TPU v7x, 128 devices: a whole 4x4x4 slice. The times are simulated.
128 devices in a mesh: fs: 16 (over z, y), tp: 8 (over x, core).
Axes of the slice: x: 4, y: 4, z: 4, core: 2. Of those that a mesh axis runs over, the one named last changes fastest.
Arguments:
- tokens: bfloat16 [8192, 4096], P('fs'), may hold values from -6 to 6
- norm_gain: float32 [4096], P('fs'), may hold values from 0.1 to 1.9
- gate_train: float32 [16, 4096, 1024], P(None, 'fs', 'tp'), may hold values from -0.09375 to 0.09375
- up_train: float32 [16, 4096, 1024], P(None, 'fs', 'tp'), may hold values from -0.09375 to 0.09375
- down_train: float32 [16, 1024, 4096], P(None, 'fs', 'tp'), may hold values from -0.1875 to 0.1875
- shared_gate_train: float32 [4096, 1024], P('fs', 'tp'), may hold values from -0.09375 to 0.09375
- shared_up_train: float32 [4096, 1024], P('fs', 'tp'), may hold values from -0.09375 to 0.09375
- shared_down_train: float32 [1024, 4096], P('fs', 'tp'), may hold values from -0.1875 to 0.1875
- route_expert: int32 [8192, 2], P('fs'), may hold values from 0 to 15, all different within a row; in each aligned block of 512 rows (0 to 511, 512 to 1023, ...) at most 96 rows name the same one
- route_weight: float32 [8192, 2], P('fs'), may hold values from 0.1 to 1
Outputs:
- expert_gate: bfloat16 [16, 4096, 1024], P('fs', None, 'tp')
- expert_up: bfloat16 [16, 4096, 1024], P('fs', None, 'tp')
- expert_down: bfloat16 [16, 1024, 4096], P('fs', 'tp')
- shared_gate: bfloat16 [4096, 1024], P(None, 'tp')
- shared_up: bfloat16 [4096, 1024], P(None, 'tp')
- shared_down: bfloat16 [1024, 4096], P('tp')
- mixed: bfloat16 [8192, 4096], P('fs', 'tp')
Inputs may be any that keep to these rules, and one draw needn't show every extreme that they name: `route_expert`: each row names 2 different experts. Within each aligned block of 512 rows no expert is named by more than 96 rows, a bound that some block reaches in every draw.
All inputs are finite; a program needn't handle non-finite values.
Results may differ from a plain program's by a relative error of at most 0.015.
Values may be sent and summed in bfloat16 or wider, within the bound.
No kernel may reach another device: no remote copies, remote signals or barrier semaphores. Data moves between devices by JAX's collectives and lax.ppermute only.
A program may use at most 128 MiB of HBM per device.

v0:
```python
import jax
import jax.numpy as jnp
from jax import lax
from jax.sharding import PartitionSpec as P

norm_eps = 1e-06


def sent_together(arrays, axis, dim, along):
    widths = [a.shape[along] for a in arrays]
    both = jnp.concatenate(arrays, axis=along)
    result = lax.all_gather(both, axis, axis=dim, tiled=True)
    return tuple(jnp.split(result, [sum(widths[:k]) for k in range(1, len(widths))], axis=along))


def blockwise_down(hidden, weight_down, pieces):
    step_width = hidden.shape[1] // pieces
    total = jnp.zeros((hidden.shape[0], weight_down.shape[1]), jnp.float32)
    for block in range(pieces):
        term = jnp.dot(
            hidden[:, block * step_width : (block + 1) * step_width],
            weight_down[block * step_width : (block + 1) * step_width],
            preferred_element_type=jnp.float32,
        )
        total = total + term.astype(jnp.bfloat16).astype(jnp.float32)
    return total


def on_device(
    tokens,
    norm_gain,
    gate_train,
    up_train,
    down_train,
    shared_gate_train,
    shared_up_train,
    shared_down_train,
    route_expert,
    route_weight,
):
    gain_rows = norm_gain[None, :, None]
    gate_local = (gain_rows * gate_train).astype(jnp.bfloat16)
    up_local = (gain_rows * up_train).astype(jnp.bfloat16)
    expert_gate, expert_up = (
        lax.all_to_all(gate_local, "fs", split_axis=0, concat_axis=1, tiled=True),
        lax.all_to_all(up_local, "fs", split_axis=0, concat_axis=1, tiled=True),
    )
    expert_down = lax.all_to_all(
        lax.all_to_all(
            down_train.astype(jnp.bfloat16), "fs", split_axis=0, concat_axis=1, tiled=True
        ),
        "tp",
        split_axis=1,
        concat_axis=2,
        tiled=True,
    )
    shared_gate_local = (norm_gain[:, None] * shared_gate_train).astype(jnp.bfloat16)
    shared_up_local = (norm_gain[:, None] * shared_up_train).astype(jnp.bfloat16)
    shared_gate, shared_up, shared_down_rows = (
        *sent_together((shared_gate_local, shared_up_local), "fs", 0, 1),
        lax.all_gather(shared_down_train.astype(jnp.bfloat16), "fs", axis=0, tiled=True),
    )
    shared_down = lax.all_to_all(shared_down_rows, "tp", split_axis=0, concat_axis=1, tiled=True)
    tok_rows, model_width = tokens.shape
    top_count = route_expert.shape[1]
    experts = lax.axis_size("fs")
    pieces = lax.axis_size("tp")
    capacity = 3 * tok_rows * top_count // (2 * experts)
    columns = model_width // pieces
    values = tokens.astype(jnp.float32)
    normed = (
        values * lax.rsqrt(jnp.mean(values * values, axis=1, keepdims=True) + norm_eps)
    ).astype(jnp.bfloat16)
    pairs = route_expert.reshape(-1)
    chosen = (pairs[:, None] == jnp.arange(experts, dtype=jnp.int32)[None, :]).astype(jnp.int32)
    earlier = jnp.cumsum(chosen, axis=0) - chosen
    slot_of = jnp.sum(earlier * chosen, axis=1)
    target = pairs * capacity + slot_of
    matches = (target[:, None] == jnp.arange(experts * capacity, dtype=jnp.int32)[None, :]).astype(
        jnp.bfloat16
    )
    placing = jnp.sum(matches.reshape(tok_rows, top_count, experts * capacity), axis=1)
    own_columns = lax.dynamic_slice_in_dim(normed, lax.axis_index("tp") * columns, columns, 1)
    outgoing = jnp.einsum("ts,td->sd", placing, own_columns, preferred_element_type=jnp.float32)
    outgoing = outgoing.astype(jnp.bfloat16).reshape(experts, capacity, columns)
    arriving = lax.all_to_all(outgoing, "fs", split_axis=0, concat_axis=0, tiled=True)
    arrived = lax.all_gather(arriving, "tp", axis=2, tiled=True)
    arrived_rows = arrived.reshape(-1, model_width)
    gate_vals = jnp.dot(arrived_rows, expert_gate[0], preferred_element_type=jnp.float32)
    up_vals = jnp.dot(arrived_rows, expert_up[0], preferred_element_type=jnp.float32)
    expert_hidden = (jax.nn.silu(gate_vals) * up_vals).astype(jnp.bfloat16)
    shared_gate_vals = jnp.dot(normed, shared_gate, preferred_element_type=jnp.float32)
    shared_up_vals = jnp.dot(normed, shared_up, preferred_element_type=jnp.float32)
    shared_hidden = (jax.nn.silu(shared_gate_vals) * shared_up_vals).astype(jnp.bfloat16)
    down_by_columns = lax.all_to_all(expert_down[0], "tp", split_axis=1, concat_axis=0, tiled=True)
    hidden_whole, shared_whole = sent_together((expert_hidden, shared_hidden), "tp", 1, 0)
    expert_sums = blockwise_down(hidden_whole, down_by_columns, pieces)
    shared_sums = blockwise_down(shared_whole, shared_down_rows, pieces)
    returning = expert_sums.astype(jnp.bfloat16).reshape(experts, capacity, columns)
    returned = lax.all_to_all(returning, "fs", split_axis=0, concat_axis=0, tiled=True).reshape(
        experts * capacity, columns
    )
    picked = jnp.take(returned, target, axis=0).reshape(tok_rows, top_count, columns)
    routed = jnp.sum(route_weight[:, :, None] * picked.astype(jnp.float32), axis=1)
    mixed = (routed + shared_sums).astype(jnp.bfloat16)
    return (expert_gate, expert_up, expert_down, shared_gate, shared_up, shared_down, mixed)


def solution(mesh):
    placed = (
        P("fs", None),
        P("fs"),
        P(None, "fs", "tp"),
        P(None, "fs", "tp"),
        P(None, "fs", "tp"),
        P("fs", "tp"),
        P("fs", "tp"),
        P("fs", "tp"),
        P("fs", None),
        P("fs", None),
    )
    return jax.shard_map(
        on_device,
        mesh=mesh,
        in_specs=placed,
        out_specs=(
            P("fs", None, "tp"),
            P("fs", None, "tp"),
            P("fs", "tp", None),
            P(None, "tp"),
            P(None, "tp"),
            P("tp", None),
            P("fs", "tp"),
        ),
        check_vma=False,
    )
```

profile of v0, /device:TPU:0, one launch (start us, length us, event | category | flops | bytes accessed | tf_op | source)
XLA Modules:
  0.0 312.0 jit_solution(5884856145658552887)
XLA Ops:
  7.2 1.1 multiply_convert_fusion.3
  8.3 0.7 pad_maximum_fusion.1
  9.1 0.8 copy.74
  10.2 4.5 %reduce-window.6 = s32[16,8,128]{2,1,0:T(8,128)S(1)} reduce-window(s32[16,8,128]{2,1,0:T(8,128)S(1)} %fusion.51, s32[]{:T(128)} %constant.18.clone.1), window={size=1x1x128 pad=0_0x0_0x127_0}, to_apply=%region_0.0 | reduce-window | flops 2080768 | bytes 131076 | tf_op jit(solution)/shard_map/reduce-window
  15.5 0.8 compare_and_fusion
  16.4 0.6 fusion.3
  17.0 3.1 fusion
  20.1 1.5 fusion.1
  21.6 1.0 convolution_convert_fusion
  22.7 0.9 copy-done.1
  23.6 33.0 %all_to_all.99 = bf16[16,96,512]{2,1,0:T(8,128)(2,1)} all-to-all(bf16[16,96,512]{2,1,0:T(8,128)(2,1)S(1)} %bitcast.97), channel_id=1, replica_groups=mesh['fs'=16,'tp'=8] {'fs'}, dimensions={0} | all-to-all | bytes 3145728 | tf_op jit(solution)/shard_map/all_to_all | solution.py:86
  56.6 3.5 %multiply_convert_fusion = (bf16[16,256,128]{2,1,0:T(8,128)(2,1)}, bf16[16,256,128]{2,1,0:T(8,128)(2,1)}) fusion(f32[16,256,128]{2,1,0:T(8,128)S(1)} %copy-done.11, f32[256]{0:T(256)S(1)} %copy-done.16, f32[16,256,128]{2,1,0:T(8,128)} %param.12), kind=kLoop, calls=%fused_computation.21 | loop fusion | flops 2097152 | bytes 6292480 | tf_op jit(solution)/shard_map/convert_element_type | solution.py:43
  60.1 3.7 %all-to-all-start = ((bf16[16,256,128]{2,1,0:T(8,128)(2,1)}), bf16[16,256,128]{2,1,0:T(8,128)(2,1)S(1)}, u32[]{:S(2)}, u32[]{:S(2)}) async-start(bf16[16,256,128]{2,1,0:T(8,128)(2,1)} %get-tuple-element.49), calls=%async_computation | async-start | bytes 2097152 | tf_op jit(solution)/shard_map/all_to_all | solution.py:45
  63.8 0.6 convert_element_type.156
  64.6 1.8 fusion.55
  66.4 1.0 copy-done.2
  67.4 1.2 fusion.57
  68.7 1.3 fusion.22
  70.0 8.6 %all-to-all-done = bf16[16,256,128]{2,1,0:T(8,128)(2,1)S(1)} async-done(((bf16[16,256,128]{2,1,0:T(8,128)(2,1)}), bf16[16,256,128]{2,1,0:T(8,128)(2,1)S(1)}, u32[]{:S(2)}, u32[]{:S(2)}) %all-to-all-start) | async-done | bytes 1048608 | tf_op jit(solution)/shard_map/all_to_all | solution.py:45
  78.6 3.7 %all-to-all-start.1 = ((bf16[16,256,128]{2,1,0:T(8,128)(2,1)}), bf16[16,256,128]{2,1,0:T(8,128)(2,1)S(1)}, u32[]{:S(2)}, u32[]{:S(2)}) async-start(bf16[16,256,128]{2,1,0:T(8,128)(2,1)} %get-tuple-element.48), calls=%async_computation.1 | async-start | bytes 2097152 | tf_op jit(solution)/shard_map/all_to_all | solution.py:46
  82.3 51.0 %all-gather.9.cloned.1.call-done = bf16[16,96,4096]{2,1,0:T(8,128)(2,1)} async-done(((bf16[16,96,512]{2,1,0:T(8,128)(2,1)}), bf16[16,96,4096]{2,1,0:T(8,128)(2,1)}) %all-gather.9.cloned.1.call-update) | async-done | bytes 12582928 | tf_op jit(solution)/shard_map/all_gather | solution.py:87
  133.2 6.4 %fusion.56 = f32[1536,128]{1,0:T(8,128)S(1)} fusion(bf16[1536,4096]{1,0:T(8,128)(2,1)} %bitcast.102, bf16[4096,128]{1,0:T(8,128)(2,1)S(1)} %bitcast.91), kind=kOutput, calls=%fused_computation.106 | convolution fusion | flops 1610612736 | bytes 14417920 | tf_op jit(solution)/shard_map/dot_general | solution.py:89
  139.7 7.0 %fusion.4 = bf16[1536,128]{1,0:T(8,128)(2,1)S(1)} fusion(bf16[1536,4096]{1,0:T(8,128)(2,1)} %bitcast.103, bf16[4096,128]{1,0:T(8,128)(2,1)S(1)} %bitcast.93, f32[1536,128]{1,0:T(8,128)S(1)} %fusion.56), kind=kOutput, calls=%fused_computation.19 | convolution fusion | flops 1611792384 | bytes 14811136 | tf_op jit(solution)/shard_map/dot_general | solution.py:90
  146.7 0.8 pad_maximum_fusion
  147.6 1.7 convert_element_type.153
  149.3 25.8 %all_to_all.100 = bf16[16,64,512]{2,1,0:T(8,128)(2,1)S(1)} all-to-all(bf16[16,64,512]{2,1,0:T(8,128)(2,1)S(1)} %convert_element_type.153), channel_id=1, replica_groups=mesh['fs'=16,'tp'=8] {'fs'}, dimensions={0} | all-to-all | bytes 2097152 | tf_op jit(solution)/shard_map/all_to_all | solution.py:49
  175.1 1.6 copy.87
  176.7 0.5 broadcast.91
  177.2 7.0 %reduce.1 = bf16[1024,512]{1,0:T(8,128)(2,1)S(1)} reduce(bf16[1024,1,512]{2,1,0:T(2,128)(2,1)S(1)} %bitcast.80, bf16[]{:T(256)} %broadcast.91), dimensions={1}, to_apply=%bitcast.77.reduce_sub_computation | reduce | bytes 2097154
  184.2 0.8 reshape.154
  185.0 24.0 %all_to_all.101 = bf16[8,2,32768]{2,1,0:T(2,128)(2,1)S(1)} all-to-all(bf16[8,2,32768]{2,1,0:T(2,128)(2,1)S(1)} %reshape.154), channel_id=1, replica_groups=mesh['fs'=16,'tp'=8] {'tp'}, dimensions={0} | all-to-all | bytes 2097152 | tf_op jit(solution)/shard_map/all_to_all | solution.py:48
  209.1 4.2 %all-to-all-start.4 = ((bf16[8,128,512]{2,1,0:T(8,128)(2,1)}), bf16[8,128,512]{2,1,0:T(8,128)(2,1)}, u32[]{:S(2)}, u32[]{:S(2)}) async-start(bf16[8,128,512]{2,1,0:T(8,128)(2,1)} %bitcast.89), calls=%async_computation.4 | async-start | bytes 2097152 | tf_op jit(solution)/shard_map/all_to_all | solution.py:63
  213.3 1.1 reshape.155
  214.4 1.3 copy.83
  215.7 17.9 %all-to-all-done.4 = bf16[8,128,512]{2,1,0:T(8,128)(2,1)} async-done(((bf16[8,128,512]{2,1,0:T(8,128)(2,1)}), bf16[8,128,512]{2,1,0:T(8,128)(2,1)}, u32[]{:S(2)}, u32[]{:S(2)}) %all-to-all-start.4) | async-done | bytes 1048608 | tf_op jit(solution)/shard_map/all_to_all | solution.py:63
  233.6 3.8 %all-to-all-start.6 = ((bf16[128,8,512]{2,0,1:T(8,128)(2,1)}), bf16[128,8,512]{2,0,1:T(8,128)(2,1)S(1)}, u32[]{:S(2)}, u32[]{:S(2)}) async-start(bf16[128,8,512]{2,0,1:T(8,128)(2,1)} %bitcast.14), calls=%async_computation.6 | async-start | bytes 2097152 | tf_op jit(solution)/shard_map/all_to_all | solution.py:95
  238.1 1.6 copy.71
  239.7 1.3 copy.81
  241.0 1.6 copy.72
  242.6 1.3 copy.82
  244.0 9.3 %all-to-all-done.6 = bf16[128,8,512]{2,0,1:T(8,128)(2,1)S(1)} async-done(((bf16[128,8,512]{2,0,1:T(8,128)(2,1)}), bf16[128,8,512]{2,0,1:T(8,128)(2,1)S(1)}, u32[]{:S(2)}, u32[]{:S(2)}) %all-to-all-start.6) | async-done | bytes 1048608 | tf_op jit(solution)/shard_map/all_to_all | solution.py:95
  253.3 1.7 convolution_convert_fusion.7
  255.0 1.5 convolution_convert_fusion.6
  256.5 0.6 convolution_convert_fusion.5
  257.1 0.5 convolution_convert_fusion.4
  257.6 0.5 convolution_convert_fusion.3
  258.2 0.5 convolution_convert_fusion.2
  258.8 0.5 convolution_convert_fusion.1
  259.3 2.8 add_convert_fusion
  262.1 3.9 %all-to-all-start.7 = ((bf16[16,96,512]{2,1,0:T(8,128)(2,1)}), bf16[16,96,512]{2,1,0:T(8,128)(2,1)S(1)}, u32[]{:S(2)}, u32[]{:S(2)}) async-start(bf16[16,96,512]{2,1,0:T(8,128)(2,1)} %bitcast.24), calls=%async_computation.7 | async-start | bytes 3145728 | tf_op jit(solution)/shard_map/all_to_all | solution.py:100
  266.0 1.2 fusion.21
  267.2 1.2 fusion.20
  268.4 1.2 fusion.18
  269.6 1.2 fusion.16
  270.8 1.2 fusion.14
  272.0 1.2 fusion.12
  273.2 2.2 fusion.10
  275.4 15.1 %all-to-all-done.7 = bf16[16,96,512]{2,1,0:T(8,128)(2,1)S(1)} async-done(((bf16[16,96,512]{2,1,0:T(8,128)(2,1)}), bf16[16,96,512]{2,1,0:T(8,128)(2,1)S(1)}, u32[]{:S(2)}, u32[]{:S(2)}) %all-to-all-start.7) | async-done | bytes 1572896 | tf_op jit(solution)/shard_map/all_to_all | solution.py:100
  290.4 5.1 %gather_fusion = bf16[1024,512]{1,0:T(8,128)(2,1)} fusion(bf16[1536,512]{1,0:T(8,128)(2,1)S(1)} %bitcast.78, s32[1024]{0:T(1024)S(1)} %broadcast_clamp_fusion), kind=kCustom, calls=%fused_computation | custom fusion | bytes 2101248 | tf_op jit(solution)/shard_map/jit(_take)/gather | solution.py:103
  295.5 1.6 gather.7
  297.1 4.4 %multiply_reduce_fusion = f32[512,512]{1,0:T(8,128)S(1)} fusion(bf16[512,2,512]{2,1,0:T(2,128)(2,1)S(1)} %gather.7, pred[512,2]{1,0:T(8,128)(4,1)S(1)} %copy.79, f32[512,2]{1,0:T(8,128)S(1)} %copy.73), kind=kLoop, calls=%fused_computation.20 | loop fusion | flops 1835008 | bytes 2102272 | tf_op jit(solution)/shard_map/reduce_sum | solution.py:104
  301.5 2.0 fusion.8
  303.5 1.0 copy.90
  304.4 1.0 copy.91
  (64 shorter events, 2.1 us)
Async XLA Ops:
  7.2 57.4 %all-gather.5.cloned.1.call-start = ((), (), s32[]{:S(2)}) async-start(), calls=%async_computation.8 | async-start | bytes 2228224 | tf_op jit(solution)/shard_map/all_gather | solution.py:12
  9.0 124.2 %all-gather.9.cloned.1.call-start = ((), (), s32[]{:S(2)}) async-start(), calls=%async_computation.10 | async-start | bytes 14155776 | tf_op jit(solution)/shard_map/all_gather | solution.py:87
  15.5 4.6 %copy-start = (bf16[512,4096]{1,0:T(8,128)(2,1)S(1)}, bf16[512,4096]{1,0:T(8,128)(2,1)}, u32[]{:S(2)}) copy-start(bf16[512,4096]{1,0:T(8,128)(2,1)} %param.10) | copy-start | bytes 12582916
  21.6 1.9 copy-start.1
  23.6 33.0 %copy-start.11 = (f32[16,256,128]{2,1,0:T(8,128)S(1)}, f32[16,256,128]{2,1,0:T(8,128)}, u32[]{:S(2)}) copy-start(f32[16,256,128]{2,1,0:T(8,128)} %param.13) | copy-start | bytes 6291460
  23.6 33.0 %copy-start.16 = (f32[256]{0:T(256)S(1)}, f32[256]{0:T(256)}, u32[]{:S(2)}) copy-start(f32[256]{0:T(256)} %param.11) | copy-start | bytes 3076
  56.6 7.3 %copy-start.13 = (f32[64,512]{1,0:T(8,128)S(1)}, f32[64,512]{1,0:T(8,128)}, u32[]{:S(2)}) copy-start(f32[64,512]{1,0:T(8,128)} %param.17) | copy-start | bytes 393220
  60.1 18.4 %all-to-all-start = ((bf16[16,256,128]{2,1,0:T(8,128)(2,1)}), bf16[16,256,128]{2,1,0:T(8,128)(2,1)S(1)}, u32[]{:S(2)}, u32[]{:S(2)}) async-start(bf16[16,256,128]{2,1,0:T(8,128)(2,1)} %get-tuple-element.49), calls=%async_computation | async-start | bytes 2097152 | tf_op jit(solution)/shard_map/all_to_all | solution.py:45
  63.8 145.3 %all-gather.7.cloned.1.call-start = ((), (), s32[]{:S(2)}) async-start(), calls=%async_computation.9 | async-start | bytes 1114112 | tf_op jit(solution)/shard_map/all_gather | solution.py:61
  64.5 2.9 copy-start.2
  66.4 2.3 copy-start.10
  66.4 2.3 copy-start.12
  78.6 61.1 %copy-start.5 = (bf16[16,256,128]{2,1,0:T(8,128)(2,1)}, bf16[16,256,128]{2,1,0:T(8,128)(2,1)S(1)}, u32[]{:S(2)}) copy-start(bf16[16,256,128]{2,1,0:T(8,128)(2,1)S(1)} %all-to-all-done) | copy-start | bytes 3145732
  78.6 61.1 %all-to-all-start.1 = ((bf16[16,256,128]{2,1,0:T(8,128)(2,1)}), bf16[16,256,128]{2,1,0:T(8,128)(2,1)S(1)}, u32[]{:S(2)}, u32[]{:S(2)}) async-start(bf16[16,256,128]{2,1,0:T(8,128)(2,1)} %get-tuple-element.48), calls=%async_computation.1 | async-start | bytes 2097152 | tf_op jit(solution)/shard_map/all_to_all | solution.py:46
  82.2 171.0 %all-gather.11.cloned.1.call-start = ((), (), s32[]{:S(2)}) async-start(), calls=%async_computation.11 | async-start | bytes 4718592 | tf_op jit(solution)/shard_map/all_gather | solution.py:12
  139.7 7.0 %copy-start.7 = (bf16[16,256,128]{2,1,0:T(8,128)(2,1)}, bf16[16,256,128]{2,1,0:T(8,128)(2,1)S(1)}, u32[]{:S(2)}) copy-start(bf16[16,256,128]{2,1,0:T(8,128)(2,1)S(1)} %all-to-all-done.1) | copy-start | bytes 3145732
  209.1 24.5 %all-to-all-start.4 = ((bf16[8,128,512]{2,1,0:T(8,128)(2,1)}), bf16[8,128,512]{2,1,0:T(8,128)(2,1)}, u32[]{:S(2)}, u32[]{:S(2)}) async-start(bf16[8,128,512]{2,1,0:T(8,128)(2,1)} %bitcast.89), calls=%async_computation.4 | async-start | bytes 2097152 | tf_op jit(solution)/shard_map/all_to_all | solution.py:63
  214.4 22.9 %copy-start.14 = (s32[512,2]{0,1:T(2,128)S(1)}, s32[512,2]{0,1:T(2,128)}, u32[]{:S(2)}) copy-start(s32[512,2]{0,1:T(2,128)} %param.18) | copy-start | bytes 12292
  214.4 23.5 %copy-start.15 = (f32[512,2]{0,1:T(2,128)S(1)}, f32[512,2]{0,1:T(2,128)}, u32[]{:S(2)}) copy-start(f32[512,2]{0,1:T(2,128)} %param.19) | copy-start | bytes 12292
  233.6 19.7 %all-to-all-start.6 = ((bf16[128,8,512]{2,0,1:T(8,128)(2,1)}), bf16[128,8,512]{2,0,1:T(8,128)(2,1)S(1)}, u32[]{:S(2)}, u32[]{:S(2)}) async-start(bf16[128,8,512]{2,0,1:T(8,128)(2,1)} %bitcast.14), calls=%async_computation.6 | async-start | bytes 2097152 | tf_op jit(solution)/shard_map/all_to_all | solution.py:95
  253.3 3.3 %copy-start.3 = (bf16[2048,1024]{1,0:T(8,128)(2,1)S(1)}, bf16[2048,1024]{1,0:T(8,128)(2,1)}, u32[]{:S(2)}) copy-start(bf16[2048,1024]{1,0:T(8,128)(2,1)} %all-gather.11.cloned.1.call-done) | copy-start | bytes 12582916
  262.1 3.9 %copy-start.4 = (bf16[1024,512]{1,0:T(8,128)(2,1)S(1)}, bf16[1024,512]{1,0:T(8,128)(2,1)}, u32[]{:S(2)}) copy-start(bf16[1024,512]{1,0:T(8,128)(2,1)} %all-gather.7.cloned.1.call-done) | copy-start | bytes 3145732
  262.1 28.3 %all-to-all-start.7 = ((bf16[16,96,512]{2,1,0:T(8,128)(2,1)}), bf16[16,96,512]{2,1,0:T(8,128)(2,1)S(1)}, u32[]{:S(2)}, u32[]{:S(2)}) async-start(bf16[16,96,512]{2,1,0:T(8,128)(2,1)} %bitcast.24), calls=%async_computation.7 | async-start | bytes 3145728 | tf_op jit(solution)/shard_map/all_to_all | solution.py:100
  295.5 6.0 %copy-start.9 = (f32[512,512]{1,0:T(8,128)S(1)}, f32[512,512]{1,0:T(8,128)}, u32[]{:S(2)}) copy-start(f32[512,512]{1,0:T(8,128)} %fusion.10) | copy-start | bytes 3145732
  297.0 6.4 %copy-start.6 = (bf16[16,256,128]{2,1,0:T(8,128)(2,1)S(1)}, bf16[16,256,128]{2,1,0:T(8,128)(2,1)}, u32[]{:S(2)}) copy-start(bf16[16,256,128]{2,1,0:T(8,128)(2,1)} %copy-done.5) | copy-start | bytes 3145732
  297.1 7.4 %copy-start.8 = (bf16[16,256,128]{2,1,0:T(8,128)(2,1)S(1)}, bf16[16,256,128]{2,1,0:T(8,128)(2,1)}, u32[]{:S(2)}) copy-start(bf16[16,256,128]{2,1,0:T(8,128)(2,1)} %copy-done.7) | copy-start | bytes 3145732
Sparse Core Ops, SparseCore 0:
  10.7 52.8 all-gather.4
  65.3 67.9 all-gather.8
  135.9 44.8 all-gather.6
  183.0 52.5 all-gather.10
where the time goes:
time: 313 us; the launch traced here: 312 us
  waiting for transfers between devices  102 us (33%)
  blocking collectives  82.7 us (26%)
  matrix products  37 us (12%)
  other arithmetic  30.7 us (10%)
  local copies, waits for them, and re-layouts  25.9 us (8%)
  starting transfers between devices  19.4 us (6%)
  between operations  14.3 us (5%)
    all_gather x1, waiting for transfers between devices, on_device(): arrived = lax.all_gather(arriving, 'tp', axis=2, tiled=True)  51 us
    all_to_all x1, blocking collectives, on_device(): lax.all_to_all(outgoing, 'fs', split_axis=0, concat_axis=0, tiled=True)  33 us
    all_to_all x1, blocking collectives, on_device(): lax.all_to_all(down_train.astype(jnp.bfloat16), 'fs', split_axis=0, conca...  25.8 us
    all_to_all x1, blocking collectives, on_device(): lax.all_to_all(lax.all_to_all(down_train.astype(jnp.bfloat16), 'fs', spli...  24 us
    dot_general x16, matrix products, blockwise_down(): jnp.dot(hidden[:, block * step_width:(block + 1) * step_width], weight_do...  20.1 us
    all_to_all x1, waiting for transfers between devices, on_device(): lax.all_to_all(shared_down_rows, 'tp', split_axis=0, concat_axis=1, tiled...  17.9 us
    all_to_all x1, waiting for transfers between devices, on_device(): lax.all_to_all(returning, 'fs', split_axis=0, concat_axis=0, tiled=True)  15.1 us
    unnamed x44, local copies, waits for them, and re-layouts  11.2 us
  transfers between devices with their start and end apart: 9, of which 5 were waited for; matrix products, arithmetic and copies ran while one was open for 21% of the time, Pallas kernels for 0%

commit v1 on v0

v1 whole, which is shorter than its diff:
```python
import functools

import jax
import jax.numpy as jnp
from jax import lax
from jax.experimental import pallas as pl
from jax.experimental.pallas import tpu as pltpu
from jax.sharding import PartitionSpec as P

norm_eps = 1e-06
bf16 = jnp.bfloat16
f32 = jnp.float32


def dot(a, b):
    return jnp.dot(a, b, preferred_element_type=f32)


def together(*values):
    return lax.optimization_barrier(values)


def cost(flops, moved):
    return pl.CostEstimate(flops=flops, bytes_accessed=moved, transcendentals=0)


def vmem_limit(mib):
    return pltpu.CompilerParams(vmem_limit_bytes=mib << 20)


def dispatch_kernel(half, place_ref, route_ref, tok_ref, normed_ref, out_ref, slot_ref, kept, placing):
    step = pl.program_id(0)
    chip, core = place_ref[0], place_ref[1]
    rows, _ = tok_ref.shape
    quarter = out_ref.shape[1]
    spots, tok_rows = placing.shape
    experts = spots // half

    @pl.when(step == 0)
    def _():
        ids = lax.broadcasted_iota(jnp.int32, (experts, tok_rows), 0)
        hot = [route_ref[k : k + 1, :] == ids for k in range(route_ref.shape[0])]
        named = sum(jnp.where(x, 1.0, 0.0) for x in hot).astype(bf16)
        ahead = lax.broadcasted_iota(jnp.int32, (tok_rows, tok_rows), 0) < (
            lax.broadcasted_iota(jnp.int32, (tok_rows, tok_rows), 1)
        )
        earlier = dot(named, jnp.where(ahead, 1.0, 0.0).astype(bf16))
        spot = lax.broadcasted_iota(jnp.int32, (spots, tok_rows), 0)
        total = jnp.zeros((spots, tok_rows), f32)
        for k, x in enumerate(hot):
            slot = jnp.sum(jnp.where(x, earlier, 0.0), axis=0, keepdims=True).astype(jnp.int32)
            slot_ref[k : k + 1, :] = slot
            local = slot - core * half
            here = (local >= 0) & (local < half)
            target = jnp.where(here, route_ref[k : k + 1, :] * half + local, -1)
            total = total + jnp.where(spot == target, 1.0, 0.0)
        placing[...] = total.astype(bf16)

    values = tok_ref[...].astype(f32)
    scale = lax.rsqrt(jnp.mean(values * values, axis=1, keepdims=True) + norm_eps)
    normed_ref[...] = (values * scale).astype(bf16)
    at = pl.multiple_of(chip * quarter, quarter)
    kept[pl.ds(pl.multiple_of(step * rows, rows), rows), :] = normed_ref[:, pl.ds(at, quarter)]

    @pl.when(step == pl.num_programs(0) - 1)
    def _():
        for c in range(0, spots, 256):
            out_ref[c : c + 256, :] = dot(placing[c : c + 256, :], kept[...]).astype(bf16)


def mark_kernel(a_ref, b_ref, out_ref):
    out_ref[...] = a_ref[...] + b_ref[...]


def first_kernel(place_ref, *refs):
    x_refs, (w_own_ref, w_other_ref, _, acc_ref) = refs[:6], refs[6:]
    chip = place_ref[0]
    quarter, wide = x_refs[0].shape[1], w_own_ref.shape[1]
    chips = w_own_ref.shape[0] // quarter
    for part in range(2):
        for half, w_ref in ((0, w_own_ref), (1, w_other_ref)):
            total = None
            for x_ref, shift in zip(x_refs[3 * part : 3 * part + 3], (0, chips - 1, 1)):
                at = pl.multiple_of(lax.rem(chip + shift, chips) * quarter, quarter)
                term = dot(x_ref[...], w_ref[pl.ds(at, quarter), :])
                total = term if total is None else total + term
            acc_ref[part, :, half * wide : (half + 1) * wide] = total


def hidden_kernel(place_ref, far0_ref, far1_ref, acc_ref, w_own_ref, w_other_ref, out_ref):
    core = place_ref[1]
    wide = w_own_ref.shape[1]
    hs = wide // 2
    for part, far_ref in enumerate((far0_ref, far1_ref)):
        for half, w_ref, slot in ((0, w_own_ref, core), (1, w_other_ref, 1 - core)):
            total = acc_ref[part, :, half * wide : (half + 1) * wide]
            total = total + dot(far_ref[...], w_ref[...])
            gate, up = total[:, :hs], total[:, hs:]
            value = (gate / (1.0 + jnp.exp(-gate)) * up).astype(bf16)
            out_ref[part, :, pl.ds(pl.multiple_of(slot * hs, hs), hs)] = value


def down_kernel(place_ref, h0_ref, h1_ref, h2_ref, h3_ref, w_own_ref, w_other_ref, out_ref):
    chip = place_ref[0]
    depth, cols = h0_ref.shape[1], w_own_ref.shape[1]
    chips = w_own_ref.shape[0] // depth
    parts = ((h0_ref, 0), (h1_ref, chips - 1), (h2_ref, 1), (h3_ref, chips // 2))
    for half, w_ref in ((0, w_own_ref), (1, w_other_ref)):
        total = None
        for h_ref, shift in parts:
            at = pl.multiple_of(lax.rem(chip + shift, chips) * depth, depth)
            term = dot(h_ref[...], w_ref[pl.ds(at, depth), :])
            total = term if total is None else total + term
        out_ref[:, half * cols : (half + 1) * cols] = total.astype(bf16)


def mix_kernel(high_ref, low_ref, got_ref, base_ref, out_ref):
    got = got_ref[...]
    total = base_ref[...] + dot(high_ref[...], got) + dot(low_ref[...], got)
    out_ref[...] = total.astype(out_ref.dtype)


def join_kernel(place_ref, p0_ref, p1_ref, p2_ref, p3_ref, routed_ref, shared_ref):
    chip, core = place_ref[0], place_ref[1]
    hs = routed_ref.shape[0]
    cols = p0_ref.shape[1] // 2
    for shift, ref in enumerate((p0_ref, p1_ref, p2_ref, p3_ref)):
        source = lax.rem(chip + 4 - shift, 4)
        for half, lane in ((0, core), (1, 1 - core)):
            at = pl.multiple_of((source * 2 + lane) * cols, cols)
            block = ref[:, half * cols : (half + 1) * cols]
            routed_ref[:, pl.ds(at, cols)] = block[:hs]
            shared_ref[:, pl.ds(at, cols)] = block[hs:]


def whole(shape):
    return pl.BlockSpec(shape, lambda *_: (0,) * len(shape))


def on_device(
    tokens,
    norm_gain,
    gate_train,
    up_train,
    down_train,
    shared_gate_train,
    shared_up_train,
    shared_down_train,
    route_expert,
    route_weight,
):
    experts = lax.axis_size("fs")
    tp = lax.axis_size("tp")
    t = lax.axis_index("tp")
    chips = tp // 2
    chip, core = t // 2, t % 2
    place = jnp.stack([chip, core]).astype(jnp.int32)
    tok_rows, width = tokens.shape
    top_count = route_expert.shape[1]
    cap = 3 * tok_rows * top_count // (2 * experts)
    half = cap // 2
    rows = experts * half
    quarter = width // chips
    cols = width // tp
    hs = gate_train.shape[2]
    deep = down_train.shape[1]

    def shift_by(a, n):
        return lax.ppermute(a, "tp", [(i, (i + 2 * n) % tp) for i in range(tp)])

    def swap(a):
        return lax.ppermute(a, "tp", [(i, i ^ 1) for i in range(tp)])

    gain = norm_gain[:, None]
    shared_local = jnp.concatenate(
        [
            jnp.concatenate(
                [(gain * shared_gate_train).astype(bf16), (gain * shared_up_train).astype(bf16)],
                axis=1,
            ).reshape(-1, deep, 2 * hs),
            jnp.swapaxes(
                shared_down_train.astype(bf16).reshape(deep, -1, 2 * hs), 0, 1
            ),
        ],
        axis=0,
    )
    shared_all = lax.all_gather(shared_local, "fs", axis=0, tiled=False)
    gu_blocks = gain.shape[0] // deep
    shared_gu = shared_all[:, :gu_blocks].reshape(width, 2 * hs)
    shared_cols = jnp.swapaxes(shared_all[:, gu_blocks:], 1, 2).reshape(experts * deep, cols)

    steps = 8
    block = tok_rows // steps
    normed, outgoing, slots = pl.pallas_call(
        functools.partial(dispatch_kernel, half),
        grid_spec=pltpu.PrefetchScalarGridSpec(
            num_scalar_prefetch=1,
            grid=(steps,),
            in_specs=[
                whole((top_count, tok_rows)),
                pl.BlockSpec((block, width), lambda i, s: (i, 0)),
            ],
            out_specs=[
                pl.BlockSpec((block, width), lambda i, s: (i, 0)),
                whole((rows, quarter)),
                whole((top_count, tok_rows)),
            ],
            scratch_shapes=[
                pltpu.VMEM((tok_rows, quarter), bf16),
                pltpu.VMEM((rows, tok_rows), bf16),
            ],
        ),
        out_shape=[
            jax.ShapeDtypeStruct((tok_rows, width), bf16),
            jax.ShapeDtypeStruct((rows, quarter), bf16),
            jax.ShapeDtypeStruct((top_count, tok_rows), jnp.int32),
        ],
        compiler_params=vmem_limit(60),
        cost_estimate=cost(2 * rows * tok_rows * quarter, 4 * tok_rows * width),
    )(place, route_expert.T, tokens)
    arriving = lax.all_to_all(
        outgoing.reshape(experts, half, quarter), "fs", split_axis=0, concat_axis=0, tiled=True
    )

    gu_local = jnp.concatenate(
        [(gain[None] * gate_train).astype(bf16), (gain[None] * up_train).astype(bf16)], axis=2
    )
    mid = rows // 2
    arriving = arriving.reshape(rows, quarter)
    top, bottom = together(arriving[:mid], arriving[mid:])
    gu_local, top, bottom = together(gu_local, top, bottom)
    gu = lax.all_to_all(gu_local, "fs", split_axis=0, concat_axis=0, tiled=True)
    down_local, gu = together(down_train.astype(bf16), gu)
    down_cols = lax.all_to_all(down_local, "fs", split_axis=0, concat_axis=0, tiled=True)
    gu = gu.reshape(width, 2 * hs)
    gu_other = swap(gu)
    down_cols = down_cols.reshape(experts * deep, cols)
    down_other = swap(down_cols)
    shared_other = swap(shared_cols)

    left_top = shift_by(top, 1)
    right_bottom = shift_by(bottom, -1)
    right_top = shift_by(top, -1)
    left_bottom = shift_by(bottom, 1)
    far_top = shift_by(left_top, 1)
    far_bottom = shift_by(right_bottom, -1)

    tile = (16, 128)
    mark = pl.pallas_call(
        mark_kernel,
        grid=(1,),
        in_specs=[whole(tile)] * 2,
        out_specs=whole(tile),
        out_shape=jax.ShapeDtypeStruct(tile, bf16),
        cost_estimate=cost(1 << 20, 1 << 14),
    )(left_top, right_bottom)
    x_spec = pl.BlockSpec((mid // 2, quarter), lambda i, s: (i, 0))
    acc_spec = pl.BlockSpec((2, mid // 2, 4 * hs), lambda i, s: (0, i, 0))
    w_spec = pl.BlockSpec((quarter, 2 * hs), lambda i, s: (lax.rem(s[0] + chips // 2, chips), 0))
    acc = pl.pallas_call(
        first_kernel,
        grid_spec=pltpu.PrefetchScalarGridSpec(
            num_scalar_prefetch=1,
            grid=(2,),
            in_specs=[x_spec] * 6 + [whole((width, 2 * hs))] * 2 + [whole(tile)],
            out_specs=acc_spec,
        ),
        out_shape=jax.ShapeDtypeStruct((2, mid, 4 * hs), f32),
        compiler_params=vmem_limit(32),
        cost_estimate=cost(2 * rows * 3 * quarter * 4 * hs, 8 * width * hs),
    )(place, top, left_top, right_top, bottom, left_bottom, right_bottom, gu, gu_other, mark)
    hidden = pl.pallas_call(
        hidden_kernel,
        grid_spec=pltpu.PrefetchScalarGridSpec(
            num_scalar_prefetch=1,
            grid=(2,),
            in_specs=[x_spec, x_spec, acc_spec, w_spec, w_spec],
            out_specs=pl.BlockSpec((2, mid // 2, 2 * hs), lambda i, s: (0, i, 0)),
        ),
        out_shape=jax.ShapeDtypeStruct((2, mid, 2 * hs), bf16),
        compiler_params=vmem_limit(32),
        cost_estimate=cost(2 * rows * quarter * 4 * hs, 8 * quarter * hs),
    )(place, far_top, far_bottom, acc, gu, gu_other).reshape(rows, 2 * hs)

    sg = dot(normed, shared_gu)
    gate, up = sg[:, :hs], sg[:, hs:]
    shared_hid = (gate / (1.0 + jnp.exp(-gate)) * up).astype(bf16)
    shared_whole = lax.all_gather(shared_hid, "tp", axis=1, tiled=True)

    h_spec = pl.BlockSpec((rows // 3, 2 * hs), lambda i, s: (i, 0))
    sums = pl.pallas_call(
        down_kernel,
        grid_spec=pltpu.PrefetchScalarGridSpec(
            num_scalar_prefetch=1,
            grid=(3,),
            in_specs=[h_spec] * 4 + [whole((experts * deep, cols))] * 2,
            out_specs=pl.BlockSpec((rows // 3, 2 * cols), lambda i, s: (i, 0)),
        ),
        out_shape=jax.ShapeDtypeStruct((rows, 2 * cols), bf16),
        compiler_params=vmem_limit(60),
        cost_estimate=cost(4 * rows * experts * deep * cols, 8 * experts * deep * cols),
    )(
        place,
        hidden,
        shift_by(hidden, 1),
        shift_by(hidden, -1),
        shift_by(hidden, 2),
        down_cols,
        down_other,
    )
    returned = lax.all_to_all(
        sums.reshape(experts, half, 2 * cols), "fs", split_axis=0, concat_axis=0, tiled=True
    ).reshape(rows, 2 * cols)
    got_other = swap(returned[:, cols:])

    spots = jnp.arange(rows, dtype=jnp.int32)[None, :]

    def mixing(which):
        high, low = 0, 0
        for k in range(top_count):
            local = slots[k] - which * half
            here = (local >= 0) & (local < half)
            target = jnp.where(here, route_expert[:, k] * half + local, -1)
            at = target[:, None] == spots
            weight = route_weight[:, k][:, None]
            most = weight.astype(bf16)
            rest = (weight - most.astype(f32)).astype(bf16)
            high = high + jnp.where(at, most, 0)
            low = low + jnp.where(at, rest, 0)
        return together(high.astype(bf16), low.astype(bf16))

    def mix(pair, got, base, dtype):
        return pl.pallas_call(
            mix_kernel,
            grid=(2,),
            in_specs=[
                pl.BlockSpec((tok_rows // 2, rows), lambda i: (i, 0)),
                pl.BlockSpec((tok_rows // 2, rows), lambda i: (i, 0)),
                pl.BlockSpec((rows, cols), lambda i: (0, 0)),
                pl.BlockSpec((tok_rows // 2, cols), lambda i: (i, 0)),
            ],
            out_specs=pl.BlockSpec((tok_rows // 2, cols), lambda i: (i, 0)),
            out_shape=jax.ShapeDtypeStruct((tok_rows, cols), dtype),
            compiler_params=vmem_limit(24),
            cost_estimate=cost(4 * tok_rows * rows * cols, 4 * tok_rows * rows),
        )(*pair, got, base)

    shared_sums = dot(shared_whole, shared_cols)
    part = mix(mixing(core), returned, shared_sums, f32)
    mixed = mix(mixing(1 - core), got_other, part, bf16)

    def chunk(n):
        at = (lax.rem(chip + n, chips) * 2 + core) * hs
        block = [
            lax.dynamic_slice_in_dim(a, at, hs, 0)
            for a in (down_cols, down_other, shared_cols, shared_other)
        ]
        return jnp.concatenate(
            [jnp.concatenate(block[:2], axis=1), jnp.concatenate(block[2:], axis=1)], axis=0
        )

    chunks = together(*(chunk(n) for n in range(chips)), sums)[:chips]
    pieces = [chunks[0]]
    for n in range(1, chips):
        pieces.append(shift_by(chunks[n], n))
    expert_down, shared_down = pl.pallas_call(
        join_kernel,
        grid_spec=pltpu.PrefetchScalarGridSpec(
            num_scalar_prefetch=1,
            grid=(1,),
            in_specs=[whole((2 * hs, 2 * cols))] * 4,
            out_specs=[whole((hs, width))] * 2,
        ),
        out_shape=[jax.ShapeDtypeStruct((hs, width), bf16)] * 2,
        compiler_params=vmem_limit(24),
        cost_estimate=cost(1 << 20, 8 * hs * width),
    )(place, *pieces)
    expert_gate = gu[None, :, :hs]
    expert_up = gu[None, :, hs:]
    shared_gate = shared_gu[:, :hs]
    shared_up = shared_gu[:, hs:]
    return (
        expert_gate,
        expert_up,
        expert_down[None],
        shared_gate,
        shared_up,
        shared_down,
        mixed,
    )


def solution(mesh):
    placed = (
        P("fs", None),
        P("fs"),
        P(None, "fs", "tp"),
        P(None, "fs", "tp"),
        P(None, "fs", "tp"),
        P("fs", "tp"),
        P("fs", "tp"),
        P("fs", "tp"),
        P("fs", None),
        P("fs", None),
    )

    return jax.shard_map(
        on_device,
        mesh=mesh,
        in_specs=placed,
        out_specs=(
            P("fs", None, "tp"),
            P("fs", None, "tp"),
            P("fs", "tp", None),
            P(None, "tp"),
            P(None, "tp"),
            P("tp", None),
            P("fs", "tp"),
        ),
        check_vma=False,
    )
```

time: 313 us -> 243 us (0.78)
  blocking collectives: 82.7 us -> 0 us
  Pallas kernels: 0 us -> 34 us
  matrix products: 37 us -> 3.62 us
  other arithmetic: 30.7 us -> 13.1 us
  starting transfers between devices: 19.4 us -> 36.9 us
  waiting for transfers between devices: 102 us -> 119 us
  local copies, waits for them, and re-layouts: 25.9 us -> 20.9 us
    all_to_all x3 -> x0, blocking collectives: 82.7 us -> none  [the longest x1 33 us: on_device(): lax.all_to_all(outgoing, 'fs', split_axis=0, concat_axis=0, tiled=True)]
    all_gather x4 -> x2, waiting for transfers between devices: 51 us -> 0.01 us  [the longest x1 0.01 us: on_device(): shared_all = lax.all_gather(shared_local, 'fs', axis=0, tiled=False)]
    ppermute x0 -> x16, waiting for transfers between devices: none -> 45.4 us  [the longest x12 45.4 us: shift_by(): return lax.ppermute(a, 'tp', [(i, (i + 2 * n) % tp) for i in range(tp)])]
    pallas_call x0 -> x8, Pallas kernels: none -> 34 us  [the longest x1 10.5 us: on_device(): pl.pallas_call(functools.partial(dispatch_kernel, half), grid_spec=pltpu....]
    dot_general x21 -> x2, matrix products: 37 us -> 3.62 us  [dot(): return jnp.dot(a, b, preferred_element_type=f32)]
    all_to_all x5 -> x4, waiting for transfers between devices: 50.8 us -> 73.7 us  [the longest x1 38.1 us: on_device(): gu = lax.all_to_all(gu_local, 'fs', split_axis=0, concat_axis=0, tiled=True)]
    ppermute x0 -> x16, starting transfers between devices: none -> 16.1 us  [the longest x12 16 us: shift_by(): return lax.ppermute(a, 'tp', [(i, (i + 2 * n) % tp) for i in range(tp)])]
    reduce_sum x4 -> x0, other arithmetic: 8.12 us -> none  [the longest x1 4.38 us: on_device(): jnp.sum(route_weight[:, :, None] * picked.astype(jnp.float32), axis=1)]
  transfers between devices with their start and end apart: 9 -> 22, of which waited for: 5 -> 11; matrix products, arithmetic and copies ran while one was open for 21% -> 13% of each run, Pallas kernels for 0% -> 8%
where the time goes in v1:
time: 243 us; the launch traced here: 242 us
  waiting for transfers between devices  119 us (49%)
  starting transfers between devices  36.9 us (15%)
  Pallas kernels  34 us (14%)
  local copies, waits for them, and re-layouts  20.9 us (9%)
  between operations  14.5 us (6%)
  other arithmetic  13.1 us (5%)
  matrix products  3.62 us (1%)
    ppermute x12, waiting for transfers between devices, shift_by(): return lax.ppermute(a, 'tp', [(i, (i + 2 * n) % tp) for i in range(tp)])  45.4 us
    all_to_all x1, waiting for transfers between devices, on_device(): gu = lax.all_to_all(gu_local, 'fs', split_axis=0, concat_axis=0, tiled=True)  38.1 us
    all_to_all x1, waiting for transfers between devices, on_device(): lax.all_to_all(outgoing.reshape(experts, half, quarter), 'fs', split_axis...  20 us
    ppermute x12, starting transfers between devices, shift_by(): return lax.ppermute(a, 'tp', [(i, (i + 2 * n) % tp) for i in range(tp)])  16 us
    all_to_all x1, waiting for transfers between devices, on_device(): lax.all_to_all(sums.reshape(experts, half, 2 * cols), 'fs', split_axis=0,...  15.6 us
    pallas_call x1, Pallas kernels, on_device(): pl.pallas_call(functools.partial(dispatch_kernel, half), grid_spec=pltpu....  10.5 us
    all_to_all x1, starting transfers between devices, on_device(): lax.all_to_all(outgoing.reshape(experts, half, quarter), 'fs', split_axis...  8.3 us
    pallas_call x1, Pallas kernels, on_device(): pl.pallas_call(down_kernel, grid_spec=pltpu.PrefetchScalarGridSpec(num_sc...  6.09 us
  transfers between devices with their start and end apart: 22, of which 11 were waited for; matrix products, arithmetic and copies ran while one was open for 13% of the time, Pallas kernels for 8%

profile of v1, /device:TPU:0, one launch (start us, length us, event | category | flops | bytes accessed | tf_op | source)
XLA Modules:
  0.0 242.2 jit_solution(1865842433335176291)
XLA Ops:
  7.2 0.6 pad_add_fusion.place_ref
  7.8 10.5 %shard_map.153 = (bf16[512,4096]{1,0:T(8,128)(2,1)}, bf16[768,1024]{1,0:T(8,128)(2,1)}, s32[2,512]{1,0:T(2,128)}) custom-call(s32[2]{0:T(128)} %pad_add_fusion.place_ref, s32[2,512]{1,0:T(2,128)} %bitcast.79, bf16[512,4096]{1,0:T(8,128)(2,1)} %tok_ref.1), custom_call_target="tpu_custom_call" | custom-call | flops 805306368 | bytes 8388608 | tf_op jit(solution)/shard_map/pallas_call | solution.py:194
  18.3 8.3 %all-to-all-start = ((bf16[16,48,1024]{2,1,0:T(8,128)(2,1)}), bf16[16,48,1024]{2,1,0:T(8,128)(2,1)S(1)}, u32[]{:S(2)}, u32[]{:S(2)}) async-start(bf16[16,48,1024]{2,1,0:T(8,128)(2,1)} %bitcast.76), calls=%async_computation | async-start | bytes 3145728 | tf_op jit(solution)/shard_map/all_to_all | solution.py:221
  26.8 0.1 multiply_convert_fusion.3
  26.9 0.7 pad_maximum_fusion.1
  27.7 2.8 %multiply_convert_fusion.1 = (bf16[16,256,128]{2,1,0:T(8,128)(2,1)S(1)}, bf16[16,256,128]{2,1,0:T(8,128)(2,1)S(1)}) fusion(f32[16,256,128]{2,1,0:T(8,128)} %param.12, f32[256]{0:T(256)S(1)} %copy-done.20, f32[16,256,128]{2,1,0:T(8,128)} %param.13), kind=kLoop, calls=%fused_computation.2 | loop fusion | flops 2097152 | bytes 6292480 | tf_op jit(solution)/shard_map/convert_element_type | solution.py:226
  30.5 1.7 pad_maximum_fusion
  32.2 20.0 %all-to-all-done = bf16[16,48,1024]{2,1,0:T(8,128)(2,1)S(1)} async-done(((bf16[16,48,1024]{2,1,0:T(8,128)(2,1)}), bf16[16,48,1024]{2,1,0:T(8,128)(2,1)S(1)}, u32[]{:S(2)}, u32[]{:S(2)}) %all-to-all-start) | async-done | bytes 1572896 | tf_op jit(solution)/shard_map/all_to_all | solution.py:221
  52.2 1.3 fusion.14
  53.5 3.7 %all-to-all-start.1 = ((bf16[16,256,256]{2,1,0:T(8,128)(2,1)}), bf16[16,256,256]{2,1,0:T(8,128)(2,1)S(1)}, u32[]{:S(2)}, u32[]{:S(2)}) async-start(bf16[16,256,256]{2,1,0:T(8,128)(2,1)} %pad_maximum_fusion), calls=%async_computation.1 | async-start | bytes 4194304 | tf_op jit(solution)/shard_map/all_to_all | solution.py:232
  57.3 2.7 %convert_element_type.54 = bf16[16,64,512]{2,1,0:T(8,128)(2,1)} convert(f32[16,64,512]{2,1,0:T(8,128)} %param.14) | non-fusion elementwise | flops 524288 | bytes 3145728 | tf_op jit(solution)/shard_map/convert_element_type | solution.py:233
  60.0 38.1 %all-to-all-done.1 = bf16[16,256,256]{2,1,0:T(8,128)(2,1)S(1)} async-done(((bf16[16,256,256]{2,1,0:T(8,128)(2,1)}), bf16[16,256,256]{2,1,0:T(8,128)(2,1)S(1)}, u32[]{:S(2)}, u32[]{:S(2)}) %all-to-all-start.1) | async-done | bytes 2097184 | tf_op jit(solution)/shard_map/all_to_all | solution.py:232
  98.1 1.5 collective-permute-start.2
  99.6 1.7 collective-permute-start.4
  101.3 4.3 %all-to-all-start.2 = ((bf16[16,64,512]{2,1,0:T(8,128)(2,1)}), bf16[16,64,512]{2,1,0:T(8,128)(2,1)}, u32[]{:S(2)}, u32[]{:S(2)}) async-start(bf16[16,64,512]{2,1,0:T(8,128)(2,1)} %convert_element_type.54), calls=%async_computation.2 | async-start | bytes 2097152 | tf_op jit(solution)/shard_map/all_to_all | solution.py:234
  105.7 0.0 all-gather.4.cloned.1.call-start
  105.7 1.5 collective-permute-start.6
  107.3 0.6 collective-permute-start.7
  107.8 12.1 %collective-permute-done.2.a_ref.refs_1_ = bf16[384,1024]{1,0:T(8,128)(2,1)S(1)} collective-permute-done((bf16[384,1024]{1,0:T(8,128)(2,1)}, bf16[384,1024]{1,0:T(8,128)(2,1)S(1)}, u32[]{:S(2)}, u32[]{:S(2)}) %collective-permute-start.2) | collective-permute-done | bytes 786464 | tf_op jit(solution)/shard_map/ppermute | solution.py:169
  119.9 0.3 collective-permute-start.3
  120.2 0.1 collective-permute-done.4.b_ref.refs_5_
  120.3 3.0 %collective-permute-start.5 = (bf16[384,1024]{1,0:T(8,128)(2,1)}, bf16[384,1024]{1,0:T(8,128)(2,1)}, u32[]{:S(2)}, u32[]{:S(2)}) collective-permute-start(bf16[384,1024]{1,0:T(8,128)(2,1)} %collective-permute-done.4.b_ref.refs_5_), channel_id=1, source_target_pairs={{0,6},{1,7},{2,0},{3,1},{4,2},{5,3},{6,4},{7,5},{8,14},{9,15},{10,... | collective-permute-start | bytes 2359304 | tf_op jit(solution)/shard_map/ppermute | solution.py:169
  123.3 2.5 %fusion.9 = (bf16[512,768]{1,0:T(8,128)(2,1)}, bf16[512,768]{1,0:T(8,128)(2,1)}, bf16[512,768]{1,0:T(8,128)(2,1)}, bf16[512,768]{1,0:T(8,128)(2,1)}) fusion(s32[512]{0:T(512)S(1)} %bitcast.82, s32[512]{0:T(512)S(1)} %bitcast.83, bf16[512]{0:T(512)(128)(2,1)S(1)} %get-tuple-element.48, bf16[512]{0:T(512)(128)(2,1)S(1)} %get-tuple-element.47, ...), kind=kLoop, calls=%fused_computation.19 | loop fusion | flops 11010048 | bytes 3158016 | tf_op jit(solution)/shard_map/add | solution.py:329
  125.8 1.3 shard_map.154.refs_8_
  127.1 10.1 %collective-permute-done.6.refs_2_ = bf16[384,1024]{1,0:T(8,128)(2,1)} collective-permute-done((bf16[384,1024]{1,0:T(8,128)(2,1)}, bf16[384,1024]{1,0:T(8,128)(2,1)}, u32[]{:S(2)}, u32[]{:S(2)}) %collective-permute-start.6) | collective-permute-done | bytes 786464 | tf_op jit(solution)/shard_map/ppermute | solution.py:169
  137.2 1.1 copy-done.1
  138.3 1.1 copy-done.4
  139.5 1.1 copy-done.5
  140.6 0.7 copy-done.9
  141.3 5.6 %shard_map.155.acc_ref = f32[2,384,512]{2,1,0:T(8,128)S(1)} custom-call(s32[2]{0:T(128)S(1)} %copy-done.10, bf16[384,1024]{1,0:T(8,128)(2,1)S(1)} %bitcast.62, bf16[384,1024]{1,0:T(8,128)(2,1)S(1)} %copy-done.1, bf16[384,1024]{1,0:T(8,128)(2,1)} %collective-permute-done.6.refs_2_, bf16[384,1024]{1,0:T(8,128)(2,1)S(1)} %bitcast.59, ...), custom_call_target="tpu_custom_call" | custom-call | flops 2415919104 | bytes 4194304 | tf_op jit(solution)/shard_map/pallas_call | solution.py:260
  146.9 6.4 %collective-permute-done.3.far0_ref = bf16[384,1024]{1,0:T(8,128)(2,1)} collective-permute-done((bf16[384,1024]{1,0:T(8,128)(2,1)S(1)}, bf16[384,1024]{1,0:T(8,128)(2,1)}, u32[]{:S(2)}, u32[]{:S(2)}) %collective-permute-start.3) | collective-permute-done | bytes 786464 | tf_op jit(solution)/shard_map/ppermute | solution.py:169
  153.3 3.2 %shard_map.156 = bf16[2,384,256]{2,1,0:T(8,128)(2,1)S(1)} custom-call(s32[2]{0:T(128)S(1)} %copy-done.10, bf16[384,1024]{1,0:T(8,128)(2,1)} %collective-permute-done.3.far0_ref, bf16[384,1024]{1,0:T(8,128)(2,1)} %collective-permute-done.5.far1_ref, f32[2,384,512]{2,1,0:T(8,128)S(1)} %shard_map.155.acc_ref, bf16[4096,256]{1,0:T(8,128)(2,1)S(1)} %bitcast.55, ...), custom_call_target="tpu_custom_call" | custom-call | flops 805306368 | bytes 1048576 | tf_op jit(solution)/shard_map/pallas_call | solution.py:272
  156.5 3.0 %collective-permute-start.10 = (bf16[768,256]{1,0:T(8,128)(2,1)S(1)}, bf16[768,256]{1,0:T(8,128)(2,1)}, u32[]{:S(2)}, u32[]{:S(2)}) collective-permute-start(bf16[768,256]{1,0:T(8,128)(2,1)S(1)} %bitcast.63), channel_id=1, source_target_pairs={{0,6},{1,7},{2,0},{3,1},{4,2},{5,3},{6,4},{7,5},{8,14},{9,15},{10,... | collective-permute-start | bytes 1179656 | tf_op jit(solution)/shard_map/ppermute | solution.py:169
  159.5 0.6 collective-permute-start.11
  160.1 0.5 collective-permute-start.9
  160.6 1.9 slice.87
  162.5 0.9 copy-done.21
  163.4 1.3 fusion.15
  164.7 0.7 fusion.12
  165.4 1.3 slice_bitcast_fusion
  166.7 1.1 copy.23
  167.8 0.2 copy.24
  168.1 0.1 collective-permute-start.1
  168.2 9.1 %collective-permute-done.10.h2_ref = bf16[768,256]{1,0:T(8,128)(2,1)} collective-permute-done((bf16[768,256]{1,0:T(8,128)(2,1)S(1)}, bf16[768,256]{1,0:T(8,128)(2,1)}, u32[]{:S(2)}, u32[]{:S(2)}) %collective-permute-start.10) | collective-permute-done | bytes 393248 | tf_op jit(solution)/shard_map/ppermute | solution.py:169
  177.3 4.9 %collective-permute-done.9.h1_ref = bf16[768,256]{1,0:T(8,128)(2,1)} collective-permute-done((bf16[768,256]{1,0:T(8,128)(2,1)S(1)}, bf16[768,256]{1,0:T(8,128)(2,1)}, u32[]{:S(2)}, u32[]{:S(2)}) %collective-permute-start.9) | collective-permute-done | bytes 393248 | tf_op jit(solution)/shard_map/ppermute | solution.py:169
  182.2 6.1 %shard_map.157 = bf16[768,1024]{1,0:T(8,128)(2,1)} custom-call(s32[2]{0:T(128)} %pad_add_fusion.place_ref, bf16[768,256]{1,0:T(8,128)(2,1)} %bitcast.66, bf16[768,256]{1,0:T(8,128)(2,1)} %collective-permute-done.9.h1_ref, bf16[768,256]{1,0:T(8,128)(2,1)} %collective-permute-done.10.h2_ref, bf16[768,256]{1,0:T(8,128)(2,1)} %collective-permute-done.11.h3_ref, ...), custom_call_target="tpu_custom_call" | custom-call | flops 1610612736 | bytes 4194304 | tf_op jit(solution)/shard_map/pallas_call | solution.py:291
  188.3 4.4 %all-to-all-start.3 = ((bf16[16,48,1024]{2,1,0:T(8,128)(2,1)}), bf16[16,48,1024]{2,1,0:T(8,128)(2,1)}, u32[]{:S(2)}, u32[]{:S(2)}) async-start(bf16[16,48,1024]{2,1,0:T(8,128)(2,1)} %bitcast.75), calls=%async_computation.3 | async-start | bytes 3145728 | tf_op jit(solution)/shard_map/all_to_all | solution.py:311
  192.7 1.5 slice_bitcast_fusion.1
  194.2 1.1 constant_dynamic-slice_fusion.3
  195.3 1.1 constant_dynamic-slice_fusion.2
  196.5 1.1 constant_dynamic-slice_fusion
  197.7 0.1 maximum_maximum_fusion.2
  197.8 1.0 maximum_maximum_fusion
  198.8 2.3 collective-permute-start.13
  201.1 1.0 collective-permute-start.14
  202.1 15.6 %all-to-all-done.3 = bf16[16,48,1024]{2,1,0:T(8,128)(2,1)} async-done(((bf16[16,48,1024]{2,1,0:T(8,128)(2,1)}), bf16[16,48,1024]{2,1,0:T(8,128)(2,1)}, u32[]{:S(2)}, u32[]{:S(2)}) %all-to-all-start.3) | async-done | bytes 1572896 | tf_op jit(solution)/shard_map/all_to_all | solution.py:311
  217.7 2.1 slice.90
  219.8 3.0 %fusion.13 = (bf16[4096,128]{1,0:T(8,128)(2,1)}, bf16[4096,128]{1,0:T(8,128)(2,1)}) fusion(bf16[4096,256]{1,0:T(8,128)(2,1)} %bitcast.68), kind=kLoop, calls=%fused_computation.63 | loop fusion | bytes 4194304 | tf_op jit(solution)/shard_map/slice | solution.py:381
  222.7 2.3 collective-permute-done.12.p1_ref
  225.1 0.4 collective-permute-done.14.p3_ref
  225.5 2.0 shard_map.158
  227.5 2.4 fusion.16.base_ref
  229.9 2.4 %shard_map.159.base_ref = f32[512,512]{1,0:T(8,128)S(1)} custom-call(bf16[512,768]{1,0:T(8,128)(2,1)S(1)} %copy-done.2, bf16[512,768]{1,0:T(8,128)(2,1)S(1)} %copy-done.3, bf16[768,1024]{1,0:T(8,128)(2,1)} %bitcast.22.got_ref, f32[512,512]{1,0:T(8,128)S(1)} %fusion.16.base_ref), custom_call_target="tpu_custom_call" | custom-call | flops 805306368 | bytes 1572864 | tf_op jit(solution)/shard_map/pallas_call | solution.py:333
  232.4 3.0 %shard_map.160 = bf16[512,512]{1,0:T(8,128)(2,1)} custom-call(bf16[512,768]{1,0:T(8,128)(2,1)S(1)} %copy-done.7, bf16[512,768]{1,0:T(8,128)(2,1)S(1)} %copy-done.6, bf16[768,512]{1,0:T(8,128)(2,1)} %collective-permute-done.15.got_ref, f32[512,512]{1,0:T(8,128)S(1)} %shard_map.159.base_ref), custom_call_target="tpu_custom_call" | custom-call | flops 805306368 | bytes 1572864 | tf_op jit(solution)/shard_map/pallas_call | solution.py:333
  (64 shorter events, 0.4 us)
Async XLA Ops:
  18.3 8.4 %copy-start.16 = (f32[64,512]{1,0:T(8,128)S(1)}, f32[64,512]{1,0:T(8,128)}, u32[]{:S(2)}) copy-start(f32[64,512]{1,0:T(8,128)} %param.17) | copy-start | bytes 393220
  18.3 8.5 %copy-start.14 = (f32[256,128]{1,0:T(8,128)S(1)}, f32[256,128]{1,0:T(8,128)}, u32[]{:S(2)}) copy-start(f32[256,128]{1,0:T(8,128)} %param.15) | copy-start | bytes 393220
  18.3 8.5 %copy-start.15 = (f32[256,128]{1,0:T(8,128)S(1)}, f32[256,128]{1,0:T(8,128)}, u32[]{:S(2)}) copy-start(f32[256,128]{1,0:T(8,128)} %param.16) | copy-start | bytes 393220
  18.3 8.5 %copy-start.20 = (f32[256]{0:T(256)S(1)}, f32[256]{0:T(256)}, u32[]{:S(2)}) copy-start(f32[256]{0:T(256)} %param.11) | copy-start | bytes 3076
  18.3 33.9 %all-to-all-start = ((bf16[16,48,1024]{2,1,0:T(8,128)(2,1)}), bf16[16,48,1024]{2,1,0:T(8,128)(2,1)S(1)}, u32[]{:S(2)}, u32[]{:S(2)}) async-start(bf16[16,48,1024]{2,1,0:T(8,128)(2,1)} %bitcast.76), calls=%async_computation | async-start | bytes 3145728 | tf_op jit(solution)/shard_map/all_to_all | solution.py:221
  26.6 133.9 %all-gather.6.cloned.1.call-start = ((), (), s32[]{:S(2)}) async-start(), calls=%async_computation.5 | async-start | bytes 3342336 | tf_op jit(solution)/shard_map/all_gather | solution.py:187
  53.5 44.6 %all-to-all-start.1 = ((bf16[16,256,256]{2,1,0:T(8,128)(2,1)}), bf16[16,256,256]{2,1,0:T(8,128)(2,1)S(1)}, u32[]{:S(2)}, u32[]{:S(2)}) async-start(bf16[16,256,256]{2,1,0:T(8,128)(2,1)} %pad_maximum_fusion), calls=%async_computation.1 | async-start | bytes 4194304 | tf_op jit(solution)/shard_map/all_to_all | solution.py:232
  57.2 50.6 %copy-start.19 = (f32[512,2]{0,1:T(2,128)S(1)}, f32[512,2]{0,1:T(2,128)}, u32[]{:S(2)}) copy-start(f32[512,2]{0,1:T(2,128)} %param.19) | copy-start | bytes 12292
  57.2 66.0 %copy-start.17 = (s32[512,2]{0,1:T(2,128)S(1)}, s32[512,2]{0,1:T(2,128)}, u32[]{:S(2)}) copy-start(s32[512,2]{0,1:T(2,128)} %param.18) | copy-start | bytes 12292
  57.3 66.0 %copy-start.18 = (s32[2,512]{1,0:T(2,128)S(1)}, s32[2,512]{1,0:T(2,128)}, u32[]{:S(2)}) copy-start(s32[2,512]{1,0:T(2,128)} %get-tuple-element.41) | copy-start | bytes 12292
  98.1 39.1 %collective-permute-start.8 = (bf16[4096,256]{1,0:T(8,128)(2,1)S(1)}, bf16[4096,256]{1,0:T(8,128)(2,1)}, u32[]{:S(2)}, u32[]{:S(2)}) collective-permute-start(bf16[4096,256]{1,0:T(8,128)(2,1)S(1)} %bitcast.53), channel_id=1, source_target_pairs={{0,1},{1,0},{2,3},{3,2},{4,5},{5,4},{6,7},{7,6},{8,9},{9,8},{10,11... | collective-permute-start | bytes 6291464 | tf_op jit(solution)/shard_map/ppermute | solution.py:172
  98.1 21.8 %collective-permute-start.2 = (bf16[384,1024]{1,0:T(8,128)(2,1)}, bf16[384,1024]{1,0:T(8,128)(2,1)S(1)}, u32[]{:S(2)}, u32[]{:S(2)}) collective-permute-start(bf16[384,1024]{1,0:T(8,128)(2,1)} %bitcast.60), channel_id=1, source_target_pairs={{0,2},{1,3},{2,4},{3,5},{4,6},{5,7},{6,0},{7,1},{8,10},{9,11},{10,... | collective-permute-start | bytes 2359304 | tf_op jit(solution)/shard_map/ppermute | solution.py:169
  99.6 20.7 %collective-permute-start.4 = (bf16[384,1024]{1,0:T(8,128)(2,1)}, bf16[384,1024]{1,0:T(8,128)(2,1)}, u32[]{:S(2)}, u32[]{:S(2)}) collective-permute-start(bf16[384,1024]{1,0:T(8,128)(2,1)} %bitcast.57), channel_id=1, source_target_pairs={{0,6},{1,7},{2,0},{3,1},{4,2},{5,3},{6,4},{7,5},{8,14},{9,15},{10,... | collective-permute-start | bytes 2359304 | tf_op jit(solution)/shard_map/ppermute | solution.py:169
  101.3 35.8 %all-to-all-start.2 = ((bf16[16,64,512]{2,1,0:T(8,128)(2,1)}), bf16[16,64,512]{2,1,0:T(8,128)(2,1)}, u32[]{:S(2)}, u32[]{:S(2)}) async-start(bf16[16,64,512]{2,1,0:T(8,128)(2,1)} %convert_element_type.54), calls=%async_computation.2 | async-start | bytes 2097152 | tf_op jit(solution)/shard_map/all_to_all | solution.py:234
  105.7 121.8 %all-gather.4.cloned.1.call-start = ((), (), s32[]{:S(2)}) async-start(), calls=%async_computation.4 | async-start | bytes 1179648 | tf_op jit(solution)/shard_map/all_gather | solution.py:288
  105.7 31.4 %collective-permute-start.6 = (bf16[384,1024]{1,0:T(8,128)(2,1)}, bf16[384,1024]{1,0:T(8,128)(2,1)}, u32[]{:S(2)}, u32[]{:S(2)}) collective-permute-start(bf16[384,1024]{1,0:T(8,128)(2,1)} %bitcast.61), channel_id=1, source_target_pairs={{0,6},{1,7},{2,0},{3,1},{4,2},{5,3},{6,4},{7,5},{8,14},{9,15},{10,... | collective-permute-start | bytes 2359304 | tf_op jit(solution)/shard_map/ppermute | solution.py:169
  107.3 29.9 %collective-permute-start.7 = (bf16[384,1024]{1,0:T(8,128)(2,1)}, bf16[384,1024]{1,0:T(8,128)(2,1)}, u32[]{:S(2)}, u32[]{:S(2)}) collective-permute-start(bf16[384,1024]{1,0:T(8,128)(2,1)} %bitcast.58), channel_id=1, source_target_pairs={{0,2},{1,3},{2,4},{3,5},{4,6},{5,7},{6,0},{7,1},{8,10},{9,11},{10,... | collective-permute-start | bytes 2359304 | tf_op jit(solution)/shard_map/ppermute | solution.py:169
  119.9 5.9 %copy-start = (bf16[384,1024]{1,0:T(8,128)(2,1)}, bf16[384,1024]{1,0:T(8,128)(2,1)S(1)}, u32[]{:S(2)}) copy-start(bf16[384,1024]{1,0:T(8,128)(2,1)S(1)} %collective-permute-done.2.a_ref.refs_1_) | copy-start | bytes 2359300
  119.9 33.3 %collective-permute-start.3 = (bf16[384,1024]{1,0:T(8,128)(2,1)S(1)}, bf16[384,1024]{1,0:T(8,128)(2,1)}, u32[]{:S(2)}, u32[]{:S(2)}) collective-permute-start(bf16[384,1024]{1,0:T(8,128)(2,1)S(1)} %collective-permute-done.2.a_ref.refs_1_), channel_id=1, source_target_pairs={{0,2},{1,3},{2,4},{3,5},{4,6},{5,7},{6,0},{7,1},{8,10},{9,11},{10,... | collective-permute-start | bytes 2359304 | tf_op jit(solution)/shard_map/ppermute | solution.py:169
  120.3 33.0 %collective-permute-start.5 = (bf16[384,1024]{1,0:T(8,128)(2,1)}, bf16[384,1024]{1,0:T(8,128)(2,1)}, u32[]{:S(2)}, u32[]{:S(2)}) collective-permute-start(bf16[384,1024]{1,0:T(8,128)(2,1)} %collective-permute-done.4.b_ref.refs_5_), channel_id=1, source_target_pairs={{0,6},{1,7},{2,0},{3,1},{4,2},{5,3},{6,4},{7,5},{8,14},{9,15},{10,... | collective-permute-start | bytes 2359304 | tf_op jit(solution)/shard_map/ppermute | solution.py:169
  123.3 13.9 %copy-start.10 = (s32[2]{0:T(128)S(1)}, s32[2]{0:T(128)}, u32[]{:S(2)}) copy-start(s32[2]{0:T(128)} %pad_add_fusion.place_ref) | copy-start | bytes 28
  137.2 31.0 %collective-permute-start = (bf16[1024,512]{1,0:T(8,128)(2,1)}, bf16[1024,512]{1,0:T(8,128)(2,1)}, u32[]{:S(2)}, u32[]{:S(2)}) collective-permute-start(bf16[1024,512]{1,0:T(8,128)(2,1)} %bitcast.9.w_own_ref), channel_id=1, source_target_pairs={{0,1},{1,0},{2,3},{3,2},{4,5},{5,4},{6,7},{7,6},{8,9},{9,8},{10,11... | collective-permute-start | bytes 3145736 | tf_op jit(solution)/shard_map/ppermute | solution.py:172
  137.2 1.1 copy-start.1
  138.3 1.1 copy-start.4
  139.5 1.1 copy-start.5
  140.6 0.7 copy-start.9
  156.4 6.0 %copy-start.8 = (bf16[2,384,256]{2,1,0:T(8,128)(2,1)}, bf16[2,384,256]{2,1,0:T(8,128)(2,1)S(1)}, u32[]{:S(2)}) copy-start(bf16[2,384,256]{2,1,0:T(8,128)(2,1)S(1)} %shard_map.156) | copy-start | bytes 1179652
  156.5 20.8 %collective-permute-start.10 = (bf16[768,256]{1,0:T(8,128)(2,1)S(1)}, bf16[768,256]{1,0:T(8,128)(2,1)}, u32[]{:S(2)}, u32[]{:S(2)}) collective-permute-start(bf16[768,256]{1,0:T(8,128)(2,1)S(1)} %bitcast.63), channel_id=1, source_target_pairs={{0,6},{1,7},{2,0},{3,1},{4,2},{5,3},{6,4},{7,5},{8,14},{9,15},{10,... | collective-permute-start | bytes 1179656 | tf_op jit(solution)/shard_map/ppermute | solution.py:169
  159.5 17.8 %collective-permute-start.11 = (bf16[768,256]{1,0:T(8,128)(2,1)S(1)}, bf16[768,256]{1,0:T(8,128)(2,1)}, u32[]{:S(2)}, u32[]{:S(2)}) collective-permute-start(bf16[768,256]{1,0:T(8,128)(2,1)S(1)} %bitcast.64), channel_id=1, source_target_pairs={{0,4},{1,5},{2,6},{3,7},{4,0},{5,1},{6,2},{7,3},{8,12},{9,13},{10,... | collective-permute-start | bytes 1179656 | tf_op jit(solution)/shard_map/ppermute | solution.py:169
  160.1 22.1 %collective-permute-start.9 = (bf16[768,256]{1,0:T(8,128)(2,1)S(1)}, bf16[768,256]{1,0:T(8,128)(2,1)}, u32[]{:S(2)}, u32[]{:S(2)}) collective-permute-start(bf16[768,256]{1,0:T(8,128)(2,1)S(1)} %bitcast.65), channel_id=1, source_target_pairs={{0,2},{1,3},{2,4},{3,5},{4,6},{5,7},{6,0},{7,1},{8,10},{9,11},{10,... | collective-permute-start | bytes 1179656 | tf_op jit(solution)/shard_map/ppermute | solution.py:169
  160.6 2.8 %copy-start.21 = (bf16[512,4096]{1,0:T(8,128)(2,1)S(1)}, bf16[512,4096]{1,0:T(8,128)(2,1)}, u32[]{:S(2)}) copy-start(bf16[512,4096]{1,0:T(8,128)(2,1)} %get-tuple-element.46) | copy-start | bytes 12582916
  162.5 2.2 copy-start.12
  168.1 28.4 %copy-start.13 = (bf16[128,8,2,256]{3,1,2,0:T(8,128)(2,1)}, bf16[128,8,2,256]{3,1,2,0:T(8,128)(2,1)S(1)}, u32[]{:S(2)}) copy-start(bf16[128,8,2,256]{3,1,2,0:T(8,128)(2,1)S(1)} %copy.24) | copy-start | bytes 3145732
  168.1 28.4 %collective-permute-start.1 = (bf16[1024,512]{1,0:T(8,128)(2,1)S(1)}, bf16[1024,512]{1,0:T(8,128)(2,1)}, u32[]{:S(2)}, u32[]{:S(2)}) collective-permute-start(bf16[1024,512]{1,0:T(8,128)(2,1)S(1)} %bitcast.72), channel_id=1, source_target_pairs={{0,1},{1,0},{2,3},{3,2},{4,5},{5,4},{6,7},{7,6},{8,9},{9,8},{10,11... | collective-permute-start | bytes 3145736 | tf_op jit(solution)/shard_map/ppermute | solution.py:172
  188.3 29.4 %all-to-all-start.3 = ((bf16[16,48,1024]{2,1,0:T(8,128)(2,1)}), bf16[16,48,1024]{2,1,0:T(8,128)(2,1)}, u32[]{:S(2)}, u32[]{:S(2)}) async-start(bf16[16,48,1024]{2,1,0:T(8,128)(2,1)} %bitcast.75), calls=%async_computation.3 | async-start | bytes 3145728 | tf_op jit(solution)/shard_map/all_to_all | solution.py:311
  198.8 26.3 %collective-permute-start.12 = (bf16[256,1024]{1,0:T(8,128)(2,1)}, bf16[256,1024]{1,0:T(8,128)(2,1)S(1)}, u32[]{:S(2)}, u32[]{:S(2)}) collective-permute-start(bf16[256,1024]{1,0:T(8,128)(2,1)} %get-tuple-element.36), channel_id=1, source_target_pairs={{0,2},{1,3},{2,4},{3,5},{4,6},{5,7},{6,0},{7,1},{8,10},{9,11},{10,... | collective-permute-start | bytes 1572872 | tf_op jit(solution)/shard_map/ppermute | solution.py:169
  198.8 26.3 %collective-permute-start.13 = (bf16[256,1024]{1,0:T(8,128)(2,1)S(1)}, bf16[256,1024]{1,0:T(8,128)(2,1)S(1)}, u32[]{:S(2)}, u32[]{:S(2)}) collective-permute-start(bf16[256,1024]{1,0:T(8,128)(2,1)S(1)} %get-tuple-element.37), channel_id=1, source_target_pairs={{0,4},{1,5},{2,6},{3,7},{4,0},{5,1},{6,2},{7,3},{8,12},{9,13},{10,... | collective-permute-start | bytes 1572872 | tf_op jit(solution)/shard_map/ppermute | solution.py:169
  201.1 24.4 %collective-permute-start.14 = (bf16[256,1024]{1,0:T(8,128)(2,1)S(1)}, bf16[256,1024]{1,0:T(8,128)(2,1)S(1)}, u32[]{:S(2)}, u32[]{:S(2)}) collective-permute-start(bf16[256,1024]{1,0:T(8,128)(2,1)S(1)} %get-tuple-element.38), channel_id=1, source_target_pairs={{0,6},{1,7},{2,0},{3,1},{4,2},{5,3},{6,4},{7,5},{8,14},{9,15},{10,... | collective-permute-start | bytes 1572872 | tf_op jit(solution)/shard_map/ppermute | solution.py:169
  219.8 5.7 %copy-start.11 = (s32[2]{0:T(128)S(1)}, s32[2]{0:T(128)}, u32[]{:S(2)}) copy-start(s32[2]{0:T(128)} %pad_add_fusion.place_ref) | copy-start | bytes 28
  219.8 12.6 %collective-permute-start.15 = (bf16[768,512]{1,0:T(8,128)(2,1)}, bf16[768,512]{1,0:T(8,128)(2,1)}, u32[]{:S(2)}, u32[]{:S(2)}) collective-permute-start(bf16[768,512]{1,0:T(8,128)(2,1)} %slice.90), channel_id=1, source_target_pairs={{0,1},{1,0},{2,3},{3,2},{4,5},{5,4},{6,7},{7,6},{8,9},{9,8},{10,11... | collective-permute-start | bytes 2359304 | tf_op jit(solution)/shard_map/ppermute | solution.py:172
  227.5 2.4 copy-start.2
  227.5 2.4 copy-start.3
  229.9 2.5 %copy-start.6 = (bf16[512,768]{1,0:T(8,128)(2,1)S(1)}, bf16[512,768]{1,0:T(8,128)(2,1)}, u32[]{:S(2)}) copy-start(bf16[512,768]{1,0:T(8,128)(2,1)} %get-tuple-element.43.low_ref) | copy-start | bytes 2359300
  229.9 2.5 %copy-start.7 = (bf16[512,768]{1,0:T(8,128)(2,1)S(1)}, bf16[512,768]{1,0:T(8,128)(2,1)}, u32[]{:S(2)}) copy-start(bf16[512,768]{1,0:T(8,128)(2,1)} %get-tuple-element.42.high_ref) | copy-start | bytes 2359300
Sparse Core Ops, SparseCore 0:
  30.2 67.4 all-gather.5
  165.6 21.2 all-gather.3

commit v2 on v1

--- a/solution.py
+++ b/solution.py
@@ -56,9 +56,10 @@
             total = total + jnp.where(spot == target, 1.0, 0.0)
         placing[...] = total.astype(bf16)
 
-    values = tok_ref[...].astype(f32)
-    scale = lax.rsqrt(jnp.mean(values * values, axis=1, keepdims=True) + norm_eps)
-    normed_ref[...] = (values * scale).astype(bf16)
+    for r in range(0, rows, 16):
+        values = tok_ref[r : r + 16, :].astype(f32)
+        scale = lax.rsqrt(jnp.mean(values * values, axis=1, keepdims=True) + norm_eps)
+        normed_ref[r : r + 16, :] = (values * scale).astype(bf16)
     at = pl.multiple_of(chip * quarter, quarter)
     kept[pl.ds(pl.multiple_of(step * rows, rows), rows), :] = normed_ref[:, pl.ds(at, quarter)]
 
@@ -100,24 +101,72 @@
             out_ref[part, :, pl.ds(pl.multiple_of(slot * hs, hs), hs)] = value
 
 
-def down_kernel(place_ref, h0_ref, h1_ref, h2_ref, h3_ref, w_own_ref, w_other_ref, out_ref):
+def down_kernel(place_ref, h0_ref, h1_ref, h2_ref, h3_ref, w_own_ref, w_other_ref, out_ref, line):
     chip = place_ref[0]
     depth, cols = h0_ref.shape[1], w_own_ref.shape[1]
     chips = w_own_ref.shape[0] // depth
     parts = ((h0_ref, 0), (h1_ref, chips - 1), (h2_ref, 1), (h3_ref, chips // 2))
-    for half, w_ref in ((0, w_own_ref), (1, w_other_ref)):
-        total = None
-        for h_ref, shift in parts:
-            at = pl.multiple_of(lax.rem(chip + shift, chips) * depth, depth)
-            term = dot(h_ref[...], w_ref[pl.ds(at, depth), :])
-            total = term if total is None else total + term
-        out_ref[:, half * cols : (half + 1) * cols] = total.astype(bf16)
-
-
-def mix_kernel(high_ref, low_ref, got_ref, base_ref, out_ref):
-    got = got_ref[...]
-    total = base_ref[...] + dot(high_ref[...], got) + dot(low_ref[...], got)
-    out_ref[...] = total.astype(out_ref.dtype)
+    for h_ref, shift in parts:
+        at = pl.multiple_of(lax.rem(chip + shift, chips) * depth, depth)
+        line[:, pl.ds(at, depth)] = h_ref[...]
+    for part, w_ref in enumerate((w_own_ref, w_other_ref)):
+        total = dot(line[...], w_ref[...]).astype(bf16)
+        out_ref[:, part] = total.reshape(out_ref.shape[0], out_ref.shape[2], cols)
+
+
+def shared_kernel(place_ref, x_ref, gu_ref, sd_ref, gate_ref, up_ref, hid_ref, sd_out_ref, acc):
+    step = pl.program_id(0)
+    core = place_ref[1]
+    wide = acc.shape[1]
+    hs = wide // 2
+    deep = gu_ref.shape[0] // 4
+    fold = gu_ref.shape[1] // wide
+    for f in range(4):
+        block = gu_ref[f * deep : (f + 1) * deep, :]
+        weight = jnp.concatenate([block[:, j * wide : (j + 1) * wide] for j in range(fold)], axis=0)
+        size = fold * deep
+        gate_ref[f * size : (f + 1) * size, :] = weight[:, :hs]
+        up_ref[f * size : (f + 1) * size, :] = weight[:, hs:]
+        term = dot(x_ref[:, f * size : (f + 1) * size], weight)
+        first = (step == 0) if f == 0 else False
+        if f == 0:
+            @pl.when(first)
+            def _():
+                acc[...] = term
+
+            @pl.when(step > 0)
+            def _():
+                acc[...] += term
+        else:
+            acc[...] += term
+    rows = sd_out_ref.shape[0]
+    sd_out_ref[...] = sd_ref[pl.ds(pl.multiple_of((1 - core) * rows, rows), rows), :]
+
+    @pl.when(step == pl.num_programs(0) - 1)
+    def _():
+        gate, up = acc[:, :hs], acc[:, hs:]
+        hid_ref[...] = (gate / (1.0 + jnp.exp(-gate)) * up).astype(bf16)
+
+
+def base_kernel(hid_ref, sd_ref, out_ref):
+    out_ref[...] = dot(hid_ref[...], sd_ref[...])
+
+
+def mix_kernel(weight_ref, got_ref, base_ref, out_ref):
+    out_ref[...] = (base_ref[...] + dot(weight_ref[...], got_ref[...])).astype(out_ref.dtype)
+
+
+def chunk_kernel(place_ref, own_ref, other_ref, sd_ref, sd_other_ref, *out_refs):
+    chip, core = place_ref[0], place_ref[1]
+    hs, cols = out_refs[0].shape[0] // 2, own_ref.shape[1]
+    for n, out_ref in enumerate(out_refs):
+        target = lax.rem(chip + n, 4)
+        at = pl.ds(pl.multiple_of((target * 2 + core) * hs, hs), hs)
+        far = pl.ds(pl.multiple_of(target * hs, hs), hs)
+        out_ref[:hs, :cols] = own_ref[at, :]
+        out_ref[:hs, cols:] = other_ref[at, :]
+        out_ref[hs:, :cols] = sd_ref[at, :]
+        out_ref[hs:, cols:] = sd_other_ref[far, :]
 
 
 def join_kernel(place_ref, p0_ref, p1_ref, p2_ref, p3_ref, routed_ref, shared_ref):
@@ -172,22 +221,20 @@
         return lax.ppermute(a, "tp", [(i, i ^ 1) for i in range(tp)])
 
     gain = norm_gain[:, None]
-    shared_local = jnp.concatenate(
-        [
-            jnp.concatenate(
-                [(gain * shared_gate_train).astype(bf16), (gain * shared_up_train).astype(bf16)],
-                axis=1,
-            ).reshape(-1, deep, 2 * hs),
-            jnp.swapaxes(
-                shared_down_train.astype(bf16).reshape(deep, -1, 2 * hs), 0, 1
-            ),
-        ],
+    shared_gu_local = jnp.concatenate(
+        [(gain * shared_gate_train).astype(bf16), (gain * shared_up_train).astype(bf16)], axis=1
+    )
+    fold = shared_gu_local.shape[0] // deep
+    shared_all = lax.all_gather(
+        jnp.concatenate(
+            [shared_gu_local[j * deep : (j + 1) * deep] for j in range(fold)]
+            + [shared_down_train.astype(bf16)],
+            axis=1,
+        ),
+        "fs",
         axis=0,
-    )
-    shared_all = lax.all_gather(shared_local, "fs", axis=0, tiled=False)
-    gu_blocks = gain.shape[0] // deep
-    shared_gu = shared_all[:, :gu_blocks].reshape(width, 2 * hs)
-    shared_cols = jnp.swapaxes(shared_all[:, gu_blocks:], 1, 2).reshape(experts * deep, cols)
+        tiled=True,
+    )
 
     steps = 8
     block = tok_rows // steps
@@ -236,7 +283,6 @@
     gu_other = swap(gu)
     down_cols = down_cols.reshape(experts * deep, cols)
     down_other = swap(down_cols)
-    shared_other = swap(shared_cols)
 
     left_top = shift_by(top, 1)
     right_bottom = shift_by(bottom, -1)
@@ -273,93 +319,113 @@
         hidden_kernel,
         grid_spec=pltpu.PrefetchScalarGridSpec(
             num_scalar_prefetch=1,
-            grid=(2,),
-            in_specs=[x_spec, x_spec, acc_spec, w_spec, w_spec],
-            out_specs=pl.BlockSpec((2, mid // 2, 2 * hs), lambda i, s: (0, i, 0)),
+            grid=(1,),
+            in_specs=[whole((mid, quarter))] * 2 + [whole((2, mid, 4 * hs)), w_spec, w_spec],
+            out_specs=whole((2, mid, 2 * hs)),
         ),
         out_shape=jax.ShapeDtypeStruct((2, mid, 2 * hs), bf16),
         compiler_params=vmem_limit(32),
         cost_estimate=cost(2 * rows * quarter * 4 * hs, 8 * quarter * hs),
     )(place, far_top, far_bottom, acc, gu, gu_other).reshape(rows, 2 * hs)
 
-    sg = dot(normed, shared_gu)
-    gate, up = sg[:, :hs], sg[:, hs:]
-    shared_hid = (gate / (1.0 + jnp.exp(-gate)) * up).astype(bf16)
+    sd_spec = pl.BlockSpec((experts * deep, cols), lambda *_: (0, fold * 2 * hs // cols))
+    shared_gate, shared_up, shared_hid, shared_out = pl.pallas_call(
+        shared_kernel,
+        grid_spec=pltpu.PrefetchScalarGridSpec(
+            num_scalar_prefetch=1,
+            grid=(experts // 4,),
+            in_specs=[
+                pl.BlockSpec((tok_rows, 4 * fold * deep), lambda i, s: (0, i)),
+                pl.BlockSpec((4 * deep, fold * 2 * hs), lambda i, s: (i, 0)),
+                pl.BlockSpec((4 * deep, cols), lambda i, s: (i, fold * 2 * hs // cols)),
+            ],
+            out_specs=[
+                pl.BlockSpec((4 * fold * deep, hs), lambda i, s: (i, 0)),
+                pl.BlockSpec((4 * fold * deep, hs), lambda i, s: (i, 0)),
+                whole((tok_rows, hs)),
+                pl.BlockSpec((2 * deep, cols), lambda i, s: (i, 0)),
+            ],
+            scratch_shapes=[pltpu.VMEM((tok_rows, 2 * hs), f32)],
+        ),
+        out_shape=[
+            jax.ShapeDtypeStruct((width, hs), bf16),
+            jax.ShapeDtypeStruct((width, hs), bf16),
+            jax.ShapeDtypeStruct((tok_rows, hs), bf16),
+            jax.ShapeDtypeStruct((experts * deep // 2, cols), bf16),
+        ],
+        compiler_params=vmem_limit(36),
+        cost_estimate=cost(4 * tok_rows * width * hs, 8 * width * hs),
+    )(place, normed, shared_all, shared_all)
+    shared_other = swap(shared_out)
     shared_whole = lax.all_gather(shared_hid, "tp", axis=1, tiled=True)
 
-    h_spec = pl.BlockSpec((rows // 3, 2 * hs), lambda i, s: (i, 0))
+    hid_left = shift_by(hidden, 1)
+    hid_right = shift_by(hidden, -1)
+    hid_far = shift_by(hidden, 2)
     sums = pl.pallas_call(
         down_kernel,
         grid_spec=pltpu.PrefetchScalarGridSpec(
             num_scalar_prefetch=1,
-            grid=(3,),
-            in_specs=[h_spec] * 4 + [whole((experts * deep, cols))] * 2,
-            out_specs=pl.BlockSpec((rows // 3, 2 * cols), lambda i, s: (i, 0)),
-        ),
-        out_shape=jax.ShapeDtypeStruct((rows, 2 * cols), bf16),
-        compiler_params=vmem_limit(60),
+            grid=(1,),
+            in_specs=[whole((rows, 2 * hs))] * 4 + [whole((experts * deep, cols))] * 2,
+            out_specs=whole((experts, 2, half, cols)),
+            scratch_shapes=[pltpu.VMEM((rows, experts * deep), bf16)],
+        ),
+        out_shape=jax.ShapeDtypeStruct((experts, 2, half, cols), bf16),
+        compiler_params=vmem_limit(40),
         cost_estimate=cost(4 * rows * experts * deep * cols, 8 * experts * deep * cols),
-    )(
-        place,
-        hidden,
-        shift_by(hidden, 1),
-        shift_by(hidden, -1),
-        shift_by(hidden, 2),
-        down_cols,
-        down_other,
-    )
-    returned = lax.all_to_all(
-        sums.reshape(experts, half, 2 * cols), "fs", split_axis=0, concat_axis=0, tiled=True
-    ).reshape(rows, 2 * cols)
-    got_other = swap(returned[:, cols:])
+    )(place, hidden, hid_left, hid_right, hid_far, down_cols, down_other)
+    returned = lax.all_to_all(sums, "fs", split_axis=0, concat_axis=0, tiled=True)
+    got_other = swap(returned[:, 1].reshape(rows, cols))
+    got_own = returned[:, 0].reshape(rows, cols)
 
     spots = jnp.arange(rows, dtype=jnp.int32)[None, :]
 
     def mixing(which):
-        high, low = 0, 0
+        weights = 0
         for k in range(top_count):
             local = slots[k] - which * half
             here = (local >= 0) & (local < half)
             target = jnp.where(here, route_expert[:, k] * half + local, -1)
             at = target[:, None] == spots
-            weight = route_weight[:, k][:, None]
-            most = weight.astype(bf16)
-            rest = (weight - most.astype(f32)).astype(bf16)
-            high = high + jnp.where(at, most, 0)
-            low = low + jnp.where(at, rest, 0)
-        return together(high.astype(bf16), low.astype(bf16))
-
-    def mix(pair, got, base, dtype):
+            weights = weights + jnp.where(at, route_weight[:, k][:, None].astype(bf16), 0)
+        return weights
+
+    mix_own, mix_other = together(mixing(core), mixing(1 - core))
+
+    def mix(weights, got, base, dtype):
         return pl.pallas_call(
             mix_kernel,
-            grid=(2,),
-            in_specs=[
-                pl.BlockSpec((tok_rows // 2, rows), lambda i: (i, 0)),
-                pl.BlockSpec((tok_rows // 2, rows), lambda i: (i, 0)),
-                pl.BlockSpec((rows, cols), lambda i: (0, 0)),
-                pl.BlockSpec((tok_rows // 2, cols), lambda i: (i, 0)),
-            ],
-            out_specs=pl.BlockSpec((tok_rows // 2, cols), lambda i: (i, 0)),
             out_shape=jax.ShapeDtypeStruct((tok_rows, cols), dtype),
             compiler_params=vmem_limit(24),
-            cost_estimate=cost(4 * tok_rows * rows * cols, 4 * tok_rows * rows),
-        )(*pair, got, base)
-
-    shared_sums = dot(shared_whole, shared_cols)
-    part = mix(mixing(core), returned, shared_sums, f32)
-    mixed = mix(mixing(1 - core), got_other, part, bf16)
-
-    def chunk(n):
-        at = (lax.rem(chip + n, chips) * 2 + core) * hs
-        block = [
-            lax.dynamic_slice_in_dim(a, at, hs, 0)
-            for a in (down_cols, down_other, shared_cols, shared_other)
-        ]
-        return jnp.concatenate(
-            [jnp.concatenate(block[:2], axis=1), jnp.concatenate(block[2:], axis=1)], axis=0
-        )
-
-    chunks = together(*(chunk(n) for n in range(chips)), sums)[:chips]
+            cost_estimate=cost(2 * tok_rows * rows * cols, 4 * tok_rows * rows),
+        )(weights, got, base)
+
+    base = pl.pallas_call(
+        base_kernel,
+        grid=(1,),
+        in_specs=[whole((tok_rows, experts * deep)), sd_spec],
+        out_specs=whole((tok_rows, cols)),
+        out_shape=jax.ShapeDtypeStruct((tok_rows, cols), f32),
+        compiler_params=vmem_limit(24),
+        cost_estimate=cost(2 * tok_rows * experts * deep * cols, 4 * tok_rows * rows),
+    )(shared_whole, shared_all)
+    part = mix(mix_own, got_own, base, f32)
+    mixed = mix(mix_other, got_other, part, bf16)
+
+    chunks = pl.pallas_call(
+        chunk_kernel,
+        grid_spec=pltpu.PrefetchScalarGridSpec(
+            num_scalar_prefetch=1,
+            grid=(1,),
+            in_specs=[whole((experts * deep, cols))] * 2
+            + [sd_spec, whole((experts * deep // 2, cols))],
+            out_specs=[whole((2 * hs, 2 * cols))] * chips,
+        ),
+        out_shape=[jax.ShapeDtypeStruct((2 * hs, 2 * cols), bf16)] * chips,
+        compiler_params=vmem_limit(36),
+        cost_estimate=cost(1 << 30, 8 * hs * width),
+    )(place, down_cols, down_other, shared_all, shared_other)
     pieces = [chunks[0]]
     for n in range(1, chips):
         pieces.append(shift_by(chunks[n], n))
@@ -377,8 +443,6 @@
     )(place, *pieces)
     expert_gate = gu[None, :, :hs]
     expert_up = gu[None, :, hs:]
-    shared_gate = shared_gu[:, :hs]
-    shared_up = shared_gu[:, hs:]
     return (
         expert_gate,
         expert_up,

time: 243 us -> 252 us (1.037)
  waiting for transfers between devices: 119 us -> 130 us
  Pallas kernels: 34 us -> 41 us
  local copies, waits for them, and re-layouts: 20.9 us -> 15.8 us
  matrix products: 3.62 us -> 0 us
  other arithmetic: 13.1 us -> 9.76 us
    ppermute x12, waiting for transfers between devices: 45.4 us -> 68.6 us  [shift_by(): return lax.ppermute(a, 'tp', [(i, (i + 2 * n) % tp) for i in range(tp)])]
    all_to_all x1, waiting for transfers between devices: 15.6 us -> 2.99 us  [on_device(): lax.all_to_all(sums, 'fs', split_axis=0, concat_axis=0, tiled=True)]
    pallas_call x2 -> x5, Pallas kernels: 5.44 us -> 12 us  [the longest x1 5.12 us: on_device(): pl.pallas_call(shared_kernel, grid_spec=pltpu.PrefetchScalarGridSpec(num_...]
    unnamed x45 -> x50, local copies, waits for them, and re-layouts: 5.32 us -> 10.2 us
    slice x3 -> x2, local copies, waits for them, and re-layouts: 6.94 us -> 2.83 us  [the longest x1 2.81 us: on_device(): got_own = returned[:, 0].reshape(rows, cols)]
    dot_general x2 -> x0, matrix products: 3.62 us -> none  [dot(): return jnp.dot(a, b, preferred_element_type=f32)]
    dynamic_slice x4 -> x0, local copies, waits for them, and re-layouts: 3.46 us -> none  [chunk(): lax.dynamic_slice_in_dim(a, at, hs, 0)]
  transfers between devices with their start and end apart: 22 -> 22, of which waited for: 11 -> 13; matrix products, arithmetic and copies ran while one was open for 13% -> 6% of each run, Pallas kernels for 8% -> 11%
where the time goes in v2:
time: 252 us; the launch traced here: 250 us
  waiting for transfers between devices  130 us (52%)
  Pallas kernels  41 us (16%)
  starting transfers between devices  39 us (15%)
  local copies, waits for them, and re-layouts  15.8 us (6%)
  between operations  14.4 us (6%)
  other arithmetic  9.76 us (4%)
    ppermute x12, waiting for transfers between devices, shift_by(): return lax.ppermute(a, 'tp', [(i, (i + 2 * n) % tp) for i in range(tp)])  68.6 us
    all_to_all x1, waiting for transfers between devices, on_device(): gu = lax.all_to_all(gu_local, 'fs', split_axis=0, concat_axis=0, tiled=True)  38.1 us
    all_to_all x1, waiting for transfers between devices, on_device(): lax.all_to_all(outgoing.reshape(experts, half, quarter), 'fs', split_axis...  20.1 us
    ppermute x12, starting transfers between devices, shift_by(): return lax.ppermute(a, 'tp', [(i, (i + 2 * n) % tp) for i in range(tp)])  18.5 us
    pallas_call x1, Pallas kernels, on_device(): pl.pallas_call(functools.partial(dispatch_kernel, half), grid_spec=pltpu....  10.4 us
    unnamed x50, local copies, waits for them, and re-layouts  10.2 us
    all_to_all x1, starting transfers between devices, on_device(): lax.all_to_all(outgoing.reshape(experts, half, quarter), 'fs', split_axis...  8.3 us
    pallas_call x1, Pallas kernels, on_device(): pl.pallas_call(first_kernel, grid_spec=pltpu.PrefetchScalarGridSpec(num_s...  5.96 us
  transfers between devices with their start and end apart: 22, of which 13 were waited for; matrix products, arithmetic and copies ran while one was open for 6% of the time, Pallas kernels for 11%

profile of v2, /device:TPU:0, one launch (start us, length us, event | category | flops | bytes accessed | tf_op | source)
XLA Modules:
  0.0 250.2 jit_solution(10150655875175284747)
XLA Ops:
  7.2 0.7 pad_add_fusion.place_ref
  7.8 10.4 %shard_map.153 = (bf16[512,4096]{1,0:T(8,128)(2,1)}, bf16[768,1024]{1,0:T(8,128)(2,1)}, s32[2,512]{1,0:T(2,128)}) custom-call(s32[2]{0:T(128)} %pad_add_fusion.place_ref, s32[2,512]{1,0:T(2,128)} %bitcast.53, bf16[512,4096]{1,0:T(8,128)(2,1)} %tok_ref.1), custom_call_target="tpu_custom_call" | custom-call | flops 805306368 | bytes 8388608 | tf_op jit(solution)/shard_map/pallas_call | solution.py:241
  18.3 8.3 %all-to-all-start = ((bf16[16,48,1024]{2,1,0:T(8,128)(2,1)}), bf16[16,48,1024]{2,1,0:T(8,128)(2,1)S(1)}, u32[]{:S(2)}, u32[]{:S(2)}) async-start(bf16[16,48,1024]{2,1,0:T(8,128)(2,1)} %bitcast.52), calls=%async_computation | async-start | bytes 3145728 | tf_op jit(solution)/shard_map/all_to_all | solution.py:268
  26.6 0.0 all-gather.3.cloned.1.call-start
  26.7 0.1 multiply_convert_fusion.2
  26.9 0.7 copy-done.17
  27.6 2.8 %multiply_convert_fusion.1 = (bf16[16,256,128]{2,1,0:T(8,128)(2,1)S(1)}, bf16[16,256,128]{2,1,0:T(8,128)(2,1)S(1)}) fusion(f32[16,256,128]{2,1,0:T(8,128)} %param.12, f32[256]{0:T(256)S(1)} %copy-done.24, f32[16,256,128]{2,1,0:T(8,128)} %param.13), kind=kLoop, calls=%fused_computation.2 | loop fusion | flops 2097152 | bytes 6292480 | tf_op jit(solution)/shard_map/convert_element_type | solution.py:273
  30.4 1.7 pad_maximum_fusion
  32.1 20.1 %all-to-all-done = bf16[16,48,1024]{2,1,0:T(8,128)(2,1)S(1)} async-done(((bf16[16,48,1024]{2,1,0:T(8,128)(2,1)}), bf16[16,48,1024]{2,1,0:T(8,128)(2,1)S(1)}, u32[]{:S(2)}, u32[]{:S(2)}) %all-to-all-start) | async-done | bytes 1572896 | tf_op jit(solution)/shard_map/all_to_all | solution.py:268
  52.2 1.3 fusion.14
  53.5 3.7 %all-to-all-start.1 = ((bf16[16,256,256]{2,1,0:T(8,128)(2,1)}), bf16[16,256,256]{2,1,0:T(8,128)(2,1)S(1)}, u32[]{:S(2)}, u32[]{:S(2)}) async-start(bf16[16,256,256]{2,1,0:T(8,128)(2,1)} %pad_maximum_fusion), calls=%async_computation.1 | async-start | bytes 4194304 | tf_op jit(solution)/shard_map/all_to_all | solution.py:279
  57.2 2.7 %convert_element_type.27 = bf16[16,64,512]{2,1,0:T(8,128)(2,1)} convert(f32[16,64,512]{2,1,0:T(8,128)} %param.14) | non-fusion elementwise | flops 524288 | bytes 3145728 | tf_op jit(solution)/shard_map/convert_element_type | solution.py:280
  59.9 38.1 %all-to-all-done.1 = bf16[16,256,256]{2,1,0:T(8,128)(2,1)S(1)} async-done(((bf16[16,256,256]{2,1,0:T(8,128)(2,1)}), bf16[16,256,256]{2,1,0:T(8,128)(2,1)S(1)}, u32[]{:S(2)}, u32[]{:S(2)}) %all-to-all-start.1) | async-done | bytes 2097184 | tf_op jit(solution)/shard_map/all_to_all | solution.py:279
  98.0 1.3 collective-permute-start.5
  99.4 1.9 collective-permute-start.7
  101.3 3.7 %all-to-all-start.2 = ((bf16[16,64,512]{2,1,0:T(8,128)(2,1)}), bf16[16,64,512]{2,1,0:T(8,128)(2,1)S(1)}, u32[]{:S(2)}, u32[]{:S(2)}) async-start(bf16[16,64,512]{2,1,0:T(8,128)(2,1)} %convert_element_type.27), calls=%async_computation.2 | async-start | bytes 2097152 | tf_op jit(solution)/shard_map/all_to_all | solution.py:281
  104.9 0.2 collective-permute-start.10
  105.1 3.1 %collective-permute-start.9 = (bf16[384,1024]{1,0:T(8,128)(2,1)}, bf16[384,1024]{1,0:T(8,128)(2,1)}, u32[]{:S(2)}, u32[]{:S(2)}) collective-permute-start(bf16[384,1024]{1,0:T(8,128)(2,1)} %bitcast.4.refs_0_), channel_id=1, source_target_pairs={{0,6},{1,7},{2,0},{3,1},{4,2},{5,3},{6,4},{7,5},{8,14},{9,15},{10,... | collective-permute-start | bytes 2359304 | tf_op jit(solution)/shard_map/ppermute | solution.py:218
  108.2 11.7 %collective-permute-done.5.a_ref.refs_1_ = bf16[384,1024]{1,0:T(8,128)(2,1)} collective-permute-done((bf16[384,1024]{1,0:T(8,128)(2,1)}, bf16[384,1024]{1,0:T(8,128)(2,1)}, u32[]{:S(2)}, u32[]{:S(2)}) %collective-permute-start.5) | collective-permute-done | bytes 786464 | tf_op jit(solution)/shard_map/ppermute | solution.py:218
  120.0 0.1 collective-permute-start.6
  120.1 3.1 %collective-permute-start.8 = (bf16[384,1024]{1,0:T(8,128)(2,1)}, bf16[384,1024]{1,0:T(8,128)(2,1)}, u32[]{:S(2)}, u32[]{:S(2)}) collective-permute-start(bf16[384,1024]{1,0:T(8,128)(2,1)} %collective-permute-done.7.b_ref.refs_5_), channel_id=1, source_target_pairs={{0,6},{1,7},{2,0},{3,1},{4,2},{5,3},{6,4},{7,5},{8,14},{9,15},{10,... | collective-permute-start | bytes 2359304 | tf_op jit(solution)/shard_map/ppermute | solution.py:218
  123.2 13.5 %collective-permute-done.10.refs_4_ = bf16[384,1024]{1,0:T(8,128)(2,1)S(1)} collective-permute-done((bf16[384,1024]{1,0:T(8,128)(2,1)}, bf16[384,1024]{1,0:T(8,128)(2,1)S(1)}, u32[]{:S(2)}, u32[]{:S(2)}) %collective-permute-start.10) | collective-permute-done | bytes 786464 | tf_op jit(solution)/shard_map/ppermute | solution.py:218
  136.7 0.9 copy-done.11
  137.6 1.3 shard_map.157.refs_8_
  138.9 1.1 copy-done.12
  140.0 0.7 copy-done.16
  140.7 6.0 %shard_map.158.acc_ref = f32[2,384,512]{2,1,0:T(8,128)S(1)} custom-call(s32[2]{0:T(128)S(1)} %copy-done.15, bf16[384,1024]{1,0:T(8,128)(2,1)} %bitcast.4.refs_0_, bf16[384,1024]{1,0:T(8,128)(2,1)} %collective-permute-done.5.a_ref.refs_1_, bf16[384,1024]{1,0:T(8,128)(2,1)} %collective-permute-done.9.refs_2_, bf16[384,1024]{1,0:T(8,128)(2,1)} %bitcast.5.refs_3_, ...), custom_call_target="tpu_custom_call" | custom-call | flops 2415919104 | bytes 4194304 | tf_op jit(solution)/shard_map/pallas_call | solution.py:306
  146.7 6.5 %collective-permute-done.6.far0_ref = bf16[384,1024]{1,0:T(8,128)(2,1)} collective-permute-done((bf16[384,1024]{1,0:T(8,128)(2,1)}, bf16[384,1024]{1,0:T(8,128)(2,1)}, u32[]{:S(2)}, u32[]{:S(2)}) %collective-permute-start.6) | collective-permute-done | bytes 786464 | tf_op jit(solution)/shard_map/ppermute | solution.py:218
  153.2 3.2 %shard_map.159 = bf16[2,384,256]{2,1,0:T(8,128)(2,1)S(1)} custom-call(s32[2]{0:T(128)S(1)} %copy-done.15, bf16[384,1024]{1,0:T(8,128)(2,1)} %collective-permute-done.6.far0_ref, bf16[384,1024]{1,0:T(8,128)(2,1)} %collective-permute-done.8.far1_ref, f32[2,384,512]{2,1,0:T(8,128)S(1)} %shard_map.158.acc_ref, bf16[4096,256]{1,0:T(8,128)(2,1)S(1)} %bitcast.42, ...), custom_call_target="tpu_custom_call" | custom-call | flops 805306368 | bytes 1048576 | tf_op jit(solution)/shard_map/pallas_call | solution.py:318
  156.4 1.6 collective-permute-start.12
  158.0 1.7 collective-permute-start.13
  159.7 1.6 collective-permute-start.14
  161.3 7.7 %collective-permute-done.12.h1_ref = bf16[768,256]{1,0:T(8,128)(2,1)S(1)} collective-permute-done((bf16[768,256]{1,0:T(8,128)(2,1)S(1)}, bf16[768,256]{1,0:T(8,128)(2,1)S(1)}, u32[]{:S(2)}, u32[]{:S(2)}) %collective-permute-start.12) | collective-permute-done | bytes 393248 | tf_op jit(solution)/shard_map/ppermute | solution.py:218
  169.0 7.0 %collective-permute-done.13.h2_ref = bf16[768,256]{1,0:T(8,128)(2,1)S(1)} collective-permute-done((bf16[768,256]{1,0:T(8,128)(2,1)S(1)}, bf16[768,256]{1,0:T(8,128)(2,1)S(1)}, u32[]{:S(2)}, u32[]{:S(2)}) %collective-permute-start.13) | collective-permute-done | bytes 393248 | tf_op jit(solution)/shard_map/ppermute | solution.py:218
  176.1 1.6 collective-permute-done.14.h3_ref
  177.7 4.8 %shard_map.160 = bf16[16,2,48,512]{3,2,1,0:T(8,128)(2,1)} custom-call(s32[2]{0:T(128)S(1)} %copy-done.15, bf16[768,256]{1,0:T(8,128)(2,1)S(1)} %bitcast.51, bf16[768,256]{1,0:T(8,128)(2,1)S(1)} %collective-permute-done.12.h1_ref, bf16[768,256]{1,0:T(8,128)(2,1)S(1)} %collective-permute-done.13.h2_ref, bf16[768,256]{1,0:T(8,128)(2,1)S(1)} %collective-permute-done.14.h3_ref, ...), custom_call_target="tpu_custom_call" | custom-call | flops 1610612736 | bytes 4194304 | tf_op jit(solution)/shard_map/pallas_call | solution.py:365
  182.5 4.5 %all-to-all-start.3 = ((bf16[16,2,48,512]{3,2,1,0:T(8,128)(2,1)}), bf16[16,2,48,512]{3,2,1,0:T(8,128)(2,1)}, u32[]{:S(2)}, u32[]{:S(2)}) async-start(bf16[16,2,48,512]{3,2,1,0:T(8,128)(2,1)} %shard_map.160), calls=%async_computation.3 | async-start | bytes 3145728 | tf_op jit(solution)/shard_map/all_to_all | solution.py:378
  187.0 0.2 all-gather.5.cloned.1.call-start
  187.3 0.0 all-gather.3.cloned.1.call-done.gu_ref.sd_ref
  187.3 1.9 copy-done
  189.2 2.2 copy-done.4
  191.4 5.1 %shard_map.154 = (bf16[4096,128]{1,0:T(8,128)(2,1)}, bf16[4096,128]{1,0:T(8,128)(2,1)}, bf16[512,128]{1,0:T(8,128)(2,1)}, bf16[512,512]{1,0:T(8,128)(2,1)}) custom-call(s32[2]{0:T(128)S(1)} %copy-done.15, bf16[512,4096]{1,0:T(8,128)(2,1)S(1)} %copy-done.4, bf16[1024,1536]{1,0:T(8,128)(2,1)S(1)} %copy-done, bf16[1024,1536]{1,0:T(8,128)(2,1)S(1)} %copy-done), custom_call_target="tpu_custom_call" | custom-call | flops 1073741824 | bytes 4194304 | tf_op jit(solution)/shard_map/pallas_call | solution.py:332
  196.5 0.0 collective-permute-start.1
  196.6 0.0 all-gather.5.cloned.1.call-update
  196.7 1.7 fusion.4
  198.4 0.4 collective-permute-done.1.sd_other_ref
  198.8 3.2 %shard_map.155 = (bf16[256,1024]{1,0:T(8,128)(2,1)S(1)}, bf16[256,1024]{1,0:T(8,128)(2,1)}, bf16[256,1024]{1,0:T(8,128)(2,1)}, bf16[256,1024]{1,0:T(8,128)(2,1)}) custom-call(s32[2]{0:T(128)S(1)} %copy-done.15, bf16[1024,512]{1,0:T(8,128)(2,1)S(1)} %bitcast.46, bf16[1024,512]{1,0:T(8,128)(2,1)} %collective-permute-done.other_ref.w_other_ref, ...), custom_call_target="tpu_custom_call" | custom-call | flops 1073741824 | bytes 4194304 | tf_op jit(solution)/shard_map/pallas_call | solution.py:416
  202.0 0.8 copy-done.13
  202.8 1.1 collective-permute-start.2
  203.9 2.4 collective-permute-start.3
  206.3 0.3 collective-permute-start.4
  206.6 3.0 %all-to-all-done.3 = bf16[16,2,48,512]{3,2,1,0:T(8,128)(2,1)} async-done(((bf16[16,2,48,512]{3,2,1,0:T(8,128)(2,1)}), bf16[16,2,48,512]{3,2,1,0:T(8,128)(2,1)}, u32[]{:S(2)}, u32[]{:S(2)}) %all-to-all-start.3) | async-done | bytes 1572896 | tf_op jit(solution)/shard_map/all_to_all | solution.py:378
  209.6 2.8 %fusion.13 = (bf16[16,1,48,512]{3,2,1,0:T(8,128)(2,1)}, bf16[16,1,48,512]{3,2,1,0:T(8,128)(2,1)}) fusion(bf16[16,2,48,512]{3,2,1,0:T(8,128)(2,1)} %all-to-all-done.3), kind=kLoop, calls=%fused_computation.45 | loop fusion | bytes 3145728 | tf_op jit(solution)/shard_map/slice | solution.py:380
  212.4 1.5 slice_bitcast_fusion
  213.9 7.2 %collective-permute-done.2.p1_ref = bf16[256,1024]{1,0:T(8,128)(2,1)} collective-permute-done((bf16[256,1024]{1,0:T(8,128)(2,1)}, bf16[256,1024]{1,0:T(8,128)(2,1)}, u32[]{:S(2)}, u32[]{:S(2)}) %collective-permute-start.2) | collective-permute-done | bytes 524320 | tf_op jit(solution)/shard_map/ppermute | solution.py:218
  221.1 13.0 %collective-permute-done.3.p2_ref = bf16[256,1024]{1,0:T(8,128)(2,1)} collective-permute-done((bf16[256,1024]{1,0:T(8,128)(2,1)}, bf16[256,1024]{1,0:T(8,128)(2,1)}, u32[]{:S(2)}, u32[]{:S(2)}) %collective-permute-start.3) | collective-permute-done | bytes 524320 | tf_op jit(solution)/shard_map/ppermute | solution.py:218
  234.1 0.2 collective-permute-done.4.p3_ref
  234.3 3.3 %shard_map.156 = (bf16[128,4096]{1,0:T(8,128)(2,1)}, bf16[128,4096]{1,0:T(8,128)(2,1)}) custom-call(s32[2]{0:T(128)S(1)} %copy-done.15, bf16[256,1024]{1,0:T(8,128)(2,1)S(1)} %copy-done.14, bf16[256,1024]{1,0:T(8,128)(2,1)} %collective-permute-done.2.p1_ref, bf16[256,1024]{1,0:T(8,128)(2,1)} %collective-permute-done.3.p2_ref, ...), custom_call_target="tpu_custom_call" | custom-call | flops 1048576 | bytes 4194304 | tf_op jit(solution)/shard_map/pallas_call | solution.py:432
  237.7 1.2 copy-done.10
  238.9 0.7 shard_map.161.base_ref
  239.6 0.4 copy-done.7
  240.0 0.2 copy-done.8
  240.3 0.6 shard_map.162.base_ref
  240.9 2.5 shard_map.163
  (60 shorter events, 0.2 us)
Async XLA Ops:
  18.3 8.4 %copy-start.18 = (f32[256,128]{1,0:T(8,128)S(1)}, f32[256,128]{1,0:T(8,128)}, u32[]{:S(2)}) copy-start(f32[256,128]{1,0:T(8,128)} %param.16) | copy-start | bytes 393220
  18.3 8.4 %copy-start.19 = (f32[256,128]{1,0:T(8,128)S(1)}, f32[256,128]{1,0:T(8,128)}, u32[]{:S(2)}) copy-start(f32[256,128]{1,0:T(8,128)} %param.15) | copy-start | bytes 393220
  18.3 8.4 %copy-start.24 = (f32[256]{0:T(256)S(1)}, f32[256]{0:T(256)}, u32[]{:S(2)}) copy-start(f32[256]{0:T(256)} %param.11) | copy-start | bytes 3076
  18.3 8.6 %copy-start.20 = (f32[64,512]{1,0:T(8,128)S(1)}, f32[64,512]{1,0:T(8,128)}, u32[]{:S(2)}) copy-start(f32[64,512]{1,0:T(8,128)} %param.17) | copy-start | bytes 393220
  18.3 33.9 %all-to-all-start = ((bf16[16,48,1024]{2,1,0:T(8,128)(2,1)}), bf16[16,48,1024]{2,1,0:T(8,128)(2,1)S(1)}, u32[]{:S(2)}, u32[]{:S(2)}) async-start(bf16[16,48,1024]{2,1,0:T(8,128)(2,1)} %bitcast.52), calls=%async_computation | async-start | bytes 3145728 | tf_op jit(solution)/shard_map/all_to_all | solution.py:268
  26.6 160.7 %all-gather.3.cloned.1.call-start = ((), (), s32[]{:S(2)}) async-start(), calls=%async_computation.4 | async-start | bytes 3342336 | tf_op jit(solution)/shard_map/all_gather | solution.py:228
  26.9 0.7 copy-start.17
  53.5 44.5 %all-to-all-start.1 = ((bf16[16,256,256]{2,1,0:T(8,128)(2,1)}), bf16[16,256,256]{2,1,0:T(8,128)(2,1)S(1)}, u32[]{:S(2)}, u32[]{:S(2)}) async-start(bf16[16,256,256]{2,1,0:T(8,128)(2,1)} %pad_maximum_fusion), calls=%async_computation.1 | async-start | bytes 4194304 | tf_op jit(solution)/shard_map/all_to_all | solution.py:279
  59.9 79.0 %copy-start.15 = (s32[2]{0:T(128)S(1)}, s32[2]{0:T(128)}, u32[]{:S(2)}) copy-start(s32[2]{0:T(128)} %pad_add_fusion.place_ref) | copy-start | bytes 28
  98.0 55.2 %copy-start.2 = (bf16[16,256,256]{2,1,0:T(8,128)(2,1)}, bf16[16,256,256]{2,1,0:T(8,128)(2,1)S(1)}, u32[]{:S(2)}) copy-start(bf16[16,256,256]{2,1,0:T(8,128)(2,1)S(1)} %all-to-all-done.1) | copy-start | bytes 6291460
  98.0 40.9 %collective-permute-start.11 = (bf16[4096,256]{1,0:T(8,128)(2,1)S(1)}, bf16[4096,256]{1,0:T(8,128)(2,1)}, u32[]{:S(2)}, u32[]{:S(2)}) collective-permute-start(bf16[4096,256]{1,0:T(8,128)(2,1)S(1)} %bitcast.40), channel_id=1, source_target_pairs={{0,1},{1,0},{2,3},{3,2},{4,5},{5,4},{6,7},{7,6},{8,9},{9,8},{10,11... | collective-permute-start | bytes 6291464 | tf_op jit(solution)/shard_map/ppermute | solution.py:221
  98.0 21.9 %collective-permute-start.5 = (bf16[384,1024]{1,0:T(8,128)(2,1)}, bf16[384,1024]{1,0:T(8,128)(2,1)}, u32[]{:S(2)}, u32[]{:S(2)}) collective-permute-start(bf16[384,1024]{1,0:T(8,128)(2,1)} %bitcast.4.refs_0_), channel_id=1, source_target_pairs={{0,2},{1,3},{2,4},{3,5},{4,6},{5,7},{6,0},{7,1},{8,10},{9,11},{10,... | collective-permute-start | bytes 2359304 | tf_op jit(solution)/shard_map/ppermute | solution.py:218
  99.4 20.7 %collective-permute-start.7 = (bf16[384,1024]{1,0:T(8,128)(2,1)}, bf16[384,1024]{1,0:T(8,128)(2,1)}, u32[]{:S(2)}, u32[]{:S(2)}) collective-permute-start(bf16[384,1024]{1,0:T(8,128)(2,1)} %bitcast.5.refs_3_), channel_id=1, source_target_pairs={{0,6},{1,7},{2,0},{3,1},{4,2},{5,3},{6,4},{7,5},{8,14},{9,15},{10,... | collective-permute-start | bytes 2359304 | tf_op jit(solution)/shard_map/ppermute | solution.py:218
  101.3 36.3 %all-to-all-start.2 = ((bf16[16,64,512]{2,1,0:T(8,128)(2,1)}), bf16[16,64,512]{2,1,0:T(8,128)(2,1)S(1)}, u32[]{:S(2)}, u32[]{:S(2)}) async-start(bf16[16,64,512]{2,1,0:T(8,128)(2,1)} %convert_element_type.27), calls=%async_computation.2 | async-start | bytes 2097152 | tf_op jit(solution)/shard_map/all_to_all | solution.py:281
  104.9 31.8 %collective-permute-start.10 = (bf16[384,1024]{1,0:T(8,128)(2,1)}, bf16[384,1024]{1,0:T(8,128)(2,1)S(1)}, u32[]{:S(2)}, u32[]{:S(2)}) collective-permute-start(bf16[384,1024]{1,0:T(8,128)(2,1)} %bitcast.5.refs_3_), channel_id=1, source_target_pairs={{0,2},{1,3},{2,4},{3,5},{4,6},{5,7},{6,0},{7,1},{8,10},{9,11},{10,... | collective-permute-start | bytes 2359304 | tf_op jit(solution)/shard_map/ppermute | solution.py:218
  105.1 33.8 %collective-permute-start.9 = (bf16[384,1024]{1,0:T(8,128)(2,1)}, bf16[384,1024]{1,0:T(8,128)(2,1)}, u32[]{:S(2)}, u32[]{:S(2)}) collective-permute-start(bf16[384,1024]{1,0:T(8,128)(2,1)} %bitcast.4.refs_0_), channel_id=1, source_target_pairs={{0,6},{1,7},{2,0},{3,1},{4,2},{5,3},{6,4},{7,5},{8,14},{9,15},{10,... | collective-permute-start | bytes 2359304 | tf_op jit(solution)/shard_map/ppermute | solution.py:218
  120.0 33.2 %collective-permute-start.6 = (bf16[384,1024]{1,0:T(8,128)(2,1)}, bf16[384,1024]{1,0:T(8,128)(2,1)}, u32[]{:S(2)}, u32[]{:S(2)}) collective-permute-start(bf16[384,1024]{1,0:T(8,128)(2,1)} %collective-permute-done.5.a_ref.refs_1_), channel_id=1, source_target_pairs={{0,2},{1,3},{2,4},{3,5},{4,6},{5,7},{6,0},{7,1},{8,10},{9,11},{10,... | collective-permute-start | bytes 2359304 | tf_op jit(solution)/shard_map/ppermute | solution.py:218
  120.1 33.1 %collective-permute-start.8 = (bf16[384,1024]{1,0:T(8,128)(2,1)}, bf16[384,1024]{1,0:T(8,128)(2,1)}, u32[]{:S(2)}, u32[]{:S(2)}) collective-permute-start(bf16[384,1024]{1,0:T(8,128)(2,1)} %collective-permute-done.7.b_ref.refs_5_), channel_id=1, source_target_pairs={{0,6},{1,7},{2,0},{3,1},{4,2},{5,3},{6,4},{7,5},{8,14},{9,15},{10,... | collective-permute-start | bytes 2359304 | tf_op jit(solution)/shard_map/ppermute | solution.py:218
  136.7 0.9 copy-start.11
  137.6 40.1 %copy-start.5 = (bf16[16,64,512]{2,1,0:T(8,128)(2,1)}, bf16[16,64,512]{2,1,0:T(8,128)(2,1)S(1)}, u32[]{:S(2)}) copy-start(bf16[16,64,512]{2,1,0:T(8,128)(2,1)S(1)} %all-to-all-done.2) | copy-start | bytes 3145732
  137.6 23.7 %collective-permute-start = (bf16[1024,512]{1,0:T(8,128)(2,1)S(1)}, bf16[1024,512]{1,0:T(8,128)(2,1)}, u32[]{:S(2)}, u32[]{:S(2)}) collective-permute-start(bf16[1024,512]{1,0:T(8,128)(2,1)S(1)} %bitcast.44), channel_id=1, source_target_pairs={{0,1},{1,0},{2,3},{3,2},{4,5},{5,4},{6,7},{7,6},{8,9},{9,8},{10,11... | collective-permute-start | bytes 3145736 | tf_op jit(solution)/shard_map/ppermute | solution.py:221
  138.9 1.1 copy-start.12
  140.0 0.7 copy-start.16
  156.4 12.7 %collective-permute-start.12 = (bf16[768,256]{1,0:T(8,128)(2,1)S(1)}, bf16[768,256]{1,0:T(8,128)(2,1)S(1)}, u32[]{:S(2)}, u32[]{:S(2)}) collective-permute-start(bf16[768,256]{1,0:T(8,128)(2,1)S(1)} %bitcast.48), channel_id=1, source_target_pairs={{0,2},{1,3},{2,4},{3,5},{4,6},{5,7},{6,0},{7,1},{8,10},{9,11},{10,... | collective-permute-start | bytes 1179656 | tf_op jit(solution)/shard_map/ppermute | solution.py:218
  158.0 18.1 %collective-permute-start.13 = (bf16[768,256]{1,0:T(8,128)(2,1)S(1)}, bf16[768,256]{1,0:T(8,128)(2,1)S(1)}, u32[]{:S(2)}, u32[]{:S(2)}) collective-permute-start(bf16[768,256]{1,0:T(8,128)(2,1)S(1)} %bitcast.49), channel_id=1, source_target_pairs={{0,6},{1,7},{2,0},{3,1},{4,2},{5,3},{6,4},{7,5},{8,14},{9,15},{10,... | collective-permute-start | bytes 1179656 | tf_op jit(solution)/shard_map/ppermute | solution.py:218
  159.7 18.0 %collective-permute-start.14 = (bf16[768,256]{1,0:T(8,128)(2,1)S(1)}, bf16[768,256]{1,0:T(8,128)(2,1)S(1)}, u32[]{:S(2)}, u32[]{:S(2)}) collective-permute-start(bf16[768,256]{1,0:T(8,128)(2,1)S(1)} %bitcast.50), channel_id=1, source_target_pairs={{0,4},{1,5},{2,6},{3,7},{4,0},{5,1},{6,2},{7,3},{8,12},{9,13},{10,... | collective-permute-start | bytes 1179656 | tf_op jit(solution)/shard_map/ppermute | solution.py:218
  182.5 4.8 %copy-start.23 = (f32[512,2]{0,1:T(2,128)S(1)}, f32[512,2]{0,1:T(2,128)}, u32[]{:S(2)}) copy-start(f32[512,2]{0,1:T(2,128)} %param.19) | copy-start | bytes 12292
  182.5 27.1 %all-to-all-start.3 = ((bf16[16,2,48,512]{3,2,1,0:T(8,128)(2,1)}), bf16[16,2,48,512]{3,2,1,0:T(8,128)(2,1)}, u32[]{:S(2)}, u32[]{:S(2)}) async-start(bf16[16,2,48,512]{3,2,1,0:T(8,128)(2,1)} %shard_map.160), calls=%async_computation.3 | async-start | bytes 3145728 | tf_op jit(solution)/shard_map/all_to_all | solution.py:378
  187.0 50.6 %all-gather.5.cloned.1.call-start = ((), (), s32[]{:S(2)}) async-start(), calls=%async_computation.5 | async-start | bytes 1179648 | tf_op jit(solution)/shard_map/all_gather | solution.py:360
  187.3 1.9 copy-start
  189.2 2.2 copy-start.4
  191.4 5.2 %copy-start.21 = (s32[512,2]{0,1:T(2,128)S(1)}, s32[512,2]{0,1:T(2,128)}, u32[]{:S(2)}) copy-start(s32[512,2]{0,1:T(2,128)} %param.18) | copy-start | bytes 12292
  191.4 5.3 %copy-start.22 = (s32[2,512]{1,0:T(2,128)S(1)}, s32[2,512]{1,0:T(2,128)}, u32[]{:S(2)}) copy-start(s32[2,512]{1,0:T(2,128)} %get-tuple-element.45) | copy-start | bytes 12292
  191.4 7.4 %copy-start.1 = (bf16[1024,1536]{1,0:T(8,128)(2,1)S(1)}, bf16[1024,1536]{1,0:T(8,128)(2,1)}, u32[]{:S(2)}) copy-start(bf16[1024,1536]{1,0:T(8,128)(2,1)} %all-gather.3.cloned.1.call-done.gu_ref.sd_ref) | copy-start | bytes 9437188
  196.5 2.3 collective-permute-start.1
  196.6 2.2 copy-start.6
  202.0 0.8 copy-start.13
  202.8 18.3 %collective-permute-start.2 = (bf16[256,1024]{1,0:T(8,128)(2,1)}, bf16[256,1024]{1,0:T(8,128)(2,1)}, u32[]{:S(2)}, u32[]{:S(2)}) collective-permute-start(bf16[256,1024]{1,0:T(8,128)(2,1)} %get-tuple-element.38), channel_id=1, source_target_pairs={{0,2},{1,3},{2,4},{3,5},{4,6},{5,7},{6,0},{7,1},{8,10},{9,11},{10,... | collective-permute-start | bytes 1572872 | tf_op jit(solution)/shard_map/ppermute | solution.py:218
  203.9 30.2 %collective-permute-start.3 = (bf16[256,1024]{1,0:T(8,128)(2,1)}, bf16[256,1024]{1,0:T(8,128)(2,1)}, u32[]{:S(2)}, u32[]{:S(2)}) collective-permute-start(bf16[256,1024]{1,0:T(8,128)(2,1)} %get-tuple-element.39), channel_id=1, source_target_pairs={{0,4},{1,5},{2,6},{3,7},{4,0},{5,1},{6,2},{7,3},{8,12},{9,13},{10,... | collective-permute-start | bytes 1572872 | tf_op jit(solution)/shard_map/ppermute | solution.py:218
  206.3 28.0 %collective-permute-start.4 = (bf16[256,1024]{1,0:T(8,128)(2,1)}, bf16[256,1024]{1,0:T(8,128)(2,1)}, u32[]{:S(2)}, u32[]{:S(2)}) collective-permute-start(bf16[256,1024]{1,0:T(8,128)(2,1)} %get-tuple-element.40), channel_id=1, source_target_pairs={{0,6},{1,7},{2,0},{3,1},{4,2},{5,3},{6,4},{7,5},{8,14},{9,15},{10,... | collective-permute-start | bytes 1572872 | tf_op jit(solution)/shard_map/ppermute | solution.py:218
  209.6 2.8 %copy-start.3 = (bf16[16,256,256]{2,1,0:T(8,128)(2,1)S(1)}, bf16[16,256,256]{2,1,0:T(8,128)(2,1)}, u32[]{:S(2)}) copy-start(bf16[16,256,256]{2,1,0:T(8,128)(2,1)} %copy-done.2) | copy-start | bytes 6291460
  212.4 21.9 %copy-start.14 = (bf16[256,1024]{1,0:T(8,128)(2,1)S(1)}, bf16[256,1024]{1,0:T(8,128)(2,1)}, u32[]{:S(2)}) copy-start(bf16[256,1024]{1,0:T(8,128)(2,1)} %copy-done.13) | copy-start | bytes 1572868
  212.4 28.4 %collective-permute-start.15 = (bf16[768,512]{1,0:T(8,128)(2,1)}, bf16[768,512]{1,0:T(8,128)(2,1)}, u32[]{:S(2)}, u32[]{:S(2)}) collective-permute-start(bf16[768,512]{1,0:T(8,128)(2,1)} %bitcast.20), channel_id=1, source_target_pairs={{0,1},{1,0},{2,3},{3,2},{4,5},{5,4},{6,7},{7,6},{8,9},{9,8},{10,11... | collective-permute-start | bytes 2359304 | tf_op jit(solution)/shard_map/ppermute | solution.py:221
  237.7 1.2 copy-start.10
  238.9 1.1 copy-start.7
  238.9 1.4 copy-start.8
  239.6 1.3 copy-start.9
Sparse Core Ops, SparseCore 0:
  30.1 67.4 all-gather.2
  196.8 40.1 all-gather.4

commit v3 on v2

--- a/solution.py
+++ b/solution.py
@@ -28,45 +28,63 @@
     return pltpu.CompilerParams(vmem_limit_bytes=mib << 20)
 
 
-def dispatch_kernel(half, place_ref, route_ref, tok_ref, normed_ref, out_ref, slot_ref, kept, placing):
-    step = pl.program_id(0)
+def dispatch_kernel(half, place_ref, route_ref, tok_ref, normed_ref, out_ref, slot_ref, *scratch):
+    taken, given, kept, placing, in_sem, out_sem = scratch
     chip, core = place_ref[0], place_ref[1]
-    rows, _ = tok_ref.shape
+    steps = in_sem.shape[0]
+    tok_rows = taken.shape[0]
+    rows = tok_rows // steps
     quarter = out_ref.shape[1]
-    spots, tok_rows = placing.shape
+    spots = placing.shape[0]
     experts = spots // half
 
-    @pl.when(step == 0)
-    def _():
-        ids = lax.broadcasted_iota(jnp.int32, (experts, tok_rows), 0)
-        hot = [route_ref[k : k + 1, :] == ids for k in range(route_ref.shape[0])]
-        named = sum(jnp.where(x, 1.0, 0.0) for x in hot).astype(bf16)
-        ahead = lax.broadcasted_iota(jnp.int32, (tok_rows, tok_rows), 0) < (
-            lax.broadcasted_iota(jnp.int32, (tok_rows, tok_rows), 1)
-        )
-        earlier = dot(named, jnp.where(ahead, 1.0, 0.0).astype(bf16))
-        spot = lax.broadcasted_iota(jnp.int32, (spots, tok_rows), 0)
-        total = jnp.zeros((spots, tok_rows), f32)
-        for k, x in enumerate(hot):
-            slot = jnp.sum(jnp.where(x, earlier, 0.0), axis=0, keepdims=True).astype(jnp.int32)
-            slot_ref[k : k + 1, :] = slot
-            local = slot - core * half
-            here = (local >= 0) & (local < half)
-            target = jnp.where(here, route_ref[k : k + 1, :] * half + local, -1)
-            total = total + jnp.where(spot == target, 1.0, 0.0)
-        placing[...] = total.astype(bf16)
-
-    for r in range(0, rows, 16):
-        values = tok_ref[r : r + 16, :].astype(f32)
-        scale = lax.rsqrt(jnp.mean(values * values, axis=1, keepdims=True) + norm_eps)
-        normed_ref[r : r + 16, :] = (values * scale).astype(bf16)
+    def span(step):
+        return pl.ds(step * rows, rows)
+
+    reads = [
+        pltpu.make_async_copy(tok_ref.at[span(i)], taken.at[span(i)], in_sem.at[i])
+        for i in range(steps)
+    ]
+    writes = [
+        pltpu.make_async_copy(given.at[span(i)], normed_ref.at[span(i)], out_sem.at[i])
+        for i in range(steps)
+    ]
+    for read in reads:
+        read.start()
+
+    ids = lax.broadcasted_iota(jnp.int32, (experts, tok_rows), 0)
+    hot = [route_ref[k : k + 1, :] == ids for k in range(route_ref.shape[0])]
+    named = sum(jnp.where(x, 1.0, 0.0) for x in hot).astype(bf16)
+    ahead = lax.broadcasted_iota(jnp.int32, (tok_rows, tok_rows), 0) < (
+        lax.broadcasted_iota(jnp.int32, (tok_rows, tok_rows), 1)
+    )
+    earlier = dot(named, jnp.where(ahead, 1.0, 0.0).astype(bf16))
+    spot = lax.broadcasted_iota(jnp.int32, (spots, tok_rows), 0)
+    total = jnp.zeros((spots, tok_rows), f32)
+    for k, x in enumerate(hot):
+        slot = jnp.sum(jnp.where(x, earlier, 0.0), axis=0, keepdims=True).astype(jnp.int32)
+        slot_ref[k : k + 1, :] = slot
+        local = slot - core * half
+        here = (local >= 0) & (local < half)
+        target = jnp.where(here, route_ref[k : k + 1, :] * half + local, -1)
+        total = total + jnp.where(spot == target, 1.0, 0.0)
+    placing[...] = total.astype(bf16)
+
     at = pl.multiple_of(chip * quarter, quarter)
-    kept[pl.ds(pl.multiple_of(step * rows, rows), rows), :] = normed_ref[:, pl.ds(at, quarter)]
-
-    @pl.when(step == pl.num_programs(0) - 1)
-    def _():
-        for c in range(0, spots, 256):
-            out_ref[c : c + 256, :] = dot(placing[c : c + 256, :], kept[...]).astype(bf16)
+    for i in range(steps):
+        reads[i].wait()
+        for r in range(i * rows, (i + 1) * rows, 16):
+            values = taken[r : r + 16, :].astype(f32)
+            scale = lax.rsqrt(jnp.mean(values * values, axis=1, keepdims=True) + norm_eps)
+            given[r : r + 16, :] = (values * scale).astype(bf16)
+        kept[i * rows : (i + 1) * rows, :] = given[i * rows : (i + 1) * rows, pl.ds(at, quarter)]
+        if i:
+            writes[i - 1].start()
+    for c in range(0, spots, 256):
+        out_ref[c : c + 256, :] = dot(placing[c : c + 256, :], kept[...]).astype(bf16)
+    writes[steps - 1].start()
+    for write in writes:
+        write.wait()
 
 
 def mark_kernel(a_ref, b_ref, out_ref):
@@ -114,42 +132,42 @@
         out_ref[:, part] = total.reshape(out_ref.shape[0], out_ref.shape[2], cols)
 
 
-def shared_kernel(place_ref, x_ref, gu_ref, sd_ref, gate_ref, up_ref, hid_ref, sd_out_ref, acc):
-    step = pl.program_id(0)
-    core = place_ref[1]
-    wide = acc.shape[1]
-    hs = wide // 2
-    deep = gu_ref.shape[0] // 4
-    fold = gu_ref.shape[1] // wide
-    for f in range(4):
-        block = gu_ref[f * deep : (f + 1) * deep, :]
-        weight = jnp.concatenate([block[:, j * wide : (j + 1) * wide] for j in range(fold)], axis=0)
-        size = fold * deep
-        gate_ref[f * size : (f + 1) * size, :] = weight[:, :hs]
-        up_ref[f * size : (f + 1) * size, :] = weight[:, hs:]
-        term = dot(x_ref[:, f * size : (f + 1) * size], weight)
-        first = (step == 0) if f == 0 else False
-        if f == 0:
-            @pl.when(first)
-            def _():
-                acc[...] = term
-
-            @pl.when(step > 0)
-            def _():
-                acc[...] += term
-        else:
-            acc[...] += term
-    rows = sd_out_ref.shape[0]
-    sd_out_ref[...] = sd_ref[pl.ds(pl.multiple_of((1 - core) * rows, rows), rows), :]
-
-    @pl.when(step == pl.num_programs(0) - 1)
-    def _():
-        gate, up = acc[:, :hs], acc[:, hs:]
-        hid_ref[...] = (gate / (1.0 + jnp.exp(-gate)) * up).astype(bf16)
-
-
-def base_kernel(hid_ref, sd_ref, out_ref):
-    out_ref[...] = dot(hid_ref[...], sd_ref[...])
+def shared_kernel(place_ref, x_ref, *refs):
+    groups, outs, (line,) = (refs[:4], refs[4:8]), refs[8:13], refs[13:]
+    gate_ref, up_ref, hid_ref, sd_ref, sd_out_ref = outs
+    core, z, y = place_ref[1], place_ref[2], place_ref[3]
+    hs = gate_ref.shape[1]
+    side, size = groups[0][0].shape[0], line.shape[0] // 16
+    deep = sd_ref.shape[0] // 16
+    for h, out_ref in ((0, gate_ref), (1, up_ref)):
+        for m, ref in enumerate(groups[h]):
+            for n in range(side):
+                dz, dy = (m, n) if h == 0 else (n, m)
+                source = lax.rem(z + side - dz, side) * side + lax.rem(y + side - dy, side)
+                block = ref[n, :size, :]
+                at = pl.ds(pl.multiple_of(source * size, size), size)
+                out_ref[at, :] = block
+                line[at, h * hs : (h + 1) * hs] = block
+                at = pl.ds(pl.multiple_of(source * deep, deep), deep)
+                for c in range(2):
+                    col = (2 * h + c) * hs
+                    sd_ref[at, col : col + hs] = ref[n, size + c * deep : size + (c + 1) * deep, :]
+    for c in range(4):
+        at = pl.ds(pl.multiple_of((2 * c + 1 - core) * hs, hs), hs)
+        sd_out_ref[c * hs : (c + 1) * hs, :] = sd_ref[at, :]
+    total = dot(x_ref[...], line[...])
+    gate, up = total[:, :hs], total[:, hs:]
+    hid_ref[...] = (gate / (1.0 + jnp.exp(-gate)) * up).astype(bf16)
+
+
+def base_kernel(place_ref, own_ref, other_ref, sd_ref, out_ref, line):
+    chip, core = place_ref[0], place_ref[1]
+    hs = own_ref.shape[2]
+    for ref, lane in ((own_ref, core), (other_ref, 1 - core)):
+        for n, shift in enumerate((0, 3, 1, 2)):
+            at = pl.multiple_of((lax.rem(chip + shift, 4) * 2 + lane) * hs, hs)
+            line[:, pl.ds(at, hs)] = ref[n]
+    out_ref[...] = dot(line[...], sd_ref[...])
 
 
 def mix_kernel(weight_ref, got_ref, base_ref, out_ref):
@@ -203,7 +221,6 @@
     t = lax.axis_index("tp")
     chips = tp // 2
     chip, core = t // 2, t % 2
-    place = jnp.stack([chip, core]).astype(jnp.int32)
     tok_rows, width = tokens.shape
     top_count = route_expert.shape[1]
     cap = 3 * tok_rows * top_count // (2 * experts)
@@ -221,40 +238,54 @@
         return lax.ppermute(a, "tp", [(i, i ^ 1) for i in range(tp)])
 
     gain = norm_gain[:, None]
-    shared_gu_local = jnp.concatenate(
-        [(gain * shared_gate_train).astype(bf16), (gain * shared_up_train).astype(bf16)], axis=1
-    )
-    fold = shared_gu_local.shape[0] // deep
-    shared_all = lax.all_gather(
-        jnp.concatenate(
-            [shared_gu_local[j * deep : (j + 1) * deep] for j in range(fold)]
-            + [shared_down_train.astype(bf16)],
-            axis=1,
-        ),
-        "fs",
-        axis=0,
-        tiled=True,
-    )
+    side = 4
+    f = lax.axis_index("fs")
+    place = jnp.stack([chip, core, f // side, f % side]).astype(jnp.int32)
+
+    def along(a, n, y):
+        pairs = []
+        for i in range(experts):
+            z_at, y_at = i // side, i % side
+            to = z_at * side + (y_at + n) % side if y else ((z_at + n) % side) * side + y_at
+            pairs.append((i, to))
+        return lax.ppermute(a, "fs", pairs)
+
+    shared_down_local = shared_down_train.astype(bf16)
+
+    def pack(train, half_at):
+        first_col = half_at * cols // 2
+        return jnp.concatenate(
+            [(gain * train).astype(bf16)]
+            + [shared_down_local[:, first_col + c : first_col + c + hs] for c in (0, hs)],
+            axis=0,
+        )
+
+    packs = (pack(shared_gate_train, 0), pack(shared_up_train, 1))
+    groups = [[p] for p in packs]
+    for n in range(1, side):
+        for h, group in enumerate(groups):
+            group.append(along(packs[h], n, h == 0))
+    groups = [[jnp.stack(g)] for g in groups]
+    for n in range(1, side):
+        for h, group in enumerate(groups):
+            group.append(along(group[0], n, h == 1))
 
     steps = 8
-    block = tok_rows // steps
+    anywhere = pl.BlockSpec(memory_space=pl.ANY)
     normed, outgoing, slots = pl.pallas_call(
         functools.partial(dispatch_kernel, half),
         grid_spec=pltpu.PrefetchScalarGridSpec(
             num_scalar_prefetch=1,
-            grid=(steps,),
-            in_specs=[
-                whole((top_count, tok_rows)),
-                pl.BlockSpec((block, width), lambda i, s: (i, 0)),
-            ],
-            out_specs=[
-                pl.BlockSpec((block, width), lambda i, s: (i, 0)),
-                whole((rows, quarter)),
-                whole((top_count, tok_rows)),
-            ],
+            grid=(1,),
+            in_specs=[whole((top_count, tok_rows)), anywhere],
+            out_specs=[anywhere, whole((rows, quarter)), whole((top_count, tok_rows))],
             scratch_shapes=[
+                pltpu.VMEM((tok_rows, width), bf16),
+                pltpu.VMEM((tok_rows, width), bf16),
                 pltpu.VMEM((tok_rows, quarter), bf16),
                 pltpu.VMEM((rows, tok_rows), bf16),
+                pltpu.SemaphoreType.DMA((steps,)),
+                pltpu.SemaphoreType.DMA((steps,)),
             ],
         ),
         out_shape=[
@@ -291,15 +322,20 @@
     far_top = shift_by(left_top, 1)
     far_bottom = shift_by(right_bottom, -1)
 
+    def marker(a, b):
+        return pl.pallas_call(
+            mark_kernel,
+            grid=(1,),
+            in_specs=[whole(tile)] * 2,
+            out_specs=whole(tile),
+            out_shape=jax.ShapeDtypeStruct(tile, bf16),
+            cost_estimate=cost(1 << 20, 1 << 14),
+        )(a, b)
+
     tile = (16, 128)
-    mark = pl.pallas_call(
-        mark_kernel,
-        grid=(1,),
-        in_specs=[whole(tile)] * 2,
-        out_specs=whole(tile),
-        out_shape=jax.ShapeDtypeStruct(tile, bf16),
-        cost_estimate=cost(1 << 20, 1 << 14),
-    )(left_top, right_bottom)
+    mark = marker(left_top, right_bottom)
+    soon = marker(*packs)
+    mark = marker(mark, soon)
     x_spec = pl.BlockSpec((mid // 2, quarter), lambda i, s: (i, 0))
     acc_spec = pl.BlockSpec((2, mid // 2, 4 * hs), lambda i, s: (0, i, 0))
     w_spec = pl.BlockSpec((quarter, 2 * hs), lambda i, s: (lax.rem(s[0] + chips // 2, chips), 0))
@@ -328,36 +364,37 @@
         cost_estimate=cost(2 * rows * quarter * 4 * hs, 8 * quarter * hs),
     )(place, far_top, far_bottom, acc, gu, gu_other).reshape(rows, 2 * hs)
 
-    sd_spec = pl.BlockSpec((experts * deep, cols), lambda *_: (0, fold * 2 * hs // cols))
-    shared_gate, shared_up, shared_hid, shared_out = pl.pallas_call(
+    shared_gate, shared_up, shared_hid, shared_cols, shared_out = pl.pallas_call(
         shared_kernel,
         grid_spec=pltpu.PrefetchScalarGridSpec(
             num_scalar_prefetch=1,
-            grid=(experts // 4,),
-            in_specs=[
-                pl.BlockSpec((tok_rows, 4 * fold * deep), lambda i, s: (0, i)),
-                pl.BlockSpec((4 * deep, fold * 2 * hs), lambda i, s: (i, 0)),
-                pl.BlockSpec((4 * deep, cols), lambda i, s: (i, fold * 2 * hs // cols)),
+            grid=(1,),
+            in_specs=[whole((tok_rows, width))] + [whole(groups[0][0].shape)] * 8,
+            out_specs=[
+                whole((width, hs)),
+                whole((width, hs)),
+                whole((tok_rows, hs)),
+                whole((experts * deep, cols)),
+                whole((experts * deep // 2, cols)),
             ],
-            out_specs=[
-                pl.BlockSpec((4 * fold * deep, hs), lambda i, s: (i, 0)),
-                pl.BlockSpec((4 * fold * deep, hs), lambda i, s: (i, 0)),
-                whole((tok_rows, hs)),
-                pl.BlockSpec((2 * deep, cols), lambda i, s: (i, 0)),
-            ],
-            scratch_shapes=[pltpu.VMEM((tok_rows, 2 * hs), f32)],
+            scratch_shapes=[pltpu.VMEM((width, 2 * hs), bf16)],
         ),
         out_shape=[
             jax.ShapeDtypeStruct((width, hs), bf16),
             jax.ShapeDtypeStruct((width, hs), bf16),
             jax.ShapeDtypeStruct((tok_rows, hs), bf16),
+            jax.ShapeDtypeStruct((experts * deep, cols), bf16),
             jax.ShapeDtypeStruct((experts * deep // 2, cols), bf16),
         ],
         compiler_params=vmem_limit(36),
         cost_estimate=cost(4 * tok_rows * width * hs, 8 * width * hs),
-    )(place, normed, shared_all, shared_all)
+    )(place, normed, *groups[0], *groups[1])
     shared_other = swap(shared_out)
-    shared_whole = lax.all_gather(shared_hid, "tp", axis=1, tiled=True)
+    units = [shared_hid]
+    for n in (1, -1, 2):
+        units.append(shift_by(shared_hid, n))
+    units = jnp.stack(units)
+    units_other = swap(units)
 
     hid_left = shift_by(hidden, 1)
     hid_right = shift_by(hidden, -1)
@@ -403,13 +440,17 @@
 
     base = pl.pallas_call(
         base_kernel,
-        grid=(1,),
-        in_specs=[whole((tok_rows, experts * deep)), sd_spec],
-        out_specs=whole((tok_rows, cols)),
+        grid_spec=pltpu.PrefetchScalarGridSpec(
+            num_scalar_prefetch=1,
+            grid=(1,),
+            in_specs=[whole((chips, tok_rows, hs))] * 2 + [whole((experts * deep, cols))],
+            out_specs=whole((tok_rows, cols)),
+            scratch_shapes=[pltpu.VMEM((tok_rows, experts * deep), bf16)],
+        ),
         out_shape=jax.ShapeDtypeStruct((tok_rows, cols), f32),
         compiler_params=vmem_limit(24),
         cost_estimate=cost(2 * tok_rows * experts * deep * cols, 4 * tok_rows * rows),
-    )(shared_whole, shared_all)
+    )(place, units, units_other, shared_cols)
     part = mix(mix_own, got_own, base, f32)
     mixed = mix(mix_other, got_other, part, bf16)
 
@@ -419,13 +460,13 @@
             num_scalar_prefetch=1,
             grid=(1,),
             in_specs=[whole((experts * deep, cols))] * 2
-            + [sd_spec, whole((experts * deep // 2, cols))],
+            + [whole((experts * deep, cols)), whole((experts * deep // 2, cols))],
             out_specs=[whole((2 * hs, 2 * cols))] * chips,
         ),
         out_shape=[jax.ShapeDtypeStruct((2 * hs, 2 * cols), bf16)] * chips,
         compiler_params=vmem_limit(36),
         cost_estimate=cost(1 << 30, 8 * hs * width),
-    )(place, down_cols, down_other, shared_all, shared_other)
+    )(place, down_cols, down_other, shared_cols, shared_other)
     pieces = [chunks[0]]
     for n in range(1, chips):
         pieces.append(shift_by(chunks[n], n))

time: 252 us -> 275 us (1.091)
  starting transfers between devices: 39 us -> 56.3 us
  waiting for transfers between devices: 130 us -> 147 us
  between operations: 14.4 us -> 1.07 us
  local copies, waits for them, and re-layouts: 15.8 us -> 19.8 us
  Pallas kernels: 41 us -> 37.9 us
    ppermute x0 -> x12, waiting for transfers between devices: none -> 43.3 us  [along(): return lax.ppermute(a, 'fs', pairs)]
    ppermute x0 -> x12, starting transfers between devices: none -> 15.9 us  [along(): return lax.ppermute(a, 'fs', pairs)]
    ppermute x12 -> x15, waiting for transfers between devices: 68.6 us -> 56.5 us  [shift_by(): return lax.ppermute(a, 'tp', [(i, (i + 2 * n) % tp) for i in range(tp)])]
    all_to_all x1, waiting for transfers between devices: 38.1 us -> 27.3 us  [on_device(): gu = lax.all_to_all(gu_local, 'fs', split_axis=0, concat_axis=0, tiled=True)]
    unnamed x50 -> x70, local copies, waits for them, and re-layouts: 10.2 us -> 15.5 us
    pallas_call x1, Pallas kernels: 10.4 us -> 6.54 us  [on_device(): pl.pallas_call(functools.partial(dispatch_kernel, half), grid_spec=pltpu....]
    pallas_call x2 -> x4, Pallas kernels: 1.99 us -> 5.47 us  [the longest x3 3.94 us: marker(): pl.pallas_call(mark_kernel, grid=(1,), in_specs=[whole(tile)] * 2, out_sp...]
    all_to_all x1, waiting for transfers between devices: 2.99 us -> 0.01 us  [on_device(): lax.all_to_all(sums, 'fs', split_axis=0, concat_axis=0, tiled=True)]
  transfers between devices with their start and end apart: 22 -> 36, of which waited for: 13 -> 16; matrix products, arithmetic and copies ran while one was open for 6% -> 5% of each run, Pallas kernels for 11% -> 11%
where the time goes in v3:
time: 275 us; the launch traced here: 274 us
  waiting for transfers between devices  147 us (53%)
  starting transfers between devices  56.3 us (20%)
  Pallas kernels  37.9 us (14%)
  local copies, waits for them, and re-layouts  19.8 us (7%)
  other arithmetic  11.5 us (4%)
    ppermute x15, waiting for transfers between devices, shift_by(): return lax.ppermute(a, 'tp', [(i, (i + 2 * n) % tp) for i in range(tp)])  56.5 us
    ppermute x12, waiting for transfers between devices, along(): return lax.ppermute(a, 'fs', pairs)  43.3 us
    all_to_all x1, waiting for transfers between devices, on_device(): gu = lax.all_to_all(gu_local, 'fs', split_axis=0, concat_axis=0, tiled=True)  27.3 us
    all_to_all x1, waiting for transfers between devices, on_device(): lax.all_to_all(outgoing.reshape(experts, half, quarter), 'fs', split_axis...  20.1 us
    ppermute x15, starting transfers between devices, shift_by(): return lax.ppermute(a, 'tp', [(i, (i + 2 * n) % tp) for i in range(tp)])  18.9 us
    ppermute x12, starting transfers between devices, along(): return lax.ppermute(a, 'fs', pairs)  15.9 us
    unnamed x70, local copies, waits for them, and re-layouts  15.5 us
    all_to_all x1, starting transfers between devices, on_device(): lax.all_to_all(outgoing.reshape(experts, half, quarter), 'fs', split_axis...  8.17 us
  transfers between devices with their start and end apart: 36, of which 16 were waited for; matrix products, arithmetic and copies ran while one was open for 5% of the time, Pallas kernels for 11%

profile of v3, /device:TPU:0, one launch (start us, length us, event | category | flops | bytes accessed | tf_op | source)
XLA Modules:
  0.0 273.8 jit_solution(8559559000322019272)
XLA Ops:
  1.3 6.5 %shard_map.153 = (bf16[512,4096]{1,0:T(8,128)(2,1)}, bf16[768,1024]{1,0:T(8,128)(2,1)}, s32[2,512]{1,0:T(2,128)}) custom-call(s32[4]{0:T(128)} %pad_add_fusion.place_ref, s32[2,512]{1,0:T(2,128)} %bitcast.83, bf16[512,4096]{1,0:T(8,128)(2,1)} %tok_ref.1), custom_call_target="tpu_custom_call" | custom-call | flops 805306368 | bytes 8388608 | tf_op jit(solution)/shard_map/pallas_call | solution.py:275
  7.9 8.2 %all-to-all-start = ((bf16[16,48,1024]{2,1,0:T(8,128)(2,1)}), bf16[16,48,1024]{2,1,0:T(8,128)(2,1)S(1)}, u32[]{:S(2)}, u32[]{:S(2)}) async-start(bf16[16,48,1024]{2,1,0:T(8,128)(2,1)} %bitcast.72), calls=%async_computation | async-start | bytes 3145728 | tf_op jit(solution)/shard_map/all_to_all | solution.py:299
  16.1 2.8 %multiply_convert_fusion.1 = (bf16[16,256,128]{2,1,0:T(8,128)(2,1)S(1)}, bf16[16,256,128]{2,1,0:T(8,128)(2,1)S(1)}) fusion(f32[16,256,128]{2,1,0:T(8,128)} %param.12, f32[256]{0:T(256)S(1)} %copy-done.34, f32[16,256,128]{2,1,0:T(8,128)} %param.13), kind=kLoop, calls=%fused_computation.2 | loop fusion | flops 2097152 | bytes 6292480 | tf_op jit(solution)/shard_map/convert_element_type | solution.py:304
  18.9 1.6 pad_maximum_fusion
  20.5 20.1 %all-to-all-done = bf16[16,48,1024]{2,1,0:T(8,128)(2,1)S(1)} async-done(((bf16[16,48,1024]{2,1,0:T(8,128)(2,1)}), bf16[16,48,1024]{2,1,0:T(8,128)(2,1)S(1)}, u32[]{:S(2)}, u32[]{:S(2)}) %all-to-all-start) | async-done | bytes 1572896 | tf_op jit(solution)/shard_map/all_to_all | solution.py:299
  40.6 1.3 fusion.9
  41.9 3.7 %all-to-all-start.1 = ((bf16[16,256,256]{2,1,0:T(8,128)(2,1)}), bf16[16,256,256]{2,1,0:T(8,128)(2,1)S(1)}, u32[]{:S(2)}, u32[]{:S(2)}) async-start(bf16[16,256,256]{2,1,0:T(8,128)(2,1)} %pad_maximum_fusion), calls=%async_computation.1 | async-start | bytes 4194304 | tf_op jit(solution)/shard_map/all_to_all | solution.py:310
  45.7 2.8 %convert_element_type.27 = bf16[16,64,512]{2,1,0:T(8,128)(2,1)} convert(f32[16,64,512]{2,1,0:T(8,128)} %param.14) | non-fusion elementwise | flops 524288 | bytes 3145728 | tf_op jit(solution)/shard_map/convert_element_type | solution.py:311
  48.4 27.3 %all-to-all-done.1 = bf16[16,256,256]{2,1,0:T(8,128)(2,1)S(1)} async-done(((bf16[16,256,256]{2,1,0:T(8,128)(2,1)}), bf16[16,256,256]{2,1,0:T(8,128)(2,1)S(1)}, u32[]{:S(2)}, u32[]{:S(2)}) %all-to-all-start.1) | async-done | bytes 2097184 | tf_op jit(solution)/shard_map/all_to_all | solution.py:310
  75.8 1.6 collective-permute-start.17
  77.5 1.8 collective-permute-start.19
  79.3 4.3 %all-to-all-start.2 = ((bf16[16,64,512]{2,1,0:T(8,128)(2,1)}), bf16[16,64,512]{2,1,0:T(8,128)(2,1)}, u32[]{:S(2)}, u32[]{:S(2)}) async-start(bf16[16,64,512]{2,1,0:T(8,128)(2,1)} %convert_element_type.27), calls=%async_computation.2 | async-start | bytes 2097152 | tf_op jit(solution)/shard_map/all_to_all | solution.py:312
  83.7 1.6 collective-permute-start.21
  85.3 1.8 collective-permute-start.7
  87.1 13.1 %collective-permute-done.7 = bf16[384,128]{1,0:T(8,128)(2,1)S(1)} collective-permute-done((bf16[384,128]{1,0:T(8,128)(2,1)S(1)}, bf16[384,128]{1,0:T(8,128)(2,1)S(1)}, u32[]{:S(2)}, u32[]{:S(2)}) %collective-permute-start.7) | collective-permute-done | bytes 98336 | tf_op jit(solution)/shard_map/ppermute | solution.py:251
  100.8 5.6 %collective-permute-done.8 = bf16[384,128]{1,0:T(8,128)(2,1)S(1)} collective-permute-done((bf16[384,128]{1,0:T(8,128)(2,1)S(1)}, bf16[384,128]{1,0:T(8,128)(2,1)S(1)}, u32[]{:S(2)}, u32[]{:S(2)}) %collective-permute-start.8) | collective-permute-done | bytes 98336 | tf_op jit(solution)/shard_map/ppermute | solution.py:251
  106.9 4.1 %collective-permute-done.9 = bf16[384,128]{1,0:T(8,128)(2,1)S(1)} collective-permute-done((bf16[384,128]{1,0:T(8,128)(2,1)S(1)}, bf16[384,128]{1,0:T(8,128)(2,1)S(1)}, u32[]{:S(2)}, u32[]{:S(2)}) %collective-permute-start.9) | collective-permute-done | bytes 98336 | tf_op jit(solution)/shard_map/ppermute | solution.py:251
  111.3 1.1 collective-permute-start.18
  112.5 2.1 collective-permute-start.20
  115.0 0.9 copy-done.12
  116.6 1.3 shard_map.158.b_ref
  117.9 1.0 pad_maximum_fusion.3.refs_4_
  118.9 1.3 shard_map.157.a_ref
  120.3 1.3 shard_map.159.refs_8_
  121.6 11.4 %collective-permute-done.22.refs_4_ = bf16[384,1024]{1,0:T(8,128)(2,1)} collective-permute-done((bf16[384,1024]{1,0:T(8,128)(2,1)}, bf16[384,1024]{1,0:T(8,128)(2,1)}, u32[]{:S(2)}, u32[]{:S(2)}) %collective-permute-start.22) | collective-permute-done | bytes 786464 | tf_op jit(solution)/shard_map/ppermute | solution.py:235
  133.0 2.1 collective-permute-start.1
  135.1 10.8 %collective-permute-done.18.far0_ref = bf16[384,1024]{1,0:T(8,128)(2,1)} collective-permute-done((bf16[384,1024]{1,0:T(8,128)(2,1)S(1)}, bf16[384,1024]{1,0:T(8,128)(2,1)}, u32[]{:S(2)}, u32[]{:S(2)}) %collective-permute-start.18) | collective-permute-done | bytes 786464 | tf_op jit(solution)/shard_map/ppermute | solution.py:235
  145.9 4.1 %collective-permute-start.2 = (bf16[384,128]{1,0:T(8,128)(2,1)S(1)}, bf16[384,128]{1,0:T(8,128)(2,1)S(1)}, u32[]{:S(2)}, u32[]{:S(2)}) collective-permute-start(bf16[384,128]{1,0:T(8,128)(2,1)S(1)} %copy-done.23), channel_id=1, source_target_pairs={{0,16},{8,24},{16,0},{24,8},{32,48},{40,56},{48,32},{56,40},{64,80... | collective-permute-start | bytes 294920 | tf_op jit(solution)/shard_map/ppermute | solution.py:251
  150.0 1.1 collective-permute-start.3
  151.1 1.1 copy-done.2
  152.3 1.1 copy-done.4
  153.4 1.1 copy-done.5
  154.5 1.1 copy-done.13
  156.3 5.3 %shard_map.160.acc_ref = f32[2,384,512]{2,1,0:T(8,128)S(1)} custom-call(s32[4]{0:T(128)S(1)} %copy-done.20, bf16[384,1024]{1,0:T(8,128)(2,1)S(1)} %bitcast.65, bf16[384,1024]{1,0:T(8,128)(2,1)S(1)} %copy-done.2, bf16[384,1024]{1,0:T(8,128)(2,1)S(1)} %copy-done.13, bf16[384,1024]{1,0:T(8,128)(2,1)S(1)} %bitcast.62, ...), custom_call_target="tpu_custom_call" | custom-call | flops 2415919104 | bytes 4194304 | tf_op jit(solution)/shard_map/pallas_call | solution.py:342
  161.7 1.2 collective-permute-start.10
  162.9 3.1 %shard_map.161 = bf16[2,384,256]{2,1,0:T(8,128)(2,1)S(1)} custom-call(s32[4]{0:T(128)S(1)} %copy-done.20, bf16[384,1024]{1,0:T(8,128)(2,1)} %collective-permute-done.18.far0_ref, bf16[384,1024]{1,0:T(8,128)(2,1)} %collective-permute-done.20.far1_ref, f32[2,384,512]{2,1,0:T(8,128)S(1)} %shard_map.160.acc_ref, bf16[4096,256]{1,0:T(8,128)(2,1)S(1)} %bitcast.58, ...), custom_call_target="tpu_custom_call" | custom-call | flops 805306368 | bytes 1048576 | tf_op jit(solution)/shard_map/pallas_call | solution.py:354
  166.1 3.2 %collective-permute-start.25 = (bf16[768,256]{1,0:T(8,128)(2,1)S(1)}, bf16[768,256]{1,0:T(8,128)(2,1)S(1)}, u32[]{:S(2)}, u32[]{:S(2)}) collective-permute-start(bf16[768,256]{1,0:T(8,128)(2,1)S(1)} %bitcast.68), channel_id=1, source_target_pairs={{0,6},{1,7},{2,0},{3,1},{4,2},{5,3},{6,4},{7,5},{8,14},{9,15},{10,... | collective-permute-start | bytes 1179656 | tf_op jit(solution)/shard_map/ppermute | solution.py:235
  169.4 5.7 %collective-permute-done.10.refs_5_ = bf16[4,384,128]{2,1,0:T(8,128)(2,1)S(1)} collective-permute-done((bf16[4,384,128]{2,1,0:T(8,128)(2,1)S(1)}, bf16[4,384,128]{2,1,0:T(8,128)(2,1)S(1)}, u32[]{:S(2)}, u32[]{:S(2)}) %collective-permute-start.10) | collective-permute-done | bytes 393248 | tf_op jit(solution)/shard_map/ppermute | solution.py:251
  175.9 7.0 %collective-permute-done.24.h1_ref = bf16[768,256]{1,0:T(8,128)(2,1)S(1)} collective-permute-done((bf16[768,256]{1,0:T(8,128)(2,1)S(1)}, bf16[768,256]{1,0:T(8,128)(2,1)S(1)}, u32[]{:S(2)}, u32[]{:S(2)}) %collective-permute-start.24) | collective-permute-done | bytes 393248 | tf_op jit(solution)/shard_map/ppermute | solution.py:235
  183.1 3.8 %collective-permute-start.5 = (bf16[4,384,128]{2,1,0:T(8,128)(2,1)S(1)}, bf16[4,384,128]{2,1,0:T(8,128)(2,1)}, u32[]{:S(2)}, u32[]{:S(2)}) collective-permute-start(bf16[4,384,128]{2,1,0:T(8,128)(2,1)S(1)} %pad_maximum_fusion.2.refs_0_), channel_id=1, source_target_pairs={{0,64},{8,72},{16,80},{24,88},{32,96},{40,104},{48,112},{56,120},{... | collective-permute-start | bytes 1179656 | tf_op jit(solution)/shard_map/ppermute | solution.py:251
  187.4 3.9 %shard_map.162 = bf16[16,2,48,512]{3,2,1,0:T(8,128)(2,1)S(1)} custom-call(s32[4]{0:T(128)S(1)} %copy-done.20, bf16[768,256]{1,0:T(8,128)(2,1)S(1)} %bitcast.70, bf16[768,256]{1,0:T(8,128)(2,1)S(1)} %collective-permute-done.24.h1_ref, bf16[768,256]{1,0:T(8,128)(2,1)S(1)} %collective-permute-done.25.h2_ref, ...), custom_call_target="tpu_custom_call" | custom-call | flops 1610612736 | bytes 4194304 | tf_op jit(solution)/shard_map/pallas_call | solution.py:402
  191.3 1.1 copy-done.9
  192.5 4.6 %all-to-all-start.3 = ((bf16[16,2,48,512]{3,2,1,0:T(8,128)(2,1)}), bf16[16,2,48,512]{3,2,1,0:T(8,128)(2,1)}, u32[]{:S(2)}, u32[]{:S(2)}) async-start(bf16[16,2,48,512]{3,2,1,0:T(8,128)(2,1)} %copy-done.9), calls=%async_computation.3 | async-start | bytes 3145728 | tf_op jit(solution)/shard_map/all_to_all | solution.py:415
  197.1 7.6 %collective-permute-done.5.refs_2_ = bf16[4,384,128]{2,1,0:T(8,128)(2,1)} collective-permute-done((bf16[4,384,128]{2,1,0:T(8,128)(2,1)S(1)}, bf16[4,384,128]{2,1,0:T(8,128)(2,1)}, u32[]{:S(2)}, u32[]{:S(2)}) %collective-permute-start.5) | collective-permute-done | bytes 393248 | tf_op jit(solution)/shard_map/ppermute | solution.py:251
  204.6 7.2 %collective-permute-done.6.refs_3_ = bf16[4,384,128]{2,1,0:T(8,128)(2,1)} collective-permute-done((bf16[4,384,128]{2,1,0:T(8,128)(2,1)S(1)}, bf16[4,384,128]{2,1,0:T(8,128)(2,1)}, u32[]{:S(2)}, u32[]{:S(2)}) %collective-permute-start.6) | collective-permute-done | bytes 393248 | tf_op jit(solution)/shard_map/ppermute | solution.py:251
  211.8 2.2 copy-done
  214.0 4.9 %shard_map.154 = (bf16[4096,128]{1,0:T(8,128)(2,1)}, bf16[4096,128]{1,0:T(8,128)(2,1)}, bf16[512,128]{1,0:T(8,128)(2,1)S(1)}, bf16[1024,512]{1,0:T(8,128)(2,1)S(1)}, bf16[512,512]{1,0:T(8,128)(2,1)S(1)}) custom-call(s32[4]{0:T(128)S(1)} %copy-done.20, bf16[512,4096]{1,0:T(8,128)(2,1)S(1)} %copy-done, bf16[4,384,128]{2,1,0:T(8,128)(2,1)S(1)} %pad_maximum_fusion.2.refs_0_, ...), custom_call_target="tpu_custom_call" | custom-call | flops 1073741824 | bytes 4194304 | tf_op jit(solution)/shard_map/pallas_call | solution.py:367
  218.9 1.0 copy-done.10
  219.8 3.2 %collective-permute-start.29 = (bf16[512,128]{1,0:T(8,128)(2,1)S(1)}, bf16[512,128]{1,0:T(8,128)(2,1)S(1)}, u32[]{:S(2)}, u32[]{:S(2)}) collective-permute-start(bf16[512,128]{1,0:T(8,128)(2,1)S(1)} %get-tuple-element.52), channel_id=1, source_target_pairs={{0,6},{1,7},{2,0},{3,1},{4,2},{5,3},{6,4},{7,5},{8,14},{9,15},{10,... | collective-permute-start | bytes 393224 | tf_op jit(solution)/shard_map/ppermute | solution.py:235
  223.7 2.4 collective-permute-done.28
  226.0 3.5 %collective-permute-done.30 = bf16[512,128]{1,0:T(8,128)(2,1)S(1)} collective-permute-done((bf16[512,128]{1,0:T(8,128)(2,1)S(1)}, bf16[512,128]{1,0:T(8,128)(2,1)S(1)}, u32[]{:S(2)}, u32[]{:S(2)}) %collective-permute-start.30) | collective-permute-done | bytes 131104 | tf_op jit(solution)/shard_map/ppermute | solution.py:235
  230.4 1.7 fusion.4
  232.1 0.8 copy-done.16
  232.9 1.0 copy-done.8
  234.0 1.0 copy-done.17
  235.0 1.5 shard_map.163.base_ref
  236.5 3.3 %shard_map.155 = (bf16[256,1024]{1,0:T(8,128)(2,1)S(1)}, bf16[256,1024]{1,0:T(8,128)(2,1)}, bf16[256,1024]{1,0:T(8,128)(2,1)}, bf16[256,1024]{1,0:T(8,128)(2,1)}) custom-call(s32[4]{0:T(128)S(1)} %copy-done.20, bf16[1024,512]{1,0:T(8,128)(2,1)} %bitcast.11.own_ref.w_own_ref, bf16[1024,512]{1,0:T(8,128)(2,1)} %collective-permute-done.other_ref.w_other_ref, ...), custom_call_target="tpu_custom_call" | custom-call | flops 1073741824 | bytes 4194304 | tf_op jit(solution)/shard_map/pallas_call | solution.py:457
  239.9 0.8 copy-done.14
  240.7 2.6 collective-permute-start.15
  243.9 1.5 fusion.8
  245.5 1.5 slice_bitcast_fusion
  247.0 20.3 %collective-permute-done.14.p1_ref = bf16[256,1024]{1,0:T(8,128)(2,1)} collective-permute-done((bf16[256,1024]{1,0:T(8,128)(2,1)}, bf16[256,1024]{1,0:T(8,128)(2,1)}, u32[]{:S(2)}, u32[]{:S(2)}) %collective-permute-start.14) | collective-permute-done | bytes 524320 | tf_op jit(solution)/shard_map/ppermute | solution.py:235
  267.9 3.3 %shard_map.156 = (bf16[128,4096]{1,0:T(8,128)(2,1)}, bf16[128,4096]{1,0:T(8,128)(2,1)}) custom-call(s32[4]{0:T(128)S(1)} %copy-done.20, bf16[256,1024]{1,0:T(8,128)(2,1)S(1)} %copy-done.15, bf16[256,1024]{1,0:T(8,128)(2,1)} %collective-permute-done.14.p1_ref, bf16[256,1024]{1,0:T(8,128)(2,1)} %collective-permute-done.15.p2_ref, ...), custom_call_target="tpu_custom_call" | custom-call | flops 1048576 | bytes 4194304 | tf_op jit(solution)/shard_map/pallas_call | solution.py:473
  272.4 1.4 shard_map.165
  (110 shorter events, 9.5 us)
Async XLA Ops:
  7.9 8.2 %copy-start.34 = (f32[256]{0:T(256)S(1)}, f32[256]{0:T(256)}, u32[]{:S(2)}) copy-start(f32[256]{0:T(256)} %param.11) | copy-start | bytes 3076
  7.9 32.7 %all-to-all-start = ((bf16[16,48,1024]{2,1,0:T(8,128)(2,1)}), bf16[16,48,1024]{2,1,0:T(8,128)(2,1)S(1)}, u32[]{:S(2)}, u32[]{:S(2)}) async-start(bf16[16,48,1024]{2,1,0:T(8,128)(2,1)} %bitcast.72), calls=%async_computation | async-start | bytes 3145728 | tf_op jit(solution)/shard_map/all_to_all | solution.py:299
  41.9 33.9 %all-to-all-start.1 = ((bf16[16,256,256]{2,1,0:T(8,128)(2,1)}), bf16[16,256,256]{2,1,0:T(8,128)(2,1)S(1)}, u32[]{:S(2)}, u32[]{:S(2)}) async-start(bf16[16,256,256]{2,1,0:T(8,128)(2,1)} %pad_maximum_fusion), calls=%async_computation.1 | async-start | bytes 4194304 | tf_op jit(solution)/shard_map/all_to_all | solution.py:310
  45.6 30.1 %copy-start.27 = (f32[64,512]{1,0:T(8,128)S(1)}, f32[64,512]{1,0:T(8,128)}, u32[]{:S(2)}) copy-start(f32[64,512]{1,0:T(8,128)} %param.17) | copy-start | bytes 393220
  45.6 31.7 %copy-start.25 = (f32[256,128]{1,0:T(8,128)S(1)}, f32[256,128]{1,0:T(8,128)}, u32[]{:S(2)}) copy-start(f32[256,128]{1,0:T(8,128)} %param.16) | copy-start | bytes 393220
  45.7 31.7 %copy-start.26 = (f32[256,128]{1,0:T(8,128)S(1)}, f32[256,128]{1,0:T(8,128)}, u32[]{:S(2)}) copy-start(f32[256,128]{1,0:T(8,128)} %param.15) | copy-start | bytes 393220
  75.8 74.3 %collective-permute-start.23 = (bf16[4096,256]{1,0:T(8,128)(2,1)S(1)}, bf16[4096,256]{1,0:T(8,128)(2,1)}, u32[]{:S(2)}, u32[]{:S(2)}) collective-permute-start(bf16[4096,256]{1,0:T(8,128)(2,1)S(1)} %bitcast.56), channel_id=1, source_target_pairs={{0,1},{1,0},{2,3},{3,2},{4,5},{5,4},{6,7},{7,6},{8,9},{9,8},{10,11... | collective-permute-start | bytes 6291464 | tf_op jit(solution)/shard_map/ppermute | solution.py:238
  75.8 35.5 %collective-permute-start.17 = (bf16[384,1024]{1,0:T(8,128)(2,1)}, bf16[384,1024]{1,0:T(8,128)(2,1)S(1)}, u32[]{:S(2)}, u32[]{:S(2)}) collective-permute-start(bf16[384,1024]{1,0:T(8,128)(2,1)} %bitcast.63), channel_id=1, source_target_pairs={{0,2},{1,3},{2,4},{3,5},{4,6},{5,7},{6,0},{7,1},{8,10},{9,11},{10,... | collective-permute-start | bytes 2359304 | tf_op jit(solution)/shard_map/ppermute | solution.py:235
  77.5 35.0 %collective-permute-start.19 = (bf16[384,1024]{1,0:T(8,128)(2,1)}, bf16[384,1024]{1,0:T(8,128)(2,1)}, u32[]{:S(2)}, u32[]{:S(2)}) collective-permute-start(bf16[384,1024]{1,0:T(8,128)(2,1)} %bitcast.60), channel_id=1, source_target_pairs={{0,6},{1,7},{2,0},{3,1},{4,2},{5,3},{6,4},{7,5},{8,14},{9,15},{10,... | collective-permute-start | bytes 2359304 | tf_op jit(solution)/shard_map/ppermute | solution.py:235
  79.3 36.6 %all-to-all-start.2 = ((bf16[16,64,512]{2,1,0:T(8,128)(2,1)}), bf16[16,64,512]{2,1,0:T(8,128)(2,1)}, u32[]{:S(2)}, u32[]{:S(2)}) async-start(bf16[16,64,512]{2,1,0:T(8,128)(2,1)} %convert_element_type.27), calls=%async_computation.2 | async-start | bytes 2097152 | tf_op jit(solution)/shard_map/all_to_all | solution.py:312
  83.7 31.4 %collective-permute-start.21 = (bf16[384,1024]{1,0:T(8,128)(2,1)}, bf16[384,1024]{1,0:T(8,128)(2,1)S(1)}, u32[]{:S(2)}, u32[]{:S(2)}) collective-permute-start(bf16[384,1024]{1,0:T(8,128)(2,1)} %bitcast.64), channel_id=1, source_target_pairs={{0,6},{1,7},{2,0},{3,1},{4,2},{5,3},{6,4},{7,5},{8,14},{9,15},{10,... | collective-permute-start | bytes 2359304 | tf_op jit(solution)/shard_map/ppermute | solution.py:235
  85.3 65.8 %copy-start.20 = (s32[4]{0:T(128)S(1)}, s32[4]{0:T(128)}, u32[]{:S(2)}) copy-start(s32[4]{0:T(128)} %pad_add_fusion.place_ref) | copy-start | bytes 52
  85.3 31.3 %copy-start.24 = (bf16[384,128]{1,0:T(8,128)(2,1)}, bf16[384,128]{1,0:T(8,128)(2,1)S(1)}, u32[]{:S(2)}) copy-start(bf16[384,128]{1,0:T(8,128)(2,1)S(1)} %get-tuple-element.62.b_ref) | copy-start | bytes 294916
  85.3 15.0 %collective-permute-start.7 = (bf16[384,128]{1,0:T(8,128)(2,1)S(1)}, bf16[384,128]{1,0:T(8,128)(2,1)S(1)}, u32[]{:S(2)}, u32[]{:S(2)}) collective-permute-start(bf16[384,128]{1,0:T(8,128)(2,1)S(1)} %get-tuple-element.62.b_ref), channel_id=1, source_target_pairs={{0,32},{8,40},{16,48},{24,56},{32,64},{40,72},{48,80},{56,88},{64,... | collective-permute-start | bytes 294920 | tf_op jit(solution)/shard_map/ppermute | solution.py:251
  100.3 17.6 %copy-start.28 = (bf16[384,128]{1,0:T(8,128)(2,1)}, bf16[384,128]{1,0:T(8,128)(2,1)S(1)}, u32[]{:S(2)}) copy-start(bf16[384,128]{1,0:T(8,128)(2,1)S(1)} %collective-permute-done.7) | copy-start | bytes 294916
  100.3 6.1 %collective-permute-start.8 = (bf16[384,128]{1,0:T(8,128)(2,1)S(1)}, bf16[384,128]{1,0:T(8,128)(2,1)S(1)}, u32[]{:S(2)}, u32[]{:S(2)}) collective-permute-start(bf16[384,128]{1,0:T(8,128)(2,1)S(1)} %get-tuple-element.62.b_ref), channel_id=1, source_target_pairs={{0,64},{8,72},{16,80},{24,88},{32,96},{40,104},{48,112},{56,120},{... | collective-permute-start | bytes 294920 | tf_op jit(solution)/shard_map/ppermute | solution.py:251
  106.4 11.5 %copy-start.29 = (bf16[384,128]{1,0:T(8,128)(2,1)}, bf16[384,128]{1,0:T(8,128)(2,1)S(1)}, u32[]{:S(2)}) copy-start(bf16[384,128]{1,0:T(8,128)(2,1)S(1)} %collective-permute-done.8) | copy-start | bytes 294916
  106.4 4.6 %collective-permute-start.9 = (bf16[384,128]{1,0:T(8,128)(2,1)S(1)}, bf16[384,128]{1,0:T(8,128)(2,1)S(1)}, u32[]{:S(2)}, u32[]{:S(2)}) collective-permute-start(bf16[384,128]{1,0:T(8,128)(2,1)S(1)} %get-tuple-element.62.b_ref), channel_id=1, source_target_pairs={{0,96},{8,104},{16,112},{24,120},{32,0},{40,8},{48,16},{56,24},{64... | collective-permute-start | bytes 294920 | tf_op jit(solution)/shard_map/ppermute | solution.py:251
  111.0 4.9 %copy-start.30 = (bf16[384,128]{1,0:T(8,128)(2,1)}, bf16[384,128]{1,0:T(8,128)(2,1)S(1)}, u32[]{:S(2)}) copy-start(bf16[384,128]{1,0:T(8,128)(2,1)S(1)} %collective-permute-done.9) | copy-start | bytes 294916
  111.0 21.9 %collective-permute-start.22 = (bf16[384,1024]{1,0:T(8,128)(2,1)}, bf16[384,1024]{1,0:T(8,128)(2,1)}, u32[]{:S(2)}, u32[]{:S(2)}) collective-permute-start(bf16[384,1024]{1,0:T(8,128)(2,1)} %bitcast.61), channel_id=1, source_target_pairs={{0,2},{1,3},{2,4},{3,5},{4,6},{5,7},{6,0},{7,1},{8,10},{9,11},{10,... | collective-permute-start | bytes 2359304 | tf_op jit(solution)/shard_map/ppermute | solution.py:235
  111.3 7.6 %copy-start.1 = (bf16[384,1024]{1,0:T(8,128)(2,1)}, bf16[384,1024]{1,0:T(8,128)(2,1)S(1)}, u32[]{:S(2)}) copy-start(bf16[384,1024]{1,0:T(8,128)(2,1)S(1)} %collective-permute-done.17.a_ref.refs_1_) | copy-start | bytes 2359300
  111.3 34.6 %collective-permute-start.18 = (bf16[384,1024]{1,0:T(8,128)(2,1)S(1)}, bf16[384,1024]{1,0:T(8,128)(2,1)}, u32[]{:S(2)}, u32[]{:S(2)}) collective-permute-start(bf16[384,1024]{1,0:T(8,128)(2,1)S(1)} %collective-permute-done.17.a_ref.refs_1_), channel_id=1, source_target_pairs={{0,2},{1,3},{2,4},{3,5},{4,6},{5,7},{6,0},{7,1},{8,10},{9,11},{10,... | collective-permute-start | bytes 2359304 | tf_op jit(solution)/shard_map/ppermute | solution.py:235
  112.5 49.2 %collective-permute-start.20 = (bf16[384,1024]{1,0:T(8,128)(2,1)}, bf16[384,1024]{1,0:T(8,128)(2,1)}, u32[]{:S(2)}, u32[]{:S(2)}) collective-permute-start(bf16[384,1024]{1,0:T(8,128)(2,1)} %collective-permute-done.19.b_ref.refs_5_), channel_id=1, source_target_pairs={{0,6},{1,7},{2,0},{3,1},{4,2},{5,3},{6,4},{7,5},{8,14},{9,15},{10,... | collective-permute-start | bytes 2359304 | tf_op jit(solution)/shard_map/ppermute | solution.py:235
  115.9 60.0 %collective-permute-start = (bf16[1024,512]{1,0:T(8,128)(2,1)}, bf16[1024,512]{1,0:T(8,128)(2,1)}, u32[]{:S(2)}, u32[]{:S(2)}) collective-permute-start(bf16[1024,512]{1,0:T(8,128)(2,1)} %bitcast.11.own_ref.w_own_ref), channel_id=1, source_target_pairs={{0,1},{1,0},{2,3},{3,2},{4,5},{5,4},{6,7},{7,6},{8,9},{9,8},{10,11... | collective-permute-start | bytes 3145736 | tf_op jit(solution)/shard_map/ppermute | solution.py:238
  118.9 14.1 %copy-start.23 = (bf16[384,128]{1,0:T(8,128)(2,1)S(1)}, bf16[384,128]{1,0:T(8,128)(2,1)}, u32[]{:S(2)}) copy-start(bf16[384,128]{1,0:T(8,128)(2,1)} %get-tuple-element.64.a_ref) | copy-start | bytes 294916
  133.0 33.1 %collective-permute-start.1 = (bf16[384,128]{1,0:T(8,128)(2,1)S(1)}, bf16[384,128]{1,0:T(8,128)(2,1)S(1)}, u32[]{:S(2)}, u32[]{:S(2)}) collective-permute-start(bf16[384,128]{1,0:T(8,128)(2,1)S(1)} %copy-done.23), channel_id=1, source_target_pairs={{0,8},{8,16},{16,24},{24,0},{32,40},{40,48},{48,56},{56,32},{64,72... | collective-permute-start | bytes 294920 | tf_op jit(solution)/shard_map/ppermute | solution.py:251
  145.9 20.2 %collective-permute-start.2 = (bf16[384,128]{1,0:T(8,128)(2,1)S(1)}, bf16[384,128]{1,0:T(8,128)(2,1)S(1)}, u32[]{:S(2)}, u32[]{:S(2)}) collective-permute-start(bf16[384,128]{1,0:T(8,128)(2,1)S(1)} %copy-done.23), channel_id=1, source_target_pairs={{0,16},{8,24},{16,0},{24,8},{32,48},{40,56},{48,32},{56,40},{64,80... | collective-permute-start | bytes 294920 | tf_op jit(solution)/shard_map/ppermute | solution.py:251
  150.0 19.3 %collective-permute-start.3 = (bf16[384,128]{1,0:T(8,128)(2,1)S(1)}, bf16[384,128]{1,0:T(8,128)(2,1)S(1)}, u32[]{:S(2)}, u32[]{:S(2)}) collective-permute-start(bf16[384,128]{1,0:T(8,128)(2,1)S(1)} %copy-done.23), channel_id=1, source_target_pairs={{0,24},{8,0},{16,8},{24,16},{32,56},{40,32},{48,40},{56,48},{64,88... | collective-permute-start | bytes 294920 | tf_op jit(solution)/shard_map/ppermute | solution.py:251
  151.1 1.1 copy-start.2
  152.2 1.1 copy-start.4
  153.4 1.1 copy-start.5
  154.5 1.1 copy-start.13
  161.7 13.4 %collective-permute-start.10 = (bf16[4,384,128]{2,1,0:T(8,128)(2,1)S(1)}, bf16[4,384,128]{2,1,0:T(8,128)(2,1)S(1)}, u32[]{:S(2)}, u32[]{:S(2)}) collective-permute-start(bf16[4,384,128]{2,1,0:T(8,128)(2,1)S(1)} %pad_maximum_fusion.3.refs_4_), channel_id=1, source_target_pairs={{0,8},{8,16},{16,24},{24,0},{32,40},{40,48},{48,56},{56,32},{64,72... | collective-permute-start | bytes 1179656 | tf_op jit(solution)/shard_map/ppermute | solution.py:251
  166.0 16.8 %collective-permute-start.24 = (bf16[768,256]{1,0:T(8,128)(2,1)S(1)}, bf16[768,256]{1,0:T(8,128)(2,1)S(1)}, u32[]{:S(2)}, u32[]{:S(2)}) collective-permute-start(bf16[768,256]{1,0:T(8,128)(2,1)S(1)} %bitcast.67), channel_id=1, source_target_pairs={{0,2},{1,3},{2,4},{3,5},{4,6},{5,7},{6,0},{7,1},{8,10},{9,11},{10,... | collective-permute-start | bytes 1179656 | tf_op jit(solution)/shard_map/ppermute | solution.py:235
  166.1 17.0 %collective-permute-start.25 = (bf16[768,256]{1,0:T(8,128)(2,1)S(1)}, bf16[768,256]{1,0:T(8,128)(2,1)S(1)}, u32[]{:S(2)}, u32[]{:S(2)}) collective-permute-start(bf16[768,256]{1,0:T(8,128)(2,1)S(1)} %bitcast.68), channel_id=1, source_target_pairs={{0,6},{1,7},{2,0},{3,1},{4,2},{5,3},{6,4},{7,5},{8,14},{9,15},{10,... | collective-permute-start | bytes 1179656 | tf_op jit(solution)/shard_map/ppermute | solution.py:235
  169.4 17.6 %collective-permute-start.26 = (bf16[768,256]{1,0:T(8,128)(2,1)S(1)}, bf16[768,256]{1,0:T(8,128)(2,1)S(1)}, u32[]{:S(2)}, u32[]{:S(2)}) collective-permute-start(bf16[768,256]{1,0:T(8,128)(2,1)S(1)} %bitcast.69), channel_id=1, source_target_pairs={{0,4},{1,5},{2,6},{3,7},{4,0},{5,1},{6,2},{7,3},{8,12},{9,13},{10,... | collective-permute-start | bytes 1179656 | tf_op jit(solution)/shard_map/ppermute | solution.py:235
  175.9 21.2 %collective-permute-start.11 = (bf16[4,384,128]{2,1,0:T(8,128)(2,1)S(1)}, bf16[4,384,128]{2,1,0:T(8,128)(2,1)}, u32[]{:S(2)}, u32[]{:S(2)}) collective-permute-start(bf16[4,384,128]{2,1,0:T(8,128)(2,1)S(1)} %pad_maximum_fusion.3.refs_4_), channel_id=1, source_target_pairs={{0,16},{8,24},{16,0},{24,8},{32,48},{40,56},{48,32},{56,40},{64,80... | collective-permute-start | bytes 1179656 | tf_op jit(solution)/shard_map/ppermute | solution.py:251
  175.9 21.2 %collective-permute-start.12 = (bf16[4,384,128]{2,1,0:T(8,128)(2,1)S(1)}, bf16[4,384,128]{2,1,0:T(8,128)(2,1)}, u32[]{:S(2)}, u32[]{:S(2)}) collective-permute-start(bf16[4,384,128]{2,1,0:T(8,128)(2,1)S(1)} %pad_maximum_fusion.3.refs_4_), channel_id=1, source_target_pairs={{0,24},{8,0},{16,8},{24,16},{32,56},{40,32},{48,40},{56,48},{64,88... | collective-permute-start | bytes 1179656 | tf_op jit(solution)/shard_map/ppermute | solution.py:251
  182.8 14.2 %collective-permute-start.4 = (bf16[4,384,128]{2,1,0:T(8,128)(2,1)S(1)}, bf16[4,384,128]{2,1,0:T(8,128)(2,1)}, u32[]{:S(2)}, u32[]{:S(2)}) collective-permute-start(bf16[4,384,128]{2,1,0:T(8,128)(2,1)S(1)} %pad_maximum_fusion.2.refs_0_), channel_id=1, source_target_pairs={{0,32},{8,40},{16,48},{24,56},{32,64},{40,72},{48,80},{56,88},{64,... | collective-permute-start | bytes 1179656 | tf_op jit(solution)/shard_map/ppermute | solution.py:251
  183.1 21.5 %collective-permute-start.5 = (bf16[4,384,128]{2,1,0:T(8,128)(2,1)S(1)}, bf16[4,384,128]{2,1,0:T(8,128)(2,1)}, u32[]{:S(2)}, u32[]{:S(2)}) collective-permute-start(bf16[4,384,128]{2,1,0:T(8,128)(2,1)S(1)} %pad_maximum_fusion.2.refs_0_), channel_id=1, source_target_pairs={{0,64},{8,72},{16,80},{24,88},{32,96},{40,104},{48,112},{56,120},{... | collective-permute-start | bytes 1179656 | tf_op jit(solution)/shard_map/ppermute | solution.py:251
  186.9 24.9 %collective-permute-start.6 = (bf16[4,384,128]{2,1,0:T(8,128)(2,1)S(1)}, bf16[4,384,128]{2,1,0:T(8,128)(2,1)}, u32[]{:S(2)}, u32[]{:S(2)}) collective-permute-start(bf16[4,384,128]{2,1,0:T(8,128)(2,1)S(1)} %pad_maximum_fusion.2.refs_0_), channel_id=1, source_target_pairs={{0,96},{8,104},{16,112},{24,120},{32,0},{40,8},{48,16},{56,24},{64... | collective-permute-start | bytes 1179656 | tf_op jit(solution)/shard_map/ppermute | solution.py:251
  191.3 1.1 copy-start.9
  192.5 19.3 %copy-start.19 = (bf16[4,384,128]{2,1,0:T(8,128)(2,1)S(1)}, bf16[4,384,128]{2,1,0:T(8,128)(2,1)}, u32[]{:S(2)}) copy-start(bf16[4,384,128]{2,1,0:T(8,128)(2,1)} %copy-done.18) | copy-start | bytes 1179652
  192.5 51.5 %all-to-all-start.3 = ((bf16[16,2,48,512]{3,2,1,0:T(8,128)(2,1)}), bf16[16,2,48,512]{3,2,1,0:T(8,128)(2,1)}, u32[]{:S(2)}, u32[]{:S(2)}) async-start(bf16[16,2,48,512]{3,2,1,0:T(8,128)(2,1)} %copy-done.9), calls=%async_computation.3 | async-start | bytes 3145728 | tf_op jit(solution)/shard_map/all_to_all | solution.py:415
  211.8 2.2 copy-start
  214.0 9.7 %copy-start.33 = (f32[512,2]{0,1:T(2,128)S(1)}, f32[512,2]{0,1:T(2,128)}, u32[]{:S(2)}) copy-start(f32[512,2]{0,1:T(2,128)} %param.19) | copy-start | bytes 12292
  214.0 16.4 %copy-start.31 = (s32[512,2]{0,1:T(2,128)S(1)}, s32[512,2]{0,1:T(2,128)}, u32[]{:S(2)}) copy-start(s32[512,2]{0,1:T(2,128)} %param.18) | copy-start | bytes 12292
  214.0 16.4 %copy-start.32 = (s32[2,512]{1,0:T(2,128)S(1)}, s32[2,512]{1,0:T(2,128)}, u32[]{:S(2)}) copy-start(s32[2,512]{1,0:T(2,128)} %get-tuple-element.47) | copy-start | bytes 12292
  219.8 9.8 %copy-start.22 = (bf16[512,512]{1,0:T(8,128)(2,1)}, bf16[512,512]{1,0:T(8,128)(2,1)S(1)}, u32[]{:S(2)}) copy-start(bf16[512,512]{1,0:T(8,128)(2,1)S(1)} %get-tuple-element.38) | copy-start | bytes 1572868
  219.8 6.2 %collective-permute-start.28 = (bf16[512,128]{1,0:T(8,128)(2,1)S(1)}, bf16[512,128]{1,0:T(8,128)(2,1)S(1)}, u32[]{:S(2)}, u32[]{:S(2)}) collective-permute-start(bf16[512,128]{1,0:T(8,128)(2,1)S(1)} %get-tuple-element.52), channel_id=1, source_target_pairs={{0,2},{1,3},{2,4},{3,5},{4,6},{5,7},{6,0},{7,1},{8,10},{9,11},{10,... | collective-permute-start | bytes 393224 | tf_op jit(solution)/shard_map/ppermute | solution.py:235
  219.8 6.2 %collective-permute-start.29 = (bf16[512,128]{1,0:T(8,128)(2,1)S(1)}, bf16[512,128]{1,0:T(8,128)(2,1)S(1)}, u32[]{:S(2)}, u32[]{:S(2)}) collective-permute-start(bf16[512,128]{1,0:T(8,128)(2,1)S(1)} %get-tuple-element.52), channel_id=1, source_target_pairs={{0,6},{1,7},{2,0},{3,1},{4,2},{5,3},{6,4},{7,5},{8,14},{9,15},{10,... | collective-permute-start | bytes 393224 | tf_op jit(solution)/shard_map/ppermute | solution.py:235
  223.1 6.5 %collective-permute-start.30 = (bf16[512,128]{1,0:T(8,128)(2,1)S(1)}, bf16[512,128]{1,0:T(8,128)(2,1)S(1)}, u32[]{:S(2)}, u32[]{:S(2)}) collective-permute-start(bf16[512,128]{1,0:T(8,128)(2,1)S(1)} %get-tuple-element.52), channel_id=1, source_target_pairs={{0,4},{1,5},{2,6},{3,7},{4,0},{5,1},{6,2},{7,3},{8,12},{9,13},{10,... | collective-permute-start | bytes 393224 | tf_op jit(solution)/shard_map/ppermute | solution.py:235
  229.6 2.5 copy-start.7
  229.7 2.5 collective-permute-start.31
  229.8 3.1 %copy-start.11 = (bf16[1024,512]{1,0:T(8,128)(2,1)S(1)}, bf16[1024,512]{1,0:T(8,128)(2,1)}, u32[]{:S(2)}) copy-start(bf16[1024,512]{1,0:T(8,128)(2,1)} %copy-done.10) | copy-start | bytes 3145732
  229.8 6.8 %collective-permute-start.13 = (bf16[512,512]{1,0:T(8,128)(2,1)}, bf16[512,512]{1,0:T(8,128)(2,1)S(1)}, u32[]{:S(2)}, u32[]{:S(2)}) collective-permute-start(bf16[512,512]{1,0:T(8,128)(2,1)} %copy-done.22), channel_id=1, source_target_pairs={{0,1},{1,0},{2,3},{3,2},{4,5},{5,4},{6,7},{7,6},{8,9},{9,8},{10,11... | collective-permute-start | bytes 1572872 | tf_op jit(solution)/shard_map/ppermute | solution.py:238
  232.9 1.0 copy-start.8
  240.7 26.6 %collective-permute-start.14 = (bf16[256,1024]{1,0:T(8,128)(2,1)}, bf16[256,1024]{1,0:T(8,128)(2,1)}, u32[]{:S(2)}, u32[]{:S(2)}) collective-permute-start(bf16[256,1024]{1,0:T(8,128)(2,1)} %get-tuple-element.40), channel_id=1, source_target_pairs={{0,2},{1,3},{2,4},{3,5},{4,6},{5,7},{6,0},{7,1},{8,10},{9,11},{10,... | collective-permute-start | bytes 1572872 | tf_op jit(solution)/shard_map/ppermute | solution.py:235
  240.7 26.6 %collective-permute-start.15 = (bf16[256,1024]{1,0:T(8,128)(2,1)}, bf16[256,1024]{1,0:T(8,128)(2,1)}, u32[]{:S(2)}, u32[]{:S(2)}) collective-permute-start(bf16[256,1024]{1,0:T(8,128)(2,1)} %get-tuple-element.41), channel_id=1, source_target_pairs={{0,4},{1,5},{2,6},{3,7},{4,0},{5,1},{6,2},{7,3},{8,12},{9,13},{10,... | collective-permute-start | bytes 1572872 | tf_op jit(solution)/shard_map/ppermute | solution.py:235
  243.3 24.7 %collective-permute-start.16 = (bf16[256,1024]{1,0:T(8,128)(2,1)}, bf16[256,1024]{1,0:T(8,128)(2,1)}, u32[]{:S(2)}, u32[]{:S(2)}) collective-permute-start(bf16[256,1024]{1,0:T(8,128)(2,1)} %get-tuple-element.42), channel_id=1, source_target_pairs={{0,6},{1,7},{2,0},{3,1},{4,2},{5,3},{6,4},{7,5},{8,14},{9,15},{10,... | collective-permute-start | bytes 1572872 | tf_op jit(solution)/shard_map/ppermute | solution.py:235
  245.4 22.5 %copy-start.15 = (bf16[256,1024]{1,0:T(8,128)(2,1)S(1)}, bf16[256,1024]{1,0:T(8,128)(2,1)}, u32[]{:S(2)}) copy-start(bf16[256,1024]{1,0:T(8,128)(2,1)} %copy-done.14) | copy-start | bytes 1572868
  245.4 26.4 %collective-permute-start.27 = (bf16[768,512]{1,0:T(8,128)(2,1)S(1)}, bf16[768,512]{1,0:T(8,128)(2,1)S(1)}, u32[]{:S(2)}, u32[]{:S(2)}) collective-permute-start(bf16[768,512]{1,0:T(8,128)(2,1)S(1)} %bitcast.73), channel_id=1, source_target_pairs={{0,1},{1,0},{2,3},{3,2},{4,5},{5,4},{6,7},{7,6},{8,9},{9,8},{10,11... | collective-permute-start | bytes 2359304 | tf_op jit(solution)/shard_map/ppermute | solution.py:238
  247.0 24.3 %copy-start.3 = (bf16[512,768]{1,0:T(8,128)(2,1)S(1)}, bf16[512,768]{1,0:T(8,128)(2,1)}, u32[]{:S(2)}) copy-start(bf16[512,768]{1,0:T(8,128)(2,1)} %get-tuple-element.51.weight_ref) | copy-start | bytes 2359300
  271.3 1.1 copy-start.6
  (7 other events, 5.9 us)

commit v4 on v3

--- a/solution.py
+++ b/solution.py
@@ -28,14 +28,16 @@
     return pltpu.CompilerParams(vmem_limit_bytes=mib << 20)
 
 
-def dispatch_kernel(half, place_ref, route_ref, tok_ref, normed_ref, out_ref, slot_ref, *scratch):
+def dispatch_kernel(half, place_ref, route_ref, tok_ref, normed_ref, *refs):
+    out_refs, slot_ref, scratch = refs[:2], refs[2], refs[3:]
     taken, given, kept, placing, in_sem, out_sem = scratch
     chip, core = place_ref[0], place_ref[1]
     steps = in_sem.shape[0]
     tok_rows = taken.shape[0]
     rows = tok_rows // steps
-    quarter = out_ref.shape[1]
+    quarter = out_refs[0].shape[1]
     spots = placing.shape[0]
+    few = half // 2
     experts = spots // half
 
     def span(step):
@@ -66,7 +68,9 @@
         slot_ref[k : k + 1, :] = slot
         local = slot - core * half
         here = (local >= 0) & (local < half)
-        target = jnp.where(here, route_ref[k : k + 1, :] * half + local, -1)
+        line = route_ref[k : k + 1, :] * few + local
+        line = jnp.where(local < few, line, line + (spots // 2 - few))
+        target = jnp.where(here, line, -1)
         total = total + jnp.where(spot == target, 1.0, 0.0)
     placing[...] = total.astype(bf16)
 
@@ -80,8 +84,10 @@
         kept[i * rows : (i + 1) * rows, :] = given[i * rows : (i + 1) * rows, pl.ds(at, quarter)]
         if i:
             writes[i - 1].start()
-    for c in range(0, spots, 256):
-        out_ref[c : c + 256, :] = dot(placing[c : c + 256, :], kept[...]).astype(bf16)
+    for c in range(0, spots, 192):
+        part, at = divmod(c, spots // 2)
+        block = dot(placing[c : c + 192, :], kept[...])
+        out_refs[part][at : at + 192, :] = block.astype(bf16)
     writes[steps - 1].start()
     for write in writes:
         write.wait()
@@ -92,31 +98,28 @@
 
 
 def first_kernel(place_ref, *refs):
-    x_refs, (w_own_ref, w_other_ref, _, acc_ref) = refs[:6], refs[6:]
+    x_refs, w_ref, acc_ref = refs[:6], refs[6], refs[-1]
     chip = place_ref[0]
-    quarter, wide = x_refs[0].shape[1], w_own_ref.shape[1]
-    chips = w_own_ref.shape[0] // quarter
+    quarter = x_refs[0].shape[1]
+    chips = w_ref.shape[0] // quarter
     for part in range(2):
-        for half, w_ref in ((0, w_own_ref), (1, w_other_ref)):
-            total = None
-            for x_ref, shift in zip(x_refs[3 * part : 3 * part + 3], (0, chips - 1, 1)):
-                at = pl.multiple_of(lax.rem(chip + shift, chips) * quarter, quarter)
-                term = dot(x_ref[...], w_ref[pl.ds(at, quarter), :])
-                total = term if total is None else total + term
-            acc_ref[part, :, half * wide : (half + 1) * wide] = total
-
-
-def hidden_kernel(place_ref, far0_ref, far1_ref, acc_ref, w_own_ref, w_other_ref, out_ref):
+        total = None
+        for x_ref, shift in zip(x_refs[3 * part : 3 * part + 3], (0, chips - 1, 1)):
+            at = pl.multiple_of(lax.rem(chip + shift, chips) * quarter, quarter)
+            term = dot(x_ref[...], w_ref[pl.ds(at, quarter), :])
+            total = term if total is None else total + term
+        acc_ref[part] = total
+
+
+def hidden_kernel(place_ref, far0_ref, far1_ref, acc0_ref, acc1_ref, w0_ref, w1_ref, out_ref):
     core = place_ref[1]
-    wide = w_own_ref.shape[1]
-    hs = wide // 2
-    for part, far_ref in enumerate((far0_ref, far1_ref)):
-        for half, w_ref, slot in ((0, w_own_ref, core), (1, w_other_ref, 1 - core)):
-            total = acc_ref[part, :, half * wide : (half + 1) * wide]
-            total = total + dot(far_ref[...], w_ref[...])
+    hs = w0_ref.shape[1] // 2
+    for acc_ref, w_ref, slot in ((acc0_ref, w0_ref, core), (acc1_ref, w1_ref, 1 - core)):
+        at = pl.ds(pl.multiple_of(slot * hs, hs), hs)
+        for part, far_ref in enumerate((far0_ref, far1_ref)):
+            total = acc_ref[part] + dot(far_ref[...], w_ref[...])
             gate, up = total[:, :hs], total[:, hs:]
-            value = (gate / (1.0 + jnp.exp(-gate)) * up).astype(bf16)
-            out_ref[part, :, pl.ds(pl.multiple_of(slot * hs, hs), hs)] = value
+            out_ref[part, :, at] = (gate / (1.0 + jnp.exp(-gate)) * up).astype(bf16)
 
 
 def down_kernel(place_ref, h0_ref, h1_ref, h2_ref, h3_ref, w_own_ref, w_other_ref, out_ref, line):
@@ -128,8 +131,10 @@
         at = pl.multiple_of(lax.rem(chip + shift, chips) * depth, depth)
         line[:, pl.ds(at, depth)] = h_ref[...]
     for part, w_ref in enumerate((w_own_ref, w_other_ref)):
-        total = dot(line[...], w_ref[...]).astype(bf16)
-        out_ref[:, part] = total.reshape(out_ref.shape[0], out_ref.shape[2], cols)
+        total = dot(line[...], w_ref[...])
+        total = total.reshape(2, out_ref.shape[0], out_ref.shape[3], cols).astype(bf16)
+        out_ref[:, part, 0] = total[0]
+        out_ref[:, part, 1] = total[1]
 
 
 def shared_kernel(place_ref, x_ref, *refs):
@@ -171,7 +176,8 @@
 
 
 def mix_kernel(weight_ref, got_ref, base_ref, out_ref):
-    out_ref[...] = (base_ref[...] + dot(weight_ref[...], got_ref[...])).astype(out_ref.dtype)
+    got = got_ref[...].reshape(weight_ref.shape[1], out_ref.shape[1])
+    out_ref[...] = (base_ref[...] + dot(weight_ref[...], got)).astype(out_ref.dtype)
 
 
 def chunk_kernel(place_ref, own_ref, other_ref, sd_ref, sd_other_ref, *out_refs):
@@ -272,13 +278,18 @@
 
     steps = 8
     anywhere = pl.BlockSpec(memory_space=pl.ANY)
-    normed, outgoing, slots = pl.pallas_call(
+    normed, out_top, out_bottom, slots = pl.pallas_call(
         functools.partial(dispatch_kernel, half),
         grid_spec=pltpu.PrefetchScalarGridSpec(
             num_scalar_prefetch=1,
             grid=(1,),
             in_specs=[whole((top_count, tok_rows)), anywhere],
-            out_specs=[anywhere, whole((rows, quarter)), whole((top_count, tok_rows))],
+            out_specs=[
+                anywhere,
+                whole((rows // 2, quarter)),
+                whole((rows // 2, quarter)),
+                whole((top_count, tok_rows)),
+            ],
             scratch_shapes=[
                 pltpu.VMEM((tok_rows, width), bf16),
                 pltpu.VMEM((tok_rows, width), bf16),
@@ -290,23 +301,27 @@
         ),
         out_shape=[
             jax.ShapeDtypeStruct((tok_rows, width), bf16),
-            jax.ShapeDtypeStruct((rows, quarter), bf16),
+            jax.ShapeDtypeStruct((rows // 2, quarter), bf16),
+            jax.ShapeDtypeStruct((rows // 2, quarter), bf16),
             jax.ShapeDtypeStruct((top_count, tok_rows), jnp.int32),
         ],
         compiler_params=vmem_limit(60),
         cost_estimate=cost(2 * rows * tok_rows * quarter, 4 * tok_rows * width),
     )(place, route_expert.T, tokens)
-    arriving = lax.all_to_all(
-        outgoing.reshape(experts, half, quarter), "fs", split_axis=0, concat_axis=0, tiled=True
-    )
+    mid = rows // 2
+
+    def sent(a):
+        a = a.reshape(experts, half // 2, quarter)
+        return lax.all_to_all(a, "fs", split_axis=0, concat_axis=0, tiled=True).reshape(mid, quarter)
+
+    top = sent(out_top)
+    out_bottom, top = together(out_bottom, top)
+    bottom = sent(out_bottom)
 
     gu_local = jnp.concatenate(
         [(gain[None] * gate_train).astype(bf16), (gain[None] * up_train).astype(bf16)], axis=2
     )
-    mid = rows // 2
-    arriving = arriving.reshape(rows, quarter)
-    top, bottom = together(arriving[:mid], arriving[mid:])
-    gu_local, top, bottom = together(gu_local, top, bottom)
+    gu_local, bottom = together(gu_local, bottom)
     gu = lax.all_to_all(gu_local, "fs", split_axis=0, concat_axis=0, tiled=True)
     down_local, gu = together(down_train.astype(bf16), gu)
     down_cols = lax.all_to_all(down_local, "fs", split_axis=0, concat_axis=0, tiled=True)
@@ -337,32 +352,40 @@
     soon = marker(*packs)
     mark = marker(mark, soon)
     x_spec = pl.BlockSpec((mid // 2, quarter), lambda i, s: (i, 0))
-    acc_spec = pl.BlockSpec((2, mid // 2, 4 * hs), lambda i, s: (0, i, 0))
+    acc_spec = pl.BlockSpec((2, mid // 2, 2 * hs), lambda i, s: (0, i, 0))
     w_spec = pl.BlockSpec((quarter, 2 * hs), lambda i, s: (lax.rem(s[0] + chips // 2, chips), 0))
-    acc = pl.pallas_call(
-        first_kernel,
-        grid_spec=pltpu.PrefetchScalarGridSpec(
-            num_scalar_prefetch=1,
-            grid=(2,),
-            in_specs=[x_spec] * 6 + [whole((width, 2 * hs))] * 2 + [whole(tile)],
-            out_specs=acc_spec,
-        ),
-        out_shape=jax.ShapeDtypeStruct((2, mid, 4 * hs), f32),
-        compiler_params=vmem_limit(32),
-        cost_estimate=cost(2 * rows * 3 * quarter * 4 * hs, 8 * width * hs),
-    )(place, top, left_top, right_top, bottom, left_bottom, right_bottom, gu, gu_other, mark)
+
+    def first(weight, last):
+        blocks = (top, left_top, right_top, bottom, left_bottom, right_bottom)
+        return pl.pallas_call(
+            first_kernel,
+            grid_spec=pltpu.PrefetchScalarGridSpec(
+                num_scalar_prefetch=1,
+                grid=(2,),
+                in_specs=[x_spec] * 6 + [whole((width, 2 * hs)), whole(tile)],
+                out_specs=acc_spec,
+            ),
+            out_shape=jax.ShapeDtypeStruct((2, mid, 2 * hs), f32),
+            compiler_params=vmem_limit(32),
+            cost_estimate=cost(2 * rows * 3 * quarter * 2 * hs, 4 * width * hs),
+        )(place, *blocks, weight, last)
+
+    acc_own = first(gu, mark)
+    acc_other = first(gu_other, mark)
     hidden = pl.pallas_call(
         hidden_kernel,
         grid_spec=pltpu.PrefetchScalarGridSpec(
             num_scalar_prefetch=1,
             grid=(1,),
-            in_specs=[whole((mid, quarter))] * 2 + [whole((2, mid, 4 * hs)), w_spec, w_spec],
+            in_specs=[whole((mid, quarter))] * 2
+            + [whole((2, mid, 2 * hs))] * 2
+            + [w_spec, w_spec],
             out_specs=whole((2, mid, 2 * hs)),
         ),
         out_shape=jax.ShapeDtypeStruct((2, mid, 2 * hs), bf16),
         compiler_params=vmem_limit(32),
         cost_estimate=cost(2 * rows * quarter * 4 * hs, 8 * quarter * hs),
-    )(place, far_top, far_bottom, acc, gu, gu_other).reshape(rows, 2 * hs)
+    )(place, far_top, far_bottom, acc_own, acc_other, gu, gu_other).reshape(rows, 2 * hs)
 
     shared_gate, shared_up, shared_hid, shared_cols, shared_out = pl.pallas_call(
         shared_kernel,
@@ -405,16 +428,16 @@
             num_scalar_prefetch=1,
             grid=(1,),
             in_specs=[whole((rows, 2 * hs))] * 4 + [whole((experts * deep, cols))] * 2,
-            out_specs=whole((experts, 2, half, cols)),
+            out_specs=whole((experts, 2, 2, half // 2, cols)),
             scratch_shapes=[pltpu.VMEM((rows, experts * deep), bf16)],
         ),
-        out_shape=jax.ShapeDtypeStruct((experts, 2, half, cols), bf16),
-        compiler_params=vmem_limit(40),
+        out_shape=jax.ShapeDtypeStruct((experts, 2, 2, half // 2, cols), bf16),
+        compiler_params=vmem_limit(60),
         cost_estimate=cost(4 * rows * experts * deep * cols, 8 * experts * deep * cols),
     )(place, hidden, hid_left, hid_right, hid_far, down_cols, down_other)
+    sums = sums.reshape(experts, 2, half, cols)
     returned = lax.all_to_all(sums, "fs", split_axis=0, concat_axis=0, tiled=True)
     got_other = swap(returned[:, 1].reshape(rows, cols))
-    got_own = returned[:, 0].reshape(rows, cols)
 
     spots = jnp.arange(rows, dtype=jnp.int32)[None, :]
 
@@ -433,6 +456,13 @@
     def mix(weights, got, base, dtype):
         return pl.pallas_call(
             mix_kernel,
+            grid=(1,),
+            in_specs=[
+                whole((tok_rows, rows)),
+                whole((experts, 1, half, cols)) if got.ndim == 4 else whole((rows, cols)),
+                whole((tok_rows, cols)),
+            ],
+            out_specs=whole((tok_rows, cols)),
             out_shape=jax.ShapeDtypeStruct((tok_rows, cols), dtype),
             compiler_params=vmem_limit(24),
             cost_estimate=cost(2 * tok_rows * rows * cols, 4 * tok_rows * rows),
@@ -451,7 +481,7 @@
         compiler_params=vmem_limit(24),
         cost_estimate=cost(2 * tok_rows * experts * deep * cols, 4 * tok_rows * rows),
     )(place, units, units_other, shared_cols)
-    part = mix(mix_own, got_own, base, f32)
+    part = mix(mix_own, returned, base, f32)
     mixed = mix(mix_other, got_other, part, bf16)
 
     chunks = pl.pallas_call(
@@ -509,6 +539,7 @@
         P("fs", None),
     )
 
+
     return jax.shard_map(
         on_device,
         mesh=mesh,

time: 275 us -> 274 us (level)
  waiting for transfers between devices: 147 us -> 120 us
  blocking collectives: 0 us -> 22.5 us
  Pallas kernels: 37.9 us -> 43.2 us
  local copies, waits for them, and re-layouts: 19.8 us -> 15.8 us
    all_to_all x0 -> x1, blocking collectives: none -> 22.5 us  [sent(): lax.all_to_all(a, 'fs', split_axis=0, concat_axis=0, tiled=True)]
    all_to_all x1, waiting for transfers between devices: 20.1 us -> 9.17 us  [sent(): lax.all_to_all(a, 'fs', split_axis=0, concat_axis=0, tiled=True)]
    ppermute x15, waiting for transfers between devices: 56.5 us -> 48.7 us  [shift_by(): return lax.ppermute(a, 'tp', [(i, (i + 2 * n) % tp) for i in range(tp)])]
    ppermute x12, waiting for transfers between devices: 43.3 us -> 36.3 us  [along(): return lax.ppermute(a, 'fs', pairs)]
    ppermute x15, starting transfers between devices: 18.9 us -> 24.5 us  [shift_by(): return lax.ppermute(a, 'tp', [(i, (i + 2 * n) % tp) for i in range(tp)])]
    all_to_all x1, starting transfers between devices: 8.17 us -> 3.61 us  [sent(): lax.all_to_all(a, 'fs', split_axis=0, concat_axis=0, tiled=True)]
    pallas_call x3 -> x4, Pallas kernels: 7.25 us -> 10.9 us  [the longest x2 7.79 us: first(): pl.pallas_call(first_kernel, grid_spec=pltpu.PrefetchScalarGridSpec(num_s...]
    unnamed x70 -> x78, local copies, waits for them, and re-layouts: 15.5 us -> 13.1 us
  transfers between devices with their start and end apart: 36 -> 36, of which waited for: 16 -> 17; matrix products, arithmetic and copies ran while one was open for 5% -> 5% of each run, Pallas kernels for 11% -> 13%
where the time goes in v4:
time: 274 us; the launch traced here: 272 us
  waiting for transfers between devices  120 us (44%)
  starting transfers between devices  57.4 us (21%)
  Pallas kernels  43.2 us (16%)
  blocking collectives  22.5 us (8%)
  local copies, waits for them, and re-layouts  15.8 us (6%)
  other arithmetic  12.3 us (4%)
    ppermute x15, waiting for transfers between devices, shift_by(): return lax.ppermute(a, 'tp', [(i, (i + 2 * n) % tp) for i in range(tp)])  48.7 us
    ppermute x12, waiting for transfers between devices, along(): return lax.ppermute(a, 'fs', pairs)  36.3 us
    all_to_all x1, waiting for transfers between devices, on_device(): gu = lax.all_to_all(gu_local, 'fs', split_axis=0, concat_axis=0, tiled=True)  25.9 us
    ppermute x15, starting transfers between devices, shift_by(): return lax.ppermute(a, 'tp', [(i, (i + 2 * n) % tp) for i in range(tp)])  24.5 us
    all_to_all x1, blocking collectives, sent(): lax.all_to_all(a, 'fs', split_axis=0, concat_axis=0, tiled=True)  22.5 us
    ppermute x12, starting transfers between devices, along(): return lax.ppermute(a, 'fs', pairs)  15.9 us
    unnamed x78, local copies, waits for them, and re-layouts  13.1 us
    all_to_all x1, waiting for transfers between devices, sent(): lax.all_to_all(a, 'fs', split_axis=0, concat_axis=0, tiled=True)  9.17 us
  transfers between devices with their start and end apart: 36, of which 17 were waited for; matrix products, arithmetic and copies ran while one was open for 5% of the time, Pallas kernels for 13%

profile of v4, /device:TPU:0, one launch (start us, length us, event | category | flops | bytes accessed | tf_op | source)
XLA Modules:
  0.0 272.3 jit_solution(13111447339845990010)
XLA Ops:
  1.3 6.4 %shard_map.153 = (bf16[512,4096]{1,0:T(8,128)(2,1)}, bf16[384,1024]{1,0:T(8,128)(2,1)}, bf16[384,1024]{1,0:T(8,128)(2,1)}, s32[2,512]{1,0:T(2,128)}) custom-call(s32[4]{0:T(128)} %pad_add_fusion.place_ref, s32[2,512]{1,0:T(2,128)} %bitcast.87, bf16[512,4096]{1,0:T(8,128)(2,1)} %tok_ref.1), custom_call_target="tpu_custom_call" | custom-call | flops 805306368 | bytes 8388608 | tf_op jit(solution)/shard_map/pallas_call | solution.py:281
  7.7 22.5 %all_to_all.25 = bf16[16,24,1024]{2,1,0:T(8,128)(2,1)S(1)} all-to-all(bf16[16,24,1024]{2,1,0:T(8,128)(2,1)} %bitcast.77), channel_id=1, replica_groups=mesh['fs'=16,'tp'=8] {'fs'}, dimensions={0} | all-to-all | bytes 1572864 | tf_op jit(solution)/shard_map/all_to_all | solution.py:315
  30.3 3.6 %all-to-all-start.1 = ((bf16[16,24,1024]{2,1,0:T(8,128)(2,1)}), bf16[16,24,1024]{2,1,0:T(8,128)(2,1)S(1)}, u32[]{:S(2)}, u32[]{:S(2)}) async-start(bf16[16,24,1024]{2,1,0:T(8,128)(2,1)} %bitcast.76), calls=%async_computation.1 | async-start | bytes 1572864 | tf_op jit(solution)/shard_map/all_to_all | solution.py:315
  33.9 2.7 multiply_convert_fusion.1
  36.6 1.7 pad_maximum_fusion
  38.2 9.2 %all-to-all-done.1 = bf16[16,24,1024]{2,1,0:T(8,128)(2,1)S(1)} async-done(((bf16[16,24,1024]{2,1,0:T(8,128)(2,1)}), bf16[16,24,1024]{2,1,0:T(8,128)(2,1)S(1)}, u32[]{:S(2)}, u32[]{:S(2)}) %all-to-all-start.1) | async-done | bytes 786464 | tf_op jit(solution)/shard_map/all_to_all | solution.py:315
  47.4 0.9 copy-done
  48.3 3.7 %all-to-all-start.2 = ((bf16[16,256,256]{2,1,0:T(8,128)(2,1)}), bf16[16,256,256]{2,1,0:T(8,128)(2,1)S(1)}, u32[]{:S(2)}, u32[]{:S(2)}) async-start(bf16[16,256,256]{2,1,0:T(8,128)(2,1)} %pad_maximum_fusion), calls=%async_computation.2 | async-start | bytes 4194304 | tf_op jit(solution)/shard_map/all_to_all | solution.py:325
  52.0 2.7 %convert_element_type.27 = bf16[16,64,512]{2,1,0:T(8,128)(2,1)} convert(f32[16,64,512]{2,1,0:T(8,128)} %param.14) | non-fusion elementwise | flops 524288 | bytes 3145728 | tf_op jit(solution)/shard_map/convert_element_type | solution.py:326
  54.8 25.9 %all-to-all-done.2 = bf16[16,256,256]{2,1,0:T(8,128)(2,1)S(1)} async-done(((bf16[16,256,256]{2,1,0:T(8,128)(2,1)}), bf16[16,256,256]{2,1,0:T(8,128)(2,1)S(1)}, u32[]{:S(2)}, u32[]{:S(2)}) %all-to-all-start.2) | async-done | bytes 2097184 | tf_op jit(solution)/shard_map/all_to_all | solution.py:325
  80.7 1.5 collective-permute-start.17
  82.3 0.9 convert_element_type.31
  83.2 1.8 collective-permute-start.19
  85.0 4.3 %all-to-all-start.3 = ((bf16[16,64,512]{2,1,0:T(8,128)(2,1)}), bf16[16,64,512]{2,1,0:T(8,128)(2,1)}, u32[]{:S(2)}, u32[]{:S(2)}) async-start(bf16[16,64,512]{2,1,0:T(8,128)(2,1)} %convert_element_type.27), calls=%async_computation.3 | async-start | bytes 2097152 | tf_op jit(solution)/shard_map/all_to_all | solution.py:327
  89.4 1.6 collective-permute-start.21
  91.0 1.8 collective-permute-start.7
  92.9 13.1 %collective-permute-done.7 = bf16[384,128]{1,0:T(8,128)(2,1)S(1)} collective-permute-done((bf16[384,128]{1,0:T(8,128)(2,1)S(1)}, bf16[384,128]{1,0:T(8,128)(2,1)S(1)}, u32[]{:S(2)}, u32[]{:S(2)}) %collective-permute-start.7) | collective-permute-done | bytes 98336 | tf_op jit(solution)/shard_map/ppermute | solution.py:257
  106.5 5.6 %collective-permute-done.8 = bf16[384,128]{1,0:T(8,128)(2,1)S(1)} collective-permute-done((bf16[384,128]{1,0:T(8,128)(2,1)S(1)}, bf16[384,128]{1,0:T(8,128)(2,1)S(1)}, u32[]{:S(2)}, u32[]{:S(2)}) %collective-permute-start.8) | collective-permute-done | bytes 98336 | tf_op jit(solution)/shard_map/ppermute | solution.py:257
  112.6 4.1 %collective-permute-done.9 = bf16[384,128]{1,0:T(8,128)(2,1)S(1)} collective-permute-done((bf16[384,128]{1,0:T(8,128)(2,1)S(1)}, bf16[384,128]{1,0:T(8,128)(2,1)S(1)}, u32[]{:S(2)}, u32[]{:S(2)}) %collective-permute-start.9) | collective-permute-done | bytes 98336 | tf_op jit(solution)/shard_map/ppermute | solution.py:257
  117.0 1.1 collective-permute-start.18
  118.2 2.1 collective-permute-start.20
  122.3 1.3 shard_map.158.b_ref
  123.6 1.0 pad_maximum_fusion.3.refs_4_
  124.6 1.3 shard_map.157.a_ref
  125.9 1.3 shard_map.159.refs_7_
  127.2 11.5 %collective-permute-done.22.refs_4_ = bf16[384,1024]{1,0:T(8,128)(2,1)} collective-permute-done((bf16[384,1024]{1,0:T(8,128)(2,1)}, bf16[384,1024]{1,0:T(8,128)(2,1)}, u32[]{:S(2)}, u32[]{:S(2)}) %collective-permute-start.22) | collective-permute-done | bytes 786464 | tf_op jit(solution)/shard_map/ppermute | solution.py:241
  138.7 2.1 collective-permute-start.1
  140.8 1.1 copy-done.1
  141.9 1.1 copy-done.5
  143.8 3.5 %shard_map.160.acc0_ref = f32[2,384,256]{2,1,0:T(8,128)S(1)} custom-call(s32[4]{0:T(128)S(1)} %copy-done.22, bf16[384,1024]{1,0:T(8,128)(2,1)S(1)} %bitcast.63, bf16[384,1024]{1,0:T(8,128)(2,1)} %collective-permute-done.17.a_ref.refs_1_, bf16[384,1024]{1,0:T(8,128)(2,1)S(1)} %copy-done.5, bf16[384,1024]{1,0:T(8,128)(2,1)S(1)} %bitcast.67, ...), custom_call_target="tpu_custom_call" | custom-call | flops 1207959552 | bytes 2097152 | tf_op jit(solution)/shard_map/pallas_call | solution.py:360
  147.2 4.4 %collective-permute-done.18.far0_ref = bf16[384,1024]{1,0:T(8,128)(2,1)} collective-permute-done((bf16[384,1024]{1,0:T(8,128)(2,1)}, bf16[384,1024]{1,0:T(8,128)(2,1)}, u32[]{:S(2)}, u32[]{:S(2)}) %collective-permute-start.18) | collective-permute-done | bytes 786464 | tf_op jit(solution)/shard_map/ppermute | solution.py:241
  151.6 4.1 %collective-permute-start.2 = (bf16[384,128]{1,0:T(8,128)(2,1)S(1)}, bf16[384,128]{1,0:T(8,128)(2,1)S(1)}, u32[]{:S(2)}, u32[]{:S(2)}) collective-permute-start(bf16[384,128]{1,0:T(8,128)(2,1)S(1)} %copy-done.25), channel_id=1, source_target_pairs={{0,16},{8,24},{16,0},{24,8},{32,48},{40,56},{48,32},{56,40},{64,80... | collective-permute-start | bytes 294920 | tf_op jit(solution)/shard_map/ppermute | solution.py:257
  155.8 1.1 collective-permute-start.3
  156.8 4.3 %shard_map.161.acc1_ref = f32[2,384,256]{2,1,0:T(8,128)S(1)} custom-call(s32[4]{0:T(128)S(1)} %copy-done.22, bf16[384,1024]{1,0:T(8,128)(2,1)S(1)} %bitcast.64, bf16[384,1024]{1,0:T(8,128)(2,1)} %collective-permute-done.17.a_ref.refs_1_, bf16[384,1024]{1,0:T(8,128)(2,1)S(1)} %copy-done.6, bf16[384,1024]{1,0:T(8,128)(2,1)S(1)} %bitcast.68, ...), custom_call_target="tpu_custom_call" | custom-call | flops 1207959552 | bytes 2097152 | tf_op jit(solution)/shard_map/pallas_call | solution.py:360
  161.2 1.2 collective-permute-start.10
  162.4 3.1 %shard_map.162 = bf16[2,384,256]{2,1,0:T(8,128)(2,1)S(1)} custom-call(s32[4]{0:T(128)S(1)} %copy-done.22, bf16[384,1024]{1,0:T(8,128)(2,1)} %collective-permute-done.18.far0_ref, bf16[384,1024]{1,0:T(8,128)(2,1)} %collective-permute-done.20.far1_ref, f32[2,384,256]{2,1,0:T(8,128)S(1)} %shard_map.160.acc0_ref, f32[2,384,256]{2,1,0:T(8,128)S(1)} %shard_map.161.acc1_ref, ...), custom_call_target="tpu_custom_call" | custom-call | flops 805306368 | bytes 1048576 | tf_op jit(solution)/shard_map/pallas_call | solution.py:375
  165.7 3.2 %collective-permute-start.25 = (bf16[768,256]{1,0:T(8,128)(2,1)S(1)}, bf16[768,256]{1,0:T(8,128)(2,1)S(1)}, u32[]{:S(2)}, u32[]{:S(2)}) collective-permute-start(bf16[768,256]{1,0:T(8,128)(2,1)S(1)} %bitcast.70), channel_id=1, source_target_pairs={{0,6},{1,7},{2,0},{3,1},{4,2},{5,3},{6,4},{7,5},{8,14},{9,15},{10,... | collective-permute-start | bytes 1179656 | tf_op jit(solution)/shard_map/ppermute | solution.py:241
  168.9 5.7 %collective-permute-done.10.refs_5_ = bf16[4,384,128]{2,1,0:T(8,128)(2,1)S(1)} collective-permute-done((bf16[4,384,128]{2,1,0:T(8,128)(2,1)S(1)}, bf16[4,384,128]{2,1,0:T(8,128)(2,1)S(1)}, u32[]{:S(2)}, u32[]{:S(2)}) %collective-permute-start.10) | collective-permute-done | bytes 393248 | tf_op jit(solution)/shard_map/ppermute | solution.py:257
  175.4 7.0 %collective-permute-done.24.h1_ref = bf16[768,256]{1,0:T(8,128)(2,1)S(1)} collective-permute-done((bf16[768,256]{1,0:T(8,128)(2,1)S(1)}, bf16[768,256]{1,0:T(8,128)(2,1)S(1)}, u32[]{:S(2)}, u32[]{:S(2)}) %collective-permute-start.24) | collective-permute-done | bytes 393248 | tf_op jit(solution)/shard_map/ppermute | solution.py:241
  182.7 3.8 %collective-permute-start.5 = (bf16[4,384,128]{2,1,0:T(8,128)(2,1)S(1)}, bf16[4,384,128]{2,1,0:T(8,128)(2,1)}, u32[]{:S(2)}, u32[]{:S(2)}) collective-permute-start(bf16[4,384,128]{2,1,0:T(8,128)(2,1)S(1)} %pad_maximum_fusion.2.refs_0_), channel_id=1, source_target_pairs={{0,64},{8,72},{16,80},{24,88},{32,96},{40,104},{48,112},{56,120},{... | collective-permute-start | bytes 1179656 | tf_op jit(solution)/shard_map/ppermute | solution.py:257
  187.7 5.7 %shard_map.163 = bf16[16,2,2,24,512]{4,3,2,1,0:T(8,128)(2,1)} custom-call(s32[4]{0:T(128)} %pad_add_fusion.place_ref, bf16[768,256]{1,0:T(8,128)(2,1)} %bitcast.72, bf16[768,256]{1,0:T(8,128)(2,1)} %copy-done.36, bf16[768,256]{1,0:T(8,128)(2,1)} %copy-done.37, bf16[768,256]{1,0:T(8,128)(2,1)} %copy-done.38, bf16[1024,512]{1,0:T(8,128)(2,1)} %bitcast.12.own_ref.w_own_ref, ...), custom_call_target="tpu_custom_call" | custom-call | flops 1610612736 | bytes 4194304 | tf_op jit(solution)/shard_map/pallas_call | solution.py:425
  193.4 4.6 %all-to-all-start.4 = ((bf16[16,2,48,512]{3,2,1,0:T(8,128)(2,1)}), bf16[16,2,48,512]{3,2,1,0:T(8,128)(2,1)}, u32[]{:S(2)}, u32[]{:S(2)}) async-start(bf16[16,2,48,512]{3,2,1,0:T(8,128)(2,1)} %bitcast.74), calls=%async_computation.4 | async-start | bytes 3145728 | tf_op jit(solution)/shard_map/all_to_all | solution.py:439
  198.0 5.5 %collective-permute-done.5.refs_2_ = bf16[4,384,128]{2,1,0:T(8,128)(2,1)} collective-permute-done((bf16[4,384,128]{2,1,0:T(8,128)(2,1)S(1)}, bf16[4,384,128]{2,1,0:T(8,128)(2,1)}, u32[]{:S(2)}, u32[]{:S(2)}) %collective-permute-start.5) | collective-permute-done | bytes 393248 | tf_op jit(solution)/shard_map/ppermute | solution.py:257
  203.4 2.2 collective-permute-done.6.refs_3_
  205.7 2.2 copy-done.3
  207.9 4.9 %shard_map.154 = (bf16[4096,128]{1,0:T(8,128)(2,1)}, bf16[4096,128]{1,0:T(8,128)(2,1)}, bf16[512,128]{1,0:T(8,128)(2,1)S(1)}, bf16[1024,512]{1,0:T(8,128)(2,1)S(1)}, bf16[512,512]{1,0:T(8,128)(2,1)S(1)}) custom-call(s32[4]{0:T(128)S(1)} %copy-done.23, bf16[512,4096]{1,0:T(8,128)(2,1)S(1)} %copy-done.3, bf16[4,384,128]{2,1,0:T(8,128)(2,1)S(1)} %pad_maximum_fusion.2.refs_0_, ...), custom_call_target="tpu_custom_call" | custom-call | flops 1073741824 | bytes 4194304 | tf_op jit(solution)/shard_map/pallas_call | solution.py:390
  212.7 1.0 copy-done.11
  213.7 7.2 %collective-permute-start.29 = (bf16[512,128]{1,0:T(8,128)(2,1)S(1)}, bf16[512,128]{1,0:T(8,128)(2,1)S(1)}, u32[]{:S(2)}, u32[]{:S(2)}) collective-permute-start(bf16[512,128]{1,0:T(8,128)(2,1)S(1)} %get-tuple-element.52), channel_id=1, source_target_pairs={{0,6},{1,7},{2,0},{3,1},{4,2},{5,3},{6,4},{7,5},{8,14},{9,15},{10,... | collective-permute-start | bytes 393224 | tf_op jit(solution)/shard_map/ppermute | solution.py:241
  221.0 1.5 collective-permute-start.30
  222.4 1.5 collective-permute-done.28
  223.9 3.5 %collective-permute-done.30 = bf16[512,128]{1,0:T(8,128)(2,1)S(1)} collective-permute-done((bf16[512,128]{1,0:T(8,128)(2,1)S(1)}, bf16[512,128]{1,0:T(8,128)(2,1)S(1)}, u32[]{:S(2)}, u32[]{:S(2)}) %collective-permute-start.30) | collective-permute-done | bytes 131104 | tf_op jit(solution)/shard_map/ppermute | solution.py:241
  228.3 1.7 fusion.4
  230.8 1.0 copy-done.10
  231.8 1.0 copy-done.16
  232.9 1.5 shard_map.164.base_ref
  234.4 3.3 %shard_map.155 = (bf16[256,1024]{1,0:T(8,128)(2,1)S(1)}, bf16[256,1024]{1,0:T(8,128)(2,1)}, bf16[256,1024]{1,0:T(8,128)(2,1)}, bf16[256,1024]{1,0:T(8,128)(2,1)}) custom-call(s32[4]{0:T(128)S(1)} %copy-done.23, bf16[1024,512]{1,0:T(8,128)(2,1)} %bitcast.12.own_ref.w_own_ref, bf16[1024,512]{1,0:T(8,128)(2,1)} %collective-permute-done.other_ref.w_other_ref, ...), custom_call_target="tpu_custom_call" | custom-call | flops 1073741824 | bytes 4194304 | tf_op jit(solution)/shard_map/pallas_call | solution.py:487
  239.3 2.7 %collective-permute-start.15 = (bf16[256,1024]{1,0:T(8,128)(2,1)}, bf16[256,1024]{1,0:T(8,128)(2,1)}, u32[]{:S(2)}, u32[]{:S(2)}) collective-permute-start(bf16[256,1024]{1,0:T(8,128)(2,1)} %get-tuple-element.41), channel_id=1, source_target_pairs={{0,4},{1,5},{2,6},{3,7},{4,0},{5,1},{6,2},{7,3},{8,12},{9,13},{10,... | collective-permute-start | bytes 1572872 | tf_op jit(solution)/shard_map/ppermute | solution.py:241
  242.6 1.2 slice.68
  243.9 1.5 slice_bitcast_fusion
  245.4 9.2 %collective-permute-done.14.p1_ref = bf16[256,1024]{1,0:T(8,128)(2,1)} collective-permute-done((bf16[256,1024]{1,0:T(8,128)(2,1)}, bf16[256,1024]{1,0:T(8,128)(2,1)}, u32[]{:S(2)}, u32[]{:S(2)}) %collective-permute-start.14) | collective-permute-done | bytes 524320 | tf_op jit(solution)/shard_map/ppermute | solution.py:241
  254.6 10.8 %collective-permute-done.15.p2_ref = bf16[256,1024]{1,0:T(8,128)(2,1)} collective-permute-done((bf16[256,1024]{1,0:T(8,128)(2,1)}, bf16[256,1024]{1,0:T(8,128)(2,1)}, u32[]{:S(2)}, u32[]{:S(2)}) %collective-permute-start.15) | collective-permute-done | bytes 524320 | tf_op jit(solution)/shard_map/ppermute | solution.py:241
  265.8 3.3 %shard_map.156 = (bf16[128,4096]{1,0:T(8,128)(2,1)}, bf16[128,4096]{1,0:T(8,128)(2,1)}) custom-call(s32[4]{0:T(128)S(1)} %copy-done.23, bf16[256,1024]{1,0:T(8,128)(2,1)S(1)} %copy-done.14, bf16[256,1024]{1,0:T(8,128)(2,1)} %collective-permute-done.14.p1_ref, bf16[256,1024]{1,0:T(8,128)(2,1)} %collective-permute-done.15.p2_ref, ...), custom_call_target="tpu_custom_call" | custom-call | flops 1048576 | bytes 4194304 | tf_op jit(solution)/shard_map/pallas_call | solution.py:503
  269.1 1.8 shard_map.165.base_ref
  271.0 1.4 shard_map.166
  (119 shorter events, 11.5 us)
Async XLA Ops:
  7.7 26.2 %copy-start.35 = (f32[256]{0:T(256)S(1)}, f32[256]{0:T(256)}, u32[]{:S(2)}) copy-start(f32[256]{0:T(256)} %param.11) | copy-start | bytes 3076
  30.3 17.2 %all-to-all-start.1 = ((bf16[16,24,1024]{2,1,0:T(8,128)(2,1)}), bf16[16,24,1024]{2,1,0:T(8,128)(2,1)S(1)}, u32[]{:S(2)}, u32[]{:S(2)}) async-start(bf16[16,24,1024]{2,1,0:T(8,128)(2,1)} %bitcast.76), calls=%async_computation.1 | async-start | bytes 1572864 | tf_op jit(solution)/shard_map/all_to_all | solution.py:315
  48.3 32.4 %all-to-all-start.2 = ((bf16[16,256,256]{2,1,0:T(8,128)(2,1)}), bf16[16,256,256]{2,1,0:T(8,128)(2,1)S(1)}, u32[]{:S(2)}, u32[]{:S(2)}) async-start(bf16[16,256,256]{2,1,0:T(8,128)(2,1)} %pad_maximum_fusion), calls=%async_computation.2 | async-start | bytes 4194304 | tf_op jit(solution)/shard_map/all_to_all | solution.py:325
  52.0 30.1 %copy-start.27 = (f32[256,128]{1,0:T(8,128)S(1)}, f32[256,128]{1,0:T(8,128)}, u32[]{:S(2)}) copy-start(f32[256,128]{1,0:T(8,128)} %param.16) | copy-start | bytes 393220
  52.0 30.1 %copy-start.28 = (f32[256,128]{1,0:T(8,128)S(1)}, f32[256,128]{1,0:T(8,128)}, u32[]{:S(2)}) copy-start(f32[256,128]{1,0:T(8,128)} %param.15) | copy-start | bytes 393220
  80.7 75.1 %collective-permute-start.23 = (bf16[4096,256]{1,0:T(8,128)(2,1)S(1)}, bf16[4096,256]{1,0:T(8,128)(2,1)}, u32[]{:S(2)}, u32[]{:S(2)}) collective-permute-start(bf16[4096,256]{1,0:T(8,128)(2,1)S(1)} %bitcast.57), channel_id=1, source_target_pairs={{0,1},{1,0},{2,3},{3,2},{4,5},{5,4},{6,7},{7,6},{8,9},{9,8},{10,11... | collective-permute-start | bytes 6291464 | tf_op jit(solution)/shard_map/ppermute | solution.py:244
  80.7 36.4 %collective-permute-start.17 = (bf16[384,1024]{1,0:T(8,128)(2,1)S(1)}, bf16[384,1024]{1,0:T(8,128)(2,1)}, u32[]{:S(2)}, u32[]{:S(2)}) collective-permute-start(bf16[384,1024]{1,0:T(8,128)(2,1)S(1)} %bitcast.61), channel_id=1, source_target_pairs={{0,2},{1,3},{2,4},{3,5},{4,6},{5,7},{6,0},{7,1},{8,10},{9,11},{10,... | collective-permute-start | bytes 2359304 | tf_op jit(solution)/shard_map/ppermute | solution.py:241
  83.2 35.0 %collective-permute-start.19 = (bf16[384,1024]{1,0:T(8,128)(2,1)}, bf16[384,1024]{1,0:T(8,128)(2,1)}, u32[]{:S(2)}, u32[]{:S(2)}) collective-permute-start(bf16[384,1024]{1,0:T(8,128)(2,1)} %bitcast.65), channel_id=1, source_target_pairs={{0,6},{1,7},{2,0},{3,1},{4,2},{5,3},{6,4},{7,5},{8,14},{9,15},{10,... | collective-permute-start | bytes 2359304 | tf_op jit(solution)/shard_map/ppermute | solution.py:241
  85.0 36.6 %all-to-all-start.3 = ((bf16[16,64,512]{2,1,0:T(8,128)(2,1)}), bf16[16,64,512]{2,1,0:T(8,128)(2,1)}, u32[]{:S(2)}, u32[]{:S(2)}) async-start(bf16[16,64,512]{2,1,0:T(8,128)(2,1)} %convert_element_type.27), calls=%async_computation.3 | async-start | bytes 2097152 | tf_op jit(solution)/shard_map/all_to_all | solution.py:327
  89.4 51.5 %copy-start.22 = (s32[4]{0:T(128)S(1)}, s32[4]{0:T(128)}, u32[]{:S(2)}) copy-start(s32[4]{0:T(128)} %pad_add_fusion.place_ref) | copy-start | bytes 52
  89.4 31.3 %collective-permute-start.21 = (bf16[384,1024]{1,0:T(8,128)(2,1)S(1)}, bf16[384,1024]{1,0:T(8,128)(2,1)S(1)}, u32[]{:S(2)}, u32[]{:S(2)}) collective-permute-start(bf16[384,1024]{1,0:T(8,128)(2,1)S(1)} %bitcast.62), channel_id=1, source_target_pairs={{0,6},{1,7},{2,0},{3,1},{4,2},{5,3},{6,4},{7,5},{8,14},{9,15},{10,... | collective-permute-start | bytes 2359304 | tf_op jit(solution)/shard_map/ppermute | solution.py:241
  91.0 31.3 %copy-start.26 = (bf16[384,128]{1,0:T(8,128)(2,1)}, bf16[384,128]{1,0:T(8,128)(2,1)S(1)}, u32[]{:S(2)}) copy-start(bf16[384,128]{1,0:T(8,128)(2,1)S(1)} %get-tuple-element.58.b_ref) | copy-start | bytes 294916
  91.0 15.0 %collective-permute-start.7 = (bf16[384,128]{1,0:T(8,128)(2,1)S(1)}, bf16[384,128]{1,0:T(8,128)(2,1)S(1)}, u32[]{:S(2)}, u32[]{:S(2)}) collective-permute-start(bf16[384,128]{1,0:T(8,128)(2,1)S(1)} %get-tuple-element.58.b_ref), channel_id=1, source_target_pairs={{0,32},{8,40},{16,48},{24,56},{32,64},{40,72},{48,80},{56,88},{64,... | collective-permute-start | bytes 294920 | tf_op jit(solution)/shard_map/ppermute | solution.py:257
  106.0 17.6 %copy-start.29 = (bf16[384,128]{1,0:T(8,128)(2,1)}, bf16[384,128]{1,0:T(8,128)(2,1)S(1)}, u32[]{:S(2)}) copy-start(bf16[384,128]{1,0:T(8,128)(2,1)S(1)} %collective-permute-done.7) | copy-start | bytes 294916
  106.0 6.1 %collective-permute-start.8 = (bf16[384,128]{1,0:T(8,128)(2,1)S(1)}, bf16[384,128]{1,0:T(8,128)(2,1)S(1)}, u32[]{:S(2)}, u32[]{:S(2)}) collective-permute-start(bf16[384,128]{1,0:T(8,128)(2,1)S(1)} %get-tuple-element.58.b_ref), channel_id=1, source_target_pairs={{0,64},{8,72},{16,80},{24,88},{32,96},{40,104},{48,112},{56,120},{... | collective-permute-start | bytes 294920 | tf_op jit(solution)/shard_map/ppermute | solution.py:257
  112.1 11.5 %copy-start.30 = (bf16[384,128]{1,0:T(8,128)(2,1)}, bf16[384,128]{1,0:T(8,128)(2,1)S(1)}, u32[]{:S(2)}) copy-start(bf16[384,128]{1,0:T(8,128)(2,1)S(1)} %collective-permute-done.8) | copy-start | bytes 294916
  112.1 4.6 %collective-permute-start.9 = (bf16[384,128]{1,0:T(8,128)(2,1)S(1)}, bf16[384,128]{1,0:T(8,128)(2,1)S(1)}, u32[]{:S(2)}, u32[]{:S(2)}) collective-permute-start(bf16[384,128]{1,0:T(8,128)(2,1)S(1)} %get-tuple-element.58.b_ref), channel_id=1, source_target_pairs={{0,96},{8,104},{16,112},{24,120},{32,0},{40,8},{48,16},{56,24},{64... | collective-permute-start | bytes 294920 | tf_op jit(solution)/shard_map/ppermute | solution.py:257
  116.8 4.9 %copy-start.31 = (bf16[384,128]{1,0:T(8,128)(2,1)}, bf16[384,128]{1,0:T(8,128)(2,1)S(1)}, u32[]{:S(2)}) copy-start(bf16[384,128]{1,0:T(8,128)(2,1)S(1)} %collective-permute-done.9) | copy-start | bytes 294916
  116.8 21.9 %collective-permute-start.22 = (bf16[384,1024]{1,0:T(8,128)(2,1)}, bf16[384,1024]{1,0:T(8,128)(2,1)}, u32[]{:S(2)}, u32[]{:S(2)}) collective-permute-start(bf16[384,1024]{1,0:T(8,128)(2,1)} %bitcast.66), channel_id=1, source_target_pairs={{0,2},{1,3},{2,4},{3,5},{4,6},{5,7},{6,0},{7,1},{8,10},{9,11},{10,... | collective-permute-start | bytes 2359304 | tf_op jit(solution)/shard_map/ppermute | solution.py:241
  117.0 34.6 %collective-permute-start.18 = (bf16[384,1024]{1,0:T(8,128)(2,1)}, bf16[384,1024]{1,0:T(8,128)(2,1)}, u32[]{:S(2)}, u32[]{:S(2)}) collective-permute-start(bf16[384,1024]{1,0:T(8,128)(2,1)} %collective-permute-done.17.a_ref.refs_1_), channel_id=1, source_target_pairs={{0,2},{1,3},{2,4},{3,5},{4,6},{5,7},{6,0},{7,1},{8,10},{9,11},{10,... | collective-permute-start | bytes 2359304 | tf_op jit(solution)/shard_map/ppermute | solution.py:241
  118.2 43.0 %collective-permute-start.20 = (bf16[384,1024]{1,0:T(8,128)(2,1)}, bf16[384,1024]{1,0:T(8,128)(2,1)}, u32[]{:S(2)}, u32[]{:S(2)}) collective-permute-start(bf16[384,1024]{1,0:T(8,128)(2,1)} %collective-permute-done.19.b_ref.refs_5_), channel_id=1, source_target_pairs={{0,6},{1,7},{2,0},{3,1},{4,2},{5,3},{6,4},{7,5},{8,14},{9,15},{10,... | collective-permute-start | bytes 2359304 | tf_op jit(solution)/shard_map/ppermute | solution.py:241
  121.6 53.8 %collective-permute-start = (bf16[1024,512]{1,0:T(8,128)(2,1)}, bf16[1024,512]{1,0:T(8,128)(2,1)}, u32[]{:S(2)}, u32[]{:S(2)}) collective-permute-start(bf16[1024,512]{1,0:T(8,128)(2,1)} %bitcast.12.own_ref.w_own_ref), channel_id=1, source_target_pairs={{0,1},{1,0},{2,3},{3,2},{4,5},{5,4},{6,7},{7,6},{8,9},{9,8},{10,11... | collective-permute-start | bytes 3145736 | tf_op jit(solution)/shard_map/ppermute | solution.py:244
  138.7 26.9 %collective-permute-start.1 = (bf16[384,128]{1,0:T(8,128)(2,1)}, bf16[384,128]{1,0:T(8,128)(2,1)S(1)}, u32[]{:S(2)}, u32[]{:S(2)}) collective-permute-start(bf16[384,128]{1,0:T(8,128)(2,1)} %get-tuple-element.60.a_ref), channel_id=1, source_target_pairs={{0,8},{8,16},{16,24},{24,0},{32,40},{40,48},{48,56},{56,32},{64,72... | collective-permute-start | bytes 294920 | tf_op jit(solution)/shard_map/ppermute | solution.py:257
  140.8 1.1 copy-start.1
  143.8 7.9 %copy-start.25 = (bf16[384,128]{1,0:T(8,128)(2,1)S(1)}, bf16[384,128]{1,0:T(8,128)(2,1)}, u32[]{:S(2)}) copy-start(bf16[384,128]{1,0:T(8,128)(2,1)} %get-tuple-element.60.a_ref) | copy-start | bytes 294916
  143.8 13.1 %copy-start.2 = (bf16[16,24,1024]{2,1,0:T(8,128)(2,1)S(1)}, bf16[16,24,1024]{2,1,0:T(8,128)(2,1)}, u32[]{:S(2)}) copy-start(bf16[16,24,1024]{2,1,0:T(8,128)(2,1)} %copy-done) | copy-start | bytes 2359300
  143.8 13.1 %copy-start.6 = (bf16[384,1024]{1,0:T(8,128)(2,1)S(1)}, bf16[384,1024]{1,0:T(8,128)(2,1)}, u32[]{:S(2)}) copy-start(bf16[384,1024]{1,0:T(8,128)(2,1)} %copy-done.4) | copy-start | bytes 2359300
  143.8 13.1 %copy-start.21 = (bf16[16,128]{1,0:T(8,128)(2,1)S(1)}, bf16[16,128]{1,0:T(8,128)(2,1)}, u32[]{:S(2)}) copy-start(bf16[16,128]{1,0:T(8,128)(2,1)} %shard_map.159.refs_7_) | copy-start | bytes 12292
  151.6 14.0 %collective-permute-start.2 = (bf16[384,128]{1,0:T(8,128)(2,1)S(1)}, bf16[384,128]{1,0:T(8,128)(2,1)S(1)}, u32[]{:S(2)}, u32[]{:S(2)}) collective-permute-start(bf16[384,128]{1,0:T(8,128)(2,1)S(1)} %copy-done.25), channel_id=1, source_target_pairs={{0,16},{8,24},{16,0},{24,8},{32,48},{40,56},{48,32},{56,40},{64,80... | collective-permute-start | bytes 294920 | tf_op jit(solution)/shard_map/ppermute | solution.py:257
  155.8 13.1 %collective-permute-start.3 = (bf16[384,128]{1,0:T(8,128)(2,1)S(1)}, bf16[384,128]{1,0:T(8,128)(2,1)S(1)}, u32[]{:S(2)}, u32[]{:S(2)}) collective-permute-start(bf16[384,128]{1,0:T(8,128)(2,1)S(1)} %copy-done.25), channel_id=1, source_target_pairs={{0,24},{8,0},{16,8},{24,16},{32,56},{40,32},{48,40},{56,48},{64,88... | collective-permute-start | bytes 294920 | tf_op jit(solution)/shard_map/ppermute | solution.py:257
  161.2 13.4 %collective-permute-start.10 = (bf16[4,384,128]{2,1,0:T(8,128)(2,1)S(1)}, bf16[4,384,128]{2,1,0:T(8,128)(2,1)S(1)}, u32[]{:S(2)}, u32[]{:S(2)}) collective-permute-start(bf16[4,384,128]{2,1,0:T(8,128)(2,1)S(1)} %pad_maximum_fusion.3.refs_4_), channel_id=1, source_target_pairs={{0,8},{8,16},{16,24},{24,0},{32,40},{40,48},{48,56},{56,32},{64,72... | collective-permute-start | bytes 1179656 | tf_op jit(solution)/shard_map/ppermute | solution.py:257
  165.6 22.2 %copy-start.17 = (bf16[2,384,256]{2,1,0:T(8,128)(2,1)}, bf16[2,384,256]{2,1,0:T(8,128)(2,1)S(1)}, u32[]{:S(2)}) copy-start(bf16[2,384,256]{2,1,0:T(8,128)(2,1)S(1)} %shard_map.162) | copy-start | bytes 1179652
  165.6 16.8 %collective-permute-start.24 = (bf16[768,256]{1,0:T(8,128)(2,1)S(1)}, bf16[768,256]{1,0:T(8,128)(2,1)S(1)}, u32[]{:S(2)}, u32[]{:S(2)}) collective-permute-start(bf16[768,256]{1,0:T(8,128)(2,1)S(1)} %bitcast.69), channel_id=1, source_target_pairs={{0,2},{1,3},{2,4},{3,5},{4,6},{5,7},{6,0},{7,1},{8,10},{9,11},{10,... | collective-permute-start | bytes 1179656 | tf_op jit(solution)/shard_map/ppermute | solution.py:241
  165.7 17.0 %collective-permute-start.25 = (bf16[768,256]{1,0:T(8,128)(2,1)S(1)}, bf16[768,256]{1,0:T(8,128)(2,1)S(1)}, u32[]{:S(2)}, u32[]{:S(2)}) collective-permute-start(bf16[768,256]{1,0:T(8,128)(2,1)S(1)} %bitcast.70), channel_id=1, source_target_pairs={{0,6},{1,7},{2,0},{3,1},{4,2},{5,3},{6,4},{7,5},{8,14},{9,15},{10,... | collective-permute-start | bytes 1179656 | tf_op jit(solution)/shard_map/ppermute | solution.py:241
  168.9 17.6 %collective-permute-start.26 = (bf16[768,256]{1,0:T(8,128)(2,1)S(1)}, bf16[768,256]{1,0:T(8,128)(2,1)S(1)}, u32[]{:S(2)}, u32[]{:S(2)}) collective-permute-start(bf16[768,256]{1,0:T(8,128)(2,1)S(1)} %bitcast.71), channel_id=1, source_target_pairs={{0,4},{1,5},{2,6},{3,7},{4,0},{5,1},{6,2},{7,3},{8,12},{9,13},{10,... | collective-permute-start | bytes 1179656 | tf_op jit(solution)/shard_map/ppermute | solution.py:241
  175.4 22.6 %collective-permute-start.11 = (bf16[4,384,128]{2,1,0:T(8,128)(2,1)S(1)}, bf16[4,384,128]{2,1,0:T(8,128)(2,1)}, u32[]{:S(2)}, u32[]{:S(2)}) collective-permute-start(bf16[4,384,128]{2,1,0:T(8,128)(2,1)S(1)} %pad_maximum_fusion.3.refs_4_), channel_id=1, source_target_pairs={{0,16},{8,24},{16,0},{24,8},{32,48},{40,56},{48,32},{56,40},{64,80... | collective-permute-start | bytes 1179656 | tf_op jit(solution)/shard_map/ppermute | solution.py:257
  175.4 22.6 %collective-permute-start.12 = (bf16[4,384,128]{2,1,0:T(8,128)(2,1)S(1)}, bf16[4,384,128]{2,1,0:T(8,128)(2,1)}, u32[]{:S(2)}, u32[]{:S(2)}) collective-permute-start(bf16[4,384,128]{2,1,0:T(8,128)(2,1)S(1)} %pad_maximum_fusion.3.refs_4_), channel_id=1, source_target_pairs={{0,24},{8,0},{16,8},{24,16},{32,56},{40,32},{48,40},{56,48},{64,88... | collective-permute-start | bytes 1179656 | tf_op jit(solution)/shard_map/ppermute | solution.py:257
  182.4 5.3 %copy-start.36 = (bf16[768,256]{1,0:T(8,128)(2,1)}, bf16[768,256]{1,0:T(8,128)(2,1)S(1)}, u32[]{:S(2)}) copy-start(bf16[768,256]{1,0:T(8,128)(2,1)S(1)} %collective-permute-done.24.h1_ref) | copy-start | bytes 1179652
  182.4 15.6 %collective-permute-start.4 = (bf16[4,384,128]{2,1,0:T(8,128)(2,1)S(1)}, bf16[4,384,128]{2,1,0:T(8,128)(2,1)}, u32[]{:S(2)}, u32[]{:S(2)}) collective-permute-start(bf16[4,384,128]{2,1,0:T(8,128)(2,1)S(1)} %pad_maximum_fusion.2.refs_0_), channel_id=1, source_target_pairs={{0,32},{8,40},{16,48},{24,56},{32,64},{40,72},{48,80},{56,88},{64,... | collective-permute-start | bytes 1179656 | tf_op jit(solution)/shard_map/ppermute | solution.py:257
  182.7 3.8 %copy-start.37 = (bf16[768,256]{1,0:T(8,128)(2,1)}, bf16[768,256]{1,0:T(8,128)(2,1)S(1)}, u32[]{:S(2)}) copy-start(bf16[768,256]{1,0:T(8,128)(2,1)S(1)} %collective-permute-done.25.h2_ref) | copy-start | bytes 1179652
  182.7 20.8 %collective-permute-start.5 = (bf16[4,384,128]{2,1,0:T(8,128)(2,1)S(1)}, bf16[4,384,128]{2,1,0:T(8,128)(2,1)}, u32[]{:S(2)}, u32[]{:S(2)}) collective-permute-start(bf16[4,384,128]{2,1,0:T(8,128)(2,1)S(1)} %pad_maximum_fusion.2.refs_0_), channel_id=1, source_target_pairs={{0,64},{8,72},{16,80},{24,88},{32,96},{40,104},{48,112},{56,120},{... | collective-permute-start | bytes 1179656 | tf_op jit(solution)/shard_map/ppermute | solution.py:257
  187.2 18.4 %collective-permute-start.6 = (bf16[4,384,128]{2,1,0:T(8,128)(2,1)S(1)}, bf16[4,384,128]{2,1,0:T(8,128)(2,1)}, u32[]{:S(2)}, u32[]{:S(2)}) collective-permute-start(bf16[4,384,128]{2,1,0:T(8,128)(2,1)S(1)} %pad_maximum_fusion.2.refs_0_), channel_id=1, source_target_pairs={{0,96},{8,104},{16,112},{24,120},{32,0},{40,8},{48,16},{56,24},{64... | collective-permute-start | bytes 1179656 | tf_op jit(solution)/shard_map/ppermute | solution.py:257
  193.4 12.3 %copy-start.19 = (bf16[4,384,128]{2,1,0:T(8,128)(2,1)S(1)}, bf16[4,384,128]{2,1,0:T(8,128)(2,1)}, u32[]{:S(2)}) copy-start(bf16[4,384,128]{2,1,0:T(8,128)(2,1)} %copy-done.18) | copy-start | bytes 1179652
  193.4 12.3 %copy-start.23 = (s32[4]{0:T(128)S(1)}, s32[4]{0:T(128)}, u32[]{:S(2)}) copy-start(s32[4]{0:T(128)} %pad_add_fusion.place_ref) | copy-start | bytes 52
  193.4 49.2 %all-to-all-start.4 = ((bf16[16,2,48,512]{3,2,1,0:T(8,128)(2,1)}), bf16[16,2,48,512]{3,2,1,0:T(8,128)(2,1)}, u32[]{:S(2)}, u32[]{:S(2)}) async-start(bf16[16,2,48,512]{3,2,1,0:T(8,128)(2,1)} %bitcast.74), calls=%async_computation.4 | async-start | bytes 3145728 | tf_op jit(solution)/shard_map/all_to_all | solution.py:439
  205.7 2.2 copy-start.3
  207.9 14.6 %copy-start.34 = (f32[512,2]{0,1:T(2,128)S(1)}, f32[512,2]{0,1:T(2,128)}, u32[]{:S(2)}) copy-start(f32[512,2]{0,1:T(2,128)} %param.19) | copy-start | bytes 12292
  207.9 20.4 %copy-start.32 = (s32[512,2]{0,1:T(2,128)S(1)}, s32[512,2]{0,1:T(2,128)}, u32[]{:S(2)}) copy-start(s32[512,2]{0,1:T(2,128)} %param.18) | copy-start | bytes 12292
  207.9 20.4 %copy-start.33 = (s32[2,512]{1,0:T(2,128)S(1)}, s32[2,512]{1,0:T(2,128)}, u32[]{:S(2)}) copy-start(s32[2,512]{1,0:T(2,128)} %get-tuple-element.47) | copy-start | bytes 12292
  213.7 13.8 %copy-start.24 = (bf16[512,512]{1,0:T(8,128)(2,1)}, bf16[512,512]{1,0:T(8,128)(2,1)S(1)}, u32[]{:S(2)}) copy-start(bf16[512,512]{1,0:T(8,128)(2,1)S(1)} %get-tuple-element.38) | copy-start | bytes 1572868
  213.7 10.2 %collective-permute-start.28 = (bf16[512,128]{1,0:T(8,128)(2,1)S(1)}, bf16[512,128]{1,0:T(8,128)(2,1)S(1)}, u32[]{:S(2)}, u32[]{:S(2)}) collective-permute-start(bf16[512,128]{1,0:T(8,128)(2,1)S(1)} %get-tuple-element.52), channel_id=1, source_target_pairs={{0,2},{1,3},{2,4},{3,5},{4,6},{5,7},{6,0},{7,1},{8,10},{9,11},{10,... | collective-permute-start | bytes 393224 | tf_op jit(solution)/shard_map/ppermute | solution.py:241
  213.7 10.2 %collective-permute-start.29 = (bf16[512,128]{1,0:T(8,128)(2,1)S(1)}, bf16[512,128]{1,0:T(8,128)(2,1)S(1)}, u32[]{:S(2)}, u32[]{:S(2)}) collective-permute-start(bf16[512,128]{1,0:T(8,128)(2,1)S(1)} %get-tuple-element.52), channel_id=1, source_target_pairs={{0,6},{1,7},{2,0},{3,1},{4,2},{5,3},{6,4},{7,5},{8,14},{9,15},{10,... | collective-permute-start | bytes 393224 | tf_op jit(solution)/shard_map/ppermute | solution.py:241
  221.0 6.5 %collective-permute-start.30 = (bf16[512,128]{1,0:T(8,128)(2,1)S(1)}, bf16[512,128]{1,0:T(8,128)(2,1)S(1)}, u32[]{:S(2)}, u32[]{:S(2)}) collective-permute-start(bf16[512,128]{1,0:T(8,128)(2,1)S(1)} %get-tuple-element.52), channel_id=1, source_target_pairs={{0,4},{1,5},{2,6},{3,7},{4,0},{5,1},{6,2},{7,3},{8,12},{9,13},{10,... | collective-permute-start | bytes 393224 | tf_op jit(solution)/shard_map/ppermute | solution.py:241
  227.5 2.5 copy-start.9
  227.5 2.5 collective-permute-start.31
  227.6 3.1 %copy-start.12 = (bf16[1024,512]{1,0:T(8,128)(2,1)S(1)}, bf16[1024,512]{1,0:T(8,128)(2,1)}, u32[]{:S(2)}) copy-start(bf16[1024,512]{1,0:T(8,128)(2,1)} %copy-done.11) | copy-start | bytes 3145732
  227.7 6.8 %collective-permute-start.13 = (bf16[512,512]{1,0:T(8,128)(2,1)}, bf16[512,512]{1,0:T(8,128)(2,1)S(1)}, u32[]{:S(2)}, u32[]{:S(2)}) collective-permute-start(bf16[512,512]{1,0:T(8,128)(2,1)} %copy-done.24), channel_id=1, source_target_pairs={{0,1},{1,0},{2,3},{3,2},{4,5},{5,4},{6,7},{7,6},{8,9},{9,8},{10,11... | collective-permute-start | bytes 1572872 | tf_op jit(solution)/shard_map/ppermute | solution.py:244
  238.5 16.1 %collective-permute-start.14 = (bf16[256,1024]{1,0:T(8,128)(2,1)}, bf16[256,1024]{1,0:T(8,128)(2,1)}, u32[]{:S(2)}, u32[]{:S(2)}) collective-permute-start(bf16[256,1024]{1,0:T(8,128)(2,1)} %get-tuple-element.40), channel_id=1, source_target_pairs={{0,2},{1,3},{2,4},{3,5},{4,6},{5,7},{6,0},{7,1},{8,10},{9,11},{10,... | collective-permute-start | bytes 1572872 | tf_op jit(solution)/shard_map/ppermute | solution.py:241
  239.3 26.1 %collective-permute-start.15 = (bf16[256,1024]{1,0:T(8,128)(2,1)}, bf16[256,1024]{1,0:T(8,128)(2,1)}, u32[]{:S(2)}, u32[]{:S(2)}) collective-permute-start(bf16[256,1024]{1,0:T(8,128)(2,1)} %get-tuple-element.41), channel_id=1, source_target_pairs={{0,4},{1,5},{2,6},{3,7},{4,0},{5,1},{6,2},{7,3},{8,12},{9,13},{10,... | collective-permute-start | bytes 1572872 | tf_op jit(solution)/shard_map/ppermute | solution.py:241
  242.0 23.8 %collective-permute-start.16 = (bf16[256,1024]{1,0:T(8,128)(2,1)}, bf16[256,1024]{1,0:T(8,128)(2,1)}, u32[]{:S(2)}, u32[]{:S(2)}) collective-permute-start(bf16[256,1024]{1,0:T(8,128)(2,1)} %get-tuple-element.42), channel_id=1, source_target_pairs={{0,6},{1,7},{2,0},{3,1},{4,2},{5,3},{6,4},{7,5},{8,14},{9,15},{10,... | collective-permute-start | bytes 1572872 | tf_op jit(solution)/shard_map/ppermute | solution.py:241
  243.8 22.0 %copy-start.14 = (bf16[256,1024]{1,0:T(8,128)(2,1)S(1)}, bf16[256,1024]{1,0:T(8,128)(2,1)}, u32[]{:S(2)}) copy-start(bf16[256,1024]{1,0:T(8,128)(2,1)} %copy-done.13) | copy-start | bytes 1572868
  243.8 27.1 %collective-permute-start.27 = (bf16[768,512]{1,0:T(8,128)(2,1)S(1)}, bf16[768,512]{1,0:T(8,128)(2,1)S(1)}, u32[]{:S(2)}, u32[]{:S(2)}) collective-permute-start(bf16[768,512]{1,0:T(8,128)(2,1)S(1)} %bitcast.75), channel_id=1, source_target_pairs={{0,1},{1,0},{2,3},{3,2},{4,5},{5,4},{6,7},{7,6},{8,9},{9,8},{10,11... | collective-permute-start | bytes 2359304 | tf_op jit(solution)/shard_map/ppermute | solution.py:244
  245.4 23.8 %copy-start.8 = (bf16[512,768]{1,0:T(8,128)(2,1)S(1)}, bf16[512,768]{1,0:T(8,128)(2,1)}, u32[]{:S(2)}) copy-start(bf16[512,768]{1,0:T(8,128)(2,1)} %get-tuple-element.51.weight_ref) | copy-start | bytes 2359300
  269.1 1.8 copy-start.7
  (11 other events, 9.7 us)

commit v5 on v3

--- a/solution.py
+++ b/solution.py
@@ -124,12 +124,19 @@
     depth, cols = h0_ref.shape[1], w_own_ref.shape[1]
     chips = w_own_ref.shape[0] // depth
     parts = ((h0_ref, 0), (h1_ref, chips - 1), (h2_ref, 1), (h3_ref, chips // 2))
-    for h_ref, shift in parts:
-        at = pl.multiple_of(lax.rem(chip + shift, chips) * depth, depth)
-        line[:, pl.ds(at, depth)] = h_ref[...]
+
+    @pl.when(pl.program_id(0) == 0)
+    def _():
+        for h_ref, shift in parts:
+            at = pl.multiple_of(lax.rem(chip + shift, chips) * depth, depth)
+            line[:, pl.ds(at, depth)] = h_ref[...]
+
     for part, w_ref in enumerate((w_own_ref, w_other_ref)):
-        total = dot(line[...], w_ref[...]).astype(bf16)
-        out_ref[:, part] = total.reshape(out_ref.shape[0], out_ref.shape[2], cols)
+
+        @pl.when(pl.program_id(0) == part)
+        def _():
+            total = dot(line[...], w_ref[...]).astype(bf16)
+            out_ref[:, 0] = total.reshape(out_ref.shape[0], out_ref.shape[2], cols)
 
 
 def shared_kernel(place_ref, x_ref, *refs):
@@ -171,7 +178,8 @@
 
 
 def mix_kernel(weight_ref, got_ref, base_ref, out_ref):
-    out_ref[...] = (base_ref[...] + dot(weight_ref[...], got_ref[...])).astype(out_ref.dtype)
+    got = got_ref[...].reshape(weight_ref.shape[1], out_ref.shape[1])
+    out_ref[...] = (base_ref[...] + dot(weight_ref[...], got)).astype(out_ref.dtype)
 
 
 def chunk_kernel(place_ref, own_ref, other_ref, sd_ref, sd_other_ref, *out_refs):
@@ -403,18 +411,17 @@
         down_kernel,
         grid_spec=pltpu.PrefetchScalarGridSpec(
             num_scalar_prefetch=1,
-            grid=(1,),
+            grid=(2,),
             in_specs=[whole((rows, 2 * hs))] * 4 + [whole((experts * deep, cols))] * 2,
-            out_specs=whole((experts, 2, half, cols)),
+            out_specs=pl.BlockSpec((experts, 1, half, cols), lambda i, s: (0, i, 0, 0)),
             scratch_shapes=[pltpu.VMEM((rows, experts * deep), bf16)],
         ),
         out_shape=jax.ShapeDtypeStruct((experts, 2, half, cols), bf16),
-        compiler_params=vmem_limit(40),
+        compiler_params=vmem_limit(60),
         cost_estimate=cost(4 * rows * experts * deep * cols, 8 * experts * deep * cols),
     )(place, hidden, hid_left, hid_right, hid_far, down_cols, down_other)
     returned = lax.all_to_all(sums, "fs", split_axis=0, concat_axis=0, tiled=True)
     got_other = swap(returned[:, 1].reshape(rows, cols))
-    got_own = returned[:, 0].reshape(rows, cols)
 
     spots = jnp.arange(rows, dtype=jnp.int32)[None, :]
 
@@ -433,6 +440,13 @@
     def mix(weights, got, base, dtype):
         return pl.pallas_call(
             mix_kernel,
+            grid=(1,),
+            in_specs=[
+                whole((tok_rows, rows)),
+                whole((experts, 1, half, cols)) if got.ndim == 4 else whole((rows, cols)),
+                whole((tok_rows, cols)),
+            ],
+            out_specs=whole((tok_rows, cols)),
             out_shape=jax.ShapeDtypeStruct((tok_rows, cols), dtype),
             compiler_params=vmem_limit(24),
             cost_estimate=cost(2 * tok_rows * rows * cols, 4 * tok_rows * rows),
@@ -451,7 +465,7 @@
         compiler_params=vmem_limit(24),
         cost_estimate=cost(2 * tok_rows * experts * deep * cols, 4 * tok_rows * rows),
     )(place, units, units_other, shared_cols)
-    part = mix(mix_own, got_own, base, f32)
+    part = mix(mix_own, returned, base, f32)
     mixed = mix(mix_other, got_other, part, bf16)
 
     chunks = pl.pallas_call(
@@ -509,6 +523,7 @@
         P("fs", None),
     )
 
+
     return jax.shard_map(
         on_device,
         mesh=mesh,

time: 275 us -> 274 us (level)
  waiting for transfers between devices: 147 us -> 139 us
  starting transfers between devices: 56.3 us -> 62 us
  Pallas kernels: 37.9 us -> 40.7 us
    ppermute x12, waiting for transfers between devices: 43.3 us -> 36.3 us  [along(): return lax.ppermute(a, 'fs', pairs)]
    ppermute x15, starting transfers between devices: 18.9 us -> 24.5 us  [shift_by(): return lax.ppermute(a, 'tp', [(i, (i + 2 * n) % tp) for i in range(tp)])]
    unnamed x70 -> x76, local copies, waits for them, and re-layouts: 15.5 us -> 14.5 us
  transfers between devices with their start and end apart: 36 -> 36, of which waited for: 16 -> 17; matrix products, arithmetic and copies ran while one was open for 5% -> 5% of each run, Pallas kernels for 11% -> 12%
where the time goes in v5:
time: 274 us; the launch traced here: 273 us
  waiting for transfers between devices  139 us (51%)
  starting transfers between devices  62 us (23%)
  Pallas kernels  40.7 us (15%)
  local copies, waits for them, and re-layouts  18.5 us (7%)
  other arithmetic  11.6 us (4%)
    ppermute x15, waiting for transfers between devices, shift_by(): return lax.ppermute(a, 'tp', [(i, (i + 2 * n) % tp) for i in range(tp)])  55.2 us
    ppermute x12, waiting for transfers between devices, along(): return lax.ppermute(a, 'fs', pairs)  36.3 us
    all_to_all x1, waiting for transfers between devices, on_device(): gu = lax.all_to_all(gu_local, 'fs', split_axis=0, concat_axis=0, tiled=True)  27.4 us
    ppermute x15, starting transfers between devices, shift_by(): return lax.ppermute(a, 'tp', [(i, (i + 2 * n) % tp) for i in range(tp)])  24.5 us
    all_to_all x1, waiting for transfers between devices, on_device(): lax.all_to_all(outgoing.reshape(experts, half, quarter), 'fs', split_axis...  20 us
    ppermute x12, starting transfers between devices, along(): return lax.ppermute(a, 'fs', pairs)  15.9 us
    unnamed x76, local copies, waits for them, and re-layouts  14.5 us
    all_to_all x1, starting transfers between devices, on_device(): lax.all_to_all(outgoing.reshape(experts, half, quarter), 'fs', split_axis...  8.17 us
  transfers between devices with their start and end apart: 36, of which 17 were waited for; matrix products, arithmetic and copies ran while one was open for 5% of the time, Pallas kernels for 12%

profile of v5, /device:TPU:0, one launch (start us, length us, event | category | flops | bytes accessed | tf_op | source)
XLA Modules:
  0.0 272.7 jit_solution(2423439099704416135)
XLA Ops:
  1.3 6.5 %shard_map.153 = (bf16[512,4096]{1,0:T(8,128)(2,1)}, bf16[768,1024]{1,0:T(8,128)(2,1)}, s32[2,512]{1,0:T(2,128)}) custom-call(s32[4]{0:T(128)} %pad_add_fusion.place_ref, s32[2,512]{1,0:T(2,128)} %bitcast.81, bf16[512,4096]{1,0:T(8,128)(2,1)} %tok_ref.1), custom_call_target="tpu_custom_call" | custom-call | flops 805306368 | bytes 8388608 | tf_op jit(solution)/shard_map/pallas_call | solution.py:283
  7.8 8.2 %all-to-all-start = ((bf16[16,48,1024]{2,1,0:T(8,128)(2,1)}), bf16[16,48,1024]{2,1,0:T(8,128)(2,1)S(1)}, u32[]{:S(2)}, u32[]{:S(2)}) async-start(bf16[16,48,1024]{2,1,0:T(8,128)(2,1)} %bitcast.70), calls=%async_computation | async-start | bytes 3145728 | tf_op jit(solution)/shard_map/all_to_all | solution.py:307
  16.0 2.8 %multiply_convert_fusion.1 = (bf16[16,256,128]{2,1,0:T(8,128)(2,1)S(1)}, bf16[16,256,128]{2,1,0:T(8,128)(2,1)S(1)}) fusion(f32[16,256,128]{2,1,0:T(8,128)} %param.12, f32[256]{0:T(256)S(1)} %copy-done.34, f32[16,256,128]{2,1,0:T(8,128)} %param.13), kind=kLoop, calls=%fused_computation.2 | loop fusion | flops 2097152 | bytes 6292480 | tf_op jit(solution)/shard_map/convert_element_type | solution.py:312
  18.8 1.7 pad_maximum_fusion
  20.5 20.0 %all-to-all-done = bf16[16,48,1024]{2,1,0:T(8,128)(2,1)S(1)} async-done(((bf16[16,48,1024]{2,1,0:T(8,128)(2,1)}), bf16[16,48,1024]{2,1,0:T(8,128)(2,1)S(1)}, u32[]{:S(2)}, u32[]{:S(2)}) %all-to-all-start) | async-done | bytes 1572896 | tf_op jit(solution)/shard_map/all_to_all | solution.py:307
  40.5 1.3 fusion.8
  41.8 3.7 %all-to-all-start.1 = ((bf16[16,256,256]{2,1,0:T(8,128)(2,1)}), bf16[16,256,256]{2,1,0:T(8,128)(2,1)S(1)}, u32[]{:S(2)}, u32[]{:S(2)}) async-start(bf16[16,256,256]{2,1,0:T(8,128)(2,1)} %pad_maximum_fusion), calls=%async_computation.1 | async-start | bytes 4194304 | tf_op jit(solution)/shard_map/all_to_all | solution.py:318
  45.6 2.8 %convert_element_type.27 = bf16[16,64,512]{2,1,0:T(8,128)(2,1)} convert(f32[16,64,512]{2,1,0:T(8,128)} %param.14) | non-fusion elementwise | flops 524288 | bytes 3145728 | tf_op jit(solution)/shard_map/convert_element_type | solution.py:319
  48.4 27.4 %all-to-all-done.1 = bf16[16,256,256]{2,1,0:T(8,128)(2,1)S(1)} async-done(((bf16[16,256,256]{2,1,0:T(8,128)(2,1)}), bf16[16,256,256]{2,1,0:T(8,128)(2,1)S(1)}, u32[]{:S(2)}, u32[]{:S(2)}) %all-to-all-start.1) | async-done | bytes 2097184 | tf_op jit(solution)/shard_map/all_to_all | solution.py:318
  75.7 1.5 collective-permute-start.17
  77.4 1.8 collective-permute-start.19
  79.2 4.3 %all-to-all-start.2 = ((bf16[16,64,512]{2,1,0:T(8,128)(2,1)}), bf16[16,64,512]{2,1,0:T(8,128)(2,1)}, u32[]{:S(2)}, u32[]{:S(2)}) async-start(bf16[16,64,512]{2,1,0:T(8,128)(2,1)} %convert_element_type.27), calls=%async_computation.2 | async-start | bytes 2097152 | tf_op jit(solution)/shard_map/all_to_all | solution.py:320
  83.6 1.6 collective-permute-start.21
  85.2 1.8 collective-permute-start.7
  87.1 13.2 %collective-permute-done.7 = bf16[384,128]{1,0:T(8,128)(2,1)S(1)} collective-permute-done((bf16[384,128]{1,0:T(8,128)(2,1)S(1)}, bf16[384,128]{1,0:T(8,128)(2,1)S(1)}, u32[]{:S(2)}, u32[]{:S(2)}) %collective-permute-start.7) | collective-permute-done | bytes 98336 | tf_op jit(solution)/shard_map/ppermute | solution.py:259
  100.8 5.6 %collective-permute-done.8 = bf16[384,128]{1,0:T(8,128)(2,1)S(1)} collective-permute-done((bf16[384,128]{1,0:T(8,128)(2,1)S(1)}, bf16[384,128]{1,0:T(8,128)(2,1)S(1)}, u32[]{:S(2)}, u32[]{:S(2)}) %collective-permute-start.8) | collective-permute-done | bytes 98336 | tf_op jit(solution)/shard_map/ppermute | solution.py:259
  106.8 4.1 %collective-permute-done.9 = bf16[384,128]{1,0:T(8,128)(2,1)S(1)} collective-permute-done((bf16[384,128]{1,0:T(8,128)(2,1)S(1)}, bf16[384,128]{1,0:T(8,128)(2,1)S(1)}, u32[]{:S(2)}, u32[]{:S(2)}) %collective-permute-start.9) | collective-permute-done | bytes 98336 | tf_op jit(solution)/shard_map/ppermute | solution.py:259
  111.3 1.1 collective-permute-start.18
  112.4 2.1 collective-permute-start.20
  115.0 0.9 copy-done.11
  116.5 1.3 shard_map.158.b_ref
  117.8 1.0 pad_maximum_fusion.3.refs_4_
  118.8 1.3 shard_map.157.a_ref
  120.1 1.3 shard_map.159.refs_8_
  121.4 11.5 %collective-permute-done.22.refs_4_ = bf16[384,1024]{1,0:T(8,128)(2,1)} collective-permute-done((bf16[384,1024]{1,0:T(8,128)(2,1)}, bf16[384,1024]{1,0:T(8,128)(2,1)}, u32[]{:S(2)}, u32[]{:S(2)}) %collective-permute-start.22) | collective-permute-done | bytes 786464 | tf_op jit(solution)/shard_map/ppermute | solution.py:243
  132.9 2.1 collective-permute-start.1
  135.0 10.8 %collective-permute-done.18.far0_ref = bf16[384,1024]{1,0:T(8,128)(2,1)} collective-permute-done((bf16[384,1024]{1,0:T(8,128)(2,1)S(1)}, bf16[384,1024]{1,0:T(8,128)(2,1)}, u32[]{:S(2)}, u32[]{:S(2)}) %collective-permute-start.18) | collective-permute-done | bytes 786464 | tf_op jit(solution)/shard_map/ppermute | solution.py:243
  145.9 4.1 %collective-permute-start.2 = (bf16[384,128]{1,0:T(8,128)(2,1)}, bf16[384,128]{1,0:T(8,128)(2,1)S(1)}, u32[]{:S(2)}, u32[]{:S(2)}) collective-permute-start(bf16[384,128]{1,0:T(8,128)(2,1)} %get-tuple-element.62.a_ref), channel_id=1, source_target_pairs={{0,16},{8,24},{16,0},{24,8},{32,48},{40,56},{48,32},{56,40},{64,80... | collective-permute-start | bytes 294920 | tf_op jit(solution)/shard_map/ppermute | solution.py:259
  150.0 1.1 collective-permute-start.3
  151.1 1.1 copy-done.2
  152.2 1.1 copy-done.3
  153.3 1.1 copy-done.4
  154.5 1.1 copy-done.12
  156.3 5.3 %shard_map.160.acc_ref = f32[2,384,512]{2,1,0:T(8,128)S(1)} custom-call(s32[4]{0:T(128)S(1)} %copy-done.20, bf16[384,1024]{1,0:T(8,128)(2,1)S(1)} %bitcast.64, bf16[384,1024]{1,0:T(8,128)(2,1)S(1)} %copy-done.2, bf16[384,1024]{1,0:T(8,128)(2,1)S(1)} %copy-done.12, bf16[384,1024]{1,0:T(8,128)(2,1)S(1)} %bitcast.61, ...), custom_call_target="tpu_custom_call" | custom-call | flops 2415919104 | bytes 4194304 | tf_op jit(solution)/shard_map/pallas_call | solution.py:350
  161.6 1.2 collective-permute-start.10
  162.8 3.1 %shard_map.161 = bf16[2,384,256]{2,1,0:T(8,128)(2,1)S(1)} custom-call(s32[4]{0:T(128)S(1)} %copy-done.20, bf16[384,1024]{1,0:T(8,128)(2,1)} %collective-permute-done.18.far0_ref, bf16[384,1024]{1,0:T(8,128)(2,1)} %collective-permute-done.20.far1_ref, f32[2,384,512]{2,1,0:T(8,128)S(1)} %shard_map.160.acc_ref, bf16[4096,256]{1,0:T(8,128)(2,1)S(1)} %bitcast.57, ...), custom_call_target="tpu_custom_call" | custom-call | flops 805306368 | bytes 1048576 | tf_op jit(solution)/shard_map/pallas_call | solution.py:362
  166.1 3.2 %collective-permute-start.25 = (bf16[768,256]{1,0:T(8,128)(2,1)S(1)}, bf16[768,256]{1,0:T(8,128)(2,1)S(1)}, u32[]{:S(2)}, u32[]{:S(2)}) collective-permute-start(bf16[768,256]{1,0:T(8,128)(2,1)S(1)} %bitcast.66), channel_id=1, source_target_pairs={{0,6},{1,7},{2,0},{3,1},{4,2},{5,3},{6,4},{7,5},{8,14},{9,15},{10,... | collective-permute-start | bytes 1179656 | tf_op jit(solution)/shard_map/ppermute | solution.py:243
  169.4 5.7 %collective-permute-done.10.refs_5_ = bf16[4,384,128]{2,1,0:T(8,128)(2,1)S(1)} collective-permute-done((bf16[4,384,128]{2,1,0:T(8,128)(2,1)S(1)}, bf16[4,384,128]{2,1,0:T(8,128)(2,1)S(1)}, u32[]{:S(2)}, u32[]{:S(2)}) %collective-permute-start.10) | collective-permute-done | bytes 393248 | tf_op jit(solution)/shard_map/ppermute | solution.py:259
  175.8 7.0 %collective-permute-done.24.h1_ref = bf16[768,256]{1,0:T(8,128)(2,1)S(1)} collective-permute-done((bf16[768,256]{1,0:T(8,128)(2,1)S(1)}, bf16[768,256]{1,0:T(8,128)(2,1)S(1)}, u32[]{:S(2)}, u32[]{:S(2)}) %collective-permute-start.24) | collective-permute-done | bytes 393248 | tf_op jit(solution)/shard_map/ppermute | solution.py:243
  183.1 3.8 %collective-permute-start.5 = (bf16[4,384,128]{2,1,0:T(8,128)(2,1)S(1)}, bf16[4,384,128]{2,1,0:T(8,128)(2,1)}, u32[]{:S(2)}, u32[]{:S(2)}) collective-permute-start(bf16[4,384,128]{2,1,0:T(8,128)(2,1)S(1)} %pad_maximum_fusion.2.refs_0_), channel_id=1, source_target_pairs={{0,64},{8,72},{16,80},{24,88},{32,96},{40,104},{48,112},{56,120},{... | collective-permute-start | bytes 1179656 | tf_op jit(solution)/shard_map/ppermute | solution.py:259
  188.1 5.7 %shard_map.162 = bf16[16,2,48,512]{3,2,1,0:T(8,128)(2,1)} custom-call(s32[4]{0:T(128)} %pad_add_fusion.place_ref, bf16[768,256]{1,0:T(8,128)(2,1)} %bitcast.68, bf16[768,256]{1,0:T(8,128)(2,1)} %copy-done.35, bf16[768,256]{1,0:T(8,128)(2,1)} %copy-done.36, bf16[768,256]{1,0:T(8,128)(2,1)} %copy-done.37, bf16[1024,512]{1,0:T(8,128)(2,1)} %bitcast.11.own_ref.w_own_ref, ...), custom_call_target="tpu_custom_call" | custom-call | flops 1610612736 | bytes 4194304 | tf_op jit(solution)/shard_map/pallas_call | solution.py:410
  193.8 4.6 %all-to-all-start.3 = ((bf16[16,2,48,512]{3,2,1,0:T(8,128)(2,1)}), bf16[16,2,48,512]{3,2,1,0:T(8,128)(2,1)}, u32[]{:S(2)}, u32[]{:S(2)}) async-start(bf16[16,2,48,512]{3,2,1,0:T(8,128)(2,1)} %shard_map.162), calls=%async_computation.3 | async-start | bytes 3145728 | tf_op jit(solution)/shard_map/all_to_all | solution.py:423
  198.4 5.5 %collective-permute-done.5.refs_2_ = bf16[4,384,128]{2,1,0:T(8,128)(2,1)} collective-permute-done((bf16[4,384,128]{2,1,0:T(8,128)(2,1)S(1)}, bf16[4,384,128]{2,1,0:T(8,128)(2,1)}, u32[]{:S(2)}, u32[]{:S(2)}) %collective-permute-start.5) | collective-permute-done | bytes 393248 | tf_op jit(solution)/shard_map/ppermute | solution.py:259
  203.9 2.2 collective-permute-done.6.refs_3_
  206.1 2.2 copy-done
  208.3 4.9 %shard_map.154 = (bf16[4096,128]{1,0:T(8,128)(2,1)}, bf16[4096,128]{1,0:T(8,128)(2,1)}, bf16[512,128]{1,0:T(8,128)(2,1)S(1)}, bf16[1024,512]{1,0:T(8,128)(2,1)S(1)}, bf16[512,512]{1,0:T(8,128)(2,1)S(1)}) custom-call(s32[4]{0:T(128)S(1)} %copy-done.21, bf16[512,4096]{1,0:T(8,128)(2,1)S(1)} %copy-done, bf16[4,384,128]{2,1,0:T(8,128)(2,1)S(1)} %pad_maximum_fusion.2.refs_0_, ...), custom_call_target="tpu_custom_call" | custom-call | flops 1073741824 | bytes 4194304 | tf_op jit(solution)/shard_map/pallas_call | solution.py:375
  213.2 1.0 copy-done.9
  214.1 7.2 %collective-permute-start.29 = (bf16[512,128]{1,0:T(8,128)(2,1)S(1)}, bf16[512,128]{1,0:T(8,128)(2,1)S(1)}, u32[]{:S(2)}, u32[]{:S(2)}) collective-permute-start(bf16[512,128]{1,0:T(8,128)(2,1)S(1)} %get-tuple-element.52), channel_id=1, source_target_pairs={{0,6},{1,7},{2,0},{3,1},{4,2},{5,3},{6,4},{7,5},{8,14},{9,15},{10,... | collective-permute-start | bytes 393224 | tf_op jit(solution)/shard_map/ppermute | solution.py:243
  221.3 1.5 collective-permute-start.30
  222.8 1.5 collective-permute-done.28
  224.3 3.5 %collective-permute-done.30 = bf16[512,128]{1,0:T(8,128)(2,1)S(1)} collective-permute-done((bf16[512,128]{1,0:T(8,128)(2,1)S(1)}, bf16[512,128]{1,0:T(8,128)(2,1)S(1)}, u32[]{:S(2)}, u32[]{:S(2)}) %collective-permute-start.30) | collective-permute-done | bytes 131104 | tf_op jit(solution)/shard_map/ppermute | solution.py:243
  228.7 1.7 fusion.4
  231.2 1.0 copy-done.8
  232.2 1.0 copy-done.16
  233.3 1.5 shard_map.163.base_ref
  234.8 3.3 %shard_map.155 = (bf16[256,1024]{1,0:T(8,128)(2,1)S(1)}, bf16[256,1024]{1,0:T(8,128)(2,1)}, bf16[256,1024]{1,0:T(8,128)(2,1)}, bf16[256,1024]{1,0:T(8,128)(2,1)}) custom-call(s32[4]{0:T(128)S(1)} %copy-done.21, bf16[1024,512]{1,0:T(8,128)(2,1)} %bitcast.11.own_ref.w_own_ref, bf16[1024,512]{1,0:T(8,128)(2,1)} %collective-permute-done.other_ref.w_other_ref, ...), custom_call_target="tpu_custom_call" | custom-call | flops 1073741824 | bytes 4194304 | tf_op jit(solution)/shard_map/pallas_call | solution.py:471
  239.7 2.7 %collective-permute-start.15 = (bf16[256,1024]{1,0:T(8,128)(2,1)}, bf16[256,1024]{1,0:T(8,128)(2,1)}, u32[]{:S(2)}, u32[]{:S(2)}) collective-permute-start(bf16[256,1024]{1,0:T(8,128)(2,1)} %get-tuple-element.41), channel_id=1, source_target_pairs={{0,4},{1,5},{2,6},{3,7},{4,0},{5,1},{6,2},{7,3},{8,12},{9,13},{10,... | collective-permute-start | bytes 1572872 | tf_op jit(solution)/shard_map/ppermute | solution.py:243
  243.0 1.2 slice.86
  244.3 1.5 slice_bitcast_fusion
  245.8 9.2 %collective-permute-done.14.p1_ref = bf16[256,1024]{1,0:T(8,128)(2,1)} collective-permute-done((bf16[256,1024]{1,0:T(8,128)(2,1)}, bf16[256,1024]{1,0:T(8,128)(2,1)}, u32[]{:S(2)}, u32[]{:S(2)}) %collective-permute-start.14) | collective-permute-done | bytes 524320 | tf_op jit(solution)/shard_map/ppermute | solution.py:243
  255.0 10.8 %collective-permute-done.15.p2_ref = bf16[256,1024]{1,0:T(8,128)(2,1)} collective-permute-done((bf16[256,1024]{1,0:T(8,128)(2,1)}, bf16[256,1024]{1,0:T(8,128)(2,1)}, u32[]{:S(2)}, u32[]{:S(2)}) %collective-permute-start.15) | collective-permute-done | bytes 524320 | tf_op jit(solution)/shard_map/ppermute | solution.py:243
  266.2 3.3 %shard_map.156 = (bf16[128,4096]{1,0:T(8,128)(2,1)}, bf16[128,4096]{1,0:T(8,128)(2,1)}) custom-call(s32[4]{0:T(128)S(1)} %copy-done.21, bf16[256,1024]{1,0:T(8,128)(2,1)S(1)} %copy-done.14, bf16[256,1024]{1,0:T(8,128)(2,1)} %collective-permute-done.14.p1_ref, bf16[256,1024]{1,0:T(8,128)(2,1)} %collective-permute-done.15.p2_ref, ...), custom_call_target="tpu_custom_call" | custom-call | flops 1048576 | bytes 4194304 | tf_op jit(solution)/shard_map/pallas_call | solution.py:487
  269.5 1.8 shard_map.164.base_ref
  271.3 1.4 shard_map.165
  (116 shorter events, 10.6 us)
Async XLA Ops:
  7.8 8.2 %copy-start.34 = (f32[256]{0:T(256)S(1)}, f32[256]{0:T(256)}, u32[]{:S(2)}) copy-start(f32[256]{0:T(256)} %param.11) | copy-start | bytes 3076
  7.8 32.7 %all-to-all-start = ((bf16[16,48,1024]{2,1,0:T(8,128)(2,1)}), bf16[16,48,1024]{2,1,0:T(8,128)(2,1)S(1)}, u32[]{:S(2)}, u32[]{:S(2)}) async-start(bf16[16,48,1024]{2,1,0:T(8,128)(2,1)} %bitcast.70), calls=%async_computation | async-start | bytes 3145728 | tf_op jit(solution)/shard_map/all_to_all | solution.py:307
  41.8 33.9 %all-to-all-start.1 = ((bf16[16,256,256]{2,1,0:T(8,128)(2,1)}), bf16[16,256,256]{2,1,0:T(8,128)(2,1)S(1)}, u32[]{:S(2)}, u32[]{:S(2)}) async-start(bf16[16,256,256]{2,1,0:T(8,128)(2,1)} %pad_maximum_fusion), calls=%async_computation.1 | async-start | bytes 4194304 | tf_op jit(solution)/shard_map/all_to_all | solution.py:318
  45.6 30.2 %copy-start.27 = (f32[64,512]{1,0:T(8,128)S(1)}, f32[64,512]{1,0:T(8,128)}, u32[]{:S(2)}) copy-start(f32[64,512]{1,0:T(8,128)} %param.17) | copy-start | bytes 393220
  45.6 31.7 %copy-start.25 = (f32[256,128]{1,0:T(8,128)S(1)}, f32[256,128]{1,0:T(8,128)}, u32[]{:S(2)}) copy-start(f32[256,128]{1,0:T(8,128)} %param.16) | copy-start | bytes 393220
  45.6 31.7 %copy-start.26 = (f32[256,128]{1,0:T(8,128)S(1)}, f32[256,128]{1,0:T(8,128)}, u32[]{:S(2)}) copy-start(f32[256,128]{1,0:T(8,128)} %param.15) | copy-start | bytes 393220
  75.7 74.3 %collective-permute-start.23 = (bf16[4096,256]{1,0:T(8,128)(2,1)S(1)}, bf16[4096,256]{1,0:T(8,128)(2,1)}, u32[]{:S(2)}, u32[]{:S(2)}) collective-permute-start(bf16[4096,256]{1,0:T(8,128)(2,1)S(1)} %bitcast.55), channel_id=1, source_target_pairs={{0,1},{1,0},{2,3},{3,2},{4,5},{5,4},{6,7},{7,6},{8,9},{9,8},{10,11... | collective-permute-start | bytes 6291464 | tf_op jit(solution)/shard_map/ppermute | solution.py:246
  75.7 35.5 %collective-permute-start.17 = (bf16[384,1024]{1,0:T(8,128)(2,1)}, bf16[384,1024]{1,0:T(8,128)(2,1)S(1)}, u32[]{:S(2)}, u32[]{:S(2)}) collective-permute-start(bf16[384,1024]{1,0:T(8,128)(2,1)} %bitcast.62), channel_id=1, source_target_pairs={{0,2},{1,3},{2,4},{3,5},{4,6},{5,7},{6,0},{7,1},{8,10},{9,11},{10,... | collective-permute-start | bytes 2359304 | tf_op jit(solution)/shard_map/ppermute | solution.py:243
  77.4 35.0 %collective-permute-start.19 = (bf16[384,1024]{1,0:T(8,128)(2,1)}, bf16[384,1024]{1,0:T(8,128)(2,1)}, u32[]{:S(2)}, u32[]{:S(2)}) collective-permute-start(bf16[384,1024]{1,0:T(8,128)(2,1)} %bitcast.59), channel_id=1, source_target_pairs={{0,6},{1,7},{2,0},{3,1},{4,2},{5,3},{6,4},{7,5},{8,14},{9,15},{10,... | collective-permute-start | bytes 2359304 | tf_op jit(solution)/shard_map/ppermute | solution.py:243
  79.2 36.6 %all-to-all-start.2 = ((bf16[16,64,512]{2,1,0:T(8,128)(2,1)}), bf16[16,64,512]{2,1,0:T(8,128)(2,1)}, u32[]{:S(2)}, u32[]{:S(2)}) async-start(bf16[16,64,512]{2,1,0:T(8,128)(2,1)} %convert_element_type.27), calls=%async_computation.2 | async-start | bytes 2097152 | tf_op jit(solution)/shard_map/all_to_all | solution.py:320
  83.6 67.5 %copy-start.20 = (s32[4]{0:T(128)S(1)}, s32[4]{0:T(128)}, u32[]{:S(2)}) copy-start(s32[4]{0:T(128)} %pad_add_fusion.place_ref) | copy-start | bytes 52
  83.6 31.3 %collective-permute-start.21 = (bf16[384,1024]{1,0:T(8,128)(2,1)}, bf16[384,1024]{1,0:T(8,128)(2,1)S(1)}, u32[]{:S(2)}, u32[]{:S(2)}) collective-permute-start(bf16[384,1024]{1,0:T(8,128)(2,1)} %bitcast.63), channel_id=1, source_target_pairs={{0,6},{1,7},{2,0},{3,1},{4,2},{5,3},{6,4},{7,5},{8,14},{9,15},{10,... | collective-permute-start | bytes 2359304 | tf_op jit(solution)/shard_map/ppermute | solution.py:243
  85.2 31.3 %copy-start.24 = (bf16[384,128]{1,0:T(8,128)(2,1)}, bf16[384,128]{1,0:T(8,128)(2,1)S(1)}, u32[]{:S(2)}) copy-start(bf16[384,128]{1,0:T(8,128)(2,1)S(1)} %get-tuple-element.60.b_ref) | copy-start | bytes 294916
  85.2 15.0 %collective-permute-start.7 = (bf16[384,128]{1,0:T(8,128)(2,1)S(1)}, bf16[384,128]{1,0:T(8,128)(2,1)S(1)}, u32[]{:S(2)}, u32[]{:S(2)}) collective-permute-start(bf16[384,128]{1,0:T(8,128)(2,1)S(1)} %get-tuple-element.60.b_ref), channel_id=1, source_target_pairs={{0,32},{8,40},{16,48},{24,56},{32,64},{40,72},{48,80},{56,88},{64,... | collective-permute-start | bytes 294920 | tf_op jit(solution)/shard_map/ppermute | solution.py:259
  100.2 17.5 %copy-start.28 = (bf16[384,128]{1,0:T(8,128)(2,1)}, bf16[384,128]{1,0:T(8,128)(2,1)S(1)}, u32[]{:S(2)}) copy-start(bf16[384,128]{1,0:T(8,128)(2,1)S(1)} %collective-permute-done.7) | copy-start | bytes 294916
  100.2 6.1 %collective-permute-start.8 = (bf16[384,128]{1,0:T(8,128)(2,1)S(1)}, bf16[384,128]{1,0:T(8,128)(2,1)S(1)}, u32[]{:S(2)}, u32[]{:S(2)}) collective-permute-start(bf16[384,128]{1,0:T(8,128)(2,1)S(1)} %get-tuple-element.60.b_ref), channel_id=1, source_target_pairs={{0,64},{8,72},{16,80},{24,88},{32,96},{40,104},{48,112},{56,120},{... | collective-permute-start | bytes 294920 | tf_op jit(solution)/shard_map/ppermute | solution.py:259
  106.4 11.4 %copy-start.29 = (bf16[384,128]{1,0:T(8,128)(2,1)}, bf16[384,128]{1,0:T(8,128)(2,1)S(1)}, u32[]{:S(2)}) copy-start(bf16[384,128]{1,0:T(8,128)(2,1)S(1)} %collective-permute-done.8) | copy-start | bytes 294916
  106.4 4.6 %collective-permute-start.9 = (bf16[384,128]{1,0:T(8,128)(2,1)S(1)}, bf16[384,128]{1,0:T(8,128)(2,1)S(1)}, u32[]{:S(2)}, u32[]{:S(2)}) collective-permute-start(bf16[384,128]{1,0:T(8,128)(2,1)S(1)} %get-tuple-element.60.b_ref), channel_id=1, source_target_pairs={{0,96},{8,104},{16,112},{24,120},{32,0},{40,8},{48,16},{56,24},{64... | collective-permute-start | bytes 294920 | tf_op jit(solution)/shard_map/ppermute | solution.py:259
  111.0 4.9 %copy-start.30 = (bf16[384,128]{1,0:T(8,128)(2,1)}, bf16[384,128]{1,0:T(8,128)(2,1)S(1)}, u32[]{:S(2)}) copy-start(bf16[384,128]{1,0:T(8,128)(2,1)S(1)} %collective-permute-done.9) | copy-start | bytes 294916
  111.0 21.9 %collective-permute-start.22 = (bf16[384,1024]{1,0:T(8,128)(2,1)}, bf16[384,1024]{1,0:T(8,128)(2,1)}, u32[]{:S(2)}, u32[]{:S(2)}) collective-permute-start(bf16[384,1024]{1,0:T(8,128)(2,1)} %bitcast.60), channel_id=1, source_target_pairs={{0,2},{1,3},{2,4},{3,5},{4,6},{5,7},{6,0},{7,1},{8,10},{9,11},{10,... | collective-permute-start | bytes 2359304 | tf_op jit(solution)/shard_map/ppermute | solution.py:243
  111.3 7.6 %copy-start.1 = (bf16[384,1024]{1,0:T(8,128)(2,1)}, bf16[384,1024]{1,0:T(8,128)(2,1)S(1)}, u32[]{:S(2)}) copy-start(bf16[384,1024]{1,0:T(8,128)(2,1)S(1)} %collective-permute-done.17.a_ref.refs_1_) | copy-start | bytes 2359300
  111.3 34.6 %collective-permute-start.18 = (bf16[384,1024]{1,0:T(8,128)(2,1)S(1)}, bf16[384,1024]{1,0:T(8,128)(2,1)}, u32[]{:S(2)}, u32[]{:S(2)}) collective-permute-start(bf16[384,1024]{1,0:T(8,128)(2,1)S(1)} %collective-permute-done.17.a_ref.refs_1_), channel_id=1, source_target_pairs={{0,2},{1,3},{2,4},{3,5},{4,6},{5,7},{6,0},{7,1},{8,10},{9,11},{10,... | collective-permute-start | bytes 2359304 | tf_op jit(solution)/shard_map/ppermute | solution.py:243
  112.4 49.2 %collective-permute-start.20 = (bf16[384,1024]{1,0:T(8,128)(2,1)}, bf16[384,1024]{1,0:T(8,128)(2,1)}, u32[]{:S(2)}, u32[]{:S(2)}) collective-permute-start(bf16[384,1024]{1,0:T(8,128)(2,1)} %collective-permute-done.19.b_ref.refs_5_), channel_id=1, source_target_pairs={{0,6},{1,7},{2,0},{3,1},{4,2},{5,3},{6,4},{7,5},{8,14},{9,15},{10,... | collective-permute-start | bytes 2359304 | tf_op jit(solution)/shard_map/ppermute | solution.py:243
  115.8 60.0 %collective-permute-start = (bf16[1024,512]{1,0:T(8,128)(2,1)}, bf16[1024,512]{1,0:T(8,128)(2,1)}, u32[]{:S(2)}, u32[]{:S(2)}) collective-permute-start(bf16[1024,512]{1,0:T(8,128)(2,1)} %bitcast.11.own_ref.w_own_ref), channel_id=1, source_target_pairs={{0,1},{1,0},{2,3},{3,2},{4,5},{5,4},{6,7},{7,6},{8,9},{9,8},{10,11... | collective-permute-start | bytes 3145736 | tf_op jit(solution)/shard_map/ppermute | solution.py:246
  132.9 33.1 %collective-permute-start.1 = (bf16[384,128]{1,0:T(8,128)(2,1)}, bf16[384,128]{1,0:T(8,128)(2,1)S(1)}, u32[]{:S(2)}, u32[]{:S(2)}) collective-permute-start(bf16[384,128]{1,0:T(8,128)(2,1)} %get-tuple-element.62.a_ref), channel_id=1, source_target_pairs={{0,8},{8,16},{16,24},{24,0},{32,40},{40,48},{48,56},{56,32},{64,72... | collective-permute-start | bytes 294920 | tf_op jit(solution)/shard_map/ppermute | solution.py:259
  145.9 20.2 %collective-permute-start.2 = (bf16[384,128]{1,0:T(8,128)(2,1)}, bf16[384,128]{1,0:T(8,128)(2,1)S(1)}, u32[]{:S(2)}, u32[]{:S(2)}) collective-permute-start(bf16[384,128]{1,0:T(8,128)(2,1)} %get-tuple-element.62.a_ref), channel_id=1, source_target_pairs={{0,16},{8,24},{16,0},{24,8},{32,48},{40,56},{48,32},{56,40},{64,80... | collective-permute-start | bytes 294920 | tf_op jit(solution)/shard_map/ppermute | solution.py:259
  150.0 19.3 %collective-permute-start.3 = (bf16[384,128]{1,0:T(8,128)(2,1)}, bf16[384,128]{1,0:T(8,128)(2,1)S(1)}, u32[]{:S(2)}, u32[]{:S(2)}) collective-permute-start(bf16[384,128]{1,0:T(8,128)(2,1)} %get-tuple-element.62.a_ref), channel_id=1, source_target_pairs={{0,24},{8,0},{16,8},{24,16},{32,56},{40,32},{48,40},{56,48},{64,88... | collective-permute-start | bytes 294920 | tf_op jit(solution)/shard_map/ppermute | solution.py:259
  151.1 1.1 copy-start.2
  152.2 1.1 copy-start.3
  153.3 1.1 copy-start.4
  161.6 13.4 %collective-permute-start.10 = (bf16[4,384,128]{2,1,0:T(8,128)(2,1)S(1)}, bf16[4,384,128]{2,1,0:T(8,128)(2,1)S(1)}, u32[]{:S(2)}, u32[]{:S(2)}) collective-permute-start(bf16[4,384,128]{2,1,0:T(8,128)(2,1)S(1)} %pad_maximum_fusion.3.refs_4_), channel_id=1, source_target_pairs={{0,8},{8,16},{16,24},{24,0},{32,40},{40,48},{48,56},{56,32},{64,72... | collective-permute-start | bytes 1179656 | tf_op jit(solution)/shard_map/ppermute | solution.py:259
  166.0 22.2 %copy-start.17 = (bf16[2,384,256]{2,1,0:T(8,128)(2,1)}, bf16[2,384,256]{2,1,0:T(8,128)(2,1)S(1)}, u32[]{:S(2)}) copy-start(bf16[2,384,256]{2,1,0:T(8,128)(2,1)S(1)} %shard_map.161) | copy-start | bytes 1179652
  166.0 16.8 %collective-permute-start.24 = (bf16[768,256]{1,0:T(8,128)(2,1)S(1)}, bf16[768,256]{1,0:T(8,128)(2,1)S(1)}, u32[]{:S(2)}, u32[]{:S(2)}) collective-permute-start(bf16[768,256]{1,0:T(8,128)(2,1)S(1)} %bitcast.65), channel_id=1, source_target_pairs={{0,2},{1,3},{2,4},{3,5},{4,6},{5,7},{6,0},{7,1},{8,10},{9,11},{10,... | collective-permute-start | bytes 1179656 | tf_op jit(solution)/shard_map/ppermute | solution.py:243
  166.1 17.0 %collective-permute-start.25 = (bf16[768,256]{1,0:T(8,128)(2,1)S(1)}, bf16[768,256]{1,0:T(8,128)(2,1)S(1)}, u32[]{:S(2)}, u32[]{:S(2)}) collective-permute-start(bf16[768,256]{1,0:T(8,128)(2,1)S(1)} %bitcast.66), channel_id=1, source_target_pairs={{0,6},{1,7},{2,0},{3,1},{4,2},{5,3},{6,4},{7,5},{8,14},{9,15},{10,... | collective-permute-start | bytes 1179656 | tf_op jit(solution)/shard_map/ppermute | solution.py:243
  169.3 17.6 %collective-permute-start.26 = (bf16[768,256]{1,0:T(8,128)(2,1)S(1)}, bf16[768,256]{1,0:T(8,128)(2,1)S(1)}, u32[]{:S(2)}, u32[]{:S(2)}) collective-permute-start(bf16[768,256]{1,0:T(8,128)(2,1)S(1)} %bitcast.67), channel_id=1, source_target_pairs={{0,4},{1,5},{2,6},{3,7},{4,0},{5,1},{6,2},{7,3},{8,12},{9,13},{10,... | collective-permute-start | bytes 1179656 | tf_op jit(solution)/shard_map/ppermute | solution.py:243
  175.8 22.6 %collective-permute-start.11 = (bf16[4,384,128]{2,1,0:T(8,128)(2,1)S(1)}, bf16[4,384,128]{2,1,0:T(8,128)(2,1)}, u32[]{:S(2)}, u32[]{:S(2)}) collective-permute-start(bf16[4,384,128]{2,1,0:T(8,128)(2,1)S(1)} %pad_maximum_fusion.3.refs_4_), channel_id=1, source_target_pairs={{0,16},{8,24},{16,0},{24,8},{32,48},{40,56},{48,32},{56,40},{64,80... | collective-permute-start | bytes 1179656 | tf_op jit(solution)/shard_map/ppermute | solution.py:259
  175.8 22.6 %collective-permute-start.12 = (bf16[4,384,128]{2,1,0:T(8,128)(2,1)S(1)}, bf16[4,384,128]{2,1,0:T(8,128)(2,1)}, u32[]{:S(2)}, u32[]{:S(2)}) collective-permute-start(bf16[4,384,128]{2,1,0:T(8,128)(2,1)S(1)} %pad_maximum_fusion.3.refs_4_), channel_id=1, source_target_pairs={{0,24},{8,0},{16,8},{24,16},{32,56},{40,32},{48,40},{56,48},{64,88... | collective-permute-start | bytes 1179656 | tf_op jit(solution)/shard_map/ppermute | solution.py:259
  182.8 4.1 %copy-start.35 = (bf16[768,256]{1,0:T(8,128)(2,1)}, bf16[768,256]{1,0:T(8,128)(2,1)S(1)}, u32[]{:S(2)}) copy-start(bf16[768,256]{1,0:T(8,128)(2,1)S(1)} %collective-permute-done.24.h1_ref) | copy-start | bytes 1179652
  182.8 15.6 %collective-permute-start.4 = (bf16[4,384,128]{2,1,0:T(8,128)(2,1)S(1)}, bf16[4,384,128]{2,1,0:T(8,128)(2,1)}, u32[]{:S(2)}, u32[]{:S(2)}) collective-permute-start(bf16[4,384,128]{2,1,0:T(8,128)(2,1)S(1)} %pad_maximum_fusion.2.refs_0_), channel_id=1, source_target_pairs={{0,32},{8,40},{16,48},{24,56},{32,64},{40,72},{48,80},{56,88},{64,... | collective-permute-start | bytes 1179656 | tf_op jit(solution)/shard_map/ppermute | solution.py:259
  183.1 3.8 %copy-start.36 = (bf16[768,256]{1,0:T(8,128)(2,1)}, bf16[768,256]{1,0:T(8,128)(2,1)S(1)}, u32[]{:S(2)}) copy-start(bf16[768,256]{1,0:T(8,128)(2,1)S(1)} %collective-permute-done.25.h2_ref) | copy-start | bytes 1179652
  183.1 20.8 %collective-permute-start.5 = (bf16[4,384,128]{2,1,0:T(8,128)(2,1)S(1)}, bf16[4,384,128]{2,1,0:T(8,128)(2,1)}, u32[]{:S(2)}, u32[]{:S(2)}) collective-permute-start(bf16[4,384,128]{2,1,0:T(8,128)(2,1)S(1)} %pad_maximum_fusion.2.refs_0_), channel_id=1, source_target_pairs={{0,64},{8,72},{16,80},{24,88},{32,96},{40,104},{48,112},{56,120},{... | collective-permute-start | bytes 1179656 | tf_op jit(solution)/shard_map/ppermute | solution.py:259
  187.6 18.5 %collective-permute-start.6 = (bf16[4,384,128]{2,1,0:T(8,128)(2,1)S(1)}, bf16[4,384,128]{2,1,0:T(8,128)(2,1)}, u32[]{:S(2)}, u32[]{:S(2)}) collective-permute-start(bf16[4,384,128]{2,1,0:T(8,128)(2,1)S(1)} %pad_maximum_fusion.2.refs_0_), channel_id=1, source_target_pairs={{0,96},{8,104},{16,112},{24,120},{32,0},{40,8},{48,16},{56,24},{64... | collective-permute-start | bytes 1179656 | tf_op jit(solution)/shard_map/ppermute | solution.py:259
  193.8 12.3 %copy-start.19 = (bf16[4,384,128]{2,1,0:T(8,128)(2,1)S(1)}, bf16[4,384,128]{2,1,0:T(8,128)(2,1)}, u32[]{:S(2)}) copy-start(bf16[4,384,128]{2,1,0:T(8,128)(2,1)} %copy-done.18) | copy-start | bytes 1179652
  193.8 12.3 %copy-start.21 = (s32[4]{0:T(128)S(1)}, s32[4]{0:T(128)}, u32[]{:S(2)}) copy-start(s32[4]{0:T(128)} %pad_add_fusion.place_ref) | copy-start | bytes 52
  193.8 49.2 %all-to-all-start.3 = ((bf16[16,2,48,512]{3,2,1,0:T(8,128)(2,1)}), bf16[16,2,48,512]{3,2,1,0:T(8,128)(2,1)}, u32[]{:S(2)}, u32[]{:S(2)}) async-start(bf16[16,2,48,512]{3,2,1,0:T(8,128)(2,1)} %shard_map.162), calls=%async_computation.3 | async-start | bytes 3145728 | tf_op jit(solution)/shard_map/all_to_all | solution.py:423
  206.1 2.2 copy-start
  208.3 14.5 %copy-start.33 = (f32[512,2]{0,1:T(2,128)S(1)}, f32[512,2]{0,1:T(2,128)}, u32[]{:S(2)}) copy-start(f32[512,2]{0,1:T(2,128)} %param.19) | copy-start | bytes 12292
  208.3 20.3 %copy-start.31 = (s32[512,2]{0,1:T(2,128)S(1)}, s32[512,2]{0,1:T(2,128)}, u32[]{:S(2)}) copy-start(s32[512,2]{0,1:T(2,128)} %param.18) | copy-start | bytes 12292
  208.3 20.3 %copy-start.32 = (s32[2,512]{1,0:T(2,128)S(1)}, s32[2,512]{1,0:T(2,128)}, u32[]{:S(2)}) copy-start(s32[2,512]{1,0:T(2,128)} %get-tuple-element.47) | copy-start | bytes 12292
  214.1 13.8 %copy-start.23 = (bf16[512,512]{1,0:T(8,128)(2,1)}, bf16[512,512]{1,0:T(8,128)(2,1)S(1)}, u32[]{:S(2)}) copy-start(bf16[512,512]{1,0:T(8,128)(2,1)S(1)} %get-tuple-element.38) | copy-start | bytes 1572868
  214.1 10.2 %collective-permute-start.28 = (bf16[512,128]{1,0:T(8,128)(2,1)S(1)}, bf16[512,128]{1,0:T(8,128)(2,1)S(1)}, u32[]{:S(2)}, u32[]{:S(2)}) collective-permute-start(bf16[512,128]{1,0:T(8,128)(2,1)S(1)} %get-tuple-element.52), channel_id=1, source_target_pairs={{0,2},{1,3},{2,4},{3,5},{4,6},{5,7},{6,0},{7,1},{8,10},{9,11},{10,... | collective-permute-start | bytes 393224 | tf_op jit(solution)/shard_map/ppermute | solution.py:243
  214.1 10.2 %collective-permute-start.29 = (bf16[512,128]{1,0:T(8,128)(2,1)S(1)}, bf16[512,128]{1,0:T(8,128)(2,1)S(1)}, u32[]{:S(2)}, u32[]{:S(2)}) collective-permute-start(bf16[512,128]{1,0:T(8,128)(2,1)S(1)} %get-tuple-element.52), channel_id=1, source_target_pairs={{0,6},{1,7},{2,0},{3,1},{4,2},{5,3},{6,4},{7,5},{8,14},{9,15},{10,... | collective-permute-start | bytes 393224 | tf_op jit(solution)/shard_map/ppermute | solution.py:243
  221.3 6.5 %collective-permute-start.30 = (bf16[512,128]{1,0:T(8,128)(2,1)S(1)}, bf16[512,128]{1,0:T(8,128)(2,1)S(1)}, u32[]{:S(2)}, u32[]{:S(2)}) collective-permute-start(bf16[512,128]{1,0:T(8,128)(2,1)S(1)} %get-tuple-element.52), channel_id=1, source_target_pairs={{0,4},{1,5},{2,6},{3,7},{4,0},{5,1},{6,2},{7,3},{8,12},{9,13},{10,... | collective-permute-start | bytes 393224 | tf_op jit(solution)/shard_map/ppermute | solution.py:243
  227.9 2.5 copy-start.7
  227.9 2.5 collective-permute-start.31
  228.0 3.1 %copy-start.10 = (bf16[1024,512]{1,0:T(8,128)(2,1)S(1)}, bf16[1024,512]{1,0:T(8,128)(2,1)}, u32[]{:S(2)}) copy-start(bf16[1024,512]{1,0:T(8,128)(2,1)} %copy-done.9) | copy-start | bytes 3145732
  228.1 6.8 %collective-permute-start.13 = (bf16[512,512]{1,0:T(8,128)(2,1)}, bf16[512,512]{1,0:T(8,128)(2,1)S(1)}, u32[]{:S(2)}, u32[]{:S(2)}) collective-permute-start(bf16[512,512]{1,0:T(8,128)(2,1)} %copy-done.23), channel_id=1, source_target_pairs={{0,1},{1,0},{2,3},{3,2},{4,5},{5,4},{6,7},{7,6},{8,9},{9,8},{10,11... | collective-permute-start | bytes 1572872 | tf_op jit(solution)/shard_map/ppermute | solution.py:246
  238.9 16.1 %collective-permute-start.14 = (bf16[256,1024]{1,0:T(8,128)(2,1)}, bf16[256,1024]{1,0:T(8,128)(2,1)}, u32[]{:S(2)}, u32[]{:S(2)}) collective-permute-start(bf16[256,1024]{1,0:T(8,128)(2,1)} %get-tuple-element.40), channel_id=1, source_target_pairs={{0,2},{1,3},{2,4},{3,5},{4,6},{5,7},{6,0},{7,1},{8,10},{9,11},{10,... | collective-permute-start | bytes 1572872 | tf_op jit(solution)/shard_map/ppermute | solution.py:243
  239.7 26.1 %collective-permute-start.15 = (bf16[256,1024]{1,0:T(8,128)(2,1)}, bf16[256,1024]{1,0:T(8,128)(2,1)}, u32[]{:S(2)}, u32[]{:S(2)}) collective-permute-start(bf16[256,1024]{1,0:T(8,128)(2,1)} %get-tuple-element.41), channel_id=1, source_target_pairs={{0,4},{1,5},{2,6},{3,7},{4,0},{5,1},{6,2},{7,3},{8,12},{9,13},{10,... | collective-permute-start | bytes 1572872 | tf_op jit(solution)/shard_map/ppermute | solution.py:243
  242.4 23.8 %collective-permute-start.16 = (bf16[256,1024]{1,0:T(8,128)(2,1)}, bf16[256,1024]{1,0:T(8,128)(2,1)}, u32[]{:S(2)}, u32[]{:S(2)}) collective-permute-start(bf16[256,1024]{1,0:T(8,128)(2,1)} %get-tuple-element.42), channel_id=1, source_target_pairs={{0,6},{1,7},{2,0},{3,1},{4,2},{5,3},{6,4},{7,5},{8,14},{9,15},{10,... | collective-permute-start | bytes 1572872 | tf_op jit(solution)/shard_map/ppermute | solution.py:243
  244.2 22.0 %copy-start.14 = (bf16[256,1024]{1,0:T(8,128)(2,1)S(1)}, bf16[256,1024]{1,0:T(8,128)(2,1)}, u32[]{:S(2)}) copy-start(bf16[256,1024]{1,0:T(8,128)(2,1)} %copy-done.13) | copy-start | bytes 1572868
  244.2 27.1 %collective-permute-start.27 = (bf16[768,512]{1,0:T(8,128)(2,1)S(1)}, bf16[768,512]{1,0:T(8,128)(2,1)S(1)}, u32[]{:S(2)}, u32[]{:S(2)}) collective-permute-start(bf16[768,512]{1,0:T(8,128)(2,1)S(1)} %bitcast.71), channel_id=1, source_target_pairs={{0,1},{1,0},{2,3},{3,2},{4,5},{5,4},{6,7},{7,6},{8,9},{9,8},{10,11... | collective-permute-start | bytes 2359304 | tf_op jit(solution)/shard_map/ppermute | solution.py:246
  245.8 23.8 %copy-start.6 = (bf16[512,768]{1,0:T(8,128)(2,1)S(1)}, bf16[512,768]{1,0:T(8,128)(2,1)}, u32[]{:S(2)}) copy-start(bf16[512,768]{1,0:T(8,128)(2,1)} %get-tuple-element.51.weight_ref) | copy-start | bytes 2359300
  269.5 1.8 copy-start.5
  (10 other events, 8.8 us)

commit v6 on v3

--- a/solution.py
+++ b/solution.py
@@ -28,29 +28,15 @@
     return pltpu.CompilerParams(vmem_limit_bytes=mib << 20)
 
 
-def dispatch_kernel(half, place_ref, route_ref, tok_ref, normed_ref, out_ref, slot_ref, *scratch):
-    taken, given, kept, placing, in_sem, out_sem = scratch
-    chip, core = place_ref[0], place_ref[1]
-    steps = in_sem.shape[0]
-    tok_rows = taken.shape[0]
-    rows = tok_rows // steps
-    quarter = out_ref.shape[1]
+def route_kernel(half, route_ref, tok_ref, out_ref, slot_ref, kept, placing, sem):
+    t = lax.axis_index("tp")
+    chip, core = t // 2, lax.rem(t, 2)
+    tok_rows, quarter = kept.shape
     spots = placing.shape[0]
     experts = spots // half
-
-    def span(step):
-        return pl.ds(step * rows, rows)
-
-    reads = [
-        pltpu.make_async_copy(tok_ref.at[span(i)], taken.at[span(i)], in_sem.at[i])
-        for i in range(steps)
-    ]
-    writes = [
-        pltpu.make_async_copy(given.at[span(i)], normed_ref.at[span(i)], out_sem.at[i])
-        for i in range(steps)
-    ]
-    for read in reads:
-        read.start()
+    at = pl.ds(pl.multiple_of(chip * quarter, quarter), quarter)
+    read = pltpu.make_async_copy(tok_ref.at[:, at], kept, sem)
+    read.start()
 
     ids = lax.broadcasted_iota(jnp.int32, (experts, tok_rows), 0)
     hot = [route_ref[k : k + 1, :] == ids for k in range(route_ref.shape[0])]
@@ -69,51 +55,80 @@
         target = jnp.where(here, route_ref[k : k + 1, :] * half + local, -1)
         total = total + jnp.where(spot == target, 1.0, 0.0)
     placing[...] = total.astype(bf16)
-
-    at = pl.multiple_of(chip * quarter, quarter)
+    read.wait()
+    for c in range(0, spots, 256):
+        out_ref[c : c + 256, :] = dot(placing[c : c + 256, :], kept[...]).astype(bf16)
+
+
+def norm_kernel(tok_ref, normed_ref, taken, given, in_sem, out_sem):
+    steps = in_sem.shape[0]
+    rows = taken.shape[0] // steps
+
+    def span(step):
+        return pl.ds(step * rows, rows)
+
+    reads = [
+        pltpu.make_async_copy(tok_ref.at[span(i)], taken.at[span(i)], in_sem.at[i])
+        for i in range(steps)
+    ]
+    writes = [
+        pltpu.make_async_copy(given.at[span(i)], normed_ref.at[span(i)], out_sem.at[i])
+        for i in range(steps)
+    ]
+    for read in reads:
+        read.start()
     for i in range(steps):
         reads[i].wait()
         for r in range(i * rows, (i + 1) * rows, 16):
             values = taken[r : r + 16, :].astype(f32)
             scale = lax.rsqrt(jnp.mean(values * values, axis=1, keepdims=True) + norm_eps)
             given[r : r + 16, :] = (values * scale).astype(bf16)
-        kept[i * rows : (i + 1) * rows, :] = given[i * rows : (i + 1) * rows, pl.ds(at, quarter)]
         if i:
             writes[i - 1].start()
-    for c in range(0, spots, 256):
-        out_ref[c : c + 256, :] = dot(placing[c : c + 256, :], kept[...]).astype(bf16)
     writes[steps - 1].start()
     for write in writes:
         write.wait()
 
 
+def squares(x_ref):
+    total = None
+    for c in range(0, x_ref.shape[1], 128):
+        values = x_ref[:, c : c + 128].astype(f32)
+        total = values * values if total is None else total + values * values
+    return total
+
+
 def mark_kernel(a_ref, b_ref, out_ref):
     out_ref[...] = a_ref[...] + b_ref[...]
 
 
 def first_kernel(place_ref, *refs):
-    x_refs, (w_own_ref, w_other_ref, _, acc_ref) = refs[:6], refs[6:]
+    x_refs, (w_own_ref, w_other_ref, _, acc_ref, sq_ref) = refs[:6], refs[6:]
     chip = place_ref[0]
     quarter, wide = x_refs[0].shape[1], w_own_ref.shape[1]
     chips = w_own_ref.shape[0] // quarter
     for part in range(2):
+        blocks = x_refs[3 * part : 3 * part + 3]
         for half, w_ref in ((0, w_own_ref), (1, w_other_ref)):
             total = None
-            for x_ref, shift in zip(x_refs[3 * part : 3 * part + 3], (0, chips - 1, 1)):
+            for x_ref, shift in zip(blocks, (0, chips - 1, 1)):
                 at = pl.multiple_of(lax.rem(chip + shift, chips) * quarter, quarter)
                 term = dot(x_ref[...], w_ref[pl.ds(at, quarter), :])
                 total = term if total is None else total + term
             acc_ref[part, :, half * wide : (half + 1) * wide] = total
-
-
-def hidden_kernel(place_ref, far0_ref, far1_ref, acc_ref, w_own_ref, w_other_ref, out_ref):
+        sq_ref[part] = squares(blocks[0]) + squares(blocks[1]) + squares(blocks[2])
+
+
+def hidden_kernel(width, place_ref, far0_ref, far1_ref, acc_ref, sq_ref, w0_ref, w1_ref, out_ref):
     core = place_ref[1]
-    wide = w_own_ref.shape[1]
+    wide = w0_ref.shape[1]
     hs = wide // 2
     for part, far_ref in enumerate((far0_ref, far1_ref)):
-        for half, w_ref, slot in ((0, w_own_ref, core), (1, w_other_ref, 1 - core)):
+        sums = jnp.sum(sq_ref[part] + squares(far_ref), axis=1, keepdims=True)
+        scale = lax.rsqrt(sums * (1.0 / width) + norm_eps)
+        for half, w_ref, slot in ((0, w0_ref, core), (1, w1_ref, 1 - core)):
             total = acc_ref[part, :, half * wide : (half + 1) * wide]
-            total = total + dot(far_ref[...], w_ref[...])
+            total = (total + dot(far_ref[...], w_ref[...])) * scale
             gate, up = total[:, :hs], total[:, hs:]
             value = (gate / (1.0 + jnp.exp(-gate)) * up).astype(bf16)
             out_ref[part, :, pl.ds(pl.multiple_of(slot * hs, hs), hs)] = value
@@ -171,7 +186,8 @@
 
 
 def mix_kernel(weight_ref, got_ref, base_ref, out_ref):
-    out_ref[...] = (base_ref[...] + dot(weight_ref[...], got_ref[...])).astype(out_ref.dtype)
+    got = got_ref[...].reshape(weight_ref.shape[1], out_ref.shape[1])
+    out_ref[...] = (base_ref[...] + dot(weight_ref[...], got)).astype(out_ref.dtype)
 
 
 def chunk_kernel(place_ref, own_ref, other_ref, sd_ref, sd_other_ref, *out_refs):
@@ -187,17 +203,26 @@
         out_ref[hs:, cols:] = sd_other_ref[far, :]
 
 
-def join_kernel(place_ref, p0_ref, p1_ref, p2_ref, p3_ref, routed_ref, shared_ref):
+def join_kernel(place_ref, p0_ref, p1_ref, p2_ref, p3_ref, routed_ref, shared_ref, sems):
     chip, core = place_ref[0], place_ref[1]
     hs = routed_ref.shape[0]
     cols = p0_ref.shape[1] // 2
+    copies = []
     for shift, ref in enumerate((p0_ref, p1_ref, p2_ref, p3_ref)):
         source = lax.rem(chip + 4 - shift, 4)
         for half, lane in ((0, core), (1, 1 - core)):
-            at = pl.multiple_of((source * 2 + lane) * cols, cols)
-            block = ref[:, half * cols : (half + 1) * cols]
-            routed_ref[:, pl.ds(at, cols)] = block[:hs]
-            shared_ref[:, pl.ds(at, cols)] = block[hs:]
+            at = pl.ds(pl.multiple_of((source * 2 + lane) * cols, cols), cols)
+            part = pl.ds(half * cols, cols)
+            for top, out_ref in ((0, routed_ref), (hs, shared_ref)):
+                copies.append(
+                    pltpu.make_async_copy(
+                        ref.at[pl.ds(top, hs), part], out_ref.at[:, at], sems.at[len(copies)]
+                    )
+                )
+    for copy in copies:
+        copy.start()
+    for copy in copies:
+        copy.wait()
 
 
 def whole(shape):
@@ -272,30 +297,38 @@
 
     steps = 8
     anywhere = pl.BlockSpec(memory_space=pl.ANY)
-    normed, outgoing, slots = pl.pallas_call(
-        functools.partial(dispatch_kernel, half),
-        grid_spec=pltpu.PrefetchScalarGridSpec(
-            num_scalar_prefetch=1,
-            grid=(1,),
-            in_specs=[whole((top_count, tok_rows)), anywhere],
-            out_specs=[anywhere, whole((rows, quarter)), whole((top_count, tok_rows))],
-            scratch_shapes=[
-                pltpu.VMEM((tok_rows, width), bf16),
-                pltpu.VMEM((tok_rows, width), bf16),
-                pltpu.VMEM((tok_rows, quarter), bf16),
-                pltpu.VMEM((rows, tok_rows), bf16),
-                pltpu.SemaphoreType.DMA((steps,)),
-                pltpu.SemaphoreType.DMA((steps,)),
-            ],
-        ),
+    outgoing, slots = pl.pallas_call(
+        functools.partial(route_kernel, half),
+        grid=(1,),
+        in_specs=[whole((top_count, tok_rows)), anywhere],
+        out_specs=[whole((rows, quarter)), whole((top_count, tok_rows))],
         out_shape=[
-            jax.ShapeDtypeStruct((tok_rows, width), bf16),
             jax.ShapeDtypeStruct((rows, quarter), bf16),
             jax.ShapeDtypeStruct((top_count, tok_rows), jnp.int32),
         ],
+        scratch_shapes=[
+            pltpu.VMEM((tok_rows, quarter), bf16),
+            pltpu.VMEM((rows, tok_rows), bf16),
+            pltpu.SemaphoreType.DMA(()),
+        ],
         compiler_params=vmem_limit(60),
-        cost_estimate=cost(2 * rows * tok_rows * quarter, 4 * tok_rows * width),
-    )(place, route_expert.T, tokens)
+        cost_estimate=cost(2 * rows * tok_rows * quarter, 4 * tok_rows * quarter),
+    )(route_expert.T, tokens)
+    normed = pl.pallas_call(
+        norm_kernel,
+        grid=(1,),
+        in_specs=[anywhere],
+        out_specs=anywhere,
+        out_shape=jax.ShapeDtypeStruct((tok_rows, width), bf16),
+        scratch_shapes=[
+            pltpu.VMEM((tok_rows, width), bf16),
+            pltpu.VMEM((tok_rows, width), bf16),
+            pltpu.SemaphoreType.DMA((steps,)),
+            pltpu.SemaphoreType.DMA((steps,)),
+        ],
+        compiler_params=vmem_limit(60),
+        cost_estimate=cost(16 * tok_rows * width, 4 * tok_rows * width),
+    )(tokens)
     arriving = lax.all_to_all(
         outgoing.reshape(experts, half, quarter), "fs", split_axis=0, concat_axis=0, tiled=True
     )
@@ -339,30 +372,34 @@
     x_spec = pl.BlockSpec((mid // 2, quarter), lambda i, s: (i, 0))
     acc_spec = pl.BlockSpec((2, mid // 2, 4 * hs), lambda i, s: (0, i, 0))
     w_spec = pl.BlockSpec((quarter, 2 * hs), lambda i, s: (lax.rem(s[0] + chips // 2, chips), 0))
-    acc = pl.pallas_call(
+    acc, sq = pl.pallas_call(
         first_kernel,
         grid_spec=pltpu.PrefetchScalarGridSpec(
             num_scalar_prefetch=1,
             grid=(2,),
             in_specs=[x_spec] * 6 + [whole((width, 2 * hs))] * 2 + [whole(tile)],
-            out_specs=acc_spec,
-        ),
-        out_shape=jax.ShapeDtypeStruct((2, mid, 4 * hs), f32),
+            out_specs=[acc_spec, pl.BlockSpec((2, mid // 2, 128), lambda i, s: (0, i, 0))],
+        ),
+        out_shape=[
+            jax.ShapeDtypeStruct((2, mid, 4 * hs), f32),
+            jax.ShapeDtypeStruct((2, mid, 128), f32),
+        ],
         compiler_params=vmem_limit(32),
         cost_estimate=cost(2 * rows * 3 * quarter * 4 * hs, 8 * width * hs),
     )(place, top, left_top, right_top, bottom, left_bottom, right_bottom, gu, gu_other, mark)
     hidden = pl.pallas_call(
-        hidden_kernel,
-        grid_spec=pltpu.PrefetchScalarGridSpec(
-            num_scalar_prefetch=1,
-            grid=(1,),
-            in_specs=[whole((mid, quarter))] * 2 + [whole((2, mid, 4 * hs)), w_spec, w_spec],
+        functools.partial(hidden_kernel, width),
+        grid_spec=pltpu.PrefetchScalarGridSpec(
+            num_scalar_prefetch=1,
+            grid=(1,),
+            in_specs=[whole((mid, quarter))] * 2
+            + [whole((2, mid, 4 * hs)), whole((2, mid, 128)), w_spec, w_spec],
             out_specs=whole((2, mid, 2 * hs)),
         ),
         out_shape=jax.ShapeDtypeStruct((2, mid, 2 * hs), bf16),
         compiler_params=vmem_limit(32),
         cost_estimate=cost(2 * rows * quarter * 4 * hs, 8 * quarter * hs),
-    )(place, far_top, far_bottom, acc, gu, gu_other).reshape(rows, 2 * hs)
+    )(place, far_top, far_bottom, acc, sq, gu, gu_other).reshape(rows, 2 * hs)
 
     shared_gate, shared_up, shared_hid, shared_cols, shared_out = pl.pallas_call(
         shared_kernel,
@@ -414,7 +451,6 @@
     )(place, hidden, hid_left, hid_right, hid_far, down_cols, down_other)
     returned = lax.all_to_all(sums, "fs", split_axis=0, concat_axis=0, tiled=True)
     got_other = swap(returned[:, 1].reshape(rows, cols))
-    got_own = returned[:, 0].reshape(rows, cols)
 
     spots = jnp.arange(rows, dtype=jnp.int32)[None, :]
 
@@ -433,6 +469,13 @@
     def mix(weights, got, base, dtype):
         return pl.pallas_call(
             mix_kernel,
+            grid=(1,),
+            in_specs=[
+                whole((tok_rows, rows)),
+                whole((experts, 1, half, cols)) if got.ndim == 4 else whole((rows, cols)),
+                whole((tok_rows, cols)),
+            ],
+            out_specs=whole((tok_rows, cols)),
             out_shape=jax.ShapeDtypeStruct((tok_rows, cols), dtype),
             compiler_params=vmem_limit(24),
             cost_estimate=cost(2 * tok_rows * rows * cols, 4 * tok_rows * rows),
@@ -451,7 +494,7 @@
         compiler_params=vmem_limit(24),
         cost_estimate=cost(2 * tok_rows * experts * deep * cols, 4 * tok_rows * rows),
     )(place, units, units_other, shared_cols)
-    part = mix(mix_own, got_own, base, f32)
+    part = mix(mix_own, returned, base, f32)
     mixed = mix(mix_other, got_other, part, bf16)
 
     chunks = pl.pallas_call(
@@ -476,7 +519,8 @@
             num_scalar_prefetch=1,
             grid=(1,),
             in_specs=[whole((2 * hs, 2 * cols))] * 4,
-            out_specs=[whole((hs, width))] * 2,
+            out_specs=[anywhere] * 2,
+            scratch_shapes=[pltpu.SemaphoreType.DMA((4 * chips,))],
         ),
         out_shape=[jax.ShapeDtypeStruct((hs, width), bf16)] * 2,
         compiler_params=vmem_limit(24),
@@ -509,6 +553,7 @@
         P("fs", None),
     )
 
+
     return jax.shard_map(
         on_device,
         mesh=mesh,

time: 275 us -> 270 us (0.982)
  local copies, waits for them, and re-layouts: 19.8 us -> 15.5 us
  Pallas kernels: 37.9 us -> 41.8 us
  waiting for transfers between devices: 147 us -> 144 us
    unnamed x70 -> x58, local copies, waits for them, and re-layouts: 15.5 us -> 11.5 us
    ppermute x12, waiting for transfers between devices: 43.3 us -> 39.4 us  [along(): return lax.ppermute(a, 'fs', pairs)]
    pallas_call x4 -> x5, Pallas kernels: 11.6 us -> 14.1 us  [the longest x1 4.09 us: on_device(): pl.pallas_call(functools.partial(route_kernel, half), grid=(1,), in_specs...]
  transfers between devices with their start and end apart: 36 -> 36, of which waited for: 16 -> 16; matrix products, arithmetic and copies ran while one was open for 5% -> 5% of each run, Pallas kernels for 11% -> 13%
where the time goes in v6:
time: 270 us; the launch traced here: 269 us
  waiting for transfers between devices  144 us (53%)
  starting transfers between devices  56.2 us (21%)
  Pallas kernels  41.8 us (15%)
  local copies, waits for them, and re-layouts  15.5 us (6%)
  other arithmetic  11 us (4%)
    ppermute x15, waiting for transfers between devices, shift_by(): return lax.ppermute(a, 'tp', [(i, (i + 2 * n) % tp) for i in range(tp)])  56.7 us
    ppermute x12, waiting for transfers between devices, along(): return lax.ppermute(a, 'fs', pairs)  39.4 us
    all_to_all x1, waiting for transfers between devices, on_device(): gu = lax.all_to_all(gu_local, 'fs', split_axis=0, concat_axis=0, tiled=True)  27.3 us
    all_to_all x1, waiting for transfers between devices, on_device(): lax.all_to_all(outgoing.reshape(experts, half, quarter), 'fs', split_axis...  20.1 us
    ppermute x15, starting transfers between devices, shift_by(): return lax.ppermute(a, 'tp', [(i, (i + 2 * n) % tp) for i in range(tp)])  19 us
    ppermute x12, starting transfers between devices, along(): return lax.ppermute(a, 'fs', pairs)  15.8 us
    unnamed x58, local copies, waits for them, and re-layouts  11.5 us
    all_to_all x1, starting transfers between devices, on_device(): lax.all_to_all(outgoing.reshape(experts, half, quarter), 'fs', split_axis...  8.17 us
  transfers between devices with their start and end apart: 36, of which 16 were waited for; matrix products, arithmetic and copies ran while one was open for 5% of the time, Pallas kernels for 13%

profile of v6, /device:TPU:0, one launch (start us, length us, event | category | flops | bytes accessed | tf_op | source)
XLA Modules:
  0.0 269.2 jit_solution(590675740473635676)
XLA Ops:
  0.6 4.1 %shard_map.153 = (bf16[768,1024]{1,0:T(8,128)(2,1)}, s32[2,512]{1,0:T(2,128)}) custom-call(s32[2,512]{1,0:T(2,128)} %bitcast.75, bf16[512,4096]{1,0:T(8,128)(2,1)} %tok_ref.3), custom_call_target="tpu_custom_call" | custom-call | flops 805306368 | bytes 2097152 | tf_op jit(solution)/shard_map/pallas_call | solution.py:300
  4.7 8.2 %all-to-all-start = ((bf16[16,48,1024]{2,1,0:T(8,128)(2,1)}), bf16[16,48,1024]{2,1,0:T(8,128)(2,1)S(1)}, u32[]{:S(2)}, u32[]{:S(2)}) async-start(bf16[16,48,1024]{2,1,0:T(8,128)(2,1)} %bitcast.64), calls=%async_computation | async-start | bytes 3145728 | tf_op jit(solution)/shard_map/all_to_all | solution.py:332
  12.9 2.8 %multiply_convert_fusion.1 = (bf16[16,256,128]{2,1,0:T(8,128)(2,1)S(1)}, bf16[16,256,128]{2,1,0:T(8,128)(2,1)S(1)}) fusion(f32[16,256,128]{2,1,0:T(8,128)} %param.12, f32[256]{0:T(256)S(1)} %copy-done.28, f32[16,256,128]{2,1,0:T(8,128)} %param.13), kind=kLoop, calls=%fused_computation.2 | loop fusion | flops 2097152 | bytes 6292480 | tf_op jit(solution)/shard_map/convert_element_type | solution.py:337
  15.8 1.6 pad_maximum_fusion
  17.4 20.1 %all-to-all-done = bf16[16,48,1024]{2,1,0:T(8,128)(2,1)S(1)} async-done(((bf16[16,48,1024]{2,1,0:T(8,128)(2,1)}), bf16[16,48,1024]{2,1,0:T(8,128)(2,1)S(1)}, u32[]{:S(2)}, u32[]{:S(2)}) %all-to-all-start) | async-done | bytes 1572896 | tf_op jit(solution)/shard_map/all_to_all | solution.py:332
  37.4 1.3 fusion.8
  38.7 3.7 %all-to-all-start.1 = ((bf16[16,256,256]{2,1,0:T(8,128)(2,1)}), bf16[16,256,256]{2,1,0:T(8,128)(2,1)S(1)}, u32[]{:S(2)}, u32[]{:S(2)}) async-start(bf16[16,256,256]{2,1,0:T(8,128)(2,1)} %pad_maximum_fusion), calls=%async_computation.1 | async-start | bytes 4194304 | tf_op jit(solution)/shard_map/all_to_all | solution.py:343
  42.5 2.8 %convert_element_type.27 = bf16[16,64,512]{2,1,0:T(8,128)(2,1)} convert(f32[16,64,512]{2,1,0:T(8,128)} %param.14) | non-fusion elementwise | flops 524288 | bytes 3145728 | tf_op jit(solution)/shard_map/convert_element_type | solution.py:344
  45.3 27.3 %all-to-all-done.1 = bf16[16,256,256]{2,1,0:T(8,128)(2,1)S(1)} async-done(((bf16[16,256,256]{2,1,0:T(8,128)(2,1)}), bf16[16,256,256]{2,1,0:T(8,128)(2,1)S(1)}, u32[]{:S(2)}, u32[]{:S(2)}) %all-to-all-start.1) | async-done | bytes 2097184 | tf_op jit(solution)/shard_map/all_to_all | solution.py:343
  72.6 1.6 collective-permute-start.17
  74.3 1.8 collective-permute-start.19
  76.1 4.3 %all-to-all-start.2 = ((bf16[16,64,512]{2,1,0:T(8,128)(2,1)}), bf16[16,64,512]{2,1,0:T(8,128)(2,1)}, u32[]{:S(2)}, u32[]{:S(2)}) async-start(bf16[16,64,512]{2,1,0:T(8,128)(2,1)} %convert_element_type.27), calls=%async_computation.2 | async-start | bytes 2097152 | tf_op jit(solution)/shard_map/all_to_all | solution.py:345
  80.5 1.6 collective-permute-start.21
  82.1 1.8 collective-permute-start.7
  84.0 13.1 %collective-permute-done.7 = bf16[384,128]{1,0:T(8,128)(2,1)S(1)} collective-permute-done((bf16[384,128]{1,0:T(8,128)(2,1)S(1)}, bf16[384,128]{1,0:T(8,128)(2,1)S(1)}, u32[]{:S(2)}, u32[]{:S(2)}) %collective-permute-start.7) | collective-permute-done | bytes 98336 | tf_op jit(solution)/shard_map/ppermute | solution.py:276
  97.7 5.6 %collective-permute-done.8 = bf16[384,128]{1,0:T(8,128)(2,1)S(1)} collective-permute-done((bf16[384,128]{1,0:T(8,128)(2,1)S(1)}, bf16[384,128]{1,0:T(8,128)(2,1)S(1)}, u32[]{:S(2)}, u32[]{:S(2)}) %collective-permute-start.8) | collective-permute-done | bytes 98336 | tf_op jit(solution)/shard_map/ppermute | solution.py:276
  103.7 4.1 %collective-permute-done.9 = bf16[384,128]{1,0:T(8,128)(2,1)S(1)} collective-permute-done((bf16[384,128]{1,0:T(8,128)(2,1)S(1)}, bf16[384,128]{1,0:T(8,128)(2,1)S(1)}, u32[]{:S(2)}, u32[]{:S(2)}) %collective-permute-start.9) | collective-permute-done | bytes 98336 | tf_op jit(solution)/shard_map/ppermute | solution.py:276
  108.2 1.1 collective-permute-start.18
  109.3 2.1 collective-permute-start.20
  111.9 0.9 copy-done.15
  113.4 1.3 shard_map.159.b_ref
  114.8 1.0 pad_maximum_fusion.3.refs_4_
  115.8 1.3 shard_map.158.a_ref
  117.1 1.3 shard_map.160.refs_8_
  118.4 11.4 %collective-permute-done.22.refs_4_ = bf16[384,1024]{1,0:T(8,128)(2,1)} collective-permute-done((bf16[384,1024]{1,0:T(8,128)(2,1)}, bf16[384,1024]{1,0:T(8,128)(2,1)}, u32[]{:S(2)}, u32[]{:S(2)}) %collective-permute-start.22) | collective-permute-done | bytes 786464 | tf_op jit(solution)/shard_map/ppermute | solution.py:260
  129.8 2.1 collective-permute-start.1
  131.9 10.7 %collective-permute-done.18.far0_ref = bf16[384,1024]{1,0:T(8,128)(2,1)S(1)} collective-permute-done((bf16[384,1024]{1,0:T(8,128)(2,1)}, bf16[384,1024]{1,0:T(8,128)(2,1)S(1)}, u32[]{:S(2)}, u32[]{:S(2)}) %collective-permute-start.18) | collective-permute-done | bytes 786464 | tf_op jit(solution)/shard_map/ppermute | solution.py:260
  142.6 4.1 %collective-permute-start.2 = (bf16[384,128]{1,0:T(8,128)(2,1)}, bf16[384,128]{1,0:T(8,128)(2,1)S(1)}, u32[]{:S(2)}, u32[]{:S(2)}) collective-permute-start(bf16[384,128]{1,0:T(8,128)(2,1)} %get-tuple-element.64.a_ref), channel_id=1, source_target_pairs={{0,16},{8,24},{16,0},{24,8},{32,48},{40,56},{48,32},{56,40},{64,80... | collective-permute-start | bytes 294920 | tf_op jit(solution)/shard_map/ppermute | solution.py:276
  146.8 1.1 collective-permute-start.3
  148.5 1.1 copy-done.16
  149.7 7.0 %shard_map.161 = (f32[2,384,512]{2,1,0:T(8,128)S(1)}, f32[2,384,128]{2,1,0:T(8,128)S(1)}) custom-call(s32[4]{0:T(128)S(1)} %pad_add_fusion.place_ref, bf16[384,1024]{1,0:T(8,128)(2,1)} %bitcast.2.refs_0_, bf16[384,1024]{1,0:T(8,128)(2,1)} %collective-permute-done.17.a_ref.refs_1_, bf16[384,1024]{1,0:T(8,128)(2,1)S(1)} %copy-done.16, ...), custom_call_target="tpu_custom_call" | custom-call | flops 2415919104 | bytes 4194304 | tf_op jit(solution)/shard_map/pallas_call | solution.py:375
  156.6 1.0 collective-permute-start.10
  157.7 3.0 %shard_map.162 = bf16[2,384,256]{2,1,0:T(8,128)(2,1)S(1)} custom-call(s32[4]{0:T(128)S(1)} %pad_add_fusion.place_ref, bf16[384,1024]{1,0:T(8,128)(2,1)S(1)} %collective-permute-done.18.far0_ref, bf16[384,1024]{1,0:T(8,128)(2,1)} %collective-permute-done.20.far1_ref, f32[2,384,512]{2,1,0:T(8,128)S(1)} %get-tuple-element.51.acc_ref, ...), custom_call_target="tpu_custom_call" | custom-call | flops 805306368 | bytes 1048576 | tf_op jit(solution)/shard_map/pallas_call | solution.py:390
  161.0 3.2 %collective-permute-start.25 = (bf16[768,256]{1,0:T(8,128)(2,1)S(1)}, bf16[768,256]{1,0:T(8,128)(2,1)S(1)}, u32[]{:S(2)}, u32[]{:S(2)}) collective-permute-start(bf16[768,256]{1,0:T(8,128)(2,1)S(1)} %bitcast.60), channel_id=1, source_target_pairs={{0,6},{1,7},{2,0},{3,1},{4,2},{5,3},{6,4},{7,5},{8,14},{9,15},{10,... | collective-permute-start | bytes 1179656 | tf_op jit(solution)/shard_map/ppermute | solution.py:260
  164.2 5.7 %collective-permute-done.10.refs_5_ = bf16[4,384,128]{2,1,0:T(8,128)(2,1)S(1)} collective-permute-done((bf16[4,384,128]{2,1,0:T(8,128)(2,1)S(1)}, bf16[4,384,128]{2,1,0:T(8,128)(2,1)S(1)}, u32[]{:S(2)}, u32[]{:S(2)}) %collective-permute-start.10) | collective-permute-done | bytes 393248 | tf_op jit(solution)/shard_map/ppermute | solution.py:276
  169.9 0.7 copy-done.12
  170.7 7.0 %collective-permute-done.24.h1_ref = bf16[768,256]{1,0:T(8,128)(2,1)S(1)} collective-permute-done((bf16[768,256]{1,0:T(8,128)(2,1)S(1)}, bf16[768,256]{1,0:T(8,128)(2,1)S(1)}, u32[]{:S(2)}, u32[]{:S(2)}) %collective-permute-start.24) | collective-permute-done | bytes 393248 | tf_op jit(solution)/shard_map/ppermute | solution.py:260
  178.0 3.8 %collective-permute-start.5 = (bf16[4,384,128]{2,1,0:T(8,128)(2,1)S(1)}, bf16[4,384,128]{2,1,0:T(8,128)(2,1)}, u32[]{:S(2)}, u32[]{:S(2)}) collective-permute-start(bf16[4,384,128]{2,1,0:T(8,128)(2,1)S(1)} %pad_maximum_fusion.2.refs_0_), channel_id=1, source_target_pairs={{0,64},{8,72},{16,80},{24,88},{32,96},{40,104},{48,112},{56,120},{... | collective-permute-start | bytes 1179656 | tf_op jit(solution)/shard_map/ppermute | solution.py:276
  182.2 3.9 %shard_map.163 = bf16[16,2,48,512]{3,2,1,0:T(8,128)(2,1)S(1)} custom-call(s32[4]{0:T(128)S(1)} %pad_add_fusion.place_ref, bf16[768,256]{1,0:T(8,128)(2,1)S(1)} %bitcast.62, bf16[768,256]{1,0:T(8,128)(2,1)S(1)} %collective-permute-done.24.h1_ref, bf16[768,256]{1,0:T(8,128)(2,1)S(1)} %collective-permute-done.25.h2_ref, ...), custom_call_target="tpu_custom_call" | custom-call | flops 1610612736 | bytes 4194304 | tf_op jit(solution)/shard_map/pallas_call | solution.py:439
  186.2 1.2 copy-done.5
  187.3 4.4 %all-to-all-start.3 = ((bf16[16,2,48,512]{3,2,1,0:T(8,128)(2,1)}), bf16[16,2,48,512]{3,2,1,0:T(8,128)(2,1)}, u32[]{:S(2)}, u32[]{:S(2)}) async-start(bf16[16,2,48,512]{3,2,1,0:T(8,128)(2,1)} %copy-done.5), calls=%async_computation.3 | async-start | bytes 3145728 | tf_op jit(solution)/shard_map/all_to_all | solution.py:452
  191.8 3.9 %shard_map.154.x_ref = bf16[512,4096]{1,0:T(8,128)(2,1)} custom-call(bf16[512,4096]{1,0:T(8,128)(2,1)} %tok_ref.3), custom_call_target="tpu_custom_call" | custom-call | flops 33554432 | bytes 8388608 | tf_op jit(solution)/shard_map/pallas_call | solution.py:317
  195.7 3.7 %collective-permute-done.5.refs_2_ = bf16[4,384,128]{2,1,0:T(8,128)(2,1)} collective-permute-done((bf16[4,384,128]{2,1,0:T(8,128)(2,1)S(1)}, bf16[4,384,128]{2,1,0:T(8,128)(2,1)}, u32[]{:S(2)}, u32[]{:S(2)}) %collective-permute-start.5) | collective-permute-done | bytes 393248 | tf_op jit(solution)/shard_map/ppermute | solution.py:276
  199.5 7.1 %collective-permute-done.6.refs_3_ = bf16[4,384,128]{2,1,0:T(8,128)(2,1)} collective-permute-done((bf16[4,384,128]{2,1,0:T(8,128)(2,1)S(1)}, bf16[4,384,128]{2,1,0:T(8,128)(2,1)}, u32[]{:S(2)}, u32[]{:S(2)}) %collective-permute-start.6) | collective-permute-done | bytes 393248 | tf_op jit(solution)/shard_map/ppermute | solution.py:276
  206.6 2.2 copy-done
  208.8 4.8 %shard_map.155 = (bf16[4096,128]{1,0:T(8,128)(2,1)}, bf16[4096,128]{1,0:T(8,128)(2,1)}, bf16[512,128]{1,0:T(8,128)(2,1)S(1)}, bf16[1024,512]{1,0:T(8,128)(2,1)S(1)}, bf16[512,512]{1,0:T(8,128)(2,1)S(1)}) custom-call(s32[4]{0:T(128)S(1)} %pad_add_fusion.place_ref, bf16[512,4096]{1,0:T(8,128)(2,1)S(1)} %copy-done, ...), custom_call_target="tpu_custom_call" | custom-call | flops 1073741824 | bytes 4194304 | tf_op jit(solution)/shard_map/pallas_call | solution.py:404
  213.5 1.0 copy-done.6
  214.5 3.2 %collective-permute-start.29 = (bf16[512,128]{1,0:T(8,128)(2,1)S(1)}, bf16[512,128]{1,0:T(8,128)(2,1)S(1)}, u32[]{:S(2)}, u32[]{:S(2)}) collective-permute-start(bf16[512,128]{1,0:T(8,128)(2,1)S(1)} %get-tuple-element.54), channel_id=1, source_target_pairs={{0,6},{1,7},{2,0},{3,1},{4,2},{5,3},{6,4},{7,5},{8,14},{9,15},{10,... | collective-permute-start | bytes 393224 | tf_op jit(solution)/shard_map/ppermute | solution.py:260
  218.3 2.4 collective-permute-done.28
  220.7 3.5 %collective-permute-done.30 = bf16[512,128]{1,0:T(8,128)(2,1)S(1)} collective-permute-done((bf16[512,128]{1,0:T(8,128)(2,1)S(1)}, bf16[512,128]{1,0:T(8,128)(2,1)S(1)}, u32[]{:S(2)}, u32[]{:S(2)}) %collective-permute-start.30) | collective-permute-done | bytes 131104 | tf_op jit(solution)/shard_map/ppermute | solution.py:260
  225.1 1.7 fusion.4
  226.8 0.8 copy-done.10
  227.6 1.0 copy-done.4
  228.7 1.0 copy-done.11
  229.7 1.5 shard_map.164.base_ref
  231.2 3.3 %shard_map.156 = (bf16[256,1024]{1,0:T(8,128)(2,1)S(1)}, bf16[256,1024]{1,0:T(8,128)(2,1)}, bf16[256,1024]{1,0:T(8,128)(2,1)}, bf16[256,1024]{1,0:T(8,128)(2,1)}) custom-call(s32[4]{0:T(128)S(1)} %pad_add_fusion.place_ref, bf16[1024,512]{1,0:T(8,128)(2,1)} %bitcast.11.own_ref.w_own_ref, bf16[1024,512]{1,0:T(8,128)(2,1)} %collective-permute-done.other_ref.w_other_ref, ...), custom_call_target="tpu_custom_call" | custom-call | flops 1073741824 | bytes 4194304 | tf_op jit(solution)/shard_map/pallas_call | solution.py:500
  234.6 0.8 copy-done.8
  235.4 2.6 collective-permute-start.15
  238.6 1.2 slice.86
  239.9 1.5 slice_bitcast_fusion
  241.4 20.6 %collective-permute-done.14.p1_ref = bf16[256,1024]{1,0:T(8,128)(2,1)} collective-permute-done((bf16[256,1024]{1,0:T(8,128)(2,1)}, bf16[256,1024]{1,0:T(8,128)(2,1)}, u32[]{:S(2)}, u32[]{:S(2)}) %collective-permute-start.14) | collective-permute-done | bytes 524320 | tf_op jit(solution)/shard_map/ppermute | solution.py:260
  262.6 3.3 %shard_map.157 = (bf16[128,4096]{1,0:T(8,128)(2,1)}, bf16[128,4096]{1,0:T(8,128)(2,1)}) custom-call(s32[4]{0:T(128)S(1)} %pad_add_fusion.place_ref, bf16[256,1024]{1,0:T(8,128)(2,1)S(1)} %copy-done.9, bf16[256,1024]{1,0:T(8,128)(2,1)} %collective-permute-done.14.p1_ref, bf16[256,1024]{1,0:T(8,128)(2,1)} %collective-permute-done.15.p2_ref, ...), custom_call_target="tpu_custom_call" | custom-call | flops 1048576 | bytes 4194304 | tf_op jit(solution)/shard_map/pallas_call | solution.py:516
  266.0 1.8 shard_map.165.base_ref
  267.8 1.4 shard_map.166
  (99 shorter events, 7.3 us)
Async XLA Ops:
  4.7 8.2 %copy-start.28 = (f32[256]{0:T(256)S(1)}, f32[256]{0:T(256)}, u32[]{:S(2)}) copy-start(f32[256]{0:T(256)} %param.11) | copy-start | bytes 3076
  4.7 32.7 %all-to-all-start = ((bf16[16,48,1024]{2,1,0:T(8,128)(2,1)}), bf16[16,48,1024]{2,1,0:T(8,128)(2,1)S(1)}, u32[]{:S(2)}, u32[]{:S(2)}) async-start(bf16[16,48,1024]{2,1,0:T(8,128)(2,1)} %bitcast.64), calls=%async_computation | async-start | bytes 3145728 | tf_op jit(solution)/shard_map/all_to_all | solution.py:332
  38.7 33.9 %all-to-all-start.1 = ((bf16[16,256,256]{2,1,0:T(8,128)(2,1)}), bf16[16,256,256]{2,1,0:T(8,128)(2,1)S(1)}, u32[]{:S(2)}, u32[]{:S(2)}) async-start(bf16[16,256,256]{2,1,0:T(8,128)(2,1)} %pad_maximum_fusion), calls=%async_computation.1 | async-start | bytes 4194304 | tf_op jit(solution)/shard_map/all_to_all | solution.py:343
  42.5 30.1 %copy-start.21 = (f32[64,512]{1,0:T(8,128)S(1)}, f32[64,512]{1,0:T(8,128)}, u32[]{:S(2)}) copy-start(f32[64,512]{1,0:T(8,128)} %param.17) | copy-start | bytes 393220
  42.5 31.7 %copy-start.19 = (f32[256,128]{1,0:T(8,128)S(1)}, f32[256,128]{1,0:T(8,128)}, u32[]{:S(2)}) copy-start(f32[256,128]{1,0:T(8,128)} %param.16) | copy-start | bytes 393220
  42.5 31.7 %copy-start.20 = (f32[256,128]{1,0:T(8,128)S(1)}, f32[256,128]{1,0:T(8,128)}, u32[]{:S(2)}) copy-start(f32[256,128]{1,0:T(8,128)} %param.15) | copy-start | bytes 393220
  72.6 74.2 %collective-permute-start.23 = (bf16[4096,256]{1,0:T(8,128)(2,1)S(1)}, bf16[4096,256]{1,0:T(8,128)(2,1)}, u32[]{:S(2)}, u32[]{:S(2)}) collective-permute-start(bf16[4096,256]{1,0:T(8,128)(2,1)S(1)} %bitcast.55), channel_id=1, source_target_pairs={{0,1},{1,0},{2,3},{3,2},{4,5},{5,4},{6,7},{7,6},{8,9},{9,8},{10,11... | collective-permute-start | bytes 6291464 | tf_op jit(solution)/shard_map/ppermute | solution.py:263
  72.6 35.5 %collective-permute-start.17 = (bf16[384,1024]{1,0:T(8,128)(2,1)}, bf16[384,1024]{1,0:T(8,128)(2,1)}, u32[]{:S(2)}, u32[]{:S(2)}) collective-permute-start(bf16[384,1024]{1,0:T(8,128)(2,1)} %bitcast.2.refs_0_), channel_id=1, source_target_pairs={{0,2},{1,3},{2,4},{3,5},{4,6},{5,7},{6,0},{7,1},{8,10},{9,11},{10,... | collective-permute-start | bytes 2359304 | tf_op jit(solution)/shard_map/ppermute | solution.py:260
  74.3 35.0 %collective-permute-start.19 = (bf16[384,1024]{1,0:T(8,128)(2,1)}, bf16[384,1024]{1,0:T(8,128)(2,1)}, u32[]{:S(2)}, u32[]{:S(2)}) collective-permute-start(bf16[384,1024]{1,0:T(8,128)(2,1)} %bitcast.3.refs_3_), channel_id=1, source_target_pairs={{0,6},{1,7},{2,0},{3,1},{4,2},{5,3},{6,4},{7,5},{8,14},{9,15},{10,... | collective-permute-start | bytes 2359304 | tf_op jit(solution)/shard_map/ppermute | solution.py:260
  76.1 36.6 %all-to-all-start.2 = ((bf16[16,64,512]{2,1,0:T(8,128)(2,1)}), bf16[16,64,512]{2,1,0:T(8,128)(2,1)}, u32[]{:S(2)}, u32[]{:S(2)}) async-start(bf16[16,64,512]{2,1,0:T(8,128)(2,1)} %convert_element_type.27), calls=%async_computation.2 | async-start | bytes 2097152 | tf_op jit(solution)/shard_map/all_to_all | solution.py:345
  80.5 31.4 %collective-permute-start.21 = (bf16[384,1024]{1,0:T(8,128)(2,1)}, bf16[384,1024]{1,0:T(8,128)(2,1)S(1)}, u32[]{:S(2)}, u32[]{:S(2)}) collective-permute-start(bf16[384,1024]{1,0:T(8,128)(2,1)} %bitcast.2.refs_0_), channel_id=1, source_target_pairs={{0,6},{1,7},{2,0},{3,1},{4,2},{5,3},{6,4},{7,5},{8,14},{9,15},{10,... | collective-permute-start | bytes 2359304 | tf_op jit(solution)/shard_map/ppermute | solution.py:260
  82.1 31.3 %copy-start.18 = (bf16[384,128]{1,0:T(8,128)(2,1)}, bf16[384,128]{1,0:T(8,128)(2,1)S(1)}, u32[]{:S(2)}) copy-start(bf16[384,128]{1,0:T(8,128)(2,1)S(1)} %get-tuple-element.62.b_ref) | copy-start | bytes 294916
  82.1 15.0 %collective-permute-start.7 = (bf16[384,128]{1,0:T(8,128)(2,1)S(1)}, bf16[384,128]{1,0:T(8,128)(2,1)S(1)}, u32[]{:S(2)}, u32[]{:S(2)}) collective-permute-start(bf16[384,128]{1,0:T(8,128)(2,1)S(1)} %get-tuple-element.62.b_ref), channel_id=1, source_target_pairs={{0,32},{8,40},{16,48},{24,56},{32,64},{40,72},{48,80},{56,88},{64,... | collective-permute-start | bytes 294920 | tf_op jit(solution)/shard_map/ppermute | solution.py:276
  97.1 17.7 %copy-start.22 = (bf16[384,128]{1,0:T(8,128)(2,1)}, bf16[384,128]{1,0:T(8,128)(2,1)S(1)}, u32[]{:S(2)}) copy-start(bf16[384,128]{1,0:T(8,128)(2,1)S(1)} %collective-permute-done.7) | copy-start | bytes 294916
  97.1 6.1 %collective-permute-start.8 = (bf16[384,128]{1,0:T(8,128)(2,1)S(1)}, bf16[384,128]{1,0:T(8,128)(2,1)S(1)}, u32[]{:S(2)}, u32[]{:S(2)}) collective-permute-start(bf16[384,128]{1,0:T(8,128)(2,1)S(1)} %get-tuple-element.62.b_ref), channel_id=1, source_target_pairs={{0,64},{8,72},{16,80},{24,88},{32,96},{40,104},{48,112},{56,120},{... | collective-permute-start | bytes 294920 | tf_op jit(solution)/shard_map/ppermute | solution.py:276
  103.2 11.5 %copy-start.23 = (bf16[384,128]{1,0:T(8,128)(2,1)}, bf16[384,128]{1,0:T(8,128)(2,1)S(1)}, u32[]{:S(2)}) copy-start(bf16[384,128]{1,0:T(8,128)(2,1)S(1)} %collective-permute-done.8) | copy-start | bytes 294916
  103.2 4.6 %collective-permute-start.9 = (bf16[384,128]{1,0:T(8,128)(2,1)S(1)}, bf16[384,128]{1,0:T(8,128)(2,1)S(1)}, u32[]{:S(2)}, u32[]{:S(2)}) collective-permute-start(bf16[384,128]{1,0:T(8,128)(2,1)S(1)} %get-tuple-element.62.b_ref), channel_id=1, source_target_pairs={{0,96},{8,104},{16,112},{24,120},{32,0},{40,8},{48,16},{56,24},{64... | collective-permute-start | bytes 294920 | tf_op jit(solution)/shard_map/ppermute | solution.py:276
  107.9 1.4 copy-start.24
  107.9 21.9 %collective-permute-start.22 = (bf16[384,1024]{1,0:T(8,128)(2,1)}, bf16[384,1024]{1,0:T(8,128)(2,1)}, u32[]{:S(2)}, u32[]{:S(2)}) collective-permute-start(bf16[384,1024]{1,0:T(8,128)(2,1)} %bitcast.3.refs_3_), channel_id=1, source_target_pairs={{0,2},{1,3},{2,4},{3,5},{4,6},{5,7},{6,0},{7,1},{8,10},{9,11},{10,... | collective-permute-start | bytes 2359304 | tf_op jit(solution)/shard_map/ppermute | solution.py:260
  108.2 34.5 %collective-permute-start.18 = (bf16[384,1024]{1,0:T(8,128)(2,1)}, bf16[384,1024]{1,0:T(8,128)(2,1)S(1)}, u32[]{:S(2)}, u32[]{:S(2)}) collective-permute-start(bf16[384,1024]{1,0:T(8,128)(2,1)} %collective-permute-done.17.a_ref.refs_1_), channel_id=1, source_target_pairs={{0,2},{1,3},{2,4},{3,5},{4,6},{5,7},{6,0},{7,1},{8,10},{9,11},{10,... | collective-permute-start | bytes 2359304 | tf_op jit(solution)/shard_map/ppermute | solution.py:260
  109.3 47.3 %collective-permute-start.20 = (bf16[384,1024]{1,0:T(8,128)(2,1)}, bf16[384,1024]{1,0:T(8,128)(2,1)}, u32[]{:S(2)}, u32[]{:S(2)}) collective-permute-start(bf16[384,1024]{1,0:T(8,128)(2,1)} %collective-permute-done.19.b_ref.refs_5_), channel_id=1, source_target_pairs={{0,6},{1,7},{2,0},{3,1},{4,2},{5,3},{6,4},{7,5},{8,14},{9,15},{10,... | collective-permute-start | bytes 2359304 | tf_op jit(solution)/shard_map/ppermute | solution.py:260
  111.9 0.9 copy-start.15
  112.7 57.9 %collective-permute-start = (bf16[1024,512]{1,0:T(8,128)(2,1)}, bf16[1024,512]{1,0:T(8,128)(2,1)}, u32[]{:S(2)}, u32[]{:S(2)}) collective-permute-start(bf16[1024,512]{1,0:T(8,128)(2,1)} %bitcast.11.own_ref.w_own_ref), channel_id=1, source_target_pairs={{0,1},{1,0},{2,3},{3,2},{4,5},{5,4},{6,7},{7,6},{8,9},{9,8},{10,11... | collective-permute-start | bytes 3145736 | tf_op jit(solution)/shard_map/ppermute | solution.py:263
  129.8 30.9 %collective-permute-start.1 = (bf16[384,128]{1,0:T(8,128)(2,1)}, bf16[384,128]{1,0:T(8,128)(2,1)S(1)}, u32[]{:S(2)}, u32[]{:S(2)}) collective-permute-start(bf16[384,128]{1,0:T(8,128)(2,1)} %get-tuple-element.64.a_ref), channel_id=1, source_target_pairs={{0,8},{8,16},{16,24},{24,0},{32,40},{40,48},{48,56},{56,32},{64,72... | collective-permute-start | bytes 294920 | tf_op jit(solution)/shard_map/ppermute | solution.py:276
  142.6 18.3 %collective-permute-start.2 = (bf16[384,128]{1,0:T(8,128)(2,1)}, bf16[384,128]{1,0:T(8,128)(2,1)S(1)}, u32[]{:S(2)}, u32[]{:S(2)}) collective-permute-start(bf16[384,128]{1,0:T(8,128)(2,1)} %get-tuple-element.64.a_ref), channel_id=1, source_target_pairs={{0,16},{8,24},{16,0},{24,8},{32,48},{40,56},{48,32},{56,40},{64,80... | collective-permute-start | bytes 294920 | tf_op jit(solution)/shard_map/ppermute | solution.py:276
  146.8 17.4 %collective-permute-start.3 = (bf16[384,128]{1,0:T(8,128)(2,1)}, bf16[384,128]{1,0:T(8,128)(2,1)S(1)}, u32[]{:S(2)}, u32[]{:S(2)}) collective-permute-start(bf16[384,128]{1,0:T(8,128)(2,1)} %get-tuple-element.64.a_ref), channel_id=1, source_target_pairs={{0,24},{8,0},{16,8},{24,16},{32,56},{40,32},{48,40},{56,48},{64,88... | collective-permute-start | bytes 294920 | tf_op jit(solution)/shard_map/ppermute | solution.py:276
  148.5 1.1 copy-start.16
  156.6 13.3 %collective-permute-start.10 = (bf16[4,384,128]{2,1,0:T(8,128)(2,1)S(1)}, bf16[4,384,128]{2,1,0:T(8,128)(2,1)S(1)}, u32[]{:S(2)}, u32[]{:S(2)}) collective-permute-start(bf16[4,384,128]{2,1,0:T(8,128)(2,1)S(1)} %pad_maximum_fusion.3.refs_4_), channel_id=1, source_target_pairs={{0,8},{8,16},{16,24},{24,0},{32,40},{40,48},{48,56},{56,32},{64,72... | collective-permute-start | bytes 1179656 | tf_op jit(solution)/shard_map/ppermute | solution.py:276
  160.7 17.0 %collective-permute-start.24 = (bf16[768,256]{1,0:T(8,128)(2,1)S(1)}, bf16[768,256]{1,0:T(8,128)(2,1)S(1)}, u32[]{:S(2)}, u32[]{:S(2)}) collective-permute-start(bf16[768,256]{1,0:T(8,128)(2,1)S(1)} %bitcast.59), channel_id=1, source_target_pairs={{0,2},{1,3},{2,4},{3,5},{4,6},{5,7},{6,0},{7,1},{8,10},{9,11},{10,... | collective-permute-start | bytes 1179656 | tf_op jit(solution)/shard_map/ppermute | solution.py:260
  161.0 17.0 %collective-permute-start.25 = (bf16[768,256]{1,0:T(8,128)(2,1)S(1)}, bf16[768,256]{1,0:T(8,128)(2,1)S(1)}, u32[]{:S(2)}, u32[]{:S(2)}) collective-permute-start(bf16[768,256]{1,0:T(8,128)(2,1)S(1)} %bitcast.60), channel_id=1, source_target_pairs={{0,6},{1,7},{2,0},{3,1},{4,2},{5,3},{6,4},{7,5},{8,14},{9,15},{10,... | collective-permute-start | bytes 1179656 | tf_op jit(solution)/shard_map/ppermute | solution.py:260
  164.2 17.6 %collective-permute-start.26 = (bf16[768,256]{1,0:T(8,128)(2,1)S(1)}, bf16[768,256]{1,0:T(8,128)(2,1)S(1)}, u32[]{:S(2)}, u32[]{:S(2)}) collective-permute-start(bf16[768,256]{1,0:T(8,128)(2,1)S(1)} %bitcast.61), channel_id=1, source_target_pairs={{0,4},{1,5},{2,6},{3,7},{4,0},{5,1},{6,2},{7,3},{8,12},{9,13},{10,... | collective-permute-start | bytes 1179656 | tf_op jit(solution)/shard_map/ppermute | solution.py:260
  169.9 0.7 copy-start.12
  170.7 25.1 %collective-permute-start.11 = (bf16[4,384,128]{2,1,0:T(8,128)(2,1)S(1)}, bf16[4,384,128]{2,1,0:T(8,128)(2,1)S(1)}, u32[]{:S(2)}, u32[]{:S(2)}) collective-permute-start(bf16[4,384,128]{2,1,0:T(8,128)(2,1)S(1)} %pad_maximum_fusion.3.refs_4_), channel_id=1, source_target_pairs={{0,16},{8,24},{16,0},{24,8},{32,48},{40,56},{48,32},{56,40},{64,80... | collective-permute-start | bytes 1179656 | tf_op jit(solution)/shard_map/ppermute | solution.py:276
  170.7 25.1 %collective-permute-start.12 = (bf16[4,384,128]{2,1,0:T(8,128)(2,1)S(1)}, bf16[4,384,128]{2,1,0:T(8,128)(2,1)}, u32[]{:S(2)}, u32[]{:S(2)}) collective-permute-start(bf16[4,384,128]{2,1,0:T(8,128)(2,1)S(1)} %pad_maximum_fusion.3.refs_4_), channel_id=1, source_target_pairs={{0,24},{8,0},{16,8},{24,16},{32,56},{40,32},{48,40},{56,48},{64,88... | collective-permute-start | bytes 1179656 | tf_op jit(solution)/shard_map/ppermute | solution.py:276
  177.6 18.1 %collective-permute-start.4 = (bf16[4,384,128]{2,1,0:T(8,128)(2,1)S(1)}, bf16[4,384,128]{2,1,0:T(8,128)(2,1)}, u32[]{:S(2)}, u32[]{:S(2)}) collective-permute-start(bf16[4,384,128]{2,1,0:T(8,128)(2,1)S(1)} %pad_maximum_fusion.2.refs_0_), channel_id=1, source_target_pairs={{0,32},{8,40},{16,48},{24,56},{32,64},{40,72},{48,80},{56,88},{64,... | collective-permute-start | bytes 1179656 | tf_op jit(solution)/shard_map/ppermute | solution.py:276
  178.0 21.5 %collective-permute-start.5 = (bf16[4,384,128]{2,1,0:T(8,128)(2,1)S(1)}, bf16[4,384,128]{2,1,0:T(8,128)(2,1)}, u32[]{:S(2)}, u32[]{:S(2)}) collective-permute-start(bf16[4,384,128]{2,1,0:T(8,128)(2,1)S(1)} %pad_maximum_fusion.2.refs_0_), channel_id=1, source_target_pairs={{0,64},{8,72},{16,80},{24,88},{32,96},{40,104},{48,112},{56,120},{... | collective-permute-start | bytes 1179656 | tf_op jit(solution)/shard_map/ppermute | solution.py:276
  181.7 24.9 %collective-permute-start.6 = (bf16[4,384,128]{2,1,0:T(8,128)(2,1)S(1)}, bf16[4,384,128]{2,1,0:T(8,128)(2,1)}, u32[]{:S(2)}, u32[]{:S(2)}) collective-permute-start(bf16[4,384,128]{2,1,0:T(8,128)(2,1)S(1)} %pad_maximum_fusion.2.refs_0_), channel_id=1, source_target_pairs={{0,96},{8,104},{16,112},{24,120},{32,0},{40,8},{48,16},{56,24},{64... | collective-permute-start | bytes 1179656 | tf_op jit(solution)/shard_map/ppermute | solution.py:276
  186.1 1.2 copy-start.5
  187.3 51.3 %all-to-all-start.3 = ((bf16[16,2,48,512]{3,2,1,0:T(8,128)(2,1)}), bf16[16,2,48,512]{3,2,1,0:T(8,128)(2,1)}, u32[]{:S(2)}, u32[]{:S(2)}) async-start(bf16[16,2,48,512]{3,2,1,0:T(8,128)(2,1)} %copy-done.5), calls=%async_computation.3 | async-start | bytes 3145728 | tf_op jit(solution)/shard_map/all_to_all | solution.py:452
  191.8 14.8 %copy-start.13 = (bf16[4,384,128]{2,1,0:T(8,128)(2,1)S(1)}, bf16[4,384,128]{2,1,0:T(8,128)(2,1)}, u32[]{:S(2)}) copy-start(bf16[4,384,128]{2,1,0:T(8,128)(2,1)} %copy-done.12) | copy-start | bytes 1179652
  191.8 26.6 %copy-start.27 = (f32[512,2]{0,1:T(2,128)S(1)}, f32[512,2]{0,1:T(2,128)}, u32[]{:S(2)}) copy-start(f32[512,2]{0,1:T(2,128)} %param.19) | copy-start | bytes 12292
  191.8 33.2 %copy-start.25 = (s32[512,2]{0,1:T(2,128)S(1)}, s32[512,2]{0,1:T(2,128)}, u32[]{:S(2)}) copy-start(s32[512,2]{0,1:T(2,128)} %param.18) | copy-start | bytes 12292
  191.8 33.2 %copy-start.26 = (s32[2,512]{1,0:T(2,128)S(1)}, s32[2,512]{1,0:T(2,128)}, u32[]{:S(2)}) copy-start(s32[2,512]{1,0:T(2,128)} %get-tuple-element.47) | copy-start | bytes 12292
  206.6 2.2 copy-start
  213.5 1.0 copy-start.6
  214.5 9.8 %copy-start.17 = (bf16[512,512]{1,0:T(8,128)(2,1)}, bf16[512,512]{1,0:T(8,128)(2,1)S(1)}, u32[]{:S(2)}) copy-start(bf16[512,512]{1,0:T(8,128)(2,1)S(1)} %get-tuple-element.38) | copy-start | bytes 1572868
  214.5 6.2 %collective-permute-start.28 = (bf16[512,128]{1,0:T(8,128)(2,1)S(1)}, bf16[512,128]{1,0:T(8,128)(2,1)S(1)}, u32[]{:S(2)}, u32[]{:S(2)}) collective-permute-start(bf16[512,128]{1,0:T(8,128)(2,1)S(1)} %get-tuple-element.54), channel_id=1, source_target_pairs={{0,2},{1,3},{2,4},{3,5},{4,6},{5,7},{6,0},{7,1},{8,10},{9,11},{10,... | collective-permute-start | bytes 393224 | tf_op jit(solution)/shard_map/ppermute | solution.py:260
  214.5 6.2 %collective-permute-start.29 = (bf16[512,128]{1,0:T(8,128)(2,1)S(1)}, bf16[512,128]{1,0:T(8,128)(2,1)S(1)}, u32[]{:S(2)}, u32[]{:S(2)}) collective-permute-start(bf16[512,128]{1,0:T(8,128)(2,1)S(1)} %get-tuple-element.54), channel_id=1, source_target_pairs={{0,6},{1,7},{2,0},{3,1},{4,2},{5,3},{6,4},{7,5},{8,14},{9,15},{10,... | collective-permute-start | bytes 393224 | tf_op jit(solution)/shard_map/ppermute | solution.py:260
  217.8 6.5 %collective-permute-start.30 = (bf16[512,128]{1,0:T(8,128)(2,1)S(1)}, bf16[512,128]{1,0:T(8,128)(2,1)S(1)}, u32[]{:S(2)}, u32[]{:S(2)}) collective-permute-start(bf16[512,128]{1,0:T(8,128)(2,1)S(1)} %get-tuple-element.54), channel_id=1, source_target_pairs={{0,4},{1,5},{2,6},{3,7},{4,0},{5,1},{6,2},{7,3},{8,12},{9,13},{10,... | collective-permute-start | bytes 393224 | tf_op jit(solution)/shard_map/ppermute | solution.py:260
  224.3 2.5 copy-start.3
  224.3 2.5 collective-permute-start.31
  224.4 3.2 %copy-start.7 = (bf16[1024,512]{1,0:T(8,128)(2,1)S(1)}, bf16[1024,512]{1,0:T(8,128)(2,1)}, u32[]{:S(2)}) copy-start(bf16[1024,512]{1,0:T(8,128)(2,1)} %copy-done.6) | copy-start | bytes 3145732
  224.5 6.8 %collective-permute-start.13 = (bf16[512,512]{1,0:T(8,128)(2,1)}, bf16[512,512]{1,0:T(8,128)(2,1)S(1)}, u32[]{:S(2)}, u32[]{:S(2)}) collective-permute-start(bf16[512,512]{1,0:T(8,128)(2,1)} %copy-done.17), channel_id=1, source_target_pairs={{0,1},{1,0},{2,3},{3,2},{4,5},{5,4},{6,7},{7,6},{8,9},{9,8},{10,11... | collective-permute-start | bytes 1572872 | tf_op jit(solution)/shard_map/ppermute | solution.py:263
  226.8 0.8 copy-start.10
  227.6 1.0 copy-start.4
  228.7 1.0 copy-start.11
  234.6 0.8 copy-start.8
  235.4 26.6 %collective-permute-start.14 = (bf16[256,1024]{1,0:T(8,128)(2,1)}, bf16[256,1024]{1,0:T(8,128)(2,1)}, u32[]{:S(2)}, u32[]{:S(2)}) collective-permute-start(bf16[256,1024]{1,0:T(8,128)(2,1)} %get-tuple-element.40), channel_id=1, source_target_pairs={{0,2},{1,3},{2,4},{3,5},{4,6},{5,7},{6,0},{7,1},{8,10},{9,11},{10,... | collective-permute-start | bytes 1572872 | tf_op jit(solution)/shard_map/ppermute | solution.py:260
  235.4 26.6 %collective-permute-start.15 = (bf16[256,1024]{1,0:T(8,128)(2,1)}, bf16[256,1024]{1,0:T(8,128)(2,1)}, u32[]{:S(2)}, u32[]{:S(2)}) collective-permute-start(bf16[256,1024]{1,0:T(8,128)(2,1)} %get-tuple-element.41), channel_id=1, source_target_pairs={{0,4},{1,5},{2,6},{3,7},{4,0},{5,1},{6,2},{7,3},{8,12},{9,13},{10,... | collective-permute-start | bytes 1572872 | tf_op jit(solution)/shard_map/ppermute | solution.py:260
  238.0 24.7 %collective-permute-start.16 = (bf16[256,1024]{1,0:T(8,128)(2,1)}, bf16[256,1024]{1,0:T(8,128)(2,1)}, u32[]{:S(2)}, u32[]{:S(2)}) collective-permute-start(bf16[256,1024]{1,0:T(8,128)(2,1)} %get-tuple-element.42), channel_id=1, source_target_pairs={{0,6},{1,7},{2,0},{3,1},{4,2},{5,3},{6,4},{7,5},{8,14},{9,15},{10,... | collective-permute-start | bytes 1572872 | tf_op jit(solution)/shard_map/ppermute | solution.py:260
  239.8 22.8 %copy-start.9 = (bf16[256,1024]{1,0:T(8,128)(2,1)S(1)}, bf16[256,1024]{1,0:T(8,128)(2,1)}, u32[]{:S(2)}) copy-start(bf16[256,1024]{1,0:T(8,128)(2,1)} %copy-done.8) | copy-start | bytes 1572868
  239.8 28.0 %collective-permute-start.27 = (bf16[768,512]{1,0:T(8,128)(2,1)S(1)}, bf16[768,512]{1,0:T(8,128)(2,1)S(1)}, u32[]{:S(2)}, u32[]{:S(2)}) collective-permute-start(bf16[768,512]{1,0:T(8,128)(2,1)S(1)} %bitcast.65), channel_id=1, source_target_pairs={{0,1},{1,0},{2,3},{3,2},{4,5},{5,4},{6,7},{7,6},{8,9},{9,8},{10,11... | collective-permute-start | bytes 2359304 | tf_op jit(solution)/shard_map/ppermute | solution.py:263
  241.4 24.6 %copy-start.2 = (bf16[512,768]{1,0:T(8,128)(2,1)S(1)}, bf16[512,768]{1,0:T(8,128)(2,1)}, u32[]{:S(2)}) copy-start(bf16[512,768]{1,0:T(8,128)(2,1)} %get-tuple-element.53.weight_ref) | copy-start | bytes 2359300
  266.0 1.8 copy-start.1
  (1 other events, 0.7 us)

commit v7 on v6

--- a/solution.py
+++ b/solution.py
@@ -28,12 +28,12 @@
     return pltpu.CompilerParams(vmem_limit_bytes=mib << 20)
 
 
-def route_kernel(half, route_ref, tok_ref, out_ref, slot_ref, kept, placing, sem):
+def route_kernel(half, route_ref, tok_ref, top_ref, bottom_ref, slot_ref, kept, placing, sem):
     t = lax.axis_index("tp")
     chip, core = t // 2, lax.rem(t, 2)
     tok_rows, quarter = kept.shape
     spots = placing.shape[0]
-    experts = spots // half
+    experts, few = spots // half, half // 2
     at = pl.ds(pl.multiple_of(chip * quarter, quarter), quarter)
     read = pltpu.make_async_copy(tok_ref.at[:, at], kept, sem)
     read.start()
@@ -52,12 +52,16 @@
         slot_ref[k : k + 1, :] = slot
         local = slot - core * half
         here = (local >= 0) & (local < half)
-        target = jnp.where(here, route_ref[k : k + 1, :] * half + local, -1)
+        line = route_ref[k : k + 1, :] * few + local
+        line = jnp.where(local < few, line, line + (spots // 2 - few))
+        target = jnp.where(here, line, -1)
         total = total + jnp.where(spot == target, 1.0, 0.0)
     placing[...] = total.astype(bf16)
     read.wait()
-    for c in range(0, spots, 256):
-        out_ref[c : c + 256, :] = dot(placing[c : c + 256, :], kept[...]).astype(bf16)
+    for c in range(0, spots, 192):
+        part, at = divmod(c, spots // 2)
+        block = dot(placing[c : c + 192, :], kept[...]).astype(bf16)
+        (top_ref, bottom_ref)[part][at : at + 192, :] = block
 
 
 def norm_kernel(tok_ref, normed_ref, taken, given, in_sem, out_sem):
@@ -98,12 +102,15 @@
     return total
 
 
-def mark_kernel(a_ref, b_ref, out_ref):
-    out_ref[...] = a_ref[...] + b_ref[...]
+def square_kernel(*refs):
+    x_refs, sq_ref = refs[:6], refs[6]
+    for part in range(2):
+        blocks = x_refs[3 * part : 3 * part + 3]
+        sq_ref[part] = squares(blocks[0]) + squares(blocks[1]) + squares(blocks[2])
 
 
 def first_kernel(place_ref, *refs):
-    x_refs, (w_own_ref, w_other_ref, _, acc_ref, sq_ref) = refs[:6], refs[6:]
+    x_refs, (w_own_ref, w_other_ref, acc_ref) = refs[:6], refs[6:]
     chip = place_ref[0]
     quarter, wide = x_refs[0].shape[1], w_own_ref.shape[1]
     chips = w_own_ref.shape[0] // quarter
@@ -116,7 +123,6 @@
                 term = dot(x_ref[...], w_ref[pl.ds(at, quarter), :])
                 total = term if total is None else total + term
             acc_ref[part, :, half * wide : (half + 1) * wide] = total
-        sq_ref[part] = squares(blocks[0]) + squares(blocks[1]) + squares(blocks[2])
 
 
 def hidden_kernel(width, place_ref, far0_ref, far1_ref, acc_ref, sq_ref, w0_ref, w1_ref, out_ref):
@@ -134,17 +140,27 @@
             out_ref[part, :, pl.ds(pl.multiple_of(slot * hs, hs), hs)] = value
 
 
-def down_kernel(place_ref, h0_ref, h1_ref, h2_ref, h3_ref, w_own_ref, w_other_ref, out_ref, line):
+def down_kernel(place_ref, h0_ref, h1_ref, h2_ref, h3_ref, w_own_ref, w_other_ref, out_ref, *scratch):
+    line, held, sems = scratch
     chip = place_ref[0]
-    depth, cols = h0_ref.shape[1], w_own_ref.shape[1]
+    depth = h0_ref.shape[1]
     chips = w_own_ref.shape[0] // depth
     parts = ((h0_ref, 0), (h1_ref, chips - 1), (h2_ref, 1), (h3_ref, chips // 2))
     for h_ref, shift in parts:
         at = pl.multiple_of(lax.rem(chip + shift, chips) * depth, depth)
         line[:, pl.ds(at, depth)] = h_ref[...]
+    copies = []
     for part, w_ref in enumerate((w_own_ref, w_other_ref)):
-        total = dot(line[...], w_ref[...]).astype(bf16)
-        out_ref[:, part] = total.reshape(out_ref.shape[0], out_ref.shape[2], cols)
+        total = dot(line[...], w_ref[...]).reshape(held.shape[1:])
+        held[part] = total.astype(bf16)
+        for half in range(2):
+            copy = pltpu.make_async_copy(
+                held.at[part, half], out_ref.at[:, part, half], sems.at[part, half]
+            )
+            copy.start()
+            copies.append(copy)
+    for copy in copies:
+        copy.wait()
 
 
 def shared_kernel(place_ref, x_ref, *refs):
@@ -297,13 +313,15 @@
 
     steps = 8
     anywhere = pl.BlockSpec(memory_space=pl.ANY)
-    outgoing, slots = pl.pallas_call(
+    mid = rows // 2
+    out_top, out_bottom, slots = pl.pallas_call(
         functools.partial(route_kernel, half),
         grid=(1,),
         in_specs=[whole((top_count, tok_rows)), anywhere],
-        out_specs=[whole((rows, quarter)), whole((top_count, tok_rows))],
+        out_specs=[whole((mid, quarter)), whole((mid, quarter)), whole((top_count, tok_rows))],
         out_shape=[
-            jax.ShapeDtypeStruct((rows, quarter), bf16),
+            jax.ShapeDtypeStruct((mid, quarter), bf16),
+            jax.ShapeDtypeStruct((mid, quarter), bf16),
             jax.ShapeDtypeStruct((top_count, tok_rows), jnp.int32),
         ],
         scratch_shapes=[
@@ -329,17 +347,19 @@
         compiler_params=vmem_limit(60),
         cost_estimate=cost(16 * tok_rows * width, 4 * tok_rows * width),
     )(tokens)
-    arriving = lax.all_to_all(
-        outgoing.reshape(experts, half, quarter), "fs", split_axis=0, concat_axis=0, tiled=True
-    )
+
+    def sent(a):
+        a = a.reshape(experts, half // 2, quarter)
+        return lax.all_to_all(a, "fs", split_axis=0, concat_axis=0, tiled=True).reshape(mid, quarter)
+
+    top = sent(out_top)
+    out_bottom, top = together(out_bottom, top)
+    bottom = sent(out_bottom)
 
     gu_local = jnp.concatenate(
         [(gain[None] * gate_train).astype(bf16), (gain[None] * up_train).astype(bf16)], axis=2
     )
-    mid = rows // 2
-    arriving = arriving.reshape(rows, quarter)
-    top, bottom = together(arriving[:mid], arriving[mid:])
-    gu_local, top, bottom = together(gu_local, top, bottom)
+    gu_local, bottom = together(gu_local, bottom)
     gu = lax.all_to_all(gu_local, "fs", split_axis=0, concat_axis=0, tiled=True)
     down_local, gu = together(down_train.astype(bf16), gu)
     down_cols = lax.all_to_all(down_local, "fs", split_axis=0, concat_axis=0, tiled=True)
@@ -355,38 +375,31 @@
     far_top = shift_by(left_top, 1)
     far_bottom = shift_by(right_bottom, -1)
 
-    def marker(a, b):
-        return pl.pallas_call(
-            mark_kernel,
-            grid=(1,),
-            in_specs=[whole(tile)] * 2,
-            out_specs=whole(tile),
-            out_shape=jax.ShapeDtypeStruct(tile, bf16),
-            cost_estimate=cost(1 << 20, 1 << 14),
-        )(a, b)
-
-    tile = (16, 128)
-    mark = marker(left_top, right_bottom)
-    soon = marker(*packs)
-    mark = marker(mark, soon)
     x_spec = pl.BlockSpec((mid // 2, quarter), lambda i, s: (i, 0))
     acc_spec = pl.BlockSpec((2, mid // 2, 4 * hs), lambda i, s: (0, i, 0))
     w_spec = pl.BlockSpec((quarter, 2 * hs), lambda i, s: (lax.rem(s[0] + chips // 2, chips), 0))
-    acc, sq = pl.pallas_call(
+    blocks = (top, left_top, right_top, bottom, left_bottom, right_bottom)
+    sq = pl.pallas_call(
+        square_kernel,
+        grid=(2,),
+        in_specs=[pl.BlockSpec((mid // 2, quarter), lambda i: (i, 0))] * 6,
+        out_specs=pl.BlockSpec((2, mid // 2, 128), lambda i: (0, i, 0)),
+        out_shape=jax.ShapeDtypeStruct((2, mid, 128), f32),
+        compiler_params=vmem_limit(32),
+        cost_estimate=cost(6 * rows * width, 2 * rows * width),
+    )(*blocks)
+    acc = pl.pallas_call(
         first_kernel,
         grid_spec=pltpu.PrefetchScalarGridSpec(
             num_scalar_prefetch=1,
             grid=(2,),
-            in_specs=[x_spec] * 6 + [whole((width, 2 * hs))] * 2 + [whole(tile)],
-            out_specs=[acc_spec, pl.BlockSpec((2, mid // 2, 128), lambda i, s: (0, i, 0))],
-        ),
-        out_shape=[
-            jax.ShapeDtypeStruct((2, mid, 4 * hs), f32),
-            jax.ShapeDtypeStruct((2, mid, 128), f32),
-        ],
+            in_specs=[x_spec] * 6 + [whole((width, 2 * hs))] * 2,
+            out_specs=acc_spec,
+        ),
+        out_shape=jax.ShapeDtypeStruct((2, mid, 4 * hs), f32),
         compiler_params=vmem_limit(32),
         cost_estimate=cost(2 * rows * 3 * quarter * 4 * hs, 8 * width * hs),
-    )(place, top, left_top, right_top, bottom, left_bottom, right_bottom, gu, gu_other, mark)
+    )(place, *blocks, gu, gu_other)
     hidden = pl.pallas_call(
         functools.partial(hidden_kernel, width),
         grid_spec=pltpu.PrefetchScalarGridSpec(
@@ -442,13 +455,18 @@
             num_scalar_prefetch=1,
             grid=(1,),
             in_specs=[whole((rows, 2 * hs))] * 4 + [whole((experts * deep, cols))] * 2,
-            out_specs=whole((experts, 2, half, cols)),
-            scratch_shapes=[pltpu.VMEM((rows, experts * deep), bf16)],
-        ),
-        out_shape=jax.ShapeDtypeStruct((experts, 2, half, cols), bf16),
+            out_specs=pl.BlockSpec(memory_space=pltpu.HBM),
+            scratch_shapes=[
+                pltpu.VMEM((rows, experts * deep), bf16),
+                pltpu.VMEM((2, 2, experts, half // 2, cols), bf16),
+                pltpu.SemaphoreType.DMA((2, 2)),
+            ],
+        ),
+        out_shape=jax.ShapeDtypeStruct((experts, 2, 2, half // 2, cols), bf16),
         compiler_params=vmem_limit(40),
         cost_estimate=cost(4 * rows * experts * deep * cols, 8 * experts * deep * cols),
     )(place, hidden, hid_left, hid_right, hid_far, down_cols, down_other)
+    sums = sums.reshape(experts, 2, half, cols)
     returned = lax.all_to_all(sums, "fs", split_axis=0, concat_axis=0, tiled=True)
     got_other = swap(returned[:, 1].reshape(rows, cols))
 

time: 270 us -> 273 us (1.011)
  blocking collectives: 0 us -> 22.5 us
  waiting for transfers between devices: 144 us -> 133 us
  starting transfers between devices: 56.2 us -> 52.1 us
    all_to_all x0 -> x1, blocking collectives: none -> 22.5 us  [sent(): lax.all_to_all(a, 'fs', split_axis=0, concat_axis=0, tiled=True)]
    all_to_all x1, waiting for transfers between devices: 20.1 us -> 9.24 us  [sent(): lax.all_to_all(a, 'fs', split_axis=0, concat_axis=0, tiled=True)]
    all_to_all x1, starting transfers between devices: 8.17 us -> 3.61 us  [sent(): lax.all_to_all(a, 'fs', split_axis=0, concat_axis=0, tiled=True)]
    unnamed x58 -> x54, local copies, waits for them, and re-layouts: 11.5 us -> 10.8 us
where the time goes in v7:
time: 273 us; the launch traced here: 271 us
  waiting for transfers between devices  133 us (49%)
  starting transfers between devices  52.1 us (19%)
  Pallas kernels  39.4 us (14%)
  blocking collectives  22.5 us (8%)
  local copies, waits for them, and re-layouts  13.5 us (5%)
  other arithmetic  10.1 us (4%)
    ppermute x15, waiting for transfers between devices, shift_by(): return lax.ppermute(a, 'tp', [(i, (i + 2 * n) % tp) for i in range(tp)])  59 us
    ppermute x12, waiting for transfers between devices, along(): return lax.ppermute(a, 'fs', pairs)  38.6 us
    all_to_all x1, waiting for transfers between devices, on_device(): gu = lax.all_to_all(gu_local, 'fs', split_axis=0, concat_axis=0, tiled=True)  25.8 us
    all_to_all x1, blocking collectives, sent(): lax.all_to_all(a, 'fs', split_axis=0, concat_axis=0, tiled=True)  22.5 us
    ppermute x15, starting transfers between devices, shift_by(): return lax.ppermute(a, 'tp', [(i, (i + 2 * n) % tp) for i in range(tp)])  19.2 us
    ppermute x12, starting transfers between devices, along(): return lax.ppermute(a, 'fs', pairs)  16.1 us
    unnamed x54, local copies, waits for them, and re-layouts  10.8 us
    all_to_all x1, waiting for transfers between devices, sent(): lax.all_to_all(a, 'fs', split_axis=0, concat_axis=0, tiled=True)  9.24 us
  transfers between devices with their start and end apart: 36, of which 16 were waited for; matrix products, arithmetic and copies ran while one was open for 5% of the time, Pallas kernels for 13%

profile of v7, /device:TPU:0, one launch (start us, length us, event | category | flops | bytes accessed | tf_op | source)
XLA Modules:
  0.0 271.5 jit_solution(10125490546256913663)
XLA Ops:
  0.6 3.8 %shard_map.153 = (bf16[384,1024]{1,0:T(8,128)(2,1)}, bf16[384,1024]{1,0:T(8,128)(2,1)}, s32[2,512]{1,0:T(2,128)}) custom-call(s32[2,512]{1,0:T(2,128)} %bitcast.87, bf16[512,4096]{1,0:T(8,128)(2,1)} %tok_ref.3), custom_call_target="tpu_custom_call" | custom-call | flops 805306368 | bytes 2097152 | tf_op jit(solution)/shard_map/pallas_call | solution.py:317
  4.5 22.5 %all_to_all.25 = bf16[16,24,1024]{2,1,0:T(8,128)(2,1)S(1)} all-to-all(bf16[16,24,1024]{2,1,0:T(8,128)(2,1)} %bitcast.77), channel_id=1, replica_groups=mesh['fs'=16,'tp'=8] {'fs'}, dimensions={0} | all-to-all | bytes 1572864 | tf_op jit(solution)/shard_map/all_to_all | solution.py:353
  27.0 3.6 %all-to-all-start.1 = ((bf16[16,24,1024]{2,1,0:T(8,128)(2,1)}), bf16[16,24,1024]{2,1,0:T(8,128)(2,1)S(1)}, u32[]{:S(2)}, u32[]{:S(2)}) async-start(bf16[16,24,1024]{2,1,0:T(8,128)(2,1)} %bitcast.76), calls=%async_computation.1 | async-start | bytes 1572864 | tf_op jit(solution)/shard_map/all_to_all | solution.py:353
  30.6 2.7 multiply_convert_fusion.1
  33.3 1.6 pad_maximum_fusion
  34.9 9.2 %all-to-all-done.1 = bf16[16,24,1024]{2,1,0:T(8,128)(2,1)S(1)} async-done(((bf16[16,24,1024]{2,1,0:T(8,128)(2,1)}), bf16[16,24,1024]{2,1,0:T(8,128)(2,1)S(1)}, u32[]{:S(2)}, u32[]{:S(2)}) %all-to-all-start.1) | async-done | bytes 786464 | tf_op jit(solution)/shard_map/all_to_all | solution.py:353
  44.1 0.9 copy-done.1
  45.0 3.7 %all-to-all-start.2 = ((bf16[16,256,256]{2,1,0:T(8,128)(2,1)}), bf16[16,256,256]{2,1,0:T(8,128)(2,1)S(1)}, u32[]{:S(2)}, u32[]{:S(2)}) async-start(bf16[16,256,256]{2,1,0:T(8,128)(2,1)} %pad_maximum_fusion), calls=%async_computation.2 | async-start | bytes 4194304 | tf_op jit(solution)/shard_map/all_to_all | solution.py:363
  48.8 2.8 %convert_element_type.27 = bf16[16,64,512]{2,1,0:T(8,128)(2,1)} convert(f32[16,64,512]{2,1,0:T(8,128)} %param.14) | non-fusion elementwise | flops 524288 | bytes 3145728 | tf_op jit(solution)/shard_map/convert_element_type | solution.py:364
  51.5 25.8 %all-to-all-done.2 = bf16[16,256,256]{2,1,0:T(8,128)(2,1)S(1)} async-done(((bf16[16,256,256]{2,1,0:T(8,128)(2,1)}), bf16[16,256,256]{2,1,0:T(8,128)(2,1)S(1)}, u32[]{:S(2)}, u32[]{:S(2)}) %all-to-all-start.2) | async-done | bytes 2097184 | tf_op jit(solution)/shard_map/all_to_all | solution.py:363
  77.4 1.6 collective-permute-start.17
  79.1 1.8 collective-permute-start.19
  80.9 4.3 %all-to-all-start.3 = ((bf16[16,64,512]{2,1,0:T(8,128)(2,1)}), bf16[16,64,512]{2,1,0:T(8,128)(2,1)}, u32[]{:S(2)}, u32[]{:S(2)}) async-start(bf16[16,64,512]{2,1,0:T(8,128)(2,1)} %convert_element_type.27), calls=%async_computation.3 | async-start | bytes 2097152 | tf_op jit(solution)/shard_map/all_to_all | solution.py:365
  85.3 1.6 collective-permute-start.21
  86.9 1.8 collective-permute-start.7
  88.7 13.2 %collective-permute-done.7 = bf16[384,128]{1,0:T(8,128)(2,1)S(1)} collective-permute-done((bf16[384,128]{1,0:T(8,128)(2,1)S(1)}, bf16[384,128]{1,0:T(8,128)(2,1)S(1)}, u32[]{:S(2)}, u32[]{:S(2)}) %collective-permute-start.7) | collective-permute-done | bytes 98336 | tf_op jit(solution)/shard_map/ppermute | solution.py:292
  102.4 5.6 %collective-permute-done.8 = bf16[384,128]{1,0:T(8,128)(2,1)S(1)} collective-permute-done((bf16[384,128]{1,0:T(8,128)(2,1)S(1)}, bf16[384,128]{1,0:T(8,128)(2,1)S(1)}, u32[]{:S(2)}, u32[]{:S(2)}) %collective-permute-start.8) | collective-permute-done | bytes 98336 | tf_op jit(solution)/shard_map/ppermute | solution.py:292
  108.5 4.1 %collective-permute-done.9 = bf16[384,128]{1,0:T(8,128)(2,1)S(1)} collective-permute-done((bf16[384,128]{1,0:T(8,128)(2,1)S(1)}, bf16[384,128]{1,0:T(8,128)(2,1)S(1)}, u32[]{:S(2)}, u32[]{:S(2)}) %collective-permute-start.9) | collective-permute-done | bytes 98336 | tf_op jit(solution)/shard_map/ppermute | solution.py:292
  112.9 1.1 collective-permute-start.18
  114.1 2.1 collective-permute-start.20
  116.9 1.0 pad_maximum_fusion.3.refs_4_
  117.9 16.7 %collective-permute-done.22.refs_4_ = bf16[384,1024]{1,0:T(8,128)(2,1)} collective-permute-done((bf16[384,1024]{1,0:T(8,128)(2,1)}, bf16[384,1024]{1,0:T(8,128)(2,1)}, u32[]{:S(2)}, u32[]{:S(2)}) %collective-permute-start.22) | collective-permute-done | bytes 786464 | tf_op jit(solution)/shard_map/ppermute | solution.py:276
  134.6 2.1 collective-permute-start.1
  136.7 1.1 copy-done.2
  137.8 2.4 shard_map.159.sq_ref
  140.2 7.4 %collective-permute-done.18.far0_ref = bf16[384,1024]{1,0:T(8,128)(2,1)} collective-permute-done((bf16[384,1024]{1,0:T(8,128)(2,1)}, bf16[384,1024]{1,0:T(8,128)(2,1)}, u32[]{:S(2)}, u32[]{:S(2)}) %collective-permute-start.18) | collective-permute-done | bytes 786464 | tf_op jit(solution)/shard_map/ppermute | solution.py:276
  147.6 4.2 %collective-permute-start.2 = (bf16[384,128]{1,0:T(8,128)(2,1)S(1)}, bf16[384,128]{1,0:T(8,128)(2,1)S(1)}, u32[]{:S(2)}, u32[]{:S(2)}) collective-permute-start(bf16[384,128]{1,0:T(8,128)(2,1)S(1)} %get-tuple-element.58), channel_id=1, source_target_pairs={{0,16},{8,24},{16,0},{24,8},{32,48},{40,56},{48,32},{56,40},{64,80... | collective-permute-start | bytes 294920 | tf_op jit(solution)/shard_map/ppermute | solution.py:292
  151.8 1.1 collective-permute-start.3
  152.8 5.7 %shard_map.158.acc_ref = f32[2,384,512]{2,1,0:T(8,128)S(1)} custom-call(s32[4]{0:T(128)S(1)} %pad_add_fusion.place_ref, bf16[384,1024]{1,0:T(8,128)(2,1)S(1)} %bitcast.64, bf16[384,1024]{1,0:T(8,128)(2,1)} %collective-permute-done.17.refs_1_, bf16[384,1024]{1,0:T(8,128)(2,1)} %collective-permute-done.21.refs_2_, bf16[384,1024]{1,0:T(8,128)(2,1)S(1)} %bitcast.68, ...), custom_call_target="tpu_custom_call" | custom-call | flops 2415919104 | bytes 4194304 | tf_op jit(solution)/shard_map/pallas_call | solution.py:391
  158.5 1.0 collective-permute-start.10
  159.6 3.2 %shard_map.160 = bf16[2,384,256]{2,1,0:T(8,128)(2,1)S(1)} custom-call(s32[4]{0:T(128)S(1)} %pad_add_fusion.place_ref, bf16[384,1024]{1,0:T(8,128)(2,1)} %collective-permute-done.18.far0_ref, bf16[384,1024]{1,0:T(8,128)(2,1)} %collective-permute-done.20.far1_ref, f32[2,384,512]{2,1,0:T(8,128)S(1)} %shard_map.158.acc_ref, ...), custom_call_target="tpu_custom_call" | custom-call | flops 805306368 | bytes 1048576 | tf_op jit(solution)/shard_map/pallas_call | solution.py:403
  163.0 3.2 %collective-permute-start.25 = (bf16[768,256]{1,0:T(8,128)(2,1)S(1)}, bf16[768,256]{1,0:T(8,128)(2,1)S(1)}, u32[]{:S(2)}, u32[]{:S(2)}) collective-permute-start(bf16[768,256]{1,0:T(8,128)(2,1)S(1)} %bitcast.71), channel_id=1, source_target_pairs={{0,6},{1,7},{2,0},{3,1},{4,2},{5,3},{6,4},{7,5},{8,14},{9,15},{10,... | collective-permute-start | bytes 1179656 | tf_op jit(solution)/shard_map/ppermute | solution.py:276
  166.3 5.5 %collective-permute-done.10.refs_5_ = bf16[4,384,128]{2,1,0:T(8,128)(2,1)S(1)} collective-permute-done((bf16[4,384,128]{2,1,0:T(8,128)(2,1)S(1)}, bf16[4,384,128]{2,1,0:T(8,128)(2,1)S(1)}, u32[]{:S(2)}, u32[]{:S(2)}) %collective-permute-start.10) | collective-permute-done | bytes 393248 | tf_op jit(solution)/shard_map/ppermute | solution.py:292
  171.8 0.7 copy-done.15
  172.6 7.3 %collective-permute-done.24.h1_ref = bf16[768,256]{1,0:T(8,128)(2,1)S(1)} collective-permute-done((bf16[768,256]{1,0:T(8,128)(2,1)S(1)}, bf16[768,256]{1,0:T(8,128)(2,1)S(1)}, u32[]{:S(2)}, u32[]{:S(2)}) %collective-permute-start.24) | collective-permute-done | bytes 393248 | tf_op jit(solution)/shard_map/ppermute | solution.py:276
  180.2 3.9 %collective-permute-start.5 = (bf16[4,384,128]{2,1,0:T(8,128)(2,1)S(1)}, bf16[4,384,128]{2,1,0:T(8,128)(2,1)}, u32[]{:S(2)}, u32[]{:S(2)}) collective-permute-start(bf16[4,384,128]{2,1,0:T(8,128)(2,1)S(1)} %pad_maximum_fusion.2.refs_0_), channel_id=1, source_target_pairs={{0,64},{8,72},{16,80},{24,88},{32,96},{40,104},{48,112},{56,120},{... | collective-permute-start | bytes 1179656 | tf_op jit(solution)/shard_map/ppermute | solution.py:292
  184.0 0.7 collective-permute-start.6
  184.8 4.2 %shard_map.161 = bf16[16,2,2,24,512]{4,3,2,1,0:T(8,128)(2,1)S(1)} custom-call(s32[4]{0:T(128)S(1)} %pad_add_fusion.place_ref, bf16[768,256]{1,0:T(8,128)(2,1)S(1)} %bitcast.73, bf16[768,256]{1,0:T(8,128)(2,1)S(1)} %collective-permute-done.24.h1_ref, bf16[768,256]{1,0:T(8,128)(2,1)S(1)} %collective-permute-done.25.h2_ref, ...), custom_call_target="tpu_custom_call" | custom-call | flops 1610612736 | bytes 4194304 | tf_op jit(solution)/shard_map/pallas_call | solution.py:452
  189.0 1.2 copy-done.8
  190.2 4.4 %all-to-all-start.4 = ((bf16[16,2,48,512]{3,2,1,0:T(8,128)(2,1)}), bf16[16,2,48,512]{3,2,1,0:T(8,128)(2,1)}, u32[]{:S(2)}, u32[]{:S(2)}) async-start(bf16[16,2,48,512]{3,2,1,0:T(8,128)(2,1)} %bitcast.69), calls=%async_computation.4 | async-start | bytes 3145728 | tf_op jit(solution)/shard_map/all_to_all | solution.py:470
  194.7 3.9 %shard_map.154.x_ref = bf16[512,4096]{1,0:T(8,128)(2,1)} custom-call(bf16[512,4096]{1,0:T(8,128)(2,1)} %tok_ref.3), custom_call_target="tpu_custom_call" | custom-call | flops 33554432 | bytes 8388608 | tf_op jit(solution)/shard_map/pallas_call | solution.py:335
  198.6 2.9 %collective-permute-done.5.refs_2_ = bf16[4,384,128]{2,1,0:T(8,128)(2,1)} collective-permute-done((bf16[4,384,128]{2,1,0:T(8,128)(2,1)S(1)}, bf16[4,384,128]{2,1,0:T(8,128)(2,1)}, u32[]{:S(2)}, u32[]{:S(2)}) %collective-permute-start.5) | collective-permute-done | bytes 393248 | tf_op jit(solution)/shard_map/ppermute | solution.py:292
  201.5 7.3 %collective-permute-done.6.refs_3_ = bf16[4,384,128]{2,1,0:T(8,128)(2,1)} collective-permute-done((bf16[4,384,128]{2,1,0:T(8,128)(2,1)S(1)}, bf16[4,384,128]{2,1,0:T(8,128)(2,1)}, u32[]{:S(2)}, u32[]{:S(2)}) %collective-permute-start.6) | collective-permute-done | bytes 393248 | tf_op jit(solution)/shard_map/ppermute | solution.py:292
  208.8 2.2 copy-done
  211.0 4.9 %shard_map.155 = (bf16[4096,128]{1,0:T(8,128)(2,1)}, bf16[4096,128]{1,0:T(8,128)(2,1)}, bf16[512,128]{1,0:T(8,128)(2,1)S(1)}, bf16[1024,512]{1,0:T(8,128)(2,1)S(1)}, bf16[512,512]{1,0:T(8,128)(2,1)S(1)}) custom-call(s32[4]{0:T(128)S(1)} %pad_add_fusion.place_ref, bf16[512,4096]{1,0:T(8,128)(2,1)S(1)} %copy-done, ...), custom_call_target="tpu_custom_call" | custom-call | flops 1073741824 | bytes 4194304 | tf_op jit(solution)/shard_map/pallas_call | solution.py:417
  215.9 1.0 copy-done.9
  216.9 3.2 %collective-permute-start.29 = (bf16[512,128]{1,0:T(8,128)(2,1)S(1)}, bf16[512,128]{1,0:T(8,128)(2,1)S(1)}, u32[]{:S(2)}, u32[]{:S(2)}) collective-permute-start(bf16[512,128]{1,0:T(8,128)(2,1)S(1)} %get-tuple-element.50), channel_id=1, source_target_pairs={{0,6},{1,7},{2,0},{3,1},{4,2},{5,3},{6,4},{7,5},{8,14},{9,15},{10,... | collective-permute-start | bytes 393224 | tf_op jit(solution)/shard_map/ppermute | solution.py:276
  220.1 0.7 collective-permute-start.30
  220.8 2.3 collective-permute-done.28
  223.0 3.5 %collective-permute-done.30 = bf16[512,128]{1,0:T(8,128)(2,1)S(1)} collective-permute-done((bf16[512,128]{1,0:T(8,128)(2,1)S(1)}, bf16[512,128]{1,0:T(8,128)(2,1)S(1)}, u32[]{:S(2)}, u32[]{:S(2)}) %collective-permute-start.30) | collective-permute-done | bytes 131104 | tf_op jit(solution)/shard_map/ppermute | solution.py:276
  227.4 1.7 fusion.4
  229.1 0.8 copy-done.13
  229.9 1.0 copy-done.7
  231.0 1.0 copy-done.14
  232.0 1.5 shard_map.162.base_ref
  233.6 3.3 %shard_map.156 = (bf16[256,1024]{1,0:T(8,128)(2,1)S(1)}, bf16[256,1024]{1,0:T(8,128)(2,1)}, bf16[256,1024]{1,0:T(8,128)(2,1)}, bf16[256,1024]{1,0:T(8,128)(2,1)}) custom-call(s32[4]{0:T(128)S(1)} %pad_add_fusion.place_ref, bf16[1024,512]{1,0:T(8,128)(2,1)} %bitcast.12.own_ref.w_own_ref, bf16[1024,512]{1,0:T(8,128)(2,1)} %collective-permute-done.other_ref.w_other_ref, ...), custom_call_target="tpu_custom_call" | custom-call | flops 1073741824 | bytes 4194304 | tf_op jit(solution)/shard_map/pallas_call | solution.py:518
  236.9 0.8 copy-done.11
  237.7 2.7 collective-permute-start.15
  241.0 1.2 slice.68
  242.3 1.5 slice_bitcast_fusion
  243.7 20.6 %collective-permute-done.14.p1_ref = bf16[256,1024]{1,0:T(8,128)(2,1)} collective-permute-done((bf16[256,1024]{1,0:T(8,128)(2,1)}, bf16[256,1024]{1,0:T(8,128)(2,1)}, u32[]{:S(2)}, u32[]{:S(2)}) %collective-permute-start.14) | collective-permute-done | bytes 524320 | tf_op jit(solution)/shard_map/ppermute | solution.py:276
  264.9 3.3 %shard_map.157 = (bf16[128,4096]{1,0:T(8,128)(2,1)}, bf16[128,4096]{1,0:T(8,128)(2,1)}) custom-call(s32[4]{0:T(128)S(1)} %pad_add_fusion.place_ref, bf16[256,1024]{1,0:T(8,128)(2,1)S(1)} %copy-done.12, bf16[256,1024]{1,0:T(8,128)(2,1)} %collective-permute-done.14.p1_ref, bf16[256,1024]{1,0:T(8,128)(2,1)} %collective-permute-done.15.p2_ref, ...), custom_call_target="tpu_custom_call" | custom-call | flops 1048576 | bytes 4194304 | tf_op jit(solution)/shard_map/pallas_call | solution.py:534
  268.3 1.8 shard_map.163.base_ref
  270.1 1.4 shard_map.164
  (93 shorter events, 4.9 us)
Async XLA Ops:
  4.5 26.2 %copy-start.26 = (f32[256]{0:T(256)S(1)}, f32[256]{0:T(256)}, u32[]{:S(2)}) copy-start(f32[256]{0:T(256)} %param.11) | copy-start | bytes 3076
  27.0 17.2 %all-to-all-start.1 = ((bf16[16,24,1024]{2,1,0:T(8,128)(2,1)}), bf16[16,24,1024]{2,1,0:T(8,128)(2,1)S(1)}, u32[]{:S(2)}, u32[]{:S(2)}) async-start(bf16[16,24,1024]{2,1,0:T(8,128)(2,1)} %bitcast.76), calls=%async_computation.1 | async-start | bytes 1572864 | tf_op jit(solution)/shard_map/all_to_all | solution.py:353
  44.1 0.9 copy-start.1
  45.0 32.4 %all-to-all-start.2 = ((bf16[16,256,256]{2,1,0:T(8,128)(2,1)}), bf16[16,256,256]{2,1,0:T(8,128)(2,1)S(1)}, u32[]{:S(2)}, u32[]{:S(2)}) async-start(bf16[16,256,256]{2,1,0:T(8,128)(2,1)} %pad_maximum_fusion), calls=%async_computation.2 | async-start | bytes 4194304 | tf_op jit(solution)/shard_map/all_to_all | solution.py:363
  48.8 28.6 %copy-start.20 = (f32[64,512]{1,0:T(8,128)S(1)}, f32[64,512]{1,0:T(8,128)}, u32[]{:S(2)}) copy-start(f32[64,512]{1,0:T(8,128)} %param.17) | copy-start | bytes 393220
  48.8 30.2 %copy-start.18 = (f32[256,128]{1,0:T(8,128)S(1)}, f32[256,128]{1,0:T(8,128)}, u32[]{:S(2)}) copy-start(f32[256,128]{1,0:T(8,128)} %param.16) | copy-start | bytes 393220
  48.8 30.2 %copy-start.19 = (f32[256,128]{1,0:T(8,128)S(1)}, f32[256,128]{1,0:T(8,128)}, u32[]{:S(2)}) copy-start(f32[256,128]{1,0:T(8,128)} %param.15) | copy-start | bytes 393220
  77.4 74.4 %collective-permute-start.23 = (bf16[4096,256]{1,0:T(8,128)(2,1)S(1)}, bf16[4096,256]{1,0:T(8,128)(2,1)}, u32[]{:S(2)}, u32[]{:S(2)}) collective-permute-start(bf16[4096,256]{1,0:T(8,128)(2,1)S(1)} %bitcast.57), channel_id=1, source_target_pairs={{0,1},{1,0},{2,3},{3,2},{4,5},{5,4},{6,7},{7,6},{8,9},{9,8},{10,11... | collective-permute-start | bytes 6291464 | tf_op jit(solution)/shard_map/ppermute | solution.py:279
  77.4 35.5 %collective-permute-start.17 = (bf16[384,1024]{1,0:T(8,128)(2,1)S(1)}, bf16[384,1024]{1,0:T(8,128)(2,1)}, u32[]{:S(2)}, u32[]{:S(2)}) collective-permute-start(bf16[384,1024]{1,0:T(8,128)(2,1)S(1)} %bitcast.61), channel_id=1, source_target_pairs={{0,2},{1,3},{2,4},{3,5},{4,6},{5,7},{6,0},{7,1},{8,10},{9,11},{10,... | collective-permute-start | bytes 2359304 | tf_op jit(solution)/shard_map/ppermute | solution.py:276
  79.1 35.0 %collective-permute-start.19 = (bf16[384,1024]{1,0:T(8,128)(2,1)}, bf16[384,1024]{1,0:T(8,128)(2,1)}, u32[]{:S(2)}, u32[]{:S(2)}) collective-permute-start(bf16[384,1024]{1,0:T(8,128)(2,1)} %bitcast.65), channel_id=1, source_target_pairs={{0,6},{1,7},{2,0},{3,1},{4,2},{5,3},{6,4},{7,5},{8,14},{9,15},{10,... | collective-permute-start | bytes 2359304 | tf_op jit(solution)/shard_map/ppermute | solution.py:276
  80.9 35.8 %all-to-all-start.3 = ((bf16[16,64,512]{2,1,0:T(8,128)(2,1)}), bf16[16,64,512]{2,1,0:T(8,128)(2,1)}, u32[]{:S(2)}, u32[]{:S(2)}) async-start(bf16[16,64,512]{2,1,0:T(8,128)(2,1)} %convert_element_type.27), calls=%async_computation.3 | async-start | bytes 2097152 | tf_op jit(solution)/shard_map/all_to_all | solution.py:365
  85.3 31.5 %collective-permute-start.21 = (bf16[384,1024]{1,0:T(8,128)(2,1)S(1)}, bf16[384,1024]{1,0:T(8,128)(2,1)}, u32[]{:S(2)}, u32[]{:S(2)}) collective-permute-start(bf16[384,1024]{1,0:T(8,128)(2,1)S(1)} %bitcast.62), channel_id=1, source_target_pairs={{0,6},{1,7},{2,0},{3,1},{4,2},{5,3},{6,4},{7,5},{8,14},{9,15},{10,... | collective-permute-start | bytes 2359304 | tf_op jit(solution)/shard_map/ppermute | solution.py:276
  86.9 15.0 %collective-permute-start.7 = (bf16[384,128]{1,0:T(8,128)(2,1)S(1)}, bf16[384,128]{1,0:T(8,128)(2,1)S(1)}, u32[]{:S(2)}, u32[]{:S(2)}) collective-permute-start(bf16[384,128]{1,0:T(8,128)(2,1)S(1)} %get-tuple-element.56), channel_id=1, source_target_pairs={{0,32},{8,40},{16,48},{24,56},{32,64},{40,72},{48,80},{56,88},{64,... | collective-permute-start | bytes 294920 | tf_op jit(solution)/shard_map/ppermute | solution.py:292
  101.9 6.1 %collective-permute-start.8 = (bf16[384,128]{1,0:T(8,128)(2,1)S(1)}, bf16[384,128]{1,0:T(8,128)(2,1)S(1)}, u32[]{:S(2)}, u32[]{:S(2)}) collective-permute-start(bf16[384,128]{1,0:T(8,128)(2,1)S(1)} %get-tuple-element.56), channel_id=1, source_target_pairs={{0,64},{8,72},{16,80},{24,88},{32,96},{40,104},{48,112},{56,120},{... | collective-permute-start | bytes 294920 | tf_op jit(solution)/shard_map/ppermute | solution.py:292
  108.0 8.8 %copy-start.21 = (bf16[384,128]{1,0:T(8,128)(2,1)}, bf16[384,128]{1,0:T(8,128)(2,1)S(1)}, u32[]{:S(2)}) copy-start(bf16[384,128]{1,0:T(8,128)(2,1)S(1)} %collective-permute-done.8) | copy-start | bytes 294916
  108.0 4.6 %collective-permute-start.9 = (bf16[384,128]{1,0:T(8,128)(2,1)S(1)}, bf16[384,128]{1,0:T(8,128)(2,1)S(1)}, u32[]{:S(2)}, u32[]{:S(2)}) collective-permute-start(bf16[384,128]{1,0:T(8,128)(2,1)S(1)} %get-tuple-element.56), channel_id=1, source_target_pairs={{0,96},{8,104},{16,112},{24,120},{32,0},{40,8},{48,16},{56,24},{64... | collective-permute-start | bytes 294920 | tf_op jit(solution)/shard_map/ppermute | solution.py:292
  112.6 4.2 %copy-start.22 = (bf16[384,128]{1,0:T(8,128)(2,1)}, bf16[384,128]{1,0:T(8,128)(2,1)S(1)}, u32[]{:S(2)}) copy-start(bf16[384,128]{1,0:T(8,128)(2,1)S(1)} %collective-permute-done.9) | copy-start | bytes 294916
  112.6 21.9 %collective-permute-start.22 = (bf16[384,1024]{1,0:T(8,128)(2,1)}, bf16[384,1024]{1,0:T(8,128)(2,1)}, u32[]{:S(2)}, u32[]{:S(2)}) collective-permute-start(bf16[384,1024]{1,0:T(8,128)(2,1)} %bitcast.66), channel_id=1, source_target_pairs={{0,2},{1,3},{2,4},{3,5},{4,6},{5,7},{6,0},{7,1},{8,10},{9,11},{10,... | collective-permute-start | bytes 2359304 | tf_op jit(solution)/shard_map/ppermute | solution.py:276
  112.9 34.7 %collective-permute-start.18 = (bf16[384,1024]{1,0:T(8,128)(2,1)}, bf16[384,1024]{1,0:T(8,128)(2,1)}, u32[]{:S(2)}, u32[]{:S(2)}) collective-permute-start(bf16[384,1024]{1,0:T(8,128)(2,1)} %collective-permute-done.17.refs_1_), channel_id=1, source_target_pairs={{0,2},{1,3},{2,4},{3,5},{4,6},{5,7},{6,0},{7,1},{8,10},{9,11},{10,... | collective-permute-start | bytes 2359304 | tf_op jit(solution)/shard_map/ppermute | solution.py:276
  114.1 44.5 %collective-permute-start.20 = (bf16[384,1024]{1,0:T(8,128)(2,1)}, bf16[384,1024]{1,0:T(8,128)(2,1)}, u32[]{:S(2)}, u32[]{:S(2)}) collective-permute-start(bf16[384,1024]{1,0:T(8,128)(2,1)} %collective-permute-done.19.refs_5_), channel_id=1, source_target_pairs={{0,6},{1,7},{2,0},{3,1},{4,2},{5,3},{6,4},{7,5},{8,14},{9,15},{10,... | collective-permute-start | bytes 2359304 | tf_op jit(solution)/shard_map/ppermute | solution.py:276
  116.7 55.8 %collective-permute-start = (bf16[1024,512]{1,0:T(8,128)(2,1)}, bf16[1024,512]{1,0:T(8,128)(2,1)}, u32[]{:S(2)}, u32[]{:S(2)}) collective-permute-start(bf16[1024,512]{1,0:T(8,128)(2,1)} %bitcast.12.own_ref.w_own_ref), channel_id=1, source_target_pairs={{0,1},{1,0},{2,3},{3,2},{4,5},{5,4},{6,7},{7,6},{8,9},{9,8},{10,11... | collective-permute-start | bytes 3145736 | tf_op jit(solution)/shard_map/ppermute | solution.py:279
  134.6 28.2 %collective-permute-start.1 = (bf16[384,128]{1,0:T(8,128)(2,1)S(1)}, bf16[384,128]{1,0:T(8,128)(2,1)S(1)}, u32[]{:S(2)}, u32[]{:S(2)}) collective-permute-start(bf16[384,128]{1,0:T(8,128)(2,1)S(1)} %get-tuple-element.58), channel_id=1, source_target_pairs={{0,8},{8,16},{16,24},{24,0},{32,40},{40,48},{48,56},{56,32},{64,72... | collective-permute-start | bytes 294920 | tf_op jit(solution)/shard_map/ppermute | solution.py:292
  136.7 1.1 copy-start.2
  137.8 15.0 %copy-start.3 = (bf16[16,24,1024]{2,1,0:T(8,128)(2,1)S(1)}, bf16[16,24,1024]{2,1,0:T(8,128)(2,1)}, u32[]{:S(2)}) copy-start(bf16[16,24,1024]{2,1,0:T(8,128)(2,1)} %copy-done.1) | copy-start | bytes 2359300
  147.6 15.4 %collective-permute-start.2 = (bf16[384,128]{1,0:T(8,128)(2,1)S(1)}, bf16[384,128]{1,0:T(8,128)(2,1)S(1)}, u32[]{:S(2)}, u32[]{:S(2)}) collective-permute-start(bf16[384,128]{1,0:T(8,128)(2,1)S(1)} %get-tuple-element.58), channel_id=1, source_target_pairs={{0,16},{8,24},{16,0},{24,8},{32,48},{40,56},{48,32},{56,40},{64,80... | collective-permute-start | bytes 294920 | tf_op jit(solution)/shard_map/ppermute | solution.py:292
  151.8 14.5 %collective-permute-start.3 = (bf16[384,128]{1,0:T(8,128)(2,1)S(1)}, bf16[384,128]{1,0:T(8,128)(2,1)S(1)}, u32[]{:S(2)}, u32[]{:S(2)}) collective-permute-start(bf16[384,128]{1,0:T(8,128)(2,1)S(1)} %get-tuple-element.58), channel_id=1, source_target_pairs={{0,24},{8,0},{16,8},{24,16},{32,56},{40,32},{48,40},{56,48},{64,88... | collective-permute-start | bytes 294920 | tf_op jit(solution)/shard_map/ppermute | solution.py:292
  158.5 13.3 %collective-permute-start.10 = (bf16[4,384,128]{2,1,0:T(8,128)(2,1)S(1)}, bf16[4,384,128]{2,1,0:T(8,128)(2,1)S(1)}, u32[]{:S(2)}, u32[]{:S(2)}) collective-permute-start(bf16[4,384,128]{2,1,0:T(8,128)(2,1)S(1)} %pad_maximum_fusion.3.refs_4_), channel_id=1, source_target_pairs={{0,8},{8,16},{16,24},{24,0},{32,40},{40,48},{48,56},{56,32},{64,72... | collective-permute-start | bytes 1179656 | tf_op jit(solution)/shard_map/ppermute | solution.py:292
  162.8 17.1 %collective-permute-start.24 = (bf16[768,256]{1,0:T(8,128)(2,1)S(1)}, bf16[768,256]{1,0:T(8,128)(2,1)S(1)}, u32[]{:S(2)}, u32[]{:S(2)}) collective-permute-start(bf16[768,256]{1,0:T(8,128)(2,1)S(1)} %bitcast.70), channel_id=1, source_target_pairs={{0,2},{1,3},{2,4},{3,5},{4,6},{5,7},{6,0},{7,1},{8,10},{9,11},{10,... | collective-permute-start | bytes 1179656 | tf_op jit(solution)/shard_map/ppermute | solution.py:276
  163.0 17.1 %collective-permute-start.25 = (bf16[768,256]{1,0:T(8,128)(2,1)S(1)}, bf16[768,256]{1,0:T(8,128)(2,1)S(1)}, u32[]{:S(2)}, u32[]{:S(2)}) collective-permute-start(bf16[768,256]{1,0:T(8,128)(2,1)S(1)} %bitcast.71), channel_id=1, source_target_pairs={{0,6},{1,7},{2,0},{3,1},{4,2},{5,3},{6,4},{7,5},{8,14},{9,15},{10,... | collective-permute-start | bytes 1179656 | tf_op jit(solution)/shard_map/ppermute | solution.py:276
  166.3 17.8 %collective-permute-start.26 = (bf16[768,256]{1,0:T(8,128)(2,1)S(1)}, bf16[768,256]{1,0:T(8,128)(2,1)S(1)}, u32[]{:S(2)}, u32[]{:S(2)}) collective-permute-start(bf16[768,256]{1,0:T(8,128)(2,1)S(1)} %bitcast.72), channel_id=1, source_target_pairs={{0,4},{1,5},{2,6},{3,7},{4,0},{5,1},{6,2},{7,3},{8,12},{9,13},{10,... | collective-permute-start | bytes 1179656 | tf_op jit(solution)/shard_map/ppermute | solution.py:276
  171.8 0.7 copy-start.15
  172.5 26.0 %collective-permute-start.11 = (bf16[4,384,128]{2,1,0:T(8,128)(2,1)S(1)}, bf16[4,384,128]{2,1,0:T(8,128)(2,1)}, u32[]{:S(2)}, u32[]{:S(2)}) collective-permute-start(bf16[4,384,128]{2,1,0:T(8,128)(2,1)S(1)} %pad_maximum_fusion.3.refs_4_), channel_id=1, source_target_pairs={{0,16},{8,24},{16,0},{24,8},{32,48},{40,56},{48,32},{56,40},{64,80... | collective-permute-start | bytes 1179656 | tf_op jit(solution)/shard_map/ppermute | solution.py:292
  172.6 26.0 %collective-permute-start.12 = (bf16[4,384,128]{2,1,0:T(8,128)(2,1)S(1)}, bf16[4,384,128]{2,1,0:T(8,128)(2,1)}, u32[]{:S(2)}, u32[]{:S(2)}) collective-permute-start(bf16[4,384,128]{2,1,0:T(8,128)(2,1)S(1)} %pad_maximum_fusion.3.refs_4_), channel_id=1, source_target_pairs={{0,24},{8,0},{16,8},{24,16},{32,56},{40,32},{48,40},{56,48},{64,88... | collective-permute-start | bytes 1179656 | tf_op jit(solution)/shard_map/ppermute | solution.py:292
  179.9 18.7 %collective-permute-start.4 = (bf16[4,384,128]{2,1,0:T(8,128)(2,1)S(1)}, bf16[4,384,128]{2,1,0:T(8,128)(2,1)}, u32[]{:S(2)}, u32[]{:S(2)}) collective-permute-start(bf16[4,384,128]{2,1,0:T(8,128)(2,1)S(1)} %pad_maximum_fusion.2.refs_0_), channel_id=1, source_target_pairs={{0,32},{8,40},{16,48},{24,56},{32,64},{40,72},{48,80},{56,88},{64,... | collective-permute-start | bytes 1179656 | tf_op jit(solution)/shard_map/ppermute | solution.py:292
  180.2 21.3 %collective-permute-start.5 = (bf16[4,384,128]{2,1,0:T(8,128)(2,1)S(1)}, bf16[4,384,128]{2,1,0:T(8,128)(2,1)}, u32[]{:S(2)}, u32[]{:S(2)}) collective-permute-start(bf16[4,384,128]{2,1,0:T(8,128)(2,1)S(1)} %pad_maximum_fusion.2.refs_0_), channel_id=1, source_target_pairs={{0,64},{8,72},{16,80},{24,88},{32,96},{40,104},{48,112},{56,120},{... | collective-permute-start | bytes 1179656 | tf_op jit(solution)/shard_map/ppermute | solution.py:292
  184.0 24.8 %collective-permute-start.6 = (bf16[4,384,128]{2,1,0:T(8,128)(2,1)S(1)}, bf16[4,384,128]{2,1,0:T(8,128)(2,1)}, u32[]{:S(2)}, u32[]{:S(2)}) collective-permute-start(bf16[4,384,128]{2,1,0:T(8,128)(2,1)S(1)} %pad_maximum_fusion.2.refs_0_), channel_id=1, source_target_pairs={{0,96},{8,104},{16,112},{24,120},{32,0},{40,8},{48,16},{56,24},{64... | collective-permute-start | bytes 1179656 | tf_op jit(solution)/shard_map/ppermute | solution.py:292
  189.0 1.2 copy-start.8
  190.2 50.8 %all-to-all-start.4 = ((bf16[16,2,48,512]{3,2,1,0:T(8,128)(2,1)}), bf16[16,2,48,512]{3,2,1,0:T(8,128)(2,1)}, u32[]{:S(2)}, u32[]{:S(2)}) async-start(bf16[16,2,48,512]{3,2,1,0:T(8,128)(2,1)} %bitcast.69), calls=%async_computation.4 | async-start | bytes 3145728 | tf_op jit(solution)/shard_map/all_to_all | solution.py:470
  194.6 14.2 %copy-start.16 = (bf16[4,384,128]{2,1,0:T(8,128)(2,1)S(1)}, bf16[4,384,128]{2,1,0:T(8,128)(2,1)}, u32[]{:S(2)}) copy-start(bf16[4,384,128]{2,1,0:T(8,128)(2,1)} %copy-done.15) | copy-start | bytes 1179652
  194.6 26.1 %copy-start.25 = (f32[512,2]{0,1:T(2,128)S(1)}, f32[512,2]{0,1:T(2,128)}, u32[]{:S(2)}) copy-start(f32[512,2]{0,1:T(2,128)} %param.19) | copy-start | bytes 12292
  194.6 32.7 %copy-start.23 = (s32[512,2]{0,1:T(2,128)S(1)}, s32[512,2]{0,1:T(2,128)}, u32[]{:S(2)}) copy-start(s32[512,2]{0,1:T(2,128)} %param.18) | copy-start | bytes 12292
  194.6 32.7 %copy-start.24 = (s32[2,512]{1,0:T(2,128)S(1)}, s32[2,512]{1,0:T(2,128)}, u32[]{:S(2)}) copy-start(s32[2,512]{1,0:T(2,128)} %get-tuple-element.45) | copy-start | bytes 12292
  208.8 2.2 copy-start
  215.9 1.0 copy-start.9
  216.9 9.8 %copy-start.17 = (bf16[512,512]{1,0:T(8,128)(2,1)}, bf16[512,512]{1,0:T(8,128)(2,1)S(1)}, u32[]{:S(2)}) copy-start(bf16[512,512]{1,0:T(8,128)(2,1)S(1)} %get-tuple-element.36) | copy-start | bytes 1572868
  216.9 6.2 %collective-permute-start.28 = (bf16[512,128]{1,0:T(8,128)(2,1)S(1)}, bf16[512,128]{1,0:T(8,128)(2,1)S(1)}, u32[]{:S(2)}, u32[]{:S(2)}) collective-permute-start(bf16[512,128]{1,0:T(8,128)(2,1)S(1)} %get-tuple-element.50), channel_id=1, source_target_pairs={{0,2},{1,3},{2,4},{3,5},{4,6},{5,7},{6,0},{7,1},{8,10},{9,11},{10,... | collective-permute-start | bytes 393224 | tf_op jit(solution)/shard_map/ppermute | solution.py:276
  216.9 6.2 %collective-permute-start.29 = (bf16[512,128]{1,0:T(8,128)(2,1)S(1)}, bf16[512,128]{1,0:T(8,128)(2,1)S(1)}, u32[]{:S(2)}, u32[]{:S(2)}) collective-permute-start(bf16[512,128]{1,0:T(8,128)(2,1)S(1)} %get-tuple-element.50), channel_id=1, source_target_pairs={{0,6},{1,7},{2,0},{3,1},{4,2},{5,3},{6,4},{7,5},{8,14},{9,15},{10,... | collective-permute-start | bytes 393224 | tf_op jit(solution)/shard_map/ppermute | solution.py:276
  220.1 6.5 %collective-permute-start.30 = (bf16[512,128]{1,0:T(8,128)(2,1)S(1)}, bf16[512,128]{1,0:T(8,128)(2,1)S(1)}, u32[]{:S(2)}, u32[]{:S(2)}) collective-permute-start(bf16[512,128]{1,0:T(8,128)(2,1)S(1)} %get-tuple-element.50), channel_id=1, source_target_pairs={{0,4},{1,5},{2,6},{3,7},{4,0},{5,1},{6,2},{7,3},{8,12},{9,13},{10,... | collective-permute-start | bytes 393224 | tf_op jit(solution)/shard_map/ppermute | solution.py:276
  226.6 2.5 copy-start.6
  226.7 2.5 collective-permute-start.31
  226.8 3.1 %copy-start.10 = (bf16[1024,512]{1,0:T(8,128)(2,1)S(1)}, bf16[1024,512]{1,0:T(8,128)(2,1)}, u32[]{:S(2)}) copy-start(bf16[1024,512]{1,0:T(8,128)(2,1)} %copy-done.9) | copy-start | bytes 3145732
  226.8 6.8 %collective-permute-start.13 = (bf16[512,512]{1,0:T(8,128)(2,1)}, bf16[512,512]{1,0:T(8,128)(2,1)S(1)}, u32[]{:S(2)}, u32[]{:S(2)}) collective-permute-start(bf16[512,512]{1,0:T(8,128)(2,1)} %copy-done.17), channel_id=1, source_target_pairs={{0,1},{1,0},{2,3},{3,2},{4,5},{5,4},{6,7},{7,6},{8,9},{9,8},{10,11... | collective-permute-start | bytes 1572872 | tf_op jit(solution)/shard_map/ppermute | solution.py:279
  229.1 0.8 copy-start.13
  229.9 1.0 copy-start.7
  231.0 1.0 copy-start.14
  236.9 0.8 copy-start.11
  237.7 26.6 %collective-permute-start.14 = (bf16[256,1024]{1,0:T(8,128)(2,1)}, bf16[256,1024]{1,0:T(8,128)(2,1)}, u32[]{:S(2)}, u32[]{:S(2)}) collective-permute-start(bf16[256,1024]{1,0:T(8,128)(2,1)} %get-tuple-element.38), channel_id=1, source_target_pairs={{0,2},{1,3},{2,4},{3,5},{4,6},{5,7},{6,0},{7,1},{8,10},{9,11},{10,... | collective-permute-start | bytes 1572872 | tf_op jit(solution)/shard_map/ppermute | solution.py:276
  237.7 26.6 %collective-permute-start.15 = (bf16[256,1024]{1,0:T(8,128)(2,1)}, bf16[256,1024]{1,0:T(8,128)(2,1)}, u32[]{:S(2)}, u32[]{:S(2)}) collective-permute-start(bf16[256,1024]{1,0:T(8,128)(2,1)} %get-tuple-element.39), channel_id=1, source_target_pairs={{0,4},{1,5},{2,6},{3,7},{4,0},{5,1},{6,2},{7,3},{8,12},{9,13},{10,... | collective-permute-start | bytes 1572872 | tf_op jit(solution)/shard_map/ppermute | solution.py:276
  240.4 24.6 %collective-permute-start.16 = (bf16[256,1024]{1,0:T(8,128)(2,1)}, bf16[256,1024]{1,0:T(8,128)(2,1)}, u32[]{:S(2)}, u32[]{:S(2)}) collective-permute-start(bf16[256,1024]{1,0:T(8,128)(2,1)} %get-tuple-element.40), channel_id=1, source_target_pairs={{0,6},{1,7},{2,0},{3,1},{4,2},{5,3},{6,4},{7,5},{8,14},{9,15},{10,... | collective-permute-start | bytes 1572872 | tf_op jit(solution)/shard_map/ppermute | solution.py:276
  242.2 22.8 %copy-start.12 = (bf16[256,1024]{1,0:T(8,128)(2,1)S(1)}, bf16[256,1024]{1,0:T(8,128)(2,1)}, u32[]{:S(2)}) copy-start(bf16[256,1024]{1,0:T(8,128)(2,1)} %copy-done.11) | copy-start | bytes 1572868
  242.2 27.9 %collective-permute-start.27 = (bf16[768,512]{1,0:T(8,128)(2,1)S(1)}, bf16[768,512]{1,0:T(8,128)(2,1)S(1)}, u32[]{:S(2)}, u32[]{:S(2)}) collective-permute-start(bf16[768,512]{1,0:T(8,128)(2,1)S(1)} %bitcast.75), channel_id=1, source_target_pairs={{0,1},{1,0},{2,3},{3,2},{4,5},{5,4},{6,7},{7,6},{8,9},{9,8},{10,11... | collective-permute-start | bytes 2359304 | tf_op jit(solution)/shard_map/ppermute | solution.py:279
  243.7 24.5 %copy-start.5 = (bf16[512,768]{1,0:T(8,128)(2,1)S(1)}, bf16[512,768]{1,0:T(8,128)(2,1)}, u32[]{:S(2)}) copy-start(bf16[512,768]{1,0:T(8,128)(2,1)} %get-tuple-element.49.weight_ref) | copy-start | bytes 2359300
  268.3 1.8 copy-start.4

commit v8 on v6

--- a/solution.py
+++ b/solution.py
@@ -134,34 +134,41 @@
             out_ref[part, :, pl.ds(pl.multiple_of(slot * hs, hs), hs)] = value
 
 
-def down_kernel(place_ref, h0_ref, h1_ref, h2_ref, h3_ref, w_own_ref, w_other_ref, out_ref, line):
+def down_kernel(place_ref, h0_ref, h1_ref, h2_ref, h3_ref, w_own_ref, w_other_ref, out_ref, *scratch):
+    line, held, sems = scratch
     chip = place_ref[0]
-    depth, cols = h0_ref.shape[1], w_own_ref.shape[1]
+    depth = h0_ref.shape[1]
     chips = w_own_ref.shape[0] // depth
     parts = ((h0_ref, 0), (h1_ref, chips - 1), (h2_ref, 1), (h3_ref, chips // 2))
     for h_ref, shift in parts:
         at = pl.multiple_of(lax.rem(chip + shift, chips) * depth, depth)
         line[:, pl.ds(at, depth)] = h_ref[...]
+    copies = []
     for part, w_ref in enumerate((w_own_ref, w_other_ref)):
         total = dot(line[...], w_ref[...]).astype(bf16)
-        out_ref[:, part] = total.reshape(out_ref.shape[0], out_ref.shape[2], cols)
+        held[part] = total.reshape(held.shape[1:])
+        copies.append(
+            pltpu.make_async_copy(held.at[part], out_ref.at[:, part], sems.at[part])
+        )
+        copies[part].start()
+    for copy in copies:
+        copy.wait()
 
 
 def shared_kernel(place_ref, x_ref, *refs):
-    groups, outs, (line,) = (refs[:4], refs[4:8]), refs[8:13], refs[13:]
+    groups, outs, (line, sems) = (refs[:4], refs[4:8]), refs[8:13], refs[13:]
     gate_ref, up_ref, hid_ref, sd_ref, sd_out_ref = outs
     core, z, y = place_ref[1], place_ref[2], place_ref[3]
     hs = gate_ref.shape[1]
     side, size = groups[0][0].shape[0], line.shape[0] // 16
     deep = sd_ref.shape[0] // 16
-    for h, out_ref in ((0, gate_ref), (1, up_ref)):
+    for h in range(2):
         for m, ref in enumerate(groups[h]):
             for n in range(side):
                 dz, dy = (m, n) if h == 0 else (n, m)
                 source = lax.rem(z + side - dz, side) * side + lax.rem(y + side - dy, side)
                 block = ref[n, :size, :]
                 at = pl.ds(pl.multiple_of(source * size, size), size)
-                out_ref[at, :] = block
                 line[at, h * hs : (h + 1) * hs] = block
                 at = pl.ds(pl.multiple_of(source * deep, deep), deep)
                 for c in range(2):
@@ -170,9 +177,17 @@
     for c in range(4):
         at = pl.ds(pl.multiple_of((2 * c + 1 - core) * hs, hs), hs)
         sd_out_ref[c * hs : (c + 1) * hs, :] = sd_ref[at, :]
+    copies = [
+        pltpu.make_async_copy(line.at[:, pl.ds(h * hs, hs)], out_ref, sems.at[h])
+        for h, out_ref in enumerate((gate_ref, up_ref))
+    ]
+    for copy in copies:
+        copy.start()
     total = dot(x_ref[...], line[...])
     gate, up = total[:, :hs], total[:, hs:]
     hid_ref[...] = (gate / (1.0 + jnp.exp(-gate)) * up).astype(bf16)
+    for copy in copies:
+        copy.wait()
 
 
 def base_kernel(place_ref, own_ref, other_ref, sd_ref, out_ref, line):
@@ -384,7 +399,7 @@
             jax.ShapeDtypeStruct((2, mid, 4 * hs), f32),
             jax.ShapeDtypeStruct((2, mid, 128), f32),
         ],
-        compiler_params=vmem_limit(32),
+        compiler_params=vmem_limit(24),
         cost_estimate=cost(2 * rows * 3 * quarter * 4 * hs, 8 * width * hs),
     )(place, top, left_top, right_top, bottom, left_bottom, right_bottom, gu, gu_other, mark)
     hidden = pl.pallas_call(
@@ -397,7 +412,7 @@
             out_specs=whole((2, mid, 2 * hs)),
         ),
         out_shape=jax.ShapeDtypeStruct((2, mid, 2 * hs), bf16),
-        compiler_params=vmem_limit(32),
+        compiler_params=vmem_limit(24),
         cost_estimate=cost(2 * rows * quarter * 4 * hs, 8 * quarter * hs),
     )(place, far_top, far_bottom, acc, sq, gu, gu_other).reshape(rows, 2 * hs)
 
@@ -408,13 +423,16 @@
             grid=(1,),
             in_specs=[whole((tok_rows, width))] + [whole(groups[0][0].shape)] * 8,
             out_specs=[
-                whole((width, hs)),
-                whole((width, hs)),
+                pl.BlockSpec(memory_space=pltpu.HBM),
+                pl.BlockSpec(memory_space=pltpu.HBM),
                 whole((tok_rows, hs)),
                 whole((experts * deep, cols)),
                 whole((experts * deep // 2, cols)),
             ],
-            scratch_shapes=[pltpu.VMEM((width, 2 * hs), bf16)],
+            scratch_shapes=[
+                pltpu.VMEM((width, 2 * hs), bf16),
+                pltpu.SemaphoreType.DMA((2,)),
+            ],
         ),
         out_shape=[
             jax.ShapeDtypeStruct((width, hs), bf16),
@@ -423,7 +441,7 @@
             jax.ShapeDtypeStruct((experts * deep, cols), bf16),
             jax.ShapeDtypeStruct((experts * deep // 2, cols), bf16),
         ],
-        compiler_params=vmem_limit(36),
+        compiler_params=vmem_limit(60),
         cost_estimate=cost(4 * tok_rows * width * hs, 8 * width * hs),
     )(place, normed, *groups[0], *groups[1])
     shared_other = swap(shared_out)
@@ -442,11 +460,15 @@
             num_scalar_prefetch=1,
             grid=(1,),
             in_specs=[whole((rows, 2 * hs))] * 4 + [whole((experts * deep, cols))] * 2,
-            out_specs=whole((experts, 2, half, cols)),
-            scratch_shapes=[pltpu.VMEM((rows, experts * deep), bf16)],
+            out_specs=pl.BlockSpec(memory_space=pltpu.HBM),
+            scratch_shapes=[
+                pltpu.VMEM((rows, experts * deep), bf16),
+                pltpu.VMEM((2, experts, half, cols), bf16),
+                pltpu.SemaphoreType.DMA((2,)),
+            ],
         ),
         out_shape=jax.ShapeDtypeStruct((experts, 2, half, cols), bf16),
-        compiler_params=vmem_limit(40),
+        compiler_params=vmem_limit(60),
         cost_estimate=cost(4 * rows * experts * deep * cols, 8 * experts * deep * cols),
     )(place, hidden, hid_left, hid_right, hid_far, down_cols, down_other)
     returned = lax.all_to_all(sums, "fs", split_axis=0, concat_axis=0, tiled=True)
@@ -477,7 +499,7 @@
             ],
             out_specs=whole((tok_rows, cols)),
             out_shape=jax.ShapeDtypeStruct((tok_rows, cols), dtype),
-            compiler_params=vmem_limit(24),
+            compiler_params=vmem_limit(14),
             cost_estimate=cost(2 * tok_rows * rows * cols, 4 * tok_rows * rows),
         )(weights, got, base)
 
@@ -491,7 +513,7 @@
             scratch_shapes=[pltpu.VMEM((tok_rows, experts * deep), bf16)],
         ),
         out_shape=jax.ShapeDtypeStruct((tok_rows, cols), f32),
-        compiler_params=vmem_limit(24),
+        compiler_params=vmem_limit(14),
         cost_estimate=cost(2 * tok_rows * experts * deep * cols, 4 * tok_rows * rows),
     )(place, units, units_other, shared_cols)
     part = mix(mix_own, returned, base, f32)
@@ -507,7 +529,7 @@
             out_specs=[whole((2 * hs, 2 * cols))] * chips,
         ),
         out_shape=[jax.ShapeDtypeStruct((2 * hs, 2 * cols), bf16)] * chips,
-        compiler_params=vmem_limit(36),
+        compiler_params=vmem_limit(60),
         cost_estimate=cost(1 << 30, 8 * hs * width),
     )(place, down_cols, down_other, shared_cols, shared_other)
     pieces = [chunks[0]]
@@ -523,7 +545,7 @@
             scratch_shapes=[pltpu.SemaphoreType.DMA((4 * chips,))],
         ),
         out_shape=[jax.ShapeDtypeStruct((hs, width), bf16)] * 2,
-        compiler_params=vmem_limit(24),
+        compiler_params=vmem_limit(14),
         cost_estimate=cost(1 << 20, 8 * hs * width),
     )(place, *pieces)
     expert_gate = gu[None, :, :hs]

time: 270 us -> 269 us (level); the launches traced: 269 us -> 265 us
  waiting for transfers between devices: 144 us -> 137 us
  local copies, waits for them, and re-layouts: 15.5 us -> 11.2 us
  Pallas kernels: 41.8 us -> 46 us
    ppermute x12, waiting for transfers between devices: 39.4 us -> 33 us  [along(): return lax.ppermute(a, 'fs', pairs)]
    unnamed x58 -> x68, local copies, waits for them, and re-layouts: 11.5 us -> 7.23 us
  transfers between devices with their start and end apart: 36 -> 36, of which waited for: 16 -> 17; matrix products, arithmetic and copies ran while one was open for 5% -> 5% of each run, Pallas kernels for 13% -> 15%
where the time goes in v8:
time: 269 us; the launch traced here: 265 us
  waiting for transfers between devices  137 us (51%)
  starting transfers between devices  57.6 us (21%)
  Pallas kernels  46 us (17%)
  other arithmetic  11.8 us (4%)
  local copies, waits for them, and re-layouts  11.2 us (4%)
    ppermute x15, waiting for transfers between devices, shift_by(): return lax.ppermute(a, 'tp', [(i, (i + 2 * n) % tp) for i in range(tp)])  56.4 us
    ppermute x12, waiting for transfers between devices, along(): return lax.ppermute(a, 'fs', pairs)  33 us
    all_to_all x1, waiting for transfers between devices, on_device(): gu = lax.all_to_all(gu_local, 'fs', split_axis=0, concat_axis=0, tiled=True)  27.3 us
    ppermute x15, starting transfers between devices, shift_by(): return lax.ppermute(a, 'tp', [(i, (i + 2 * n) % tp) for i in range(tp)])  20.3 us
    all_to_all x1, waiting for transfers between devices, on_device(): lax.all_to_all(outgoing.reshape(experts, half, quarter), 'fs', split_axis...  20.1 us
    ppermute x12, starting transfers between devices, along(): return lax.ppermute(a, 'fs', pairs)  15.8 us
    all_to_all x1, starting transfers between devices, on_device(): lax.all_to_all(outgoing.reshape(experts, half, quarter), 'fs', split_axis...  8.17 us
    unnamed x68, local copies, waits for them, and re-layouts  7.23 us
  transfers between devices with their start and end apart: 36, of which 17 were waited for; matrix products, arithmetic and copies ran while one was open for 5% of the time, Pallas kernels for 15%

profile of v8, /device:TPU:0, one launch (start us, length us, event | category | flops | bytes accessed | tf_op | source)
XLA Modules:
  0.0 264.6 jit_solution(3237493234954342110)
XLA Ops:
  0.6 4.1 %shard_map.153 = (bf16[768,1024]{1,0:T(8,128)(2,1)}, s32[2,512]{1,0:T(2,128)}) custom-call(s32[2,512]{1,0:T(2,128)} %bitcast.75, bf16[512,4096]{1,0:T(8,128)(2,1)} %tok_ref.3), custom_call_target="tpu_custom_call" | custom-call | flops 805306368 | bytes 2097152 | tf_op jit(solution)/shard_map/pallas_call | solution.py:315
  4.7 8.2 %all-to-all-start = ((bf16[16,48,1024]{2,1,0:T(8,128)(2,1)}), bf16[16,48,1024]{2,1,0:T(8,128)(2,1)S(1)}, u32[]{:S(2)}, u32[]{:S(2)}) async-start(bf16[16,48,1024]{2,1,0:T(8,128)(2,1)} %bitcast.63), calls=%async_computation | async-start | bytes 3145728 | tf_op jit(solution)/shard_map/all_to_all | solution.py:347
  12.9 2.8 %multiply_convert_fusion.1 = (bf16[16,256,128]{2,1,0:T(8,128)(2,1)S(1)}, bf16[16,256,128]{2,1,0:T(8,128)(2,1)S(1)}) fusion(f32[16,256,128]{2,1,0:T(8,128)} %param.12, f32[256]{0:T(256)S(1)} %copy-done.29, f32[16,256,128]{2,1,0:T(8,128)} %param.13), kind=kLoop, calls=%fused_computation.2 | loop fusion | flops 2097152 | bytes 6292480 | tf_op jit(solution)/shard_map/convert_element_type | solution.py:352
  15.8 1.6 pad_maximum_fusion
  17.4 20.1 %all-to-all-done = bf16[16,48,1024]{2,1,0:T(8,128)(2,1)S(1)} async-done(((bf16[16,48,1024]{2,1,0:T(8,128)(2,1)}), bf16[16,48,1024]{2,1,0:T(8,128)(2,1)S(1)}, u32[]{:S(2)}, u32[]{:S(2)}) %all-to-all-start) | async-done | bytes 1572896 | tf_op jit(solution)/shard_map/all_to_all | solution.py:347
  37.5 1.3 fusion.8
  38.8 3.7 %all-to-all-start.1 = ((bf16[16,256,256]{2,1,0:T(8,128)(2,1)}), bf16[16,256,256]{2,1,0:T(8,128)(2,1)S(1)}, u32[]{:S(2)}, u32[]{:S(2)}) async-start(bf16[16,256,256]{2,1,0:T(8,128)(2,1)} %pad_maximum_fusion), calls=%async_computation.1 | async-start | bytes 4194304 | tf_op jit(solution)/shard_map/all_to_all | solution.py:358
  42.5 2.8 %convert_element_type.27 = bf16[16,64,512]{2,1,0:T(8,128)(2,1)} convert(f32[16,64,512]{2,1,0:T(8,128)} %param.14) | non-fusion elementwise | flops 524288 | bytes 3145728 | tf_op jit(solution)/shard_map/convert_element_type | solution.py:359
  45.3 27.3 %all-to-all-done.1 = bf16[16,256,256]{2,1,0:T(8,128)(2,1)S(1)} async-done(((bf16[16,256,256]{2,1,0:T(8,128)(2,1)}), bf16[16,256,256]{2,1,0:T(8,128)(2,1)S(1)}, u32[]{:S(2)}, u32[]{:S(2)}) %all-to-all-start.1) | async-done | bytes 2097184 | tf_op jit(solution)/shard_map/all_to_all | solution.py:358
  72.6 1.6 collective-permute-start.17
  74.3 1.8 collective-permute-start.19
  76.1 4.3 %all-to-all-start.2 = ((bf16[16,64,512]{2,1,0:T(8,128)(2,1)}), bf16[16,64,512]{2,1,0:T(8,128)(2,1)}, u32[]{:S(2)}, u32[]{:S(2)}) async-start(bf16[16,64,512]{2,1,0:T(8,128)(2,1)} %convert_element_type.27), calls=%async_computation.2 | async-start | bytes 2097152 | tf_op jit(solution)/shard_map/all_to_all | solution.py:360
  80.5 1.6 collective-permute-start.21
  82.1 1.8 collective-permute-start.7
  84.0 13.1 %collective-permute-done.7 = bf16[384,128]{1,0:T(8,128)(2,1)S(1)} collective-permute-done((bf16[384,128]{1,0:T(8,128)(2,1)S(1)}, bf16[384,128]{1,0:T(8,128)(2,1)S(1)}, u32[]{:S(2)}, u32[]{:S(2)}) %collective-permute-start.7) | collective-permute-done | bytes 98336 | tf_op jit(solution)/shard_map/ppermute | solution.py:291
  97.7 5.6 %collective-permute-done.8 = bf16[384,128]{1,0:T(8,128)(2,1)S(1)} collective-permute-done((bf16[384,128]{1,0:T(8,128)(2,1)S(1)}, bf16[384,128]{1,0:T(8,128)(2,1)S(1)}, u32[]{:S(2)}, u32[]{:S(2)}) %collective-permute-start.8) | collective-permute-done | bytes 98336 | tf_op jit(solution)/shard_map/ppermute | solution.py:291
  103.7 4.1 %collective-permute-done.9 = bf16[384,128]{1,0:T(8,128)(2,1)S(1)} collective-permute-done((bf16[384,128]{1,0:T(8,128)(2,1)S(1)}, bf16[384,128]{1,0:T(8,128)(2,1)S(1)}, u32[]{:S(2)}, u32[]{:S(2)}) %collective-permute-start.9) | collective-permute-done | bytes 98336 | tf_op jit(solution)/shard_map/ppermute | solution.py:291
  108.2 1.1 collective-permute-start.18
  109.3 2.1 collective-permute-start.20
  111.9 0.9 copy-done.13
  113.4 1.3 shard_map.159.b_ref
  114.8 1.0 pad_maximum_fusion.3.refs_4_
  115.8 1.3 shard_map.158.a_ref
  117.1 1.3 shard_map.160.refs_8_
  118.4 11.4 %collective-permute-done.22.refs_4_ = bf16[384,1024]{1,0:T(8,128)(2,1)} collective-permute-done((bf16[384,1024]{1,0:T(8,128)(2,1)}, bf16[384,1024]{1,0:T(8,128)(2,1)}, u32[]{:S(2)}, u32[]{:S(2)}) %collective-permute-start.22) | collective-permute-done | bytes 786464 | tf_op jit(solution)/shard_map/ppermute | solution.py:275
  129.8 2.1 collective-permute-start.1
  131.9 10.7 %collective-permute-done.18.far0_ref = bf16[384,1024]{1,0:T(8,128)(2,1)S(1)} collective-permute-done((bf16[384,1024]{1,0:T(8,128)(2,1)}, bf16[384,1024]{1,0:T(8,128)(2,1)S(1)}, u32[]{:S(2)}, u32[]{:S(2)}) %collective-permute-start.18) | collective-permute-done | bytes 786464 | tf_op jit(solution)/shard_map/ppermute | solution.py:275
  142.6 4.1 %collective-permute-start.2 = (bf16[384,128]{1,0:T(8,128)(2,1)}, bf16[384,128]{1,0:T(8,128)(2,1)S(1)}, u32[]{:S(2)}, u32[]{:S(2)}) collective-permute-start(bf16[384,128]{1,0:T(8,128)(2,1)} %get-tuple-element.64.a_ref), channel_id=1, source_target_pairs={{0,16},{8,24},{16,0},{24,8},{32,48},{40,56},{48,32},{56,40},{64,80... | collective-permute-start | bytes 294920 | tf_op jit(solution)/shard_map/ppermute | solution.py:291
  146.8 1.1 collective-permute-start.3
  148.5 1.1 copy-done.14
  149.7 7.0 %shard_map.161 = (f32[2,384,512]{2,1,0:T(8,128)S(1)}, f32[2,384,128]{2,1,0:T(8,128)S(1)}) custom-call(s32[4]{0:T(128)S(1)} %pad_add_fusion.place_ref, bf16[384,1024]{1,0:T(8,128)(2,1)} %bitcast.2.refs_0_, bf16[384,1024]{1,0:T(8,128)(2,1)} %collective-permute-done.17.a_ref.refs_1_, bf16[384,1024]{1,0:T(8,128)(2,1)S(1)} %copy-done.14, ...), custom_call_target="tpu_custom_call" | custom-call | flops 2415919104 | bytes 4194304 | tf_op jit(solution)/shard_map/pallas_call | solution.py:390
  156.6 1.0 collective-permute-start.10
  157.7 3.0 %shard_map.162 = bf16[2,384,256]{2,1,0:T(8,128)(2,1)S(1)} custom-call(s32[4]{0:T(128)S(1)} %pad_add_fusion.place_ref, bf16[384,1024]{1,0:T(8,128)(2,1)S(1)} %collective-permute-done.18.far0_ref, bf16[384,1024]{1,0:T(8,128)(2,1)} %collective-permute-done.20.far1_ref, f32[2,384,512]{2,1,0:T(8,128)S(1)} %get-tuple-element.51.acc_ref, ...), custom_call_target="tpu_custom_call" | custom-call | flops 805306368 | bytes 1048576 | tf_op jit(solution)/shard_map/pallas_call | solution.py:405
  160.9 3.2 %collective-permute-start.25 = (bf16[768,256]{1,0:T(8,128)(2,1)S(1)}, bf16[768,256]{1,0:T(8,128)(2,1)S(1)}, u32[]{:S(2)}, u32[]{:S(2)}) collective-permute-start(bf16[768,256]{1,0:T(8,128)(2,1)S(1)} %bitcast.60), channel_id=1, source_target_pairs={{0,6},{1,7},{2,0},{3,1},{4,2},{5,3},{6,4},{7,5},{8,14},{9,15},{10,... | collective-permute-start | bytes 1179656 | tf_op jit(solution)/shard_map/ppermute | solution.py:275
  164.2 5.7 %collective-permute-done.10.refs_5_ = bf16[4,384,128]{2,1,0:T(8,128)(2,1)S(1)} collective-permute-done((bf16[4,384,128]{2,1,0:T(8,128)(2,1)S(1)}, bf16[4,384,128]{2,1,0:T(8,128)(2,1)S(1)}, u32[]{:S(2)}, u32[]{:S(2)}) %collective-permute-start.10) | collective-permute-done | bytes 393248 | tf_op jit(solution)/shard_map/ppermute | solution.py:291
  170.0 7.6 %collective-permute-done.24.h1_ref = bf16[768,256]{1,0:T(8,128)(2,1)S(1)} collective-permute-done((bf16[768,256]{1,0:T(8,128)(2,1)S(1)}, bf16[768,256]{1,0:T(8,128)(2,1)S(1)}, u32[]{:S(2)}, u32[]{:S(2)}) %collective-permute-start.24) | collective-permute-done | bytes 393248 | tf_op jit(solution)/shard_map/ppermute | solution.py:275
  178.0 3.8 %collective-permute-start.5 = (bf16[4,384,128]{2,1,0:T(8,128)(2,1)S(1)}, bf16[4,384,128]{2,1,0:T(8,128)(2,1)}, u32[]{:S(2)}, u32[]{:S(2)}) collective-permute-start(bf16[4,384,128]{2,1,0:T(8,128)(2,1)S(1)} %pad_maximum_fusion.2.refs_0_), channel_id=1, source_target_pairs={{0,64},{8,72},{16,80},{24,88},{32,96},{40,104},{48,112},{56,120},{... | collective-permute-start | bytes 1179656 | tf_op jit(solution)/shard_map/ppermute | solution.py:291
  181.8 0.7 copy-done.33
  183.0 5.4 %shard_map.163 = bf16[16,2,48,512]{3,2,1,0:T(8,128)(2,1)} custom-call(s32[4]{0:T(128)} %copy-done.9, bf16[768,256]{1,0:T(8,128)(2,1)} %bitcast.62, bf16[768,256]{1,0:T(8,128)(2,1)} %copy-done.31, bf16[768,256]{1,0:T(8,128)(2,1)} %copy-done.32, bf16[768,256]{1,0:T(8,128)(2,1)} %copy-done.33, bf16[1024,512]{1,0:T(8,128)(2,1)} %bitcast.11.own_ref.w_own_ref, ...), custom_call_target="tpu_custom_call" | custom-call | flops 1610612736 | bytes 4194304 | tf_op jit(solution)/shard_map/pallas_call | solution.py:457
  188.4 4.4 %all-to-all-start.3 = ((bf16[16,2,48,512]{3,2,1,0:T(8,128)(2,1)}), bf16[16,2,48,512]{3,2,1,0:T(8,128)(2,1)}, u32[]{:S(2)}, u32[]{:S(2)}) async-start(bf16[16,2,48,512]{3,2,1,0:T(8,128)(2,1)} %shard_map.163), calls=%async_computation.3 | async-start | bytes 3145728 | tf_op jit(solution)/shard_map/all_to_all | solution.py:474
  192.9 3.8 %shard_map.154.x_ref = bf16[512,4096]{1,0:T(8,128)(2,1)} custom-call(bf16[512,4096]{1,0:T(8,128)(2,1)} %tok_ref.3), custom_call_target="tpu_custom_call" | custom-call | flops 33554432 | bytes 8388608 | tf_op jit(solution)/shard_map/pallas_call | solution.py:332
  196.8 2.3 collective-permute-done.5.refs_2_
  199.1 2.1 collective-permute-done.6.refs_3_
  201.2 6.8 %shard_map.155 = (bf16[4096,128]{1,0:T(8,128)(2,1)}, bf16[4096,128]{1,0:T(8,128)(2,1)}, bf16[512,128]{1,0:T(8,128)(2,1)}, bf16[1024,512]{1,0:T(8,128)(2,1)}, bf16[512,512]{1,0:T(8,128)(2,1)}) custom-call(s32[4]{0:T(128)} %copy-done.9, bf16[512,4096]{1,0:T(8,128)(2,1)} %shard_map.154.x_ref, bf16[4,384,128]{2,1,0:T(8,128)(2,1)} %copy-done.16, ...), custom_call_target="tpu_custom_call" | custom-call | flops 1073741824 | bytes 4194304 | tf_op jit(solution)/shard_map/pallas_call | solution.py:419
  208.4 2.9 %collective-permute-start.29 = (bf16[512,128]{1,0:T(8,128)(2,1)}, bf16[512,128]{1,0:T(8,128)(2,1)S(1)}, u32[]{:S(2)}, u32[]{:S(2)}) collective-permute-start(bf16[512,128]{1,0:T(8,128)(2,1)} %get-tuple-element.54), channel_id=1, source_target_pairs={{0,6},{1,7},{2,0},{3,1},{4,2},{5,3},{6,4},{7,5},{8,14},{9,15},{10,... | collective-permute-start | bytes 393224 | tf_op jit(solution)/shard_map/ppermute | solution.py:275
  211.4 1.2 collective-permute-start.30
  212.6 1.9 collective-permute-done.28
  214.5 3.5 %collective-permute-done.30 = bf16[512,128]{1,0:T(8,128)(2,1)S(1)} collective-permute-done((bf16[512,128]{1,0:T(8,128)(2,1)}, bf16[512,128]{1,0:T(8,128)(2,1)S(1)}, u32[]{:S(2)}, u32[]{:S(2)}) %collective-permute-start.30) | collective-permute-done | bytes 131104 | tf_op jit(solution)/shard_map/ppermute | solution.py:275
  218.0 1.0 pad_maximum_fusion.1.own_ref
  219.8 1.7 fusion.4
  221.5 0.8 copy-done.6
  222.3 1.0 copy-done.3
  223.3 1.0 copy-done.7
  224.4 1.5 shard_map.164.base_ref
  225.9 0.8 copy-done.30
  226.7 4.1 %shard_map.156 = (bf16[256,1024]{1,0:T(8,128)(2,1)}, bf16[256,1024]{1,0:T(8,128)(2,1)}, bf16[256,1024]{1,0:T(8,128)(2,1)}, bf16[256,1024]{1,0:T(8,128)(2,1)}) custom-call(s32[4]{0:T(128)} %copy-done.9, bf16[1024,512]{1,0:T(8,128)(2,1)} %bitcast.11.own_ref.w_own_ref, bf16[1024,512]{1,0:T(8,128)(2,1)} %collective-permute-done.other_ref.w_other_ref, ...), custom_call_target="tpu_custom_call" | custom-call | flops 1073741824 | bytes 4194304 | tf_op jit(solution)/shard_map/pallas_call | solution.py:522
  231.3 2.7 %collective-permute-start.15 = (bf16[256,1024]{1,0:T(8,128)(2,1)}, bf16[256,1024]{1,0:T(8,128)(2,1)}, u32[]{:S(2)}, u32[]{:S(2)}) collective-permute-start(bf16[256,1024]{1,0:T(8,128)(2,1)} %get-tuple-element.41), channel_id=1, source_target_pairs={{0,4},{1,5},{2,6},{3,7},{4,0},{5,1},{6,2},{7,3},{8,12},{9,13},{10,... | collective-permute-start | bytes 1572872 | tf_op jit(solution)/shard_map/ppermute | solution.py:275
  234.7 1.2 slice.86
  236.0 1.5 slice_bitcast_fusion
  237.4 9.7 %collective-permute-done.14.p1_ref = bf16[256,1024]{1,0:T(8,128)(2,1)} collective-permute-done((bf16[256,1024]{1,0:T(8,128)(2,1)}, bf16[256,1024]{1,0:T(8,128)(2,1)}, u32[]{:S(2)}, u32[]{:S(2)}) %collective-permute-start.14) | collective-permute-done | bytes 524320 | tf_op jit(solution)/shard_map/ppermute | solution.py:275
  247.2 10.3 %collective-permute-done.15.p2_ref = bf16[256,1024]{1,0:T(8,128)(2,1)} collective-permute-done((bf16[256,1024]{1,0:T(8,128)(2,1)}, bf16[256,1024]{1,0:T(8,128)(2,1)}, u32[]{:S(2)}, u32[]{:S(2)}) %collective-permute-start.15) | collective-permute-done | bytes 524320 | tf_op jit(solution)/shard_map/ppermute | solution.py:275
  258.1 3.3 %shard_map.157 = (bf16[128,4096]{1,0:T(8,128)(2,1)}, bf16[128,4096]{1,0:T(8,128)(2,1)}) custom-call(s32[4]{0:T(128)S(1)} %copy-done.11, bf16[256,1024]{1,0:T(8,128)(2,1)S(1)} %copy-done.5, bf16[256,1024]{1,0:T(8,128)(2,1)} %collective-permute-done.14.p1_ref, bf16[256,1024]{1,0:T(8,128)(2,1)} %collective-permute-done.15.p2_ref, ...), custom_call_target="tpu_custom_call" | custom-call | flops 1048576 | bytes 4194304 | tf_op jit(solution)/shard_map/pallas_call | solution.py:538
  261.4 1.8 shard_map.165.base_ref
  263.2 1.4 shard_map.166
  (109 shorter events, 7.6 us)
Async XLA Ops:
  4.7 8.2 %copy-start.29 = (f32[256]{0:T(256)S(1)}, f32[256]{0:T(256)}, u32[]{:S(2)}) copy-start(f32[256]{0:T(256)} %param.11) | copy-start | bytes 3076
  4.7 32.7 %all-to-all-start = ((bf16[16,48,1024]{2,1,0:T(8,128)(2,1)}), bf16[16,48,1024]{2,1,0:T(8,128)(2,1)S(1)}, u32[]{:S(2)}, u32[]{:S(2)}) async-start(bf16[16,48,1024]{2,1,0:T(8,128)(2,1)} %bitcast.63), calls=%async_computation | async-start | bytes 3145728 | tf_op jit(solution)/shard_map/all_to_all | solution.py:347
  38.8 33.9 %all-to-all-start.1 = ((bf16[16,256,256]{2,1,0:T(8,128)(2,1)}), bf16[16,256,256]{2,1,0:T(8,128)(2,1)S(1)}, u32[]{:S(2)}, u32[]{:S(2)}) async-start(bf16[16,256,256]{2,1,0:T(8,128)(2,1)} %pad_maximum_fusion), calls=%async_computation.1 | async-start | bytes 4194304 | tf_op jit(solution)/shard_map/all_to_all | solution.py:358
  42.5 30.1 %copy-start.22 = (f32[64,512]{1,0:T(8,128)S(1)}, f32[64,512]{1,0:T(8,128)}, u32[]{:S(2)}) copy-start(f32[64,512]{1,0:T(8,128)} %param.17) | copy-start | bytes 393220
  42.5 31.7 %copy-start.20 = (f32[256,128]{1,0:T(8,128)S(1)}, f32[256,128]{1,0:T(8,128)}, u32[]{:S(2)}) copy-start(f32[256,128]{1,0:T(8,128)} %param.16) | copy-start | bytes 393220
  42.5 31.7 %copy-start.21 = (f32[256,128]{1,0:T(8,128)S(1)}, f32[256,128]{1,0:T(8,128)}, u32[]{:S(2)}) copy-start(f32[256,128]{1,0:T(8,128)} %param.15) | copy-start | bytes 393220
  72.6 74.2 %collective-permute-start.23 = (bf16[4096,256]{1,0:T(8,128)(2,1)S(1)}, bf16[4096,256]{1,0:T(8,128)(2,1)}, u32[]{:S(2)}, u32[]{:S(2)}) collective-permute-start(bf16[4096,256]{1,0:T(8,128)(2,1)S(1)} %bitcast.55), channel_id=1, source_target_pairs={{0,1},{1,0},{2,3},{3,2},{4,5},{5,4},{6,7},{7,6},{8,9},{9,8},{10,11... | collective-permute-start | bytes 6291464 | tf_op jit(solution)/shard_map/ppermute | solution.py:278
  72.6 35.5 %collective-permute-start.17 = (bf16[384,1024]{1,0:T(8,128)(2,1)}, bf16[384,1024]{1,0:T(8,128)(2,1)}, u32[]{:S(2)}, u32[]{:S(2)}) collective-permute-start(bf16[384,1024]{1,0:T(8,128)(2,1)} %bitcast.2.refs_0_), channel_id=1, source_target_pairs={{0,2},{1,3},{2,4},{3,5},{4,6},{5,7},{6,0},{7,1},{8,10},{9,11},{10,... | collective-permute-start | bytes 2359304 | tf_op jit(solution)/shard_map/ppermute | solution.py:275
  74.3 35.0 %collective-permute-start.19 = (bf16[384,1024]{1,0:T(8,128)(2,1)}, bf16[384,1024]{1,0:T(8,128)(2,1)}, u32[]{:S(2)}, u32[]{:S(2)}) collective-permute-start(bf16[384,1024]{1,0:T(8,128)(2,1)} %bitcast.3.refs_3_), channel_id=1, source_target_pairs={{0,6},{1,7},{2,0},{3,1},{4,2},{5,3},{6,4},{7,5},{8,14},{9,15},{10,... | collective-permute-start | bytes 2359304 | tf_op jit(solution)/shard_map/ppermute | solution.py:275
  76.1 36.6 %all-to-all-start.2 = ((bf16[16,64,512]{2,1,0:T(8,128)(2,1)}), bf16[16,64,512]{2,1,0:T(8,128)(2,1)}, u32[]{:S(2)}, u32[]{:S(2)}) async-start(bf16[16,64,512]{2,1,0:T(8,128)(2,1)} %convert_element_type.27), calls=%async_computation.2 | async-start | bytes 2097152 | tf_op jit(solution)/shard_map/all_to_all | solution.py:360
  80.5 31.4 %collective-permute-start.21 = (bf16[384,1024]{1,0:T(8,128)(2,1)}, bf16[384,1024]{1,0:T(8,128)(2,1)S(1)}, u32[]{:S(2)}, u32[]{:S(2)}) collective-permute-start(bf16[384,1024]{1,0:T(8,128)(2,1)} %bitcast.2.refs_0_), channel_id=1, source_target_pairs={{0,6},{1,7},{2,0},{3,1},{4,2},{5,3},{6,4},{7,5},{8,14},{9,15},{10,... | collective-permute-start | bytes 2359304 | tf_op jit(solution)/shard_map/ppermute | solution.py:275
  82.1 31.3 %copy-start.17 = (bf16[384,128]{1,0:T(8,128)(2,1)}, bf16[384,128]{1,0:T(8,128)(2,1)S(1)}, u32[]{:S(2)}) copy-start(bf16[384,128]{1,0:T(8,128)(2,1)S(1)} %get-tuple-element.62.b_ref) | copy-start | bytes 294916
  82.1 15.0 %collective-permute-start.7 = (bf16[384,128]{1,0:T(8,128)(2,1)S(1)}, bf16[384,128]{1,0:T(8,128)(2,1)S(1)}, u32[]{:S(2)}, u32[]{:S(2)}) collective-permute-start(bf16[384,128]{1,0:T(8,128)(2,1)S(1)} %get-tuple-element.62.b_ref), channel_id=1, source_target_pairs={{0,32},{8,40},{16,48},{24,56},{32,64},{40,72},{48,80},{56,88},{64,... | collective-permute-start | bytes 294920 | tf_op jit(solution)/shard_map/ppermute | solution.py:291
  97.1 17.6 %copy-start.23 = (bf16[384,128]{1,0:T(8,128)(2,1)}, bf16[384,128]{1,0:T(8,128)(2,1)S(1)}, u32[]{:S(2)}) copy-start(bf16[384,128]{1,0:T(8,128)(2,1)S(1)} %collective-permute-done.7) | copy-start | bytes 294916
  97.1 6.1 %collective-permute-start.8 = (bf16[384,128]{1,0:T(8,128)(2,1)S(1)}, bf16[384,128]{1,0:T(8,128)(2,1)S(1)}, u32[]{:S(2)}, u32[]{:S(2)}) collective-permute-start(bf16[384,128]{1,0:T(8,128)(2,1)S(1)} %get-tuple-element.62.b_ref), channel_id=1, source_target_pairs={{0,64},{8,72},{16,80},{24,88},{32,96},{40,104},{48,112},{56,120},{... | collective-permute-start | bytes 294920 | tf_op jit(solution)/shard_map/ppermute | solution.py:291
  103.2 11.5 %copy-start.24 = (bf16[384,128]{1,0:T(8,128)(2,1)}, bf16[384,128]{1,0:T(8,128)(2,1)S(1)}, u32[]{:S(2)}) copy-start(bf16[384,128]{1,0:T(8,128)(2,1)S(1)} %collective-permute-done.8) | copy-start | bytes 294916
  103.2 4.6 %collective-permute-start.9 = (bf16[384,128]{1,0:T(8,128)(2,1)S(1)}, bf16[384,128]{1,0:T(8,128)(2,1)S(1)}, u32[]{:S(2)}, u32[]{:S(2)}) collective-permute-start(bf16[384,128]{1,0:T(8,128)(2,1)S(1)} %get-tuple-element.62.b_ref), channel_id=1, source_target_pairs={{0,96},{8,104},{16,112},{24,120},{32,0},{40,8},{48,16},{56,24},{64... | collective-permute-start | bytes 294920 | tf_op jit(solution)/shard_map/ppermute | solution.py:291
  107.9 1.4 copy-start.25
  107.9 21.9 %collective-permute-start.22 = (bf16[384,1024]{1,0:T(8,128)(2,1)}, bf16[384,1024]{1,0:T(8,128)(2,1)}, u32[]{:S(2)}, u32[]{:S(2)}) collective-permute-start(bf16[384,1024]{1,0:T(8,128)(2,1)} %bitcast.3.refs_3_), channel_id=1, source_target_pairs={{0,2},{1,3},{2,4},{3,5},{4,6},{5,7},{6,0},{7,1},{8,10},{9,11},{10,... | collective-permute-start | bytes 2359304 | tf_op jit(solution)/shard_map/ppermute | solution.py:275
  108.2 34.5 %collective-permute-start.18 = (bf16[384,1024]{1,0:T(8,128)(2,1)}, bf16[384,1024]{1,0:T(8,128)(2,1)S(1)}, u32[]{:S(2)}, u32[]{:S(2)}) collective-permute-start(bf16[384,1024]{1,0:T(8,128)(2,1)} %collective-permute-done.17.a_ref.refs_1_), channel_id=1, source_target_pairs={{0,2},{1,3},{2,4},{3,5},{4,6},{5,7},{6,0},{7,1},{8,10},{9,11},{10,... | collective-permute-start | bytes 2359304 | tf_op jit(solution)/shard_map/ppermute | solution.py:275
  109.3 47.3 %collective-permute-start.20 = (bf16[384,1024]{1,0:T(8,128)(2,1)}, bf16[384,1024]{1,0:T(8,128)(2,1)}, u32[]{:S(2)}, u32[]{:S(2)}) collective-permute-start(bf16[384,1024]{1,0:T(8,128)(2,1)} %collective-permute-done.19.b_ref.refs_5_), channel_id=1, source_target_pairs={{0,6},{1,7},{2,0},{3,1},{4,2},{5,3},{6,4},{7,5},{8,14},{9,15},{10,... | collective-permute-start | bytes 2359304 | tf_op jit(solution)/shard_map/ppermute | solution.py:275
  112.8 57.2 %collective-permute-start = (bf16[1024,512]{1,0:T(8,128)(2,1)}, bf16[1024,512]{1,0:T(8,128)(2,1)}, u32[]{:S(2)}, u32[]{:S(2)}) collective-permute-start(bf16[1024,512]{1,0:T(8,128)(2,1)} %bitcast.11.own_ref.w_own_ref), channel_id=1, source_target_pairs={{0,1},{1,0},{2,3},{3,2},{4,5},{5,4},{6,7},{7,6},{8,9},{9,8},{10,11... | collective-permute-start | bytes 3145736 | tf_op jit(solution)/shard_map/ppermute | solution.py:278
  114.8 42.9 %copy-start.9 = (s32[4]{0:T(128)}, s32[4]{0:T(128)S(1)}, u32[]{:S(2)}) copy-start(s32[4]{0:T(128)S(1)} %pad_add_fusion.place_ref) | copy-start | bytes 52
  115.8 54.1 %copy-start.15 = (bf16[4,384,128]{2,1,0:T(8,128)(2,1)}, bf16[4,384,128]{2,1,0:T(8,128)(2,1)S(1)}, u32[]{:S(2)}) copy-start(bf16[4,384,128]{2,1,0:T(8,128)(2,1)S(1)} %pad_maximum_fusion.3.refs_4_) | copy-start | bytes 1179652
  129.8 30.9 %collective-permute-start.1 = (bf16[384,128]{1,0:T(8,128)(2,1)}, bf16[384,128]{1,0:T(8,128)(2,1)S(1)}, u32[]{:S(2)}, u32[]{:S(2)}) collective-permute-start(bf16[384,128]{1,0:T(8,128)(2,1)} %get-tuple-element.64.a_ref), channel_id=1, source_target_pairs={{0,8},{8,16},{16,24},{24,0},{32,40},{40,48},{48,56},{56,32},{64,72... | collective-permute-start | bytes 294920 | tf_op jit(solution)/shard_map/ppermute | solution.py:291
  142.6 18.3 %collective-permute-start.2 = (bf16[384,128]{1,0:T(8,128)(2,1)}, bf16[384,128]{1,0:T(8,128)(2,1)S(1)}, u32[]{:S(2)}, u32[]{:S(2)}) collective-permute-start(bf16[384,128]{1,0:T(8,128)(2,1)} %get-tuple-element.64.a_ref), channel_id=1, source_target_pairs={{0,16},{8,24},{16,0},{24,8},{32,48},{40,56},{48,32},{56,40},{64,80... | collective-permute-start | bytes 294920 | tf_op jit(solution)/shard_map/ppermute | solution.py:291
  146.8 17.4 %collective-permute-start.3 = (bf16[384,128]{1,0:T(8,128)(2,1)}, bf16[384,128]{1,0:T(8,128)(2,1)S(1)}, u32[]{:S(2)}, u32[]{:S(2)}) collective-permute-start(bf16[384,128]{1,0:T(8,128)(2,1)} %get-tuple-element.64.a_ref), channel_id=1, source_target_pairs={{0,24},{8,0},{16,8},{24,16},{32,56},{40,32},{48,40},{56,48},{64,88... | collective-permute-start | bytes 294920 | tf_op jit(solution)/shard_map/ppermute | solution.py:291
  148.5 1.1 copy-start.14
  156.6 13.3 %collective-permute-start.10 = (bf16[4,384,128]{2,1,0:T(8,128)(2,1)S(1)}, bf16[4,384,128]{2,1,0:T(8,128)(2,1)S(1)}, u32[]{:S(2)}, u32[]{:S(2)}) collective-permute-start(bf16[4,384,128]{2,1,0:T(8,128)(2,1)S(1)} %pad_maximum_fusion.3.refs_4_), channel_id=1, source_target_pairs={{0,8},{8,16},{16,24},{24,0},{32,40},{40,48},{48,56},{56,32},{64,72... | collective-permute-start | bytes 1179656 | tf_op jit(solution)/shard_map/ppermute | solution.py:291
  160.6 22.4 %copy-start.8 = (bf16[2,384,256]{2,1,0:T(8,128)(2,1)}, bf16[2,384,256]{2,1,0:T(8,128)(2,1)S(1)}, u32[]{:S(2)}) copy-start(bf16[2,384,256]{2,1,0:T(8,128)(2,1)S(1)} %shard_map.162) | copy-start | bytes 1179652
  160.7 17.0 %collective-permute-start.24 = (bf16[768,256]{1,0:T(8,128)(2,1)S(1)}, bf16[768,256]{1,0:T(8,128)(2,1)S(1)}, u32[]{:S(2)}, u32[]{:S(2)}) collective-permute-start(bf16[768,256]{1,0:T(8,128)(2,1)S(1)} %bitcast.59), channel_id=1, source_target_pairs={{0,2},{1,3},{2,4},{3,5},{4,6},{5,7},{6,0},{7,1},{8,10},{9,11},{10,... | collective-permute-start | bytes 1179656 | tf_op jit(solution)/shard_map/ppermute | solution.py:275
  160.9 17.0 %collective-permute-start.25 = (bf16[768,256]{1,0:T(8,128)(2,1)S(1)}, bf16[768,256]{1,0:T(8,128)(2,1)S(1)}, u32[]{:S(2)}, u32[]{:S(2)}) collective-permute-start(bf16[768,256]{1,0:T(8,128)(2,1)S(1)} %bitcast.60), channel_id=1, source_target_pairs={{0,6},{1,7},{2,0},{3,1},{4,2},{5,3},{6,4},{7,5},{8,14},{9,15},{10,... | collective-permute-start | bytes 1179656 | tf_op jit(solution)/shard_map/ppermute | solution.py:275
  164.2 17.6 %collective-permute-start.26 = (bf16[768,256]{1,0:T(8,128)(2,1)S(1)}, bf16[768,256]{1,0:T(8,128)(2,1)S(1)}, u32[]{:S(2)}, u32[]{:S(2)}) collective-permute-start(bf16[768,256]{1,0:T(8,128)(2,1)S(1)} %bitcast.61), channel_id=1, source_target_pairs={{0,4},{1,5},{2,6},{3,7},{4,0},{5,1},{6,2},{7,3},{8,12},{9,13},{10,... | collective-permute-start | bytes 1179656 | tf_op jit(solution)/shard_map/ppermute | solution.py:275
  164.2 24.2 %copy-start.16 = (bf16[4,384,128]{2,1,0:T(8,128)(2,1)}, bf16[4,384,128]{2,1,0:T(8,128)(2,1)S(1)}, u32[]{:S(2)}) copy-start(bf16[4,384,128]{2,1,0:T(8,128)(2,1)S(1)} %pad_maximum_fusion.2.refs_0_) | copy-start | bytes 1179652
  169.9 11.8 %copy-start.18 = (bf16[4,384,128]{2,1,0:T(8,128)(2,1)}, bf16[4,384,128]{2,1,0:T(8,128)(2,1)S(1)}, u32[]{:S(2)}) copy-start(bf16[4,384,128]{2,1,0:T(8,128)(2,1)S(1)} %collective-permute-done.10.refs_5_) | copy-start | bytes 1179652
  169.9 26.9 %collective-permute-start.11 = (bf16[4,384,128]{2,1,0:T(8,128)(2,1)S(1)}, bf16[4,384,128]{2,1,0:T(8,128)(2,1)S(1)}, u32[]{:S(2)}, u32[]{:S(2)}) collective-permute-start(bf16[4,384,128]{2,1,0:T(8,128)(2,1)S(1)} %pad_maximum_fusion.3.refs_4_), channel_id=1, source_target_pairs={{0,16},{8,24},{16,0},{24,8},{32,48},{40,56},{48,32},{56,40},{64,80... | collective-permute-start | bytes 1179656 | tf_op jit(solution)/shard_map/ppermute | solution.py:291
  169.9 26.9 %collective-permute-start.12 = (bf16[4,384,128]{2,1,0:T(8,128)(2,1)S(1)}, bf16[4,384,128]{2,1,0:T(8,128)(2,1)}, u32[]{:S(2)}, u32[]{:S(2)}) collective-permute-start(bf16[4,384,128]{2,1,0:T(8,128)(2,1)S(1)} %pad_maximum_fusion.3.refs_4_), channel_id=1, source_target_pairs={{0,24},{8,0},{16,8},{24,16},{32,56},{40,32},{48,40},{56,48},{64,88... | collective-permute-start | bytes 1179656 | tf_op jit(solution)/shard_map/ppermute | solution.py:291
  177.6 4.1 %copy-start.31 = (bf16[768,256]{1,0:T(8,128)(2,1)}, bf16[768,256]{1,0:T(8,128)(2,1)S(1)}, u32[]{:S(2)}) copy-start(bf16[768,256]{1,0:T(8,128)(2,1)S(1)} %collective-permute-done.24.h1_ref) | copy-start | bytes 1179652
  177.7 19.2 %collective-permute-start.4 = (bf16[4,384,128]{2,1,0:T(8,128)(2,1)S(1)}, bf16[4,384,128]{2,1,0:T(8,128)(2,1)}, u32[]{:S(2)}, u32[]{:S(2)}) collective-permute-start(bf16[4,384,128]{2,1,0:T(8,128)(2,1)S(1)} %pad_maximum_fusion.2.refs_0_), channel_id=1, source_target_pairs={{0,32},{8,40},{16,48},{24,56},{32,64},{40,72},{48,80},{56,88},{64,... | collective-permute-start | bytes 1179656 | tf_op jit(solution)/shard_map/ppermute | solution.py:291
  178.0 3.8 %copy-start.32 = (bf16[768,256]{1,0:T(8,128)(2,1)}, bf16[768,256]{1,0:T(8,128)(2,1)S(1)}, u32[]{:S(2)}) copy-start(bf16[768,256]{1,0:T(8,128)(2,1)S(1)} %collective-permute-done.25.h2_ref) | copy-start | bytes 1179652
  178.0 21.2 %collective-permute-start.5 = (bf16[4,384,128]{2,1,0:T(8,128)(2,1)S(1)}, bf16[4,384,128]{2,1,0:T(8,128)(2,1)}, u32[]{:S(2)}, u32[]{:S(2)}) collective-permute-start(bf16[4,384,128]{2,1,0:T(8,128)(2,1)S(1)} %pad_maximum_fusion.2.refs_0_), channel_id=1, source_target_pairs={{0,64},{8,72},{16,80},{24,88},{32,96},{40,104},{48,112},{56,120},{... | collective-permute-start | bytes 1179656 | tf_op jit(solution)/shard_map/ppermute | solution.py:291
  182.5 18.7 %collective-permute-start.6 = (bf16[4,384,128]{2,1,0:T(8,128)(2,1)S(1)}, bf16[4,384,128]{2,1,0:T(8,128)(2,1)}, u32[]{:S(2)}, u32[]{:S(2)}) collective-permute-start(bf16[4,384,128]{2,1,0:T(8,128)(2,1)S(1)} %pad_maximum_fusion.2.refs_0_), channel_id=1, source_target_pairs={{0,96},{8,104},{16,112},{24,120},{32,0},{40,8},{48,16},{56,24},{64... | collective-permute-start | bytes 1179656 | tf_op jit(solution)/shard_map/ppermute | solution.py:291
  188.4 46.2 %all-to-all-start.3 = ((bf16[16,2,48,512]{3,2,1,0:T(8,128)(2,1)}), bf16[16,2,48,512]{3,2,1,0:T(8,128)(2,1)}, u32[]{:S(2)}, u32[]{:S(2)}) async-start(bf16[16,2,48,512]{3,2,1,0:T(8,128)(2,1)} %shard_map.163), calls=%async_computation.3 | async-start | bytes 3145728 | tf_op jit(solution)/shard_map/all_to_all | solution.py:474
  196.7 15.8 %copy-start.28 = (f32[512,2]{0,1:T(2,128)S(1)}, f32[512,2]{0,1:T(2,128)}, u32[]{:S(2)}) copy-start(f32[512,2]{0,1:T(2,128)} %param.19) | copy-start | bytes 12292
  196.7 23.0 %copy-start.26 = (s32[512,2]{0,1:T(2,128)S(1)}, s32[512,2]{0,1:T(2,128)}, u32[]{:S(2)}) copy-start(s32[512,2]{0,1:T(2,128)} %param.18) | copy-start | bytes 12292
  196.8 23.0 %copy-start.27 = (s32[2,512]{1,0:T(2,128)S(1)}, s32[2,512]{1,0:T(2,128)}, u32[]{:S(2)}) copy-start(s32[2,512]{1,0:T(2,128)} %get-tuple-element.47) | copy-start | bytes 12292
  196.8 4.5 %copy-start.19 = (bf16[4,384,128]{2,1,0:T(8,128)(2,1)}, bf16[4,384,128]{2,1,0:T(8,128)(2,1)S(1)}, u32[]{:S(2)}) copy-start(bf16[4,384,128]{2,1,0:T(8,128)(2,1)S(1)} %collective-permute-done.11.refs_6_) | copy-start | bytes 1179652
  208.0 14.2 %copy-start.10 = (s32[4]{0:T(128)S(1)}, s32[4]{0:T(128)}, u32[]{:S(2)}) copy-start(s32[4]{0:T(128)} %copy-done.9) | copy-start | bytes 52
  208.1 6.5 %collective-permute-start.28 = (bf16[512,128]{1,0:T(8,128)(2,1)}, bf16[512,128]{1,0:T(8,128)(2,1)S(1)}, u32[]{:S(2)}, u32[]{:S(2)}) collective-permute-start(bf16[512,128]{1,0:T(8,128)(2,1)} %get-tuple-element.54), channel_id=1, source_target_pairs={{0,2},{1,3},{2,4},{3,5},{4,6},{5,7},{6,0},{7,1},{8,10},{9,11},{10,... | collective-permute-start | bytes 393224 | tf_op jit(solution)/shard_map/ppermute | solution.py:275
  208.4 6.1 %collective-permute-start.29 = (bf16[512,128]{1,0:T(8,128)(2,1)}, bf16[512,128]{1,0:T(8,128)(2,1)S(1)}, u32[]{:S(2)}, u32[]{:S(2)}) collective-permute-start(bf16[512,128]{1,0:T(8,128)(2,1)} %get-tuple-element.54), channel_id=1, source_target_pairs={{0,6},{1,7},{2,0},{3,1},{4,2},{5,3},{6,4},{7,5},{8,14},{9,15},{10,... | collective-permute-start | bytes 393224 | tf_op jit(solution)/shard_map/ppermute | solution.py:275
  211.4 6.7 %collective-permute-start.30 = (bf16[512,128]{1,0:T(8,128)(2,1)}, bf16[512,128]{1,0:T(8,128)(2,1)S(1)}, u32[]{:S(2)}, u32[]{:S(2)}) collective-permute-start(bf16[512,128]{1,0:T(8,128)(2,1)} %get-tuple-element.54), channel_id=1, source_target_pairs={{0,4},{1,5},{2,6},{3,7},{4,0},{5,1},{6,2},{7,3},{8,12},{9,13},{10,... | collective-permute-start | bytes 393224 | tf_op jit(solution)/shard_map/ppermute | solution.py:275
  219.0 2.5 copy-start.2
  219.0 2.5 collective-permute-start.31
  219.2 3.1 %copy-start.4 = (bf16[1024,512]{1,0:T(8,128)(2,1)S(1)}, bf16[1024,512]{1,0:T(8,128)(2,1)}, u32[]{:S(2)}) copy-start(bf16[1024,512]{1,0:T(8,128)(2,1)} %get-tuple-element.37.sd_ref) | copy-start | bytes 3145732
  219.2 6.7 %collective-permute-start.13 = (bf16[512,512]{1,0:T(8,128)(2,1)}, bf16[512,512]{1,0:T(8,128)(2,1)S(1)}, u32[]{:S(2)}, u32[]{:S(2)}) collective-permute-start(bf16[512,512]{1,0:T(8,128)(2,1)} %get-tuple-element.38), channel_id=1, source_target_pairs={{0,1},{1,0},{2,3},{3,2},{4,5},{5,4},{6,7},{7,6},{8,9},{9,8},{10,11... | collective-permute-start | bytes 1572872 | tf_op jit(solution)/shard_map/ppermute | solution.py:278
  222.3 1.0 copy-start.3
  230.8 16.3 %collective-permute-start.14 = (bf16[256,1024]{1,0:T(8,128)(2,1)}, bf16[256,1024]{1,0:T(8,128)(2,1)}, u32[]{:S(2)}, u32[]{:S(2)}) collective-permute-start(bf16[256,1024]{1,0:T(8,128)(2,1)} %get-tuple-element.40), channel_id=1, source_target_pairs={{0,2},{1,3},{2,4},{3,5},{4,6},{5,7},{6,0},{7,1},{8,10},{9,11},{10,... | collective-permute-start | bytes 1572872 | tf_op jit(solution)/shard_map/ppermute | solution.py:275
  231.3 26.1 %collective-permute-start.15 = (bf16[256,1024]{1,0:T(8,128)(2,1)}, bf16[256,1024]{1,0:T(8,128)(2,1)}, u32[]{:S(2)}, u32[]{:S(2)}) collective-permute-start(bf16[256,1024]{1,0:T(8,128)(2,1)} %get-tuple-element.41), channel_id=1, source_target_pairs={{0,4},{1,5},{2,6},{3,7},{4,0},{5,1},{6,2},{7,3},{8,12},{9,13},{10,... | collective-permute-start | bytes 1572872 | tf_op jit(solution)/shard_map/ppermute | solution.py:275
  234.1 24.0 %collective-permute-start.16 = (bf16[256,1024]{1,0:T(8,128)(2,1)}, bf16[256,1024]{1,0:T(8,128)(2,1)}, u32[]{:S(2)}, u32[]{:S(2)}) collective-permute-start(bf16[256,1024]{1,0:T(8,128)(2,1)} %get-tuple-element.42), channel_id=1, source_target_pairs={{0,6},{1,7},{2,0},{3,1},{4,2},{5,3},{6,4},{7,5},{8,14},{9,15},{10,... | collective-permute-start | bytes 1572872 | tf_op jit(solution)/shard_map/ppermute | solution.py:275
  235.9 22.2 %copy-start.5 = (bf16[256,1024]{1,0:T(8,128)(2,1)S(1)}, bf16[256,1024]{1,0:T(8,128)(2,1)}, u32[]{:S(2)}) copy-start(bf16[256,1024]{1,0:T(8,128)(2,1)} %get-tuple-element.39.p0_ref) | copy-start | bytes 1572868
  235.9 22.2 %copy-start.11 = (s32[4]{0:T(128)S(1)}, s32[4]{0:T(128)}, u32[]{:S(2)}) copy-start(s32[4]{0:T(128)} %copy-done.9) | copy-start | bytes 52
  235.9 27.4 %collective-permute-start.27 = (bf16[768,512]{1,0:T(8,128)(2,1)S(1)}, bf16[768,512]{1,0:T(8,128)(2,1)S(1)}, u32[]{:S(2)}, u32[]{:S(2)}) collective-permute-start(bf16[768,512]{1,0:T(8,128)(2,1)S(1)} %bitcast.64), channel_id=1, source_target_pairs={{0,1},{1,0},{2,3},{3,2},{4,5},{5,4},{6,7},{7,6},{8,9},{9,8},{10,11... | collective-permute-start | bytes 2359304 | tf_op jit(solution)/shard_map/ppermute | solution.py:278
  237.4 24.0 %copy-start.1 = (bf16[512,768]{1,0:T(8,128)(2,1)S(1)}, bf16[512,768]{1,0:T(8,128)(2,1)}, u32[]{:S(2)}) copy-start(bf16[512,768]{1,0:T(8,128)(2,1)} %get-tuple-element.53.weight_ref) | copy-start | bytes 2359300
  261.4 1.8 copy-start
  (6 other events, 4.9 us)

commit v9 on v8

--- a/solution.py
+++ b/solution.py
@@ -98,12 +98,13 @@
     return total
 
 
-def mark_kernel(a_ref, b_ref, out_ref):
-    out_ref[...] = a_ref[...] + b_ref[...]
+def square_kernel(a_ref, b_ref, c_ref, d_ref, sq_ref):
+    sq_ref[0] = squares(a_ref) + squares(b_ref)
+    sq_ref[1] = squares(c_ref) + squares(d_ref)
 
 
 def first_kernel(place_ref, *refs):
-    x_refs, (w_own_ref, w_other_ref, _, acc_ref, sq_ref) = refs[:6], refs[6:]
+    x_refs, (w_own_ref, w_other_ref, some_ref, acc_ref, sq_ref) = refs[:6], refs[6:]
     chip = place_ref[0]
     quarter, wide = x_refs[0].shape[1], w_own_ref.shape[1]
     chips = w_own_ref.shape[0] // quarter
@@ -116,7 +117,7 @@
                 term = dot(x_ref[...], w_ref[pl.ds(at, quarter), :])
                 total = term if total is None else total + term
             acc_ref[part, :, half * wide : (half + 1) * wide] = total
-        sq_ref[part] = squares(blocks[0]) + squares(blocks[1]) + squares(blocks[2])
+        sq_ref[part] = some_ref[part] + squares(blocks[2 - part])
 
 
 def hidden_kernel(width, place_ref, far0_ref, far1_ref, acc_ref, sq_ref, w0_ref, w1_ref, out_ref):
@@ -356,7 +357,8 @@
     top, bottom = together(arriving[:mid], arriving[mid:])
     gu_local, top, bottom = together(gu_local, top, bottom)
     gu = lax.all_to_all(gu_local, "fs", split_axis=0, concat_axis=0, tiled=True)
-    down_local, gu = together(down_train.astype(bf16), gu)
+    down_local = down_train.astype(bf16)
+    down_local, gu = together(down_local, gu)
     down_cols = lax.all_to_all(down_local, "fs", split_axis=0, concat_axis=0, tiled=True)
     gu = gu.reshape(width, 2 * hs)
     gu_other = swap(gu)
@@ -370,29 +372,25 @@
     far_top = shift_by(left_top, 1)
     far_bottom = shift_by(right_bottom, -1)
 
-    def marker(a, b):
-        return pl.pallas_call(
-            mark_kernel,
-            grid=(1,),
-            in_specs=[whole(tile)] * 2,
-            out_specs=whole(tile),
-            out_shape=jax.ShapeDtypeStruct(tile, bf16),
-            cost_estimate=cost(1 << 20, 1 << 14),
-        )(a, b)
-
-    tile = (16, 128)
-    mark = marker(left_top, right_bottom)
-    soon = marker(*packs)
-    mark = marker(mark, soon)
     x_spec = pl.BlockSpec((mid // 2, quarter), lambda i, s: (i, 0))
     acc_spec = pl.BlockSpec((2, mid // 2, 4 * hs), lambda i, s: (0, i, 0))
     w_spec = pl.BlockSpec((quarter, 2 * hs), lambda i, s: (lax.rem(s[0] + chips // 2, chips), 0))
+    sq_spec = pl.BlockSpec((2, mid // 2, 128), lambda i, *s: (0, i, 0))
+    some = pl.pallas_call(
+        square_kernel,
+        grid=(2,),
+        in_specs=[pl.BlockSpec((mid // 2, quarter), lambda i: (i, 0))] * 4,
+        out_specs=sq_spec,
+        out_shape=jax.ShapeDtypeStruct((2, mid, 128), f32),
+        compiler_params=vmem_limit(24),
+        cost_estimate=cost(4 * rows * width, rows * width),
+    )(top, left_top, bottom, right_bottom)
     acc, sq = pl.pallas_call(
         first_kernel,
         grid_spec=pltpu.PrefetchScalarGridSpec(
             num_scalar_prefetch=1,
             grid=(2,),
-            in_specs=[x_spec] * 6 + [whole((width, 2 * hs))] * 2 + [whole(tile)],
+            in_specs=[x_spec] * 6 + [whole((width, 2 * hs))] * 2 + [sq_spec],
             out_specs=[acc_spec, pl.BlockSpec((2, mid // 2, 128), lambda i, s: (0, i, 0))],
         ),
         out_shape=[
@@ -401,7 +399,7 @@
         ],
         compiler_params=vmem_limit(24),
         cost_estimate=cost(2 * rows * 3 * quarter * 4 * hs, 8 * width * hs),
-    )(place, top, left_top, right_top, bottom, left_bottom, right_bottom, gu, gu_other, mark)
+    )(place, top, left_top, right_top, bottom, left_bottom, right_bottom, gu, gu_other, some)
     hidden = pl.pallas_call(
         functools.partial(hidden_kernel, width),
         grid_spec=pltpu.PrefetchScalarGridSpec(

time: 269 us -> 267 us (level)
  starting transfers between devices: 57.6 us -> 61.4 us
  Pallas kernels: 46 us -> 43.3 us
    ppermute x15, starting transfers between devices: 20.3 us -> 24.2 us  [shift_by(): return lax.ppermute(a, 'tp', [(i, (i + 2 * n) % tp) for i in range(tp)])]
    unnamed x68 -> x64, local copies, waits for them, and re-layouts: 7.23 us -> 6.53 us
  transfers between devices with their start and end apart: 36 -> 36, of which waited for: 17 -> 17; matrix products, arithmetic and copies ran while one was open for 5% -> 5% of each run, Pallas kernels for 15% -> 14%
where the time goes in v9:
time: 267 us; the launch traced here: 265 us
  waiting for transfers between devices  138 us (52%)
  starting transfers between devices  61.4 us (23%)
  Pallas kernels  43.3 us (16%)
  other arithmetic  11.2 us (4%)
  local copies, waits for them, and re-layouts  10.3 us (4%)
    ppermute x15, waiting for transfers between devices, shift_by(): return lax.ppermute(a, 'tp', [(i, (i + 2 * n) % tp) for i in range(tp)])  57.5 us
    ppermute x12, waiting for transfers between devices, along(): return lax.ppermute(a, 'fs', pairs)  32.8 us
    all_to_all x1, waiting for transfers between devices, on_device(): gu = lax.all_to_all(gu_local, 'fs', split_axis=0, concat_axis=0, tiled=True)  27.3 us
    ppermute x15, starting transfers between devices, shift_by(): return lax.ppermute(a, 'tp', [(i, (i + 2 * n) % tp) for i in range(tp)])  24.2 us
    all_to_all x1, waiting for transfers between devices, on_device(): lax.all_to_all(outgoing.reshape(experts, half, quarter), 'fs', split_axis...  20.1 us
    ppermute x12, starting transfers between devices, along(): return lax.ppermute(a, 'fs', pairs)  15.8 us
    all_to_all x1, starting transfers between devices, on_device(): lax.all_to_all(outgoing.reshape(experts, half, quarter), 'fs', split_axis...  8.17 us
    pallas_call x1, Pallas kernels, on_device(): pl.pallas_call(shared_kernel, grid_spec=pltpu.PrefetchScalarGridSpec(num_...  6.79 us
  transfers between devices with their start and end apart: 36, of which 17 were waited for; matrix products, arithmetic and copies ran while one was open for 5% of the time, Pallas kernels for 14%

profile of v9, /device:TPU:0, one launch (start us, length us, event | category | flops | bytes accessed | tf_op | source)
XLA Modules:
  0.0 265.0 jit_solution(10418808351951988981)
XLA Ops:
  0.6 4.1 %shard_map.153 = (bf16[768,1024]{1,0:T(8,128)(2,1)}, s32[2,512]{1,0:T(2,128)}) custom-call(s32[2,512]{1,0:T(2,128)} %bitcast.83, bf16[512,4096]{1,0:T(8,128)(2,1)} %tok_ref.3), custom_call_target="tpu_custom_call" | custom-call | flops 805306368 | bytes 2097152 | tf_op jit(solution)/shard_map/pallas_call | solution.py:316
  4.7 8.2 %all-to-all-start = ((bf16[16,48,1024]{2,1,0:T(8,128)(2,1)}), bf16[16,48,1024]{2,1,0:T(8,128)(2,1)S(1)}, u32[]{:S(2)}, u32[]{:S(2)}) async-start(bf16[16,48,1024]{2,1,0:T(8,128)(2,1)} %bitcast.71), calls=%async_computation | async-start | bytes 3145728 | tf_op jit(solution)/shard_map/all_to_all | solution.py:348
  12.9 2.8 %multiply_convert_fusion.1 = (bf16[16,256,128]{2,1,0:T(8,128)(2,1)S(1)}, bf16[16,256,128]{2,1,0:T(8,128)(2,1)S(1)}) fusion(f32[16,256,128]{2,1,0:T(8,128)} %param.12, f32[256]{0:T(256)S(1)} %copy-done.27, f32[16,256,128]{2,1,0:T(8,128)} %param.13), kind=kLoop, calls=%fused_computation.2 | loop fusion | flops 2097152 | bytes 6292480 | tf_op jit(solution)/shard_map/convert_element_type | solution.py:353
  15.8 1.6 pad_maximum_fusion
  17.4 20.1 %all-to-all-done = bf16[16,48,1024]{2,1,0:T(8,128)(2,1)S(1)} async-done(((bf16[16,48,1024]{2,1,0:T(8,128)(2,1)}), bf16[16,48,1024]{2,1,0:T(8,128)(2,1)S(1)}, u32[]{:S(2)}, u32[]{:S(2)}) %all-to-all-start) | async-done | bytes 1572896 | tf_op jit(solution)/shard_map/all_to_all | solution.py:348
  37.4 1.0 fusion.8
  38.5 3.7 %all-to-all-start.1 = ((bf16[16,256,256]{2,1,0:T(8,128)(2,1)}), bf16[16,256,256]{2,1,0:T(8,128)(2,1)S(1)}, u32[]{:S(2)}, u32[]{:S(2)}) async-start(bf16[16,256,256]{2,1,0:T(8,128)(2,1)} %pad_maximum_fusion), calls=%async_computation.1 | async-start | bytes 4194304 | tf_op jit(solution)/shard_map/all_to_all | solution.py:359
  42.3 2.8 %convert_element_type.27 = bf16[16,64,512]{2,1,0:T(8,128)(2,1)} convert(f32[16,64,512]{2,1,0:T(8,128)} %param.14) | non-fusion elementwise | flops 524288 | bytes 3145728 | tf_op jit(solution)/shard_map/convert_element_type | solution.py:360
  45.0 27.3 %all-to-all-done.1 = bf16[16,256,256]{2,1,0:T(8,128)(2,1)S(1)} async-done(((bf16[16,256,256]{2,1,0:T(8,128)(2,1)}), bf16[16,256,256]{2,1,0:T(8,128)(2,1)S(1)}, u32[]{:S(2)}, u32[]{:S(2)}) %all-to-all-start.1) | async-done | bytes 2097184 | tf_op jit(solution)/shard_map/all_to_all | solution.py:359
  72.4 1.6 collective-permute-start.17
  74.1 1.8 collective-permute-start.19
  75.9 4.3 %all-to-all-start.2 = ((bf16[16,64,512]{2,1,0:T(8,128)(2,1)}), bf16[16,64,512]{2,1,0:T(8,128)(2,1)}, u32[]{:S(2)}, u32[]{:S(2)}) async-start(bf16[16,64,512]{2,1,0:T(8,128)(2,1)} %convert_element_type.27), calls=%async_computation.2 | async-start | bytes 2097152 | tf_op jit(solution)/shard_map/all_to_all | solution.py:362
  80.2 1.6 collective-permute-start.21
  81.9 1.8 collective-permute-start.7
  83.7 13.2 %collective-permute-done.7 = bf16[384,128]{1,0:T(8,128)(2,1)S(1)} collective-permute-done((bf16[384,128]{1,0:T(8,128)(2,1)S(1)}, bf16[384,128]{1,0:T(8,128)(2,1)S(1)}, u32[]{:S(2)}, u32[]{:S(2)}) %collective-permute-start.7) | collective-permute-done | bytes 98336 | tf_op jit(solution)/shard_map/ppermute | solution.py:292
  97.4 5.6 %collective-permute-done.8 = bf16[384,128]{1,0:T(8,128)(2,1)S(1)} collective-permute-done((bf16[384,128]{1,0:T(8,128)(2,1)S(1)}, bf16[384,128]{1,0:T(8,128)(2,1)S(1)}, u32[]{:S(2)}, u32[]{:S(2)}) %collective-permute-start.8) | collective-permute-done | bytes 98336 | tf_op jit(solution)/shard_map/ppermute | solution.py:292
  103.5 4.1 %collective-permute-done.9 = bf16[384,128]{1,0:T(8,128)(2,1)S(1)} collective-permute-done((bf16[384,128]{1,0:T(8,128)(2,1)S(1)}, bf16[384,128]{1,0:T(8,128)(2,1)S(1)}, u32[]{:S(2)}, u32[]{:S(2)}) %collective-permute-start.9) | collective-permute-done | bytes 98336 | tf_op jit(solution)/shard_map/ppermute | solution.py:292
  107.9 1.1 collective-permute-start.18
  109.0 2.1 collective-permute-start.20
  111.4 0.9 copy-done.7
  112.4 1.1 pad_maximum_fusion.3.refs_4_
  113.5 1.1 copy-done
  114.6 1.9 shard_map.158.refs_8_
  116.6 12.8 %collective-permute-done.22.refs_4_ = bf16[384,1024]{1,0:T(8,128)(2,1)} collective-permute-done((bf16[384,1024]{1,0:T(8,128)(2,1)S(1)}, bf16[384,1024]{1,0:T(8,128)(2,1)}, u32[]{:S(2)}, u32[]{:S(2)}) %collective-permute-start.22) | collective-permute-done | bytes 786464 | tf_op jit(solution)/shard_map/ppermute | solution.py:276
  129.3 2.1 collective-permute-start.1
  131.5 10.8 %collective-permute-done.18.far0_ref = bf16[384,1024]{1,0:T(8,128)(2,1)} collective-permute-done((bf16[384,1024]{1,0:T(8,128)(2,1)}, bf16[384,1024]{1,0:T(8,128)(2,1)}, u32[]{:S(2)}, u32[]{:S(2)}) %collective-permute-start.18) | collective-permute-done | bytes 786464 | tf_op jit(solution)/shard_map/ppermute | solution.py:276
  142.3 4.1 %collective-permute-start.2 = (bf16[384,128]{1,0:T(8,128)(2,1)S(1)}, bf16[384,128]{1,0:T(8,128)(2,1)S(1)}, u32[]{:S(2)}, u32[]{:S(2)}) collective-permute-start(bf16[384,128]{1,0:T(8,128)(2,1)S(1)} %get-tuple-element.64), channel_id=1, source_target_pairs={{0,16},{8,24},{16,0},{24,8},{32,48},{40,56},{48,32},{56,40},{64,80... | collective-permute-start | bytes 294920 | tf_op jit(solution)/shard_map/ppermute | solution.py:292
  146.4 1.1 collective-permute-start.3
  147.5 5.8 %shard_map.159 = (f32[2,384,512]{2,1,0:T(8,128)S(1)}, f32[2,384,128]{2,1,0:T(8,128)S(1)}) custom-call(s32[4]{0:T(128)S(1)} %pad_add_fusion.place_ref, bf16[384,1024]{1,0:T(8,128)(2,1)S(1)} %bitcast.66, bf16[384,1024]{1,0:T(8,128)(2,1)} %collective-permute-done.17.b_ref.refs_1_, bf16[384,1024]{1,0:T(8,128)(2,1)S(1)} %copy-done.8, ...), custom_call_target="tpu_custom_call" | custom-call | flops 2415919104 | bytes 4194304 | tf_op jit(solution)/shard_map/pallas_call | solution.py:388
  153.3 1.0 collective-permute-start.10
  154.3 3.2 %shard_map.160 = bf16[2,384,256]{2,1,0:T(8,128)(2,1)S(1)} custom-call(s32[4]{0:T(128)S(1)} %pad_add_fusion.place_ref, bf16[384,1024]{1,0:T(8,128)(2,1)} %collective-permute-done.18.far0_ref, bf16[384,1024]{1,0:T(8,128)(2,1)} %collective-permute-done.20.far1_ref, f32[2,384,512]{2,1,0:T(8,128)S(1)} %get-tuple-element.51.acc_ref, ...), custom_call_target="tpu_custom_call" | custom-call | flops 805306368 | bytes 1048576 | tf_op jit(solution)/shard_map/pallas_call | solution.py:403
  157.8 3.2 %collective-permute-start.25 = (bf16[768,256]{1,0:T(8,128)(2,1)S(1)}, bf16[768,256]{1,0:T(8,128)(2,1)S(1)}, u32[]{:S(2)}, u32[]{:S(2)}) collective-permute-start(bf16[768,256]{1,0:T(8,128)(2,1)S(1)} %bitcast.68), channel_id=1, source_target_pairs={{0,6},{1,7},{2,0},{3,1},{4,2},{5,3},{6,4},{7,5},{8,14},{9,15},{10,... | collective-permute-start | bytes 1179656 | tf_op jit(solution)/shard_map/ppermute | solution.py:276
  161.1 5.5 %collective-permute-done.10.refs_5_ = bf16[4,384,128]{2,1,0:T(8,128)(2,1)S(1)} collective-permute-done((bf16[4,384,128]{2,1,0:T(8,128)(2,1)S(1)}, bf16[4,384,128]{2,1,0:T(8,128)(2,1)S(1)}, u32[]{:S(2)}, u32[]{:S(2)}) %collective-permute-start.10) | collective-permute-done | bytes 393248 | tf_op jit(solution)/shard_map/ppermute | solution.py:292
  166.7 7.9 %collective-permute-done.24.h1_ref = bf16[768,256]{1,0:T(8,128)(2,1)S(1)} collective-permute-done((bf16[768,256]{1,0:T(8,128)(2,1)S(1)}, bf16[768,256]{1,0:T(8,128)(2,1)S(1)}, u32[]{:S(2)}, u32[]{:S(2)}) %collective-permute-start.24) | collective-permute-done | bytes 393248 | tf_op jit(solution)/shard_map/ppermute | solution.py:276
  174.8 3.8 %collective-permute-start.5 = (bf16[4,384,128]{2,1,0:T(8,128)(2,1)S(1)}, bf16[4,384,128]{2,1,0:T(8,128)(2,1)}, u32[]{:S(2)}, u32[]{:S(2)}) collective-permute-start(bf16[4,384,128]{2,1,0:T(8,128)(2,1)S(1)} %pad_maximum_fusion.2.refs_0_), channel_id=1, source_target_pairs={{0,64},{8,72},{16,80},{24,88},{32,96},{40,104},{48,112},{56,120},{... | collective-permute-start | bytes 1179656 | tf_op jit(solution)/shard_map/ppermute | solution.py:292
  178.6 0.7 copy-done.31
  179.9 5.5 %shard_map.161 = bf16[16,2,48,512]{3,2,1,0:T(8,128)(2,1)} custom-call(s32[4]{0:T(128)} %copy-done.13, bf16[768,256]{1,0:T(8,128)(2,1)} %bitcast.70, bf16[768,256]{1,0:T(8,128)(2,1)} %copy-done.29, bf16[768,256]{1,0:T(8,128)(2,1)} %copy-done.30, bf16[768,256]{1,0:T(8,128)(2,1)} %copy-done.31, bf16[1024,512]{1,0:T(8,128)(2,1)} %bitcast.11.own_ref.w_own_ref, ...), custom_call_target="tpu_custom_call" | custom-call | flops 1610612736 | bytes 4194304 | tf_op jit(solution)/shard_map/pallas_call | solution.py:455
  185.4 4.4 %all-to-all-start.3 = ((bf16[16,2,48,512]{3,2,1,0:T(8,128)(2,1)}), bf16[16,2,48,512]{3,2,1,0:T(8,128)(2,1)}, u32[]{:S(2)}, u32[]{:S(2)}) async-start(bf16[16,2,48,512]{3,2,1,0:T(8,128)(2,1)} %shard_map.161), calls=%async_computation.3 | async-start | bytes 3145728 | tf_op jit(solution)/shard_map/all_to_all | solution.py:472
  189.8 3.9 %shard_map.154.x_ref = bf16[512,4096]{1,0:T(8,128)(2,1)} custom-call(bf16[512,4096]{1,0:T(8,128)(2,1)} %tok_ref.3), custom_call_target="tpu_custom_call" | custom-call | flops 33554432 | bytes 8388608 | tf_op jit(solution)/shard_map/pallas_call | solution.py:333
  193.8 2.1 collective-permute-done.5.refs_2_
  195.8 2.3 collective-permute-done.6.refs_3_
  198.2 6.8 %shard_map.155 = (bf16[4096,128]{1,0:T(8,128)(2,1)}, bf16[4096,128]{1,0:T(8,128)(2,1)}, bf16[512,128]{1,0:T(8,128)(2,1)}, bf16[1024,512]{1,0:T(8,128)(2,1)}, bf16[512,512]{1,0:T(8,128)(2,1)}) custom-call(s32[4]{0:T(128)} %copy-done.13, bf16[512,4096]{1,0:T(8,128)(2,1)} %shard_map.154.x_ref, bf16[4,384,128]{2,1,0:T(8,128)(2,1)} %copy-done.17, ...), custom_call_target="tpu_custom_call" | custom-call | flops 1073741824 | bytes 4194304 | tf_op jit(solution)/shard_map/pallas_call | solution.py:417
  205.4 6.4 %collective-permute-start.29 = (bf16[512,128]{1,0:T(8,128)(2,1)}, bf16[512,128]{1,0:T(8,128)(2,1)S(1)}, u32[]{:S(2)}, u32[]{:S(2)}) collective-permute-start(bf16[512,128]{1,0:T(8,128)(2,1)} %get-tuple-element.54), channel_id=1, source_target_pairs={{0,6},{1,7},{2,0},{3,1},{4,2},{5,3},{6,4},{7,5},{8,14},{9,15},{10,... | collective-permute-start | bytes 393224 | tf_op jit(solution)/shard_map/ppermute | solution.py:276
  211.7 1.4 collective-permute-start.30
  213.1 1.7 collective-permute-done.28
  214.8 3.6 %collective-permute-done.30 = bf16[512,128]{1,0:T(8,128)(2,1)S(1)} collective-permute-done((bf16[512,128]{1,0:T(8,128)(2,1)}, bf16[512,128]{1,0:T(8,128)(2,1)S(1)}, u32[]{:S(2)}, u32[]{:S(2)}) %collective-permute-start.30) | collective-permute-done | bytes 131104 | tf_op jit(solution)/shard_map/ppermute | solution.py:276
  218.4 1.0 pad_maximum_fusion.1.own_ref
  220.1 1.7 fusion.4
  221.9 0.8 copy-done.10
  222.7 1.0 copy-done.5
  223.7 1.0 copy-done.11
  224.7 1.5 shard_map.162.base_ref
  226.3 0.8 copy-done.28
  227.1 4.1 %shard_map.156 = (bf16[256,1024]{1,0:T(8,128)(2,1)}, bf16[256,1024]{1,0:T(8,128)(2,1)}, bf16[256,1024]{1,0:T(8,128)(2,1)}, bf16[256,1024]{1,0:T(8,128)(2,1)}) custom-call(s32[4]{0:T(128)} %copy-done.13, bf16[1024,512]{1,0:T(8,128)(2,1)} %bitcast.11.own_ref.w_own_ref, bf16[1024,512]{1,0:T(8,128)(2,1)} %collective-permute-done.other_ref.w_other_ref, ...), custom_call_target="tpu_custom_call" | custom-call | flops 1073741824 | bytes 4194304 | tf_op jit(solution)/shard_map/pallas_call | solution.py:520
  231.2 0.7 collective-permute-start.14
  231.9 2.7 %collective-permute-start.15 = (bf16[256,1024]{1,0:T(8,128)(2,1)}, bf16[256,1024]{1,0:T(8,128)(2,1)}, u32[]{:S(2)}, u32[]{:S(2)}) collective-permute-start(bf16[256,1024]{1,0:T(8,128)(2,1)} %get-tuple-element.41), channel_id=1, source_target_pairs={{0,4},{1,5},{2,6},{3,7},{4,0},{5,1},{6,2},{7,3},{8,12},{9,13},{10,... | collective-permute-start | bytes 1572872 | tf_op jit(solution)/shard_map/ppermute | solution.py:276
  234.6 0.6 collective-permute-start.16
  235.2 1.2 slice.86
  236.5 1.5 slice_bitcast_fusion
  238.0 9.4 %collective-permute-done.14.p1_ref = bf16[256,1024]{1,0:T(8,128)(2,1)} collective-permute-done((bf16[256,1024]{1,0:T(8,128)(2,1)}, bf16[256,1024]{1,0:T(8,128)(2,1)}, u32[]{:S(2)}, u32[]{:S(2)}) %collective-permute-start.14) | collective-permute-done | bytes 524320 | tf_op jit(solution)/shard_map/ppermute | solution.py:276
  247.4 10.6 %collective-permute-done.15.p2_ref = bf16[256,1024]{1,0:T(8,128)(2,1)} collective-permute-done((bf16[256,1024]{1,0:T(8,128)(2,1)}, bf16[256,1024]{1,0:T(8,128)(2,1)}, u32[]{:S(2)}, u32[]{:S(2)}) %collective-permute-start.15) | collective-permute-done | bytes 524320 | tf_op jit(solution)/shard_map/ppermute | solution.py:276
  258.5 3.3 %shard_map.157 = (bf16[128,4096]{1,0:T(8,128)(2,1)}, bf16[128,4096]{1,0:T(8,128)(2,1)}) custom-call(s32[4]{0:T(128)S(1)} %copy-done.15, bf16[256,1024]{1,0:T(8,128)(2,1)S(1)} %copy-done.9, bf16[256,1024]{1,0:T(8,128)(2,1)} %collective-permute-done.14.p1_ref, bf16[256,1024]{1,0:T(8,128)(2,1)} %collective-permute-done.15.p2_ref, ...), custom_call_target="tpu_custom_call" | custom-call | flops 1048576 | bytes 4194304 | tf_op jit(solution)/shard_map/pallas_call | solution.py:536
  261.8 1.8 shard_map.163.base_ref
  263.6 1.4 shard_map.164
  (103 shorter events, 4.8 us)
Async XLA Ops:
  4.7 8.2 %copy-start.27 = (f32[256]{0:T(256)S(1)}, f32[256]{0:T(256)}, u32[]{:S(2)}) copy-start(f32[256]{0:T(256)} %param.11) | copy-start | bytes 3076
  4.7 32.7 %all-to-all-start = ((bf16[16,48,1024]{2,1,0:T(8,128)(2,1)}), bf16[16,48,1024]{2,1,0:T(8,128)(2,1)S(1)}, u32[]{:S(2)}, u32[]{:S(2)}) async-start(bf16[16,48,1024]{2,1,0:T(8,128)(2,1)} %bitcast.71), calls=%async_computation | async-start | bytes 3145728 | tf_op jit(solution)/shard_map/all_to_all | solution.py:348
  38.5 33.9 %all-to-all-start.1 = ((bf16[16,256,256]{2,1,0:T(8,128)(2,1)}), bf16[16,256,256]{2,1,0:T(8,128)(2,1)S(1)}, u32[]{:S(2)}, u32[]{:S(2)}) async-start(bf16[16,256,256]{2,1,0:T(8,128)(2,1)} %pad_maximum_fusion), calls=%async_computation.1 | async-start | bytes 4194304 | tf_op jit(solution)/shard_map/all_to_all | solution.py:359
  42.2 30.1 %copy-start.21 = (f32[64,512]{1,0:T(8,128)S(1)}, f32[64,512]{1,0:T(8,128)}, u32[]{:S(2)}) copy-start(f32[64,512]{1,0:T(8,128)} %param.17) | copy-start | bytes 393220
  42.2 31.7 %copy-start.19 = (f32[256,128]{1,0:T(8,128)S(1)}, f32[256,128]{1,0:T(8,128)}, u32[]{:S(2)}) copy-start(f32[256,128]{1,0:T(8,128)} %param.16) | copy-start | bytes 393220
  42.2 31.7 %copy-start.20 = (f32[256,128]{1,0:T(8,128)S(1)}, f32[256,128]{1,0:T(8,128)}, u32[]{:S(2)}) copy-start(f32[256,128]{1,0:T(8,128)} %param.15) | copy-start | bytes 393220
  72.4 74.1 %collective-permute-start.23 = (bf16[4096,256]{1,0:T(8,128)(2,1)S(1)}, bf16[4096,256]{1,0:T(8,128)(2,1)}, u32[]{:S(2)}, u32[]{:S(2)}) collective-permute-start(bf16[4096,256]{1,0:T(8,128)(2,1)S(1)} %bitcast.55), channel_id=1, source_target_pairs={{0,1},{1,0},{2,3},{3,2},{4,5},{5,4},{6,7},{7,6},{8,9},{9,8},{10,11... | collective-permute-start | bytes 6291464 | tf_op jit(solution)/shard_map/ppermute | solution.py:279
  72.4 35.5 %collective-permute-start.17 = (bf16[384,1024]{1,0:T(8,128)(2,1)}, bf16[384,1024]{1,0:T(8,128)(2,1)}, u32[]{:S(2)}, u32[]{:S(2)}) collective-permute-start(bf16[384,1024]{1,0:T(8,128)(2,1)} %bitcast.63), channel_id=1, source_target_pairs={{0,2},{1,3},{2,4},{3,5},{4,6},{5,7},{6,0},{7,1},{8,10},{9,11},{10,... | collective-permute-start | bytes 2359304 | tf_op jit(solution)/shard_map/ppermute | solution.py:276
  74.1 35.0 %collective-permute-start.19 = (bf16[384,1024]{1,0:T(8,128)(2,1)S(1)}, bf16[384,1024]{1,0:T(8,128)(2,1)}, u32[]{:S(2)}, u32[]{:S(2)}) collective-permute-start(bf16[384,1024]{1,0:T(8,128)(2,1)S(1)} %bitcast.59), channel_id=1, source_target_pairs={{0,6},{1,7},{2,0},{3,1},{4,2},{5,3},{6,4},{7,5},{8,14},{9,15},{10,... | collective-permute-start | bytes 2359304 | tf_op jit(solution)/shard_map/ppermute | solution.py:276
  75.9 36.4 %all-to-all-start.2 = ((bf16[16,64,512]{2,1,0:T(8,128)(2,1)}), bf16[16,64,512]{2,1,0:T(8,128)(2,1)}, u32[]{:S(2)}, u32[]{:S(2)}) async-start(bf16[16,64,512]{2,1,0:T(8,128)(2,1)} %convert_element_type.27), calls=%async_computation.2 | async-start | bytes 2097152 | tf_op jit(solution)/shard_map/all_to_all | solution.py:362
  80.2 31.2 %collective-permute-start.21 = (bf16[384,1024]{1,0:T(8,128)(2,1)}, bf16[384,1024]{1,0:T(8,128)(2,1)S(1)}, u32[]{:S(2)}, u32[]{:S(2)}) collective-permute-start(bf16[384,1024]{1,0:T(8,128)(2,1)} %bitcast.64), channel_id=1, source_target_pairs={{0,6},{1,7},{2,0},{3,1},{4,2},{5,3},{6,4},{7,5},{8,14},{9,15},{10,... | collective-permute-start | bytes 2359304 | tf_op jit(solution)/shard_map/ppermute | solution.py:276
  81.9 15.0 %collective-permute-start.7 = (bf16[384,128]{1,0:T(8,128)(2,1)S(1)}, bf16[384,128]{1,0:T(8,128)(2,1)S(1)}, u32[]{:S(2)}, u32[]{:S(2)}) collective-permute-start(bf16[384,128]{1,0:T(8,128)(2,1)S(1)} %get-tuple-element.62), channel_id=1, source_target_pairs={{0,32},{8,40},{16,48},{24,56},{32,64},{40,72},{48,80},{56,88},{64,... | collective-permute-start | bytes 294920 | tf_op jit(solution)/shard_map/ppermute | solution.py:292
  96.9 6.1 %collective-permute-start.8 = (bf16[384,128]{1,0:T(8,128)(2,1)S(1)}, bf16[384,128]{1,0:T(8,128)(2,1)S(1)}, u32[]{:S(2)}, u32[]{:S(2)}) collective-permute-start(bf16[384,128]{1,0:T(8,128)(2,1)S(1)} %get-tuple-element.62), channel_id=1, source_target_pairs={{0,64},{8,72},{16,80},{24,88},{32,96},{40,104},{48,112},{56,120},{... | collective-permute-start | bytes 294920 | tf_op jit(solution)/shard_map/ppermute | solution.py:292
  103.0 9.4 %copy-start.22 = (bf16[384,128]{1,0:T(8,128)(2,1)}, bf16[384,128]{1,0:T(8,128)(2,1)S(1)}, u32[]{:S(2)}) copy-start(bf16[384,128]{1,0:T(8,128)(2,1)S(1)} %collective-permute-done.8) | copy-start | bytes 294916
  103.0 4.6 %collective-permute-start.9 = (bf16[384,128]{1,0:T(8,128)(2,1)S(1)}, bf16[384,128]{1,0:T(8,128)(2,1)S(1)}, u32[]{:S(2)}, u32[]{:S(2)}) collective-permute-start(bf16[384,128]{1,0:T(8,128)(2,1)S(1)} %get-tuple-element.62), channel_id=1, source_target_pairs={{0,96},{8,104},{16,112},{24,120},{32,0},{40,8},{48,16},{56,24},{64... | collective-permute-start | bytes 294920 | tf_op jit(solution)/shard_map/ppermute | solution.py:292
  107.6 4.8 %copy-start.23 = (bf16[384,128]{1,0:T(8,128)(2,1)}, bf16[384,128]{1,0:T(8,128)(2,1)S(1)}, u32[]{:S(2)}) copy-start(bf16[384,128]{1,0:T(8,128)(2,1)S(1)} %collective-permute-done.9) | copy-start | bytes 294916
  107.6 21.7 %collective-permute-start.22 = (bf16[384,1024]{1,0:T(8,128)(2,1)S(1)}, bf16[384,1024]{1,0:T(8,128)(2,1)}, u32[]{:S(2)}, u32[]{:S(2)}) collective-permute-start(bf16[384,1024]{1,0:T(8,128)(2,1)S(1)} %bitcast.60), channel_id=1, source_target_pairs={{0,2},{1,3},{2,4},{3,5},{4,6},{5,7},{6,0},{7,1},{8,10},{9,11},{10,... | collective-permute-start | bytes 2359304 | tf_op jit(solution)/shard_map/ppermute | solution.py:276
  107.9 34.4 %collective-permute-start.18 = (bf16[384,1024]{1,0:T(8,128)(2,1)}, bf16[384,1024]{1,0:T(8,128)(2,1)}, u32[]{:S(2)}, u32[]{:S(2)}) collective-permute-start(bf16[384,1024]{1,0:T(8,128)(2,1)} %collective-permute-done.17.b_ref.refs_1_), channel_id=1, source_target_pairs={{0,2},{1,3},{2,4},{3,5},{4,6},{5,7},{6,0},{7,1},{8,10},{9,11},{10,... | collective-permute-start | bytes 2359304 | tf_op jit(solution)/shard_map/ppermute | solution.py:276
  109.0 44.3 %collective-permute-start.20 = (bf16[384,1024]{1,0:T(8,128)(2,1)}, bf16[384,1024]{1,0:T(8,128)(2,1)}, u32[]{:S(2)}, u32[]{:S(2)}) collective-permute-start(bf16[384,1024]{1,0:T(8,128)(2,1)} %collective-permute-done.19.d_ref.refs_5_), channel_id=1, source_target_pairs={{0,6},{1,7},{2,0},{3,1},{4,2},{5,3},{6,4},{7,5},{8,14},{9,15},{10,... | collective-permute-start | bytes 2359304 | tf_op jit(solution)/shard_map/ppermute | solution.py:276
  112.3 54.3 %collective-permute-start = (bf16[1024,512]{1,0:T(8,128)(2,1)}, bf16[1024,512]{1,0:T(8,128)(2,1)}, u32[]{:S(2)}, u32[]{:S(2)}) collective-permute-start(bf16[1024,512]{1,0:T(8,128)(2,1)} %bitcast.11.own_ref.w_own_ref), channel_id=1, source_target_pairs={{0,1},{1,0},{2,3},{3,2},{4,5},{5,4},{6,7},{7,6},{8,9},{9,8},{10,11... | collective-permute-start | bytes 3145736 | tf_op jit(solution)/shard_map/ppermute | solution.py:279
  112.4 42.0 %copy-start.13 = (s32[4]{0:T(128)}, s32[4]{0:T(128)S(1)}, u32[]{:S(2)}) copy-start(s32[4]{0:T(128)S(1)} %pad_add_fusion.place_ref) | copy-start | bytes 52
  112.4 35.1 %copy-start.1 = (bf16[8,48,1024]{2,1,0:T(8,128)(2,1)S(1)}, bf16[8,48,1024]{2,1,0:T(8,128)(2,1)}, u32[]{:S(2)}) copy-start(bf16[8,48,1024]{2,1,0:T(8,128)(2,1)} %get-tuple-element.60) | copy-start | bytes 2359300
  113.5 1.1 copy-start
  114.6 52.0 %copy-start.16 = (bf16[4,384,128]{2,1,0:T(8,128)(2,1)}, bf16[4,384,128]{2,1,0:T(8,128)(2,1)S(1)}, u32[]{:S(2)}) copy-start(bf16[4,384,128]{2,1,0:T(8,128)(2,1)S(1)} %pad_maximum_fusion.3.refs_4_) | copy-start | bytes 1179652
  114.6 32.9 %copy-start.8 = (bf16[384,1024]{1,0:T(8,128)(2,1)S(1)}, bf16[384,1024]{1,0:T(8,128)(2,1)}, u32[]{:S(2)}) copy-start(bf16[384,1024]{1,0:T(8,128)(2,1)} %copy-done.7) | copy-start | bytes 2359300
  129.3 28.2 %collective-permute-start.1 = (bf16[384,128]{1,0:T(8,128)(2,1)S(1)}, bf16[384,128]{1,0:T(8,128)(2,1)S(1)}, u32[]{:S(2)}, u32[]{:S(2)}) collective-permute-start(bf16[384,128]{1,0:T(8,128)(2,1)S(1)} %get-tuple-element.64), channel_id=1, source_target_pairs={{0,8},{8,16},{16,24},{24,0},{32,40},{40,48},{48,56},{56,32},{64,72... | collective-permute-start | bytes 294920 | tf_op jit(solution)/shard_map/ppermute | solution.py:292
  142.3 15.5 %collective-permute-start.2 = (bf16[384,128]{1,0:T(8,128)(2,1)S(1)}, bf16[384,128]{1,0:T(8,128)(2,1)S(1)}, u32[]{:S(2)}, u32[]{:S(2)}) collective-permute-start(bf16[384,128]{1,0:T(8,128)(2,1)S(1)} %get-tuple-element.64), channel_id=1, source_target_pairs={{0,16},{8,24},{16,0},{24,8},{32,48},{40,56},{48,32},{56,40},{64,80... | collective-permute-start | bytes 294920 | tf_op jit(solution)/shard_map/ppermute | solution.py:292
  146.4 14.6 %collective-permute-start.3 = (bf16[384,128]{1,0:T(8,128)(2,1)S(1)}, bf16[384,128]{1,0:T(8,128)(2,1)S(1)}, u32[]{:S(2)}, u32[]{:S(2)}) collective-permute-start(bf16[384,128]{1,0:T(8,128)(2,1)S(1)} %get-tuple-element.64), channel_id=1, source_target_pairs={{0,24},{8,0},{16,8},{24,16},{32,56},{40,32},{48,40},{56,48},{64,88... | collective-permute-start | bytes 294920 | tf_op jit(solution)/shard_map/ppermute | solution.py:292
  153.3 13.3 %collective-permute-start.10 = (bf16[4,384,128]{2,1,0:T(8,128)(2,1)S(1)}, bf16[4,384,128]{2,1,0:T(8,128)(2,1)S(1)}, u32[]{:S(2)}, u32[]{:S(2)}) collective-permute-start(bf16[4,384,128]{2,1,0:T(8,128)(2,1)S(1)} %pad_maximum_fusion.3.refs_4_), channel_id=1, source_target_pairs={{0,8},{8,16},{16,24},{24,0},{32,40},{40,48},{48,56},{56,32},{64,72... | collective-permute-start | bytes 1179656 | tf_op jit(solution)/shard_map/ppermute | solution.py:292
  157.5 22.4 %copy-start.12 = (bf16[2,384,256]{2,1,0:T(8,128)(2,1)}, bf16[2,384,256]{2,1,0:T(8,128)(2,1)S(1)}, u32[]{:S(2)}) copy-start(bf16[2,384,256]{2,1,0:T(8,128)(2,1)S(1)} %shard_map.160) | copy-start | bytes 1179652
  157.5 17.0 %collective-permute-start.24 = (bf16[768,256]{1,0:T(8,128)(2,1)S(1)}, bf16[768,256]{1,0:T(8,128)(2,1)S(1)}, u32[]{:S(2)}, u32[]{:S(2)}) collective-permute-start(bf16[768,256]{1,0:T(8,128)(2,1)S(1)} %bitcast.67), channel_id=1, source_target_pairs={{0,2},{1,3},{2,4},{3,5},{4,6},{5,7},{6,0},{7,1},{8,10},{9,11},{10,... | collective-permute-start | bytes 1179656 | tf_op jit(solution)/shard_map/ppermute | solution.py:276
  157.8 17.0 %collective-permute-start.25 = (bf16[768,256]{1,0:T(8,128)(2,1)S(1)}, bf16[768,256]{1,0:T(8,128)(2,1)S(1)}, u32[]{:S(2)}, u32[]{:S(2)}) collective-permute-start(bf16[768,256]{1,0:T(8,128)(2,1)S(1)} %bitcast.68), channel_id=1, source_target_pairs={{0,6},{1,7},{2,0},{3,1},{4,2},{5,3},{6,4},{7,5},{8,14},{9,15},{10,... | collective-permute-start | bytes 1179656 | tf_op jit(solution)/shard_map/ppermute | solution.py:276
  161.0 17.6 %collective-permute-start.26 = (bf16[768,256]{1,0:T(8,128)(2,1)S(1)}, bf16[768,256]{1,0:T(8,128)(2,1)S(1)}, u32[]{:S(2)}, u32[]{:S(2)}) collective-permute-start(bf16[768,256]{1,0:T(8,128)(2,1)S(1)} %bitcast.69), channel_id=1, source_target_pairs={{0,4},{1,5},{2,6},{3,7},{4,0},{5,1},{6,2},{7,3},{8,12},{9,13},{10,... | collective-permute-start | bytes 1179656 | tf_op jit(solution)/shard_map/ppermute | solution.py:276
  161.1 24.3 %copy-start.17 = (bf16[4,384,128]{2,1,0:T(8,128)(2,1)}, bf16[4,384,128]{2,1,0:T(8,128)(2,1)S(1)}, u32[]{:S(2)}) copy-start(bf16[4,384,128]{2,1,0:T(8,128)(2,1)S(1)} %pad_maximum_fusion.2.refs_0_) | copy-start | bytes 1179652
  166.6 18.8 %copy-start.18 = (bf16[4,384,128]{2,1,0:T(8,128)(2,1)}, bf16[4,384,128]{2,1,0:T(8,128)(2,1)S(1)}, u32[]{:S(2)}) copy-start(bf16[4,384,128]{2,1,0:T(8,128)(2,1)S(1)} %collective-permute-done.10.refs_5_) | copy-start | bytes 1179652
  166.6 27.2 %collective-permute-start.11 = (bf16[4,384,128]{2,1,0:T(8,128)(2,1)S(1)}, bf16[4,384,128]{2,1,0:T(8,128)(2,1)}, u32[]{:S(2)}, u32[]{:S(2)}) collective-permute-start(bf16[4,384,128]{2,1,0:T(8,128)(2,1)S(1)} %pad_maximum_fusion.3.refs_4_), channel_id=1, source_target_pairs={{0,16},{8,24},{16,0},{24,8},{32,48},{40,56},{48,32},{56,40},{64,80... | collective-permute-start | bytes 1179656 | tf_op jit(solution)/shard_map/ppermute | solution.py:292
  166.6 27.1 %collective-permute-start.12 = (bf16[4,384,128]{2,1,0:T(8,128)(2,1)S(1)}, bf16[4,384,128]{2,1,0:T(8,128)(2,1)}, u32[]{:S(2)}, u32[]{:S(2)}) collective-permute-start(bf16[4,384,128]{2,1,0:T(8,128)(2,1)S(1)} %pad_maximum_fusion.3.refs_4_), channel_id=1, source_target_pairs={{0,24},{8,0},{16,8},{24,16},{32,56},{40,32},{48,40},{56,48},{64,88... | collective-permute-start | bytes 1179656 | tf_op jit(solution)/shard_map/ppermute | solution.py:292
  174.5 4.1 %copy-start.29 = (bf16[768,256]{1,0:T(8,128)(2,1)}, bf16[768,256]{1,0:T(8,128)(2,1)S(1)}, u32[]{:S(2)}) copy-start(bf16[768,256]{1,0:T(8,128)(2,1)S(1)} %collective-permute-done.24.h1_ref) | copy-start | bytes 1179652
  174.5 19.2 %collective-permute-start.4 = (bf16[4,384,128]{2,1,0:T(8,128)(2,1)S(1)}, bf16[4,384,128]{2,1,0:T(8,128)(2,1)}, u32[]{:S(2)}, u32[]{:S(2)}) collective-permute-start(bf16[4,384,128]{2,1,0:T(8,128)(2,1)S(1)} %pad_maximum_fusion.2.refs_0_), channel_id=1, source_target_pairs={{0,32},{8,40},{16,48},{24,56},{32,64},{40,72},{48,80},{56,88},{64,... | collective-permute-start | bytes 1179656 | tf_op jit(solution)/shard_map/ppermute | solution.py:292
  174.8 3.8 %copy-start.30 = (bf16[768,256]{1,0:T(8,128)(2,1)}, bf16[768,256]{1,0:T(8,128)(2,1)S(1)}, u32[]{:S(2)}) copy-start(bf16[768,256]{1,0:T(8,128)(2,1)S(1)} %collective-permute-done.25.h2_ref) | copy-start | bytes 1179652
  174.8 21.0 %collective-permute-start.5 = (bf16[4,384,128]{2,1,0:T(8,128)(2,1)S(1)}, bf16[4,384,128]{2,1,0:T(8,128)(2,1)}, u32[]{:S(2)}, u32[]{:S(2)}) collective-permute-start(bf16[4,384,128]{2,1,0:T(8,128)(2,1)S(1)} %pad_maximum_fusion.2.refs_0_), channel_id=1, source_target_pairs={{0,64},{8,72},{16,80},{24,88},{32,96},{40,104},{48,112},{56,120},{... | collective-permute-start | bytes 1179656 | tf_op jit(solution)/shard_map/ppermute | solution.py:292
  179.4 18.8 %collective-permute-start.6 = (bf16[4,384,128]{2,1,0:T(8,128)(2,1)S(1)}, bf16[4,384,128]{2,1,0:T(8,128)(2,1)}, u32[]{:S(2)}, u32[]{:S(2)}) collective-permute-start(bf16[4,384,128]{2,1,0:T(8,128)(2,1)S(1)} %pad_maximum_fusion.2.refs_0_), channel_id=1, source_target_pairs={{0,96},{8,104},{16,112},{24,120},{32,0},{40,8},{48,16},{56,24},{64... | collective-permute-start | bytes 1179656 | tf_op jit(solution)/shard_map/ppermute | solution.py:292
  185.4 49.8 %all-to-all-start.3 = ((bf16[16,2,48,512]{3,2,1,0:T(8,128)(2,1)}), bf16[16,2,48,512]{3,2,1,0:T(8,128)(2,1)}, u32[]{:S(2)}, u32[]{:S(2)}) async-start(bf16[16,2,48,512]{3,2,1,0:T(8,128)(2,1)} %shard_map.161), calls=%async_computation.3 | async-start | bytes 3145728 | tf_op jit(solution)/shard_map/all_to_all | solution.py:472
  193.7 19.4 %copy-start.26 = (f32[512,2]{0,1:T(2,128)S(1)}, f32[512,2]{0,1:T(2,128)}, u32[]{:S(2)}) copy-start(f32[512,2]{0,1:T(2,128)} %param.19) | copy-start | bytes 12292
  193.7 26.4 %copy-start.24 = (s32[512,2]{0,1:T(2,128)S(1)}, s32[512,2]{0,1:T(2,128)}, u32[]{:S(2)}) copy-start(s32[512,2]{0,1:T(2,128)} %param.18) | copy-start | bytes 12292
  193.7 26.4 %copy-start.25 = (s32[2,512]{1,0:T(2,128)S(1)}, s32[2,512]{1,0:T(2,128)}, u32[]{:S(2)}) copy-start(s32[2,512]{1,0:T(2,128)} %get-tuple-element.47) | copy-start | bytes 12292
  205.0 17.7 %copy-start.14 = (s32[4]{0:T(128)S(1)}, s32[4]{0:T(128)}, u32[]{:S(2)}) copy-start(s32[4]{0:T(128)} %copy-done.13) | copy-start | bytes 52
  205.0 9.8 %collective-permute-start.28 = (bf16[512,128]{1,0:T(8,128)(2,1)}, bf16[512,128]{1,0:T(8,128)(2,1)S(1)}, u32[]{:S(2)}, u32[]{:S(2)}) collective-permute-start(bf16[512,128]{1,0:T(8,128)(2,1)} %get-tuple-element.54), channel_id=1, source_target_pairs={{0,2},{1,3},{2,4},{3,5},{4,6},{5,7},{6,0},{7,1},{8,10},{9,11},{10,... | collective-permute-start | bytes 393224 | tf_op jit(solution)/shard_map/ppermute | solution.py:276
  205.4 9.5 %collective-permute-start.29 = (bf16[512,128]{1,0:T(8,128)(2,1)}, bf16[512,128]{1,0:T(8,128)(2,1)S(1)}, u32[]{:S(2)}, u32[]{:S(2)}) collective-permute-start(bf16[512,128]{1,0:T(8,128)(2,1)} %get-tuple-element.54), channel_id=1, source_target_pairs={{0,6},{1,7},{2,0},{3,1},{4,2},{5,3},{6,4},{7,5},{8,14},{9,15},{10,... | collective-permute-start | bytes 393224 | tf_op jit(solution)/shard_map/ppermute | solution.py:276
  211.7 6.7 %collective-permute-start.30 = (bf16[512,128]{1,0:T(8,128)(2,1)}, bf16[512,128]{1,0:T(8,128)(2,1)S(1)}, u32[]{:S(2)}, u32[]{:S(2)}) collective-permute-start(bf16[512,128]{1,0:T(8,128)(2,1)} %get-tuple-element.54), channel_id=1, source_target_pairs={{0,4},{1,5},{2,6},{3,7},{4,0},{5,1},{6,2},{7,3},{8,12},{9,13},{10,... | collective-permute-start | bytes 393224 | tf_op jit(solution)/shard_map/ppermute | solution.py:276
  219.4 2.5 copy-start.4
  219.4 2.4 collective-permute-start.31
  219.5 3.1 %copy-start.6 = (bf16[1024,512]{1,0:T(8,128)(2,1)S(1)}, bf16[1024,512]{1,0:T(8,128)(2,1)}, u32[]{:S(2)}) copy-start(bf16[1024,512]{1,0:T(8,128)(2,1)} %get-tuple-element.37.sd_ref) | copy-start | bytes 3145732
  219.5 6.7 %collective-permute-start.13 = (bf16[512,512]{1,0:T(8,128)(2,1)}, bf16[512,512]{1,0:T(8,128)(2,1)S(1)}, u32[]{:S(2)}, u32[]{:S(2)}) collective-permute-start(bf16[512,512]{1,0:T(8,128)(2,1)} %get-tuple-element.38), channel_id=1, source_target_pairs={{0,1},{1,0},{2,3},{3,2},{4,5},{5,4},{6,7},{7,6},{8,9},{9,8},{10,11... | collective-permute-start | bytes 1572872 | tf_op jit(solution)/shard_map/ppermute | solution.py:279
  222.7 1.0 copy-start.5
  223.7 1.0 copy-start.11
  231.2 16.2 %collective-permute-start.14 = (bf16[256,1024]{1,0:T(8,128)(2,1)}, bf16[256,1024]{1,0:T(8,128)(2,1)}, u32[]{:S(2)}, u32[]{:S(2)}) collective-permute-start(bf16[256,1024]{1,0:T(8,128)(2,1)} %get-tuple-element.40), channel_id=1, source_target_pairs={{0,2},{1,3},{2,4},{3,5},{4,6},{5,7},{6,0},{7,1},{8,10},{9,11},{10,... | collective-permute-start | bytes 1572872 | tf_op jit(solution)/shard_map/ppermute | solution.py:276
  231.9 26.1 %collective-permute-start.15 = (bf16[256,1024]{1,0:T(8,128)(2,1)}, bf16[256,1024]{1,0:T(8,128)(2,1)}, u32[]{:S(2)}, u32[]{:S(2)}) collective-permute-start(bf16[256,1024]{1,0:T(8,128)(2,1)} %get-tuple-element.41), channel_id=1, source_target_pairs={{0,4},{1,5},{2,6},{3,7},{4,0},{5,1},{6,2},{7,3},{8,12},{9,13},{10,... | collective-permute-start | bytes 1572872 | tf_op jit(solution)/shard_map/ppermute | solution.py:276
  234.6 23.8 %collective-permute-start.16 = (bf16[256,1024]{1,0:T(8,128)(2,1)}, bf16[256,1024]{1,0:T(8,128)(2,1)}, u32[]{:S(2)}, u32[]{:S(2)}) collective-permute-start(bf16[256,1024]{1,0:T(8,128)(2,1)} %get-tuple-element.42), channel_id=1, source_target_pairs={{0,6},{1,7},{2,0},{3,1},{4,2},{5,3},{6,4},{7,5},{8,14},{9,15},{10,... | collective-permute-start | bytes 1572872 | tf_op jit(solution)/shard_map/ppermute | solution.py:276
  236.4 22.0 %copy-start.9 = (bf16[256,1024]{1,0:T(8,128)(2,1)S(1)}, bf16[256,1024]{1,0:T(8,128)(2,1)}, u32[]{:S(2)}) copy-start(bf16[256,1024]{1,0:T(8,128)(2,1)} %get-tuple-element.39.p0_ref) | copy-start | bytes 1572868
  236.4 22.0 %copy-start.15 = (s32[4]{0:T(128)S(1)}, s32[4]{0:T(128)}, u32[]{:S(2)}) copy-start(s32[4]{0:T(128)} %copy-done.13) | copy-start | bytes 52
  236.4 27.2 %collective-permute-start.27 = (bf16[768,512]{1,0:T(8,128)(2,1)S(1)}, bf16[768,512]{1,0:T(8,128)(2,1)S(1)}, u32[]{:S(2)}, u32[]{:S(2)}) collective-permute-start(bf16[768,512]{1,0:T(8,128)(2,1)S(1)} %bitcast.72), channel_id=1, source_target_pairs={{0,1},{1,0},{2,3},{3,2},{4,5},{5,4},{6,7},{7,6},{8,9},{9,8},{10,11... | collective-permute-start | bytes 2359304 | tf_op jit(solution)/shard_map/ppermute | solution.py:279
  238.0 23.8 %copy-start.3 = (bf16[512,768]{1,0:T(8,128)(2,1)S(1)}, bf16[512,768]{1,0:T(8,128)(2,1)}, u32[]{:S(2)}) copy-start(bf16[512,768]{1,0:T(8,128)(2,1)} %get-tuple-element.53.weight_ref) | copy-start | bytes 2359300
  261.8 1.8 copy-start.2
  (4 other events, 3.2 us)

commit v10 on v8

--- a/solution.py
+++ b/solution.py
@@ -28,15 +28,19 @@
     return pltpu.CompilerParams(vmem_limit_bytes=mib << 20)
 
 
-def route_kernel(half, route_ref, tok_ref, out_ref, slot_ref, kept, placing, sem):
+def route_kernel(half, routes_ref, tok_ref, out_ref, slots_ref, *scratch):
+    route_ref, slot_ref, kept, placing, held, sems = scratch
     t = lax.axis_index("tp")
     chip, core = t // 2, lax.rem(t, 2)
     tok_rows, quarter = kept.shape
     spots = placing.shape[0]
     experts = spots // half
     at = pl.ds(pl.multiple_of(chip * quarter, quarter), quarter)
-    read = pltpu.make_async_copy(tok_ref.at[:, at], kept, sem)
+    read = pltpu.make_async_copy(tok_ref.at[:, at], kept, sems.at[0])
+    routes = pltpu.make_async_copy(routes_ref, route_ref, sems.at[1])
+    routes.start()
     read.start()
+    routes.wait()
 
     ids = lax.broadcasted_iota(jnp.int32, (experts, tok_rows), 0)
     hot = [route_ref[k : k + 1, :] == ids for k in range(route_ref.shape[0])]
@@ -54,10 +58,17 @@
         here = (local >= 0) & (local < half)
         target = jnp.where(here, route_ref[k : k + 1, :] * half + local, -1)
         total = total + jnp.where(spot == target, 1.0, 0.0)
+    writes = [pltpu.make_async_copy(slot_ref, slots_ref, sems.at[2])]
     placing[...] = total.astype(bf16)
+    writes[0].start()
     read.wait()
-    for c in range(0, spots, 256):
-        out_ref[c : c + 256, :] = dot(placing[c : c + 256, :], kept[...]).astype(bf16)
+    for n, c in enumerate(range(0, spots, 256)):
+        span = pl.ds(c, 256)
+        held[c : c + 256, :] = dot(placing[c : c + 256, :], kept[...]).astype(bf16)
+        writes.append(pltpu.make_async_copy(held.at[span], out_ref.at[span], sems.at[3 + n]))
+        writes[-1].start()
+    for write in writes:
+        write.wait()
 
 
 def norm_kernel(tok_ref, normed_ref, taken, given, in_sem, out_sem):
@@ -315,16 +326,19 @@
     outgoing, slots = pl.pallas_call(
         functools.partial(route_kernel, half),
         grid=(1,),
-        in_specs=[whole((top_count, tok_rows)), anywhere],
-        out_specs=[whole((rows, quarter)), whole((top_count, tok_rows))],
+        in_specs=[anywhere, anywhere],
+        out_specs=[anywhere, anywhere],
         out_shape=[
             jax.ShapeDtypeStruct((rows, quarter), bf16),
             jax.ShapeDtypeStruct((top_count, tok_rows), jnp.int32),
         ],
         scratch_shapes=[
+            pltpu.VMEM((top_count, tok_rows), jnp.int32),
+            pltpu.VMEM((top_count, tok_rows), jnp.int32),
             pltpu.VMEM((tok_rows, quarter), bf16),
             pltpu.VMEM((rows, tok_rows), bf16),
-            pltpu.SemaphoreType.DMA(()),
+            pltpu.VMEM((rows, quarter), bf16),
+            pltpu.SemaphoreType.DMA((3 + rows // 256,)),
         ],
         compiler_params=vmem_limit(60),
         cost_estimate=cost(2 * rows * tok_rows * quarter, 4 * tok_rows * quarter),

time: 269 us -> 269 us (level); the launches traced: 265 us -> 268 us
  starting transfers between devices: 57.6 us -> 62.5 us
    ppermute x15, starting transfers between devices: 20.3 us -> 25.2 us  [shift_by(): return lax.ppermute(a, 'tp', [(i, (i + 2 * n) % tp) for i in range(tp)])]
where the time goes in v10:
time: 269 us; the launch traced here: 268 us
  waiting for transfers between devices  136 us (51%)
  starting transfers between devices  62.5 us (23%)
  Pallas kernels  45.4 us (17%)
  other arithmetic  11.8 us (4%)
  local copies, waits for them, and re-layouts  11.2 us (4%)
    ppermute x15, waiting for transfers between devices, shift_by(): return lax.ppermute(a, 'tp', [(i, (i + 2 * n) % tp) for i in range(tp)])  56 us
    ppermute x12, waiting for transfers between devices, along(): return lax.ppermute(a, 'fs', pairs)  33 us
    all_to_all x1, waiting for transfers between devices, on_device(): gu = lax.all_to_all(gu_local, 'fs', split_axis=0, concat_axis=0, tiled=True)  27.4 us
    ppermute x15, starting transfers between devices, shift_by(): return lax.ppermute(a, 'tp', [(i, (i + 2 * n) % tp) for i in range(tp)])  25.2 us
    all_to_all x1, waiting for transfers between devices, on_device(): lax.all_to_all(outgoing.reshape(experts, half, quarter), 'fs', split_axis...  20.1 us
    ppermute x12, starting transfers between devices, along(): return lax.ppermute(a, 'fs', pairs)  15.8 us
    all_to_all x1, starting transfers between devices, on_device(): lax.all_to_all(outgoing.reshape(experts, half, quarter), 'fs', split_axis...  8.17 us
    unnamed x68, local copies, waits for them, and re-layouts  7.23 us
  transfers between devices with their start and end apart: 36, of which 17 were waited for; matrix products, arithmetic and copies ran while one was open for 5% of the time, Pallas kernels for 15%

profile of v10, /device:TPU:0, one launch (start us, length us, event | category | flops | bytes accessed | tf_op | source)
XLA Modules:
  0.0 268.5 jit_solution(16100202792221160761)
XLA Ops:
  0.6 3.4 %shard_map.153 = (bf16[768,1024]{1,0:T(8,128)(2,1)}, s32[2,512]{1,0:T(2,128)}) custom-call(s32[2,512]{1,0:T(2,128)} %bitcast.75, bf16[512,4096]{1,0:T(8,128)(2,1)} %tok_ref.3), custom_call_target="tpu_custom_call" | custom-call | flops 805306368 | bytes 2097152 | tf_op jit(solution)/shard_map/pallas_call | solution.py:326
  4.1 8.2 %all-to-all-start = ((bf16[16,48,1024]{2,1,0:T(8,128)(2,1)}), bf16[16,48,1024]{2,1,0:T(8,128)(2,1)S(1)}, u32[]{:S(2)}, u32[]{:S(2)}) async-start(bf16[16,48,1024]{2,1,0:T(8,128)(2,1)} %bitcast.63), calls=%async_computation | async-start | bytes 3145728 | tf_op jit(solution)/shard_map/all_to_all | solution.py:361
  12.2 2.8 %multiply_convert_fusion.1 = (bf16[16,256,128]{2,1,0:T(8,128)(2,1)S(1)}, bf16[16,256,128]{2,1,0:T(8,128)(2,1)S(1)}) fusion(f32[16,256,128]{2,1,0:T(8,128)} %param.12, f32[256]{0:T(256)S(1)} %copy-done.29, f32[16,256,128]{2,1,0:T(8,128)} %param.13), kind=kLoop, calls=%fused_computation.2 | loop fusion | flops 2097152 | bytes 6292480 | tf_op jit(solution)/shard_map/convert_element_type | solution.py:366
  15.1 1.6 pad_maximum_fusion
  16.7 20.1 %all-to-all-done = bf16[16,48,1024]{2,1,0:T(8,128)(2,1)S(1)} async-done(((bf16[16,48,1024]{2,1,0:T(8,128)(2,1)}), bf16[16,48,1024]{2,1,0:T(8,128)(2,1)S(1)}, u32[]{:S(2)}, u32[]{:S(2)}) %all-to-all-start) | async-done | bytes 1572896 | tf_op jit(solution)/shard_map/all_to_all | solution.py:361
  36.8 1.3 fusion.8
  38.1 3.7 %all-to-all-start.1 = ((bf16[16,256,256]{2,1,0:T(8,128)(2,1)}), bf16[16,256,256]{2,1,0:T(8,128)(2,1)S(1)}, u32[]{:S(2)}, u32[]{:S(2)}) async-start(bf16[16,256,256]{2,1,0:T(8,128)(2,1)} %pad_maximum_fusion), calls=%async_computation.1 | async-start | bytes 4194304 | tf_op jit(solution)/shard_map/all_to_all | solution.py:372
  41.8 2.8 %convert_element_type.27 = bf16[16,64,512]{2,1,0:T(8,128)(2,1)} convert(f32[16,64,512]{2,1,0:T(8,128)} %param.14) | non-fusion elementwise | flops 524288 | bytes 3145728 | tf_op jit(solution)/shard_map/convert_element_type | solution.py:373
  44.6 27.4 %all-to-all-done.1 = bf16[16,256,256]{2,1,0:T(8,128)(2,1)S(1)} async-done(((bf16[16,256,256]{2,1,0:T(8,128)(2,1)}), bf16[16,256,256]{2,1,0:T(8,128)(2,1)S(1)}, u32[]{:S(2)}, u32[]{:S(2)}) %all-to-all-start.1) | async-done | bytes 2097184 | tf_op jit(solution)/shard_map/all_to_all | solution.py:372
  72.0 1.5 collective-permute-start.17
  73.6 1.8 collective-permute-start.19
  75.4 4.3 %all-to-all-start.2 = ((bf16[16,64,512]{2,1,0:T(8,128)(2,1)}), bf16[16,64,512]{2,1,0:T(8,128)(2,1)}, u32[]{:S(2)}, u32[]{:S(2)}) async-start(bf16[16,64,512]{2,1,0:T(8,128)(2,1)} %convert_element_type.27), calls=%async_computation.2 | async-start | bytes 2097152 | tf_op jit(solution)/shard_map/all_to_all | solution.py:374
  79.8 1.6 collective-permute-start.21
  81.5 1.8 collective-permute-start.7
  83.3 13.2 %collective-permute-done.7 = bf16[384,128]{1,0:T(8,128)(2,1)S(1)} collective-permute-done((bf16[384,128]{1,0:T(8,128)(2,1)S(1)}, bf16[384,128]{1,0:T(8,128)(2,1)S(1)}, u32[]{:S(2)}, u32[]{:S(2)}) %collective-permute-start.7) | collective-permute-done | bytes 98336 | tf_op jit(solution)/shard_map/ppermute | solution.py:302
  97.0 5.6 %collective-permute-done.8 = bf16[384,128]{1,0:T(8,128)(2,1)S(1)} collective-permute-done((bf16[384,128]{1,0:T(8,128)(2,1)S(1)}, bf16[384,128]{1,0:T(8,128)(2,1)S(1)}, u32[]{:S(2)}, u32[]{:S(2)}) %collective-permute-start.8) | collective-permute-done | bytes 98336 | tf_op jit(solution)/shard_map/ppermute | solution.py:302
  103.0 4.1 %collective-permute-done.9 = bf16[384,128]{1,0:T(8,128)(2,1)S(1)} collective-permute-done((bf16[384,128]{1,0:T(8,128)(2,1)S(1)}, bf16[384,128]{1,0:T(8,128)(2,1)S(1)}, u32[]{:S(2)}, u32[]{:S(2)}) %collective-permute-start.9) | collective-permute-done | bytes 98336 | tf_op jit(solution)/shard_map/ppermute | solution.py:302
  107.5 1.1 collective-permute-start.18
  108.6 2.1 collective-permute-start.20
  111.2 0.9 copy-done.13
  112.7 1.3 shard_map.159.b_ref
  114.1 1.0 pad_maximum_fusion.3.refs_4_
  115.1 1.3 shard_map.158.a_ref
  116.4 1.3 shard_map.160.refs_8_
  117.7 11.4 %collective-permute-done.22.refs_4_ = bf16[384,1024]{1,0:T(8,128)(2,1)} collective-permute-done((bf16[384,1024]{1,0:T(8,128)(2,1)}, bf16[384,1024]{1,0:T(8,128)(2,1)}, u32[]{:S(2)}, u32[]{:S(2)}) %collective-permute-start.22) | collective-permute-done | bytes 786464 | tf_op jit(solution)/shard_map/ppermute | solution.py:286
  129.1 2.1 collective-permute-start.1
  131.2 10.7 %collective-permute-done.18.far0_ref = bf16[384,1024]{1,0:T(8,128)(2,1)S(1)} collective-permute-done((bf16[384,1024]{1,0:T(8,128)(2,1)}, bf16[384,1024]{1,0:T(8,128)(2,1)S(1)}, u32[]{:S(2)}, u32[]{:S(2)}) %collective-permute-start.18) | collective-permute-done | bytes 786464 | tf_op jit(solution)/shard_map/ppermute | solution.py:286
  142.0 4.1 %collective-permute-start.2 = (bf16[384,128]{1,0:T(8,128)(2,1)}, bf16[384,128]{1,0:T(8,128)(2,1)S(1)}, u32[]{:S(2)}, u32[]{:S(2)}) collective-permute-start(bf16[384,128]{1,0:T(8,128)(2,1)} %get-tuple-element.64.a_ref), channel_id=1, source_target_pairs={{0,16},{8,24},{16,0},{24,8},{32,48},{40,56},{48,32},{56,40},{64,80... | collective-permute-start | bytes 294920 | tf_op jit(solution)/shard_map/ppermute | solution.py:302
  146.1 1.1 collective-permute-start.3
  147.9 1.1 copy-done.14
  149.0 7.0 %shard_map.161 = (f32[2,384,512]{2,1,0:T(8,128)S(1)}, f32[2,384,128]{2,1,0:T(8,128)S(1)}) custom-call(s32[4]{0:T(128)S(1)} %pad_add_fusion.place_ref, bf16[384,1024]{1,0:T(8,128)(2,1)} %bitcast.2.refs_0_, bf16[384,1024]{1,0:T(8,128)(2,1)} %collective-permute-done.17.a_ref.refs_1_, bf16[384,1024]{1,0:T(8,128)(2,1)S(1)} %copy-done.14, ...), custom_call_target="tpu_custom_call" | custom-call | flops 2415919104 | bytes 4194304 | tf_op jit(solution)/shard_map/pallas_call | solution.py:404
  156.0 1.0 collective-permute-start.10
  157.0 3.0 %shard_map.162 = bf16[2,384,256]{2,1,0:T(8,128)(2,1)S(1)} custom-call(s32[4]{0:T(128)S(1)} %pad_add_fusion.place_ref, bf16[384,1024]{1,0:T(8,128)(2,1)S(1)} %collective-permute-done.18.far0_ref, bf16[384,1024]{1,0:T(8,128)(2,1)} %collective-permute-done.20.far1_ref, f32[2,384,512]{2,1,0:T(8,128)S(1)} %get-tuple-element.51.acc_ref, ...), custom_call_target="tpu_custom_call" | custom-call | flops 805306368 | bytes 1048576 | tf_op jit(solution)/shard_map/pallas_call | solution.py:419
  160.3 3.2 %collective-permute-start.25 = (bf16[768,256]{1,0:T(8,128)(2,1)S(1)}, bf16[768,256]{1,0:T(8,128)(2,1)S(1)}, u32[]{:S(2)}, u32[]{:S(2)}) collective-permute-start(bf16[768,256]{1,0:T(8,128)(2,1)S(1)} %bitcast.60), channel_id=1, source_target_pairs={{0,6},{1,7},{2,0},{3,1},{4,2},{5,3},{6,4},{7,5},{8,14},{9,15},{10,... | collective-permute-start | bytes 1179656 | tf_op jit(solution)/shard_map/ppermute | solution.py:286
  163.5 5.7 %collective-permute-done.10.refs_5_ = bf16[4,384,128]{2,1,0:T(8,128)(2,1)S(1)} collective-permute-done((bf16[4,384,128]{2,1,0:T(8,128)(2,1)S(1)}, bf16[4,384,128]{2,1,0:T(8,128)(2,1)S(1)}, u32[]{:S(2)}, u32[]{:S(2)}) %collective-permute-start.10) | collective-permute-done | bytes 393248 | tf_op jit(solution)/shard_map/ppermute | solution.py:302
  169.3 7.6 %collective-permute-done.24.h1_ref = bf16[768,256]{1,0:T(8,128)(2,1)S(1)} collective-permute-done((bf16[768,256]{1,0:T(8,128)(2,1)S(1)}, bf16[768,256]{1,0:T(8,128)(2,1)S(1)}, u32[]{:S(2)}, u32[]{:S(2)}) %collective-permute-start.24) | collective-permute-done | bytes 393248 | tf_op jit(solution)/shard_map/ppermute | solution.py:286
  177.2 3.8 %collective-permute-start.5 = (bf16[4,384,128]{2,1,0:T(8,128)(2,1)S(1)}, bf16[4,384,128]{2,1,0:T(8,128)(2,1)}, u32[]{:S(2)}, u32[]{:S(2)}) collective-permute-start(bf16[4,384,128]{2,1,0:T(8,128)(2,1)S(1)} %pad_maximum_fusion.2.refs_0_), channel_id=1, source_target_pairs={{0,64},{8,72},{16,80},{24,88},{32,96},{40,104},{48,112},{56,120},{... | collective-permute-start | bytes 1179656 | tf_op jit(solution)/shard_map/ppermute | solution.py:302
  181.1 0.7 copy-done.33
  182.3 5.4 %shard_map.163 = bf16[16,2,48,512]{3,2,1,0:T(8,128)(2,1)} custom-call(s32[4]{0:T(128)} %copy-done.9, bf16[768,256]{1,0:T(8,128)(2,1)} %bitcast.62, bf16[768,256]{1,0:T(8,128)(2,1)} %copy-done.31, bf16[768,256]{1,0:T(8,128)(2,1)} %copy-done.32, bf16[768,256]{1,0:T(8,128)(2,1)} %copy-done.33, bf16[1024,512]{1,0:T(8,128)(2,1)} %bitcast.11.own_ref.w_own_ref, ...), custom_call_target="tpu_custom_call" | custom-call | flops 1610612736 | bytes 4194304 | tf_op jit(solution)/shard_map/pallas_call | solution.py:471
  187.8 4.4 %all-to-all-start.3 = ((bf16[16,2,48,512]{3,2,1,0:T(8,128)(2,1)}), bf16[16,2,48,512]{3,2,1,0:T(8,128)(2,1)}, u32[]{:S(2)}, u32[]{:S(2)}) async-start(bf16[16,2,48,512]{3,2,1,0:T(8,128)(2,1)} %shard_map.163), calls=%async_computation.3 | async-start | bytes 3145728 | tf_op jit(solution)/shard_map/all_to_all | solution.py:488
  192.2 3.8 %shard_map.154.x_ref = bf16[512,4096]{1,0:T(8,128)(2,1)} custom-call(bf16[512,4096]{1,0:T(8,128)(2,1)} %tok_ref.3), custom_call_target="tpu_custom_call" | custom-call | flops 33554432 | bytes 8388608 | tf_op jit(solution)/shard_map/pallas_call | solution.py:346
  196.1 2.4 collective-permute-done.5.refs_2_
  198.5 2.1 collective-permute-done.6.refs_3_
  200.6 6.8 %shard_map.155 = (bf16[4096,128]{1,0:T(8,128)(2,1)}, bf16[4096,128]{1,0:T(8,128)(2,1)}, bf16[512,128]{1,0:T(8,128)(2,1)}, bf16[1024,512]{1,0:T(8,128)(2,1)}, bf16[512,512]{1,0:T(8,128)(2,1)}) custom-call(s32[4]{0:T(128)} %copy-done.9, bf16[512,4096]{1,0:T(8,128)(2,1)} %shard_map.154.x_ref, bf16[4,384,128]{2,1,0:T(8,128)(2,1)} %copy-done.16, ...), custom_call_target="tpu_custom_call" | custom-call | flops 1073741824 | bytes 4194304 | tf_op jit(solution)/shard_map/pallas_call | solution.py:433
  207.8 7.5 %collective-permute-start.29 = (bf16[512,128]{1,0:T(8,128)(2,1)}, bf16[512,128]{1,0:T(8,128)(2,1)S(1)}, u32[]{:S(2)}, u32[]{:S(2)}) collective-permute-start(bf16[512,128]{1,0:T(8,128)(2,1)} %get-tuple-element.54), channel_id=1, source_target_pairs={{0,6},{1,7},{2,0},{3,1},{4,2},{5,3},{6,4},{7,5},{8,14},{9,15},{10,... | collective-permute-start | bytes 393224 | tf_op jit(solution)/shard_map/ppermute | solution.py:286
  215.2 1.4 collective-permute-start.30
  216.6 1.7 collective-permute-done.28
  218.3 3.6 %collective-permute-done.30 = bf16[512,128]{1,0:T(8,128)(2,1)S(1)} collective-permute-done((bf16[512,128]{1,0:T(8,128)(2,1)}, bf16[512,128]{1,0:T(8,128)(2,1)S(1)}, u32[]{:S(2)}, u32[]{:S(2)}) %collective-permute-start.30) | collective-permute-done | bytes 131104 | tf_op jit(solution)/shard_map/ppermute | solution.py:286
  221.9 1.0 pad_maximum_fusion.1.own_ref
  223.6 1.7 fusion.4
  225.4 0.8 copy-done.6
  226.2 1.0 copy-done.3
  227.2 1.0 copy-done.7
  228.2 1.5 shard_map.164.base_ref
  229.8 0.8 copy-done.30
  230.6 4.1 %shard_map.156 = (bf16[256,1024]{1,0:T(8,128)(2,1)}, bf16[256,1024]{1,0:T(8,128)(2,1)}, bf16[256,1024]{1,0:T(8,128)(2,1)}, bf16[256,1024]{1,0:T(8,128)(2,1)}) custom-call(s32[4]{0:T(128)} %copy-done.9, bf16[1024,512]{1,0:T(8,128)(2,1)} %bitcast.11.own_ref.w_own_ref, bf16[1024,512]{1,0:T(8,128)(2,1)} %collective-permute-done.other_ref.w_other_ref, ...), custom_call_target="tpu_custom_call" | custom-call | flops 1073741824 | bytes 4194304 | tf_op jit(solution)/shard_map/pallas_call | solution.py:536
  235.4 2.7 %collective-permute-start.15 = (bf16[256,1024]{1,0:T(8,128)(2,1)}, bf16[256,1024]{1,0:T(8,128)(2,1)}, u32[]{:S(2)}, u32[]{:S(2)}) collective-permute-start(bf16[256,1024]{1,0:T(8,128)(2,1)} %get-tuple-element.41), channel_id=1, source_target_pairs={{0,4},{1,5},{2,6},{3,7},{4,0},{5,1},{6,2},{7,3},{8,12},{9,13},{10,... | collective-permute-start | bytes 1572872 | tf_op jit(solution)/shard_map/ppermute | solution.py:286
  238.7 1.2 slice.86
  240.0 1.5 slice_bitcast_fusion
  241.5 9.4 %collective-permute-done.14.p1_ref = bf16[256,1024]{1,0:T(8,128)(2,1)} collective-permute-done((bf16[256,1024]{1,0:T(8,128)(2,1)}, bf16[256,1024]{1,0:T(8,128)(2,1)}, u32[]{:S(2)}, u32[]{:S(2)}) %collective-permute-start.14) | collective-permute-done | bytes 524320 | tf_op jit(solution)/shard_map/ppermute | solution.py:286
  250.8 10.6 %collective-permute-done.15.p2_ref = bf16[256,1024]{1,0:T(8,128)(2,1)} collective-permute-done((bf16[256,1024]{1,0:T(8,128)(2,1)}, bf16[256,1024]{1,0:T(8,128)(2,1)}, u32[]{:S(2)}, u32[]{:S(2)}) %collective-permute-start.15) | collective-permute-done | bytes 524320 | tf_op jit(solution)/shard_map/ppermute | solution.py:286
  261.9 3.3 %shard_map.157 = (bf16[128,4096]{1,0:T(8,128)(2,1)}, bf16[128,4096]{1,0:T(8,128)(2,1)}) custom-call(s32[4]{0:T(128)S(1)} %copy-done.11, bf16[256,1024]{1,0:T(8,128)(2,1)S(1)} %copy-done.5, bf16[256,1024]{1,0:T(8,128)(2,1)} %collective-permute-done.14.p1_ref, bf16[256,1024]{1,0:T(8,128)(2,1)} %collective-permute-done.15.p2_ref, ...), custom_call_target="tpu_custom_call" | custom-call | flops 1048576 | bytes 4194304 | tf_op jit(solution)/shard_map/pallas_call | solution.py:552
  265.3 1.8 shard_map.165.base_ref
  267.1 1.4 shard_map.166
  (109 shorter events, 7.6 us)
Async XLA Ops:
  4.0 8.2 %copy-start.29 = (f32[256]{0:T(256)S(1)}, f32[256]{0:T(256)}, u32[]{:S(2)}) copy-start(f32[256]{0:T(256)} %param.11) | copy-start | bytes 3076
  4.1 32.7 %all-to-all-start = ((bf16[16,48,1024]{2,1,0:T(8,128)(2,1)}), bf16[16,48,1024]{2,1,0:T(8,128)(2,1)S(1)}, u32[]{:S(2)}, u32[]{:S(2)}) async-start(bf16[16,48,1024]{2,1,0:T(8,128)(2,1)} %bitcast.63), calls=%async_computation | async-start | bytes 3145728 | tf_op jit(solution)/shard_map/all_to_all | solution.py:361
  38.1 33.9 %all-to-all-start.1 = ((bf16[16,256,256]{2,1,0:T(8,128)(2,1)}), bf16[16,256,256]{2,1,0:T(8,128)(2,1)S(1)}, u32[]{:S(2)}, u32[]{:S(2)}) async-start(bf16[16,256,256]{2,1,0:T(8,128)(2,1)} %pad_maximum_fusion), calls=%async_computation.1 | async-start | bytes 4194304 | tf_op jit(solution)/shard_map/all_to_all | solution.py:372
  41.8 30.2 %copy-start.22 = (f32[64,512]{1,0:T(8,128)S(1)}, f32[64,512]{1,0:T(8,128)}, u32[]{:S(2)}) copy-start(f32[64,512]{1,0:T(8,128)} %param.17) | copy-start | bytes 393220
  41.8 31.7 %copy-start.20 = (f32[256,128]{1,0:T(8,128)S(1)}, f32[256,128]{1,0:T(8,128)}, u32[]{:S(2)}) copy-start(f32[256,128]{1,0:T(8,128)} %param.16) | copy-start | bytes 393220
  41.8 31.7 %copy-start.21 = (f32[256,128]{1,0:T(8,128)S(1)}, f32[256,128]{1,0:T(8,128)}, u32[]{:S(2)}) copy-start(f32[256,128]{1,0:T(8,128)} %param.15) | copy-start | bytes 393220
  71.9 74.2 %collective-permute-start.23 = (bf16[4096,256]{1,0:T(8,128)(2,1)S(1)}, bf16[4096,256]{1,0:T(8,128)(2,1)}, u32[]{:S(2)}, u32[]{:S(2)}) collective-permute-start(bf16[4096,256]{1,0:T(8,128)(2,1)S(1)} %bitcast.55), channel_id=1, source_target_pairs={{0,1},{1,0},{2,3},{3,2},{4,5},{5,4},{6,7},{7,6},{8,9},{9,8},{10,11... | collective-permute-start | bytes 6291464 | tf_op jit(solution)/shard_map/ppermute | solution.py:289
  72.0 35.5 %collective-permute-start.17 = (bf16[384,1024]{1,0:T(8,128)(2,1)}, bf16[384,1024]{1,0:T(8,128)(2,1)}, u32[]{:S(2)}, u32[]{:S(2)}) collective-permute-start(bf16[384,1024]{1,0:T(8,128)(2,1)} %bitcast.2.refs_0_), channel_id=1, source_target_pairs={{0,2},{1,3},{2,4},{3,5},{4,6},{5,7},{6,0},{7,1},{8,10},{9,11},{10,... | collective-permute-start | bytes 2359304 | tf_op jit(solution)/shard_map/ppermute | solution.py:286
  73.6 35.0 %collective-permute-start.19 = (bf16[384,1024]{1,0:T(8,128)(2,1)}, bf16[384,1024]{1,0:T(8,128)(2,1)}, u32[]{:S(2)}, u32[]{:S(2)}) collective-permute-start(bf16[384,1024]{1,0:T(8,128)(2,1)} %bitcast.3.refs_3_), channel_id=1, source_target_pairs={{0,6},{1,7},{2,0},{3,1},{4,2},{5,3},{6,4},{7,5},{8,14},{9,15},{10,... | collective-permute-start | bytes 2359304 | tf_op jit(solution)/shard_map/ppermute | solution.py:286
  75.4 36.6 %all-to-all-start.2 = ((bf16[16,64,512]{2,1,0:T(8,128)(2,1)}), bf16[16,64,512]{2,1,0:T(8,128)(2,1)}, u32[]{:S(2)}, u32[]{:S(2)}) async-start(bf16[16,64,512]{2,1,0:T(8,128)(2,1)} %convert_element_type.27), calls=%async_computation.2 | async-start | bytes 2097152 | tf_op jit(solution)/shard_map/all_to_all | solution.py:374
  79.8 31.4 %collective-permute-start.21 = (bf16[384,1024]{1,0:T(8,128)(2,1)}, bf16[384,1024]{1,0:T(8,128)(2,1)S(1)}, u32[]{:S(2)}, u32[]{:S(2)}) collective-permute-start(bf16[384,1024]{1,0:T(8,128)(2,1)} %bitcast.2.refs_0_), channel_id=1, source_target_pairs={{0,6},{1,7},{2,0},{3,1},{4,2},{5,3},{6,4},{7,5},{8,14},{9,15},{10,... | collective-permute-start | bytes 2359304 | tf_op jit(solution)/shard_map/ppermute | solution.py:286
  81.4 31.3 %copy-start.17 = (bf16[384,128]{1,0:T(8,128)(2,1)}, bf16[384,128]{1,0:T(8,128)(2,1)S(1)}, u32[]{:S(2)}) copy-start(bf16[384,128]{1,0:T(8,128)(2,1)S(1)} %get-tuple-element.62.b_ref) | copy-start | bytes 294916
  81.5 15.0 %collective-permute-start.7 = (bf16[384,128]{1,0:T(8,128)(2,1)S(1)}, bf16[384,128]{1,0:T(8,128)(2,1)S(1)}, u32[]{:S(2)}, u32[]{:S(2)}) collective-permute-start(bf16[384,128]{1,0:T(8,128)(2,1)S(1)} %get-tuple-element.62.b_ref), channel_id=1, source_target_pairs={{0,32},{8,40},{16,48},{24,56},{32,64},{40,72},{48,80},{56,88},{64,... | collective-permute-start | bytes 294920 | tf_op jit(solution)/shard_map/ppermute | solution.py:302
  96.4 17.6 %copy-start.23 = (bf16[384,128]{1,0:T(8,128)(2,1)}, bf16[384,128]{1,0:T(8,128)(2,1)S(1)}, u32[]{:S(2)}) copy-start(bf16[384,128]{1,0:T(8,128)(2,1)S(1)} %collective-permute-done.7) | copy-start | bytes 294916
  96.4 6.1 %collective-permute-start.8 = (bf16[384,128]{1,0:T(8,128)(2,1)S(1)}, bf16[384,128]{1,0:T(8,128)(2,1)S(1)}, u32[]{:S(2)}, u32[]{:S(2)}) collective-permute-start(bf16[384,128]{1,0:T(8,128)(2,1)S(1)} %get-tuple-element.62.b_ref), channel_id=1, source_target_pairs={{0,64},{8,72},{16,80},{24,88},{32,96},{40,104},{48,112},{56,120},{... | collective-permute-start | bytes 294920 | tf_op jit(solution)/shard_map/ppermute | solution.py:302
  102.6 11.5 %copy-start.24 = (bf16[384,128]{1,0:T(8,128)(2,1)}, bf16[384,128]{1,0:T(8,128)(2,1)S(1)}, u32[]{:S(2)}) copy-start(bf16[384,128]{1,0:T(8,128)(2,1)S(1)} %collective-permute-done.8) | copy-start | bytes 294916
  102.6 4.6 %collective-permute-start.9 = (bf16[384,128]{1,0:T(8,128)(2,1)S(1)}, bf16[384,128]{1,0:T(8,128)(2,1)S(1)}, u32[]{:S(2)}, u32[]{:S(2)}) collective-permute-start(bf16[384,128]{1,0:T(8,128)(2,1)S(1)} %get-tuple-element.62.b_ref), channel_id=1, source_target_pairs={{0,96},{8,104},{16,112},{24,120},{32,0},{40,8},{48,16},{56,24},{64... | collective-permute-start | bytes 294920 | tf_op jit(solution)/shard_map/ppermute | solution.py:302
  107.2 1.4 copy-start.25
  107.2 21.9 %collective-permute-start.22 = (bf16[384,1024]{1,0:T(8,128)(2,1)}, bf16[384,1024]{1,0:T(8,128)(2,1)}, u32[]{:S(2)}, u32[]{:S(2)}) collective-permute-start(bf16[384,1024]{1,0:T(8,128)(2,1)} %bitcast.3.refs_3_), channel_id=1, source_target_pairs={{0,2},{1,3},{2,4},{3,5},{4,6},{5,7},{6,0},{7,1},{8,10},{9,11},{10,... | collective-permute-start | bytes 2359304 | tf_op jit(solution)/shard_map/ppermute | solution.py:286
  107.5 34.5 %collective-permute-start.18 = (bf16[384,1024]{1,0:T(8,128)(2,1)}, bf16[384,1024]{1,0:T(8,128)(2,1)S(1)}, u32[]{:S(2)}, u32[]{:S(2)}) collective-permute-start(bf16[384,1024]{1,0:T(8,128)(2,1)} %collective-permute-done.17.a_ref.refs_1_), channel_id=1, source_target_pairs={{0,2},{1,3},{2,4},{3,5},{4,6},{5,7},{6,0},{7,1},{8,10},{9,11},{10,... | collective-permute-start | bytes 2359304 | tf_op jit(solution)/shard_map/ppermute | solution.py:286
  108.6 47.3 %collective-permute-start.20 = (bf16[384,1024]{1,0:T(8,128)(2,1)}, bf16[384,1024]{1,0:T(8,128)(2,1)}, u32[]{:S(2)}, u32[]{:S(2)}) collective-permute-start(bf16[384,1024]{1,0:T(8,128)(2,1)} %collective-permute-done.19.b_ref.refs_5_), channel_id=1, source_target_pairs={{0,6},{1,7},{2,0},{3,1},{4,2},{5,3},{6,4},{7,5},{8,14},{9,15},{10,... | collective-permute-start | bytes 2359304 | tf_op jit(solution)/shard_map/ppermute | solution.py:286
  112.1 57.2 %collective-permute-start = (bf16[1024,512]{1,0:T(8,128)(2,1)}, bf16[1024,512]{1,0:T(8,128)(2,1)}, u32[]{:S(2)}, u32[]{:S(2)}) collective-permute-start(bf16[1024,512]{1,0:T(8,128)(2,1)} %bitcast.11.own_ref.w_own_ref), channel_id=1, source_target_pairs={{0,1},{1,0},{2,3},{3,2},{4,5},{5,4},{6,7},{7,6},{8,9},{9,8},{10,11... | collective-permute-start | bytes 3145736 | tf_op jit(solution)/shard_map/ppermute | solution.py:289
  114.1 42.9 %copy-start.9 = (s32[4]{0:T(128)}, s32[4]{0:T(128)S(1)}, u32[]{:S(2)}) copy-start(s32[4]{0:T(128)S(1)} %pad_add_fusion.place_ref) | copy-start | bytes 52
  115.1 54.1 %copy-start.15 = (bf16[4,384,128]{2,1,0:T(8,128)(2,1)}, bf16[4,384,128]{2,1,0:T(8,128)(2,1)S(1)}, u32[]{:S(2)}) copy-start(bf16[4,384,128]{2,1,0:T(8,128)(2,1)S(1)} %pad_maximum_fusion.3.refs_4_) | copy-start | bytes 1179652
  129.1 30.8 %collective-permute-start.1 = (bf16[384,128]{1,0:T(8,128)(2,1)}, bf16[384,128]{1,0:T(8,128)(2,1)S(1)}, u32[]{:S(2)}, u32[]{:S(2)}) collective-permute-start(bf16[384,128]{1,0:T(8,128)(2,1)} %get-tuple-element.64.a_ref), channel_id=1, source_target_pairs={{0,8},{8,16},{16,24},{24,0},{32,40},{40,48},{48,56},{56,32},{64,72... | collective-permute-start | bytes 294920 | tf_op jit(solution)/shard_map/ppermute | solution.py:302
  142.0 18.3 %collective-permute-start.2 = (bf16[384,128]{1,0:T(8,128)(2,1)}, bf16[384,128]{1,0:T(8,128)(2,1)S(1)}, u32[]{:S(2)}, u32[]{:S(2)}) collective-permute-start(bf16[384,128]{1,0:T(8,128)(2,1)} %get-tuple-element.64.a_ref), channel_id=1, source_target_pairs={{0,16},{8,24},{16,0},{24,8},{32,48},{40,56},{48,32},{56,40},{64,80... | collective-permute-start | bytes 294920 | tf_op jit(solution)/shard_map/ppermute | solution.py:302
  146.1 17.4 %collective-permute-start.3 = (bf16[384,128]{1,0:T(8,128)(2,1)}, bf16[384,128]{1,0:T(8,128)(2,1)S(1)}, u32[]{:S(2)}, u32[]{:S(2)}) collective-permute-start(bf16[384,128]{1,0:T(8,128)(2,1)} %get-tuple-element.64.a_ref), channel_id=1, source_target_pairs={{0,24},{8,0},{16,8},{24,16},{32,56},{40,32},{48,40},{56,48},{64,88... | collective-permute-start | bytes 294920 | tf_op jit(solution)/shard_map/ppermute | solution.py:302
  147.9 1.1 copy-start.14
  156.0 13.3 %collective-permute-start.10 = (bf16[4,384,128]{2,1,0:T(8,128)(2,1)S(1)}, bf16[4,384,128]{2,1,0:T(8,128)(2,1)S(1)}, u32[]{:S(2)}, u32[]{:S(2)}) collective-permute-start(bf16[4,384,128]{2,1,0:T(8,128)(2,1)S(1)} %pad_maximum_fusion.3.refs_4_), channel_id=1, source_target_pairs={{0,8},{8,16},{16,24},{24,0},{32,40},{40,48},{48,56},{56,32},{64,72... | collective-permute-start | bytes 1179656 | tf_op jit(solution)/shard_map/ppermute | solution.py:302
  160.0 22.4 %copy-start.8 = (bf16[2,384,256]{2,1,0:T(8,128)(2,1)}, bf16[2,384,256]{2,1,0:T(8,128)(2,1)S(1)}, u32[]{:S(2)}) copy-start(bf16[2,384,256]{2,1,0:T(8,128)(2,1)S(1)} %shard_map.162) | copy-start | bytes 1179652
  160.0 17.0 %collective-permute-start.24 = (bf16[768,256]{1,0:T(8,128)(2,1)S(1)}, bf16[768,256]{1,0:T(8,128)(2,1)S(1)}, u32[]{:S(2)}, u32[]{:S(2)}) collective-permute-start(bf16[768,256]{1,0:T(8,128)(2,1)S(1)} %bitcast.59), channel_id=1, source_target_pairs={{0,2},{1,3},{2,4},{3,5},{4,6},{5,7},{6,0},{7,1},{8,10},{9,11},{10,... | collective-permute-start | bytes 1179656 | tf_op jit(solution)/shard_map/ppermute | solution.py:286
  160.3 17.0 %collective-permute-start.25 = (bf16[768,256]{1,0:T(8,128)(2,1)S(1)}, bf16[768,256]{1,0:T(8,128)(2,1)S(1)}, u32[]{:S(2)}, u32[]{:S(2)}) collective-permute-start(bf16[768,256]{1,0:T(8,128)(2,1)S(1)} %bitcast.60), channel_id=1, source_target_pairs={{0,6},{1,7},{2,0},{3,1},{4,2},{5,3},{6,4},{7,5},{8,14},{9,15},{10,... | collective-permute-start | bytes 1179656 | tf_op jit(solution)/shard_map/ppermute | solution.py:286
  163.5 17.6 %collective-permute-start.26 = (bf16[768,256]{1,0:T(8,128)(2,1)S(1)}, bf16[768,256]{1,0:T(8,128)(2,1)S(1)}, u32[]{:S(2)}, u32[]{:S(2)}) collective-permute-start(bf16[768,256]{1,0:T(8,128)(2,1)S(1)} %bitcast.61), channel_id=1, source_target_pairs={{0,4},{1,5},{2,6},{3,7},{4,0},{5,1},{6,2},{7,3},{8,12},{9,13},{10,... | collective-permute-start | bytes 1179656 | tf_op jit(solution)/shard_map/ppermute | solution.py:286
  163.5 24.2 %copy-start.16 = (bf16[4,384,128]{2,1,0:T(8,128)(2,1)}, bf16[4,384,128]{2,1,0:T(8,128)(2,1)S(1)}, u32[]{:S(2)}) copy-start(bf16[4,384,128]{2,1,0:T(8,128)(2,1)S(1)} %pad_maximum_fusion.2.refs_0_) | copy-start | bytes 1179652
  169.2 11.8 %copy-start.18 = (bf16[4,384,128]{2,1,0:T(8,128)(2,1)}, bf16[4,384,128]{2,1,0:T(8,128)(2,1)S(1)}, u32[]{:S(2)}) copy-start(bf16[4,384,128]{2,1,0:T(8,128)(2,1)S(1)} %collective-permute-done.10.refs_5_) | copy-start | bytes 1179652
  169.2 26.9 %collective-permute-start.11 = (bf16[4,384,128]{2,1,0:T(8,128)(2,1)S(1)}, bf16[4,384,128]{2,1,0:T(8,128)(2,1)S(1)}, u32[]{:S(2)}, u32[]{:S(2)}) collective-permute-start(bf16[4,384,128]{2,1,0:T(8,128)(2,1)S(1)} %pad_maximum_fusion.3.refs_4_), channel_id=1, source_target_pairs={{0,16},{8,24},{16,0},{24,8},{32,48},{40,56},{48,32},{56,40},{64,80... | collective-permute-start | bytes 1179656 | tf_op jit(solution)/shard_map/ppermute | solution.py:302
  169.3 26.9 %collective-permute-start.12 = (bf16[4,384,128]{2,1,0:T(8,128)(2,1)S(1)}, bf16[4,384,128]{2,1,0:T(8,128)(2,1)}, u32[]{:S(2)}, u32[]{:S(2)}) collective-permute-start(bf16[4,384,128]{2,1,0:T(8,128)(2,1)S(1)} %pad_maximum_fusion.3.refs_4_), channel_id=1, source_target_pairs={{0,24},{8,0},{16,8},{24,16},{32,56},{40,32},{48,40},{56,48},{64,88... | collective-permute-start | bytes 1179656 | tf_op jit(solution)/shard_map/ppermute | solution.py:302
  177.0 4.1 %copy-start.31 = (bf16[768,256]{1,0:T(8,128)(2,1)}, bf16[768,256]{1,0:T(8,128)(2,1)S(1)}, u32[]{:S(2)}) copy-start(bf16[768,256]{1,0:T(8,128)(2,1)S(1)} %collective-permute-done.24.h1_ref) | copy-start | bytes 1179652
  177.0 19.2 %collective-permute-start.4 = (bf16[4,384,128]{2,1,0:T(8,128)(2,1)S(1)}, bf16[4,384,128]{2,1,0:T(8,128)(2,1)}, u32[]{:S(2)}, u32[]{:S(2)}) collective-permute-start(bf16[4,384,128]{2,1,0:T(8,128)(2,1)S(1)} %pad_maximum_fusion.2.refs_0_), channel_id=1, source_target_pairs={{0,32},{8,40},{16,48},{24,56},{32,64},{40,72},{48,80},{56,88},{64,... | collective-permute-start | bytes 1179656 | tf_op jit(solution)/shard_map/ppermute | solution.py:302
  177.2 3.8 %copy-start.32 = (bf16[768,256]{1,0:T(8,128)(2,1)}, bf16[768,256]{1,0:T(8,128)(2,1)S(1)}, u32[]{:S(2)}) copy-start(bf16[768,256]{1,0:T(8,128)(2,1)S(1)} %collective-permute-done.25.h2_ref) | copy-start | bytes 1179652
  177.2 21.2 %collective-permute-start.5 = (bf16[4,384,128]{2,1,0:T(8,128)(2,1)S(1)}, bf16[4,384,128]{2,1,0:T(8,128)(2,1)}, u32[]{:S(2)}, u32[]{:S(2)}) collective-permute-start(bf16[4,384,128]{2,1,0:T(8,128)(2,1)S(1)} %pad_maximum_fusion.2.refs_0_), channel_id=1, source_target_pairs={{0,64},{8,72},{16,80},{24,88},{32,96},{40,104},{48,112},{56,120},{... | collective-permute-start | bytes 1179656 | tf_op jit(solution)/shard_map/ppermute | solution.py:302
  181.8 18.7 %collective-permute-start.6 = (bf16[4,384,128]{2,1,0:T(8,128)(2,1)S(1)}, bf16[4,384,128]{2,1,0:T(8,128)(2,1)}, u32[]{:S(2)}, u32[]{:S(2)}) collective-permute-start(bf16[4,384,128]{2,1,0:T(8,128)(2,1)S(1)} %pad_maximum_fusion.2.refs_0_), channel_id=1, source_target_pairs={{0,96},{8,104},{16,112},{24,120},{32,0},{40,8},{48,16},{56,24},{64... | collective-permute-start | bytes 1179656 | tf_op jit(solution)/shard_map/ppermute | solution.py:302
  187.8 51.0 %all-to-all-start.3 = ((bf16[16,2,48,512]{3,2,1,0:T(8,128)(2,1)}), bf16[16,2,48,512]{3,2,1,0:T(8,128)(2,1)}, u32[]{:S(2)}, u32[]{:S(2)}) async-start(bf16[16,2,48,512]{3,2,1,0:T(8,128)(2,1)} %shard_map.163), calls=%async_computation.3 | async-start | bytes 3145728 | tf_op jit(solution)/shard_map/all_to_all | solution.py:488
  196.1 20.6 %copy-start.28 = (f32[512,2]{0,1:T(2,128)S(1)}, f32[512,2]{0,1:T(2,128)}, u32[]{:S(2)}) copy-start(f32[512,2]{0,1:T(2,128)} %param.19) | copy-start | bytes 12292
  196.1 27.5 %copy-start.26 = (s32[512,2]{0,1:T(2,128)S(1)}, s32[512,2]{0,1:T(2,128)}, u32[]{:S(2)}) copy-start(s32[512,2]{0,1:T(2,128)} %param.18) | copy-start | bytes 12292
  196.1 27.5 %copy-start.27 = (s32[2,512]{1,0:T(2,128)S(1)}, s32[2,512]{1,0:T(2,128)}, u32[]{:S(2)}) copy-start(s32[2,512]{1,0:T(2,128)} %get-tuple-element.47) | copy-start | bytes 12292
  196.1 4.4 %copy-start.19 = (bf16[4,384,128]{2,1,0:T(8,128)(2,1)}, bf16[4,384,128]{2,1,0:T(8,128)(2,1)S(1)}, u32[]{:S(2)}) copy-start(bf16[4,384,128]{2,1,0:T(8,128)(2,1)S(1)} %collective-permute-done.11.refs_6_) | copy-start | bytes 1179652
  207.4 18.8 %copy-start.10 = (s32[4]{0:T(128)S(1)}, s32[4]{0:T(128)}, u32[]{:S(2)}) copy-start(s32[4]{0:T(128)} %copy-done.9) | copy-start | bytes 52
  207.4 10.9 %collective-permute-start.28 = (bf16[512,128]{1,0:T(8,128)(2,1)}, bf16[512,128]{1,0:T(8,128)(2,1)S(1)}, u32[]{:S(2)}, u32[]{:S(2)}) collective-permute-start(bf16[512,128]{1,0:T(8,128)(2,1)} %get-tuple-element.54), channel_id=1, source_target_pairs={{0,2},{1,3},{2,4},{3,5},{4,6},{5,7},{6,0},{7,1},{8,10},{9,11},{10,... | collective-permute-start | bytes 393224 | tf_op jit(solution)/shard_map/ppermute | solution.py:286
  207.8 10.5 %collective-permute-start.29 = (bf16[512,128]{1,0:T(8,128)(2,1)}, bf16[512,128]{1,0:T(8,128)(2,1)S(1)}, u32[]{:S(2)}, u32[]{:S(2)}) collective-permute-start(bf16[512,128]{1,0:T(8,128)(2,1)} %get-tuple-element.54), channel_id=1, source_target_pairs={{0,6},{1,7},{2,0},{3,1},{4,2},{5,3},{6,4},{7,5},{8,14},{9,15},{10,... | collective-permute-start | bytes 393224 | tf_op jit(solution)/shard_map/ppermute | solution.py:286
  215.2 6.7 %collective-permute-start.30 = (bf16[512,128]{1,0:T(8,128)(2,1)}, bf16[512,128]{1,0:T(8,128)(2,1)S(1)}, u32[]{:S(2)}, u32[]{:S(2)}) collective-permute-start(bf16[512,128]{1,0:T(8,128)(2,1)} %get-tuple-element.54), channel_id=1, source_target_pairs={{0,4},{1,5},{2,6},{3,7},{4,0},{5,1},{6,2},{7,3},{8,12},{9,13},{10,... | collective-permute-start | bytes 393224 | tf_op jit(solution)/shard_map/ppermute | solution.py:286
  222.9 2.5 copy-start.2
  222.9 2.5 collective-permute-start.31
  223.0 3.1 %copy-start.4 = (bf16[1024,512]{1,0:T(8,128)(2,1)S(1)}, bf16[1024,512]{1,0:T(8,128)(2,1)}, u32[]{:S(2)}) copy-start(bf16[1024,512]{1,0:T(8,128)(2,1)} %get-tuple-element.37.sd_ref) | copy-start | bytes 3145732
  223.0 6.7 %collective-permute-start.13 = (bf16[512,512]{1,0:T(8,128)(2,1)}, bf16[512,512]{1,0:T(8,128)(2,1)S(1)}, u32[]{:S(2)}, u32[]{:S(2)}) collective-permute-start(bf16[512,512]{1,0:T(8,128)(2,1)} %get-tuple-element.38), channel_id=1, source_target_pairs={{0,1},{1,0},{2,3},{3,2},{4,5},{5,4},{6,7},{7,6},{8,9},{9,8},{10,11... | collective-permute-start | bytes 1572872 | tf_op jit(solution)/shard_map/ppermute | solution.py:289
  226.2 1.0 copy-start.3
  234.7 16.2 %collective-permute-start.14 = (bf16[256,1024]{1,0:T(8,128)(2,1)}, bf16[256,1024]{1,0:T(8,128)(2,1)}, u32[]{:S(2)}, u32[]{:S(2)}) collective-permute-start(bf16[256,1024]{1,0:T(8,128)(2,1)} %get-tuple-element.40), channel_id=1, source_target_pairs={{0,2},{1,3},{2,4},{3,5},{4,6},{5,7},{6,0},{7,1},{8,10},{9,11},{10,... | collective-permute-start | bytes 1572872 | tf_op jit(solution)/shard_map/ppermute | solution.py:286
  235.4 26.1 %collective-permute-start.15 = (bf16[256,1024]{1,0:T(8,128)(2,1)}, bf16[256,1024]{1,0:T(8,128)(2,1)}, u32[]{:S(2)}, u32[]{:S(2)}) collective-permute-start(bf16[256,1024]{1,0:T(8,128)(2,1)} %get-tuple-element.41), channel_id=1, source_target_pairs={{0,4},{1,5},{2,6},{3,7},{4,0},{5,1},{6,2},{7,3},{8,12},{9,13},{10,... | collective-permute-start | bytes 1572872 | tf_op jit(solution)/shard_map/ppermute | solution.py:286
  238.1 23.8 %collective-permute-start.16 = (bf16[256,1024]{1,0:T(8,128)(2,1)}, bf16[256,1024]{1,0:T(8,128)(2,1)}, u32[]{:S(2)}, u32[]{:S(2)}) collective-permute-start(bf16[256,1024]{1,0:T(8,128)(2,1)} %get-tuple-element.42), channel_id=1, source_target_pairs={{0,6},{1,7},{2,0},{3,1},{4,2},{5,3},{6,4},{7,5},{8,14},{9,15},{10,... | collective-permute-start | bytes 1572872 | tf_op jit(solution)/shard_map/ppermute | solution.py:286
  239.9 22.0 %copy-start.5 = (bf16[256,1024]{1,0:T(8,128)(2,1)S(1)}, bf16[256,1024]{1,0:T(8,128)(2,1)}, u32[]{:S(2)}) copy-start(bf16[256,1024]{1,0:T(8,128)(2,1)} %get-tuple-element.39.p0_ref) | copy-start | bytes 1572868
  239.9 22.0 %copy-start.11 = (s32[4]{0:T(128)S(1)}, s32[4]{0:T(128)}, u32[]{:S(2)}) copy-start(s32[4]{0:T(128)} %copy-done.9) | copy-start | bytes 52
  239.9 27.2 %collective-permute-start.27 = (bf16[768,512]{1,0:T(8,128)(2,1)S(1)}, bf16[768,512]{1,0:T(8,128)(2,1)S(1)}, u32[]{:S(2)}, u32[]{:S(2)}) collective-permute-start(bf16[768,512]{1,0:T(8,128)(2,1)S(1)} %bitcast.64), channel_id=1, source_target_pairs={{0,1},{1,0},{2,3},{3,2},{4,5},{5,4},{6,7},{7,6},{8,9},{9,8},{10,11... | collective-permute-start | bytes 2359304 | tf_op jit(solution)/shard_map/ppermute | solution.py:289
  241.5 23.8 %copy-start.1 = (bf16[512,768]{1,0:T(8,128)(2,1)S(1)}, bf16[512,768]{1,0:T(8,128)(2,1)}, u32[]{:S(2)}) copy-start(bf16[512,768]{1,0:T(8,128)(2,1)} %get-tuple-element.53.weight_ref) | copy-start | bytes 2359300
  265.3 1.8 copy-start
  (6 other events, 4.9 us)
